TPU v7x, 32 devices: a whole 2x2x4 slice. The times are simulated.
32 devices in a mesh: sp: 8 (over z, x), tp: 4 (over y, core).
Axes of the slice: x: 2, y: 2, z: 4, core: 2. Of those that a mesh axis runs over, the one named last changes fastest.
Arguments:
- query: bfloat16 [2048, 1024], P('sp', 'tp'), may hold values from -6 to 6
- forget_logits: bfloat16 [2048, 1024], P('sp', 'tp'), may hold values from -5.5 to 5.5
- written_values: bfloat16 [2048, 1024], P('sp', 'tp'), may hold values from -6 to 6
- output_gate_logits: bfloat16 [2048, 1024], P('sp', 'tp'), may hold values from -6 to 6
- forget_floor_gap: float32 [1024], P('tp'), may hold values from 0 to 0.08
- extra_log_decay: float32 [2048, 1024], P('sp', 'tp'), may hold values from -0.7 to 0
- head_norm_gain: float32 [128], replicated, may hold values from 0.1 to 1.9
- output_weight: bfloat16 [1024, 2048], P('tp'), may hold values from -0.1875 to 0.1875
- residual: bfloat16 [2048, 2048], P(('sp', 'tp')), may hold values from -6 to 6
- mixer_norm_gain: float32 [2048], replicated, may hold values from 0.1 to 1.9
- mixer_up_weight: bfloat16 [2048, 8192], P('sp', 'tp'), may hold values from -0.125 to 0.125
- mixer_down_weight: bfloat16 [8192, 2048], P(('tp', 'sp')), may hold values from -0.0625 to 0.0625
Outputs:
- layer_out: bfloat16 [2048, 2048], P(('sp', 'tp'))
All inputs are finite; a program needn't handle non-finite values.
Results may differ from a plain program's by a relative error of at most 0.015.
Values may be sent and summed in bfloat16 or wider, within the bound.
No kernel may reach another device: no remote copies, remote signals or barrier semaphores. Data moves between devices by JAX's collectives and lax.ppermute only.
A program may use at most 128 MiB of HBM per device.

v0:
```python
import jax
import jax.numpy as jnp
from jax import lax
from jax.experimental import pallas as pl
from jax.experimental.pallas import tpu as pltpu
from jax.sharding import PartitionSpec as P


HEAD = 128
SUB = 64
EPS = 1e-06
HI = lax.Precision.HIGHEST
AXES = ("sp", "tp")
F32 = jnp.float32
BF16 = jnp.bfloat16


HEAD_K = 128
HEAD_V = 128
BLOCK = 64


def exact_parts(x):
    first = x.astype(BF16)
    rest = x - first.astype(F32)
    second = rest.astype(BF16)
    third = (rest - second.astype(F32)).astype(BF16)
    return first, second, third


def pack_logs(totals):
    lines = []
    for x in totals:
        lines += list(exact_parts(x))
    pad = 16 - len(lines)
    return jnp.concatenate(
        [x.astype(F32) for x in lines] + [jnp.zeros((pad, HEAD), F32)], axis=0
    ).astype(BF16)


def log_of(packed, heads, h):
    parts = packed[heads * HEAD :, :].astype(F32)
    return sum(parts[3 * h + k : 3 * h + k + 1, :] for k in range(3))


def as_column(row):
    return jnp.transpose(jnp.broadcast_to(row, (HEAD, HEAD)))


def gates_body(logits, values, gap, extra, gate_out, cum_out, packed):
    rows, width = logits.shape
    heads = width // HEAD
    z = logits[...].astype(F32)
    gate = gap[...] / (1.0 + jnp.exp(z))
    log_forget = jnp.log1p(-gate) + extra[...]
    r = lax.broadcasted_iota(jnp.int32, (rows, rows), 0)
    c = lax.broadcasted_iota(jnp.int32, (rows, rows), 1)
    lower = (r >= c).astype(F32)
    cum = jnp.dot(lower, log_forget, precision=HI, preferred_element_type=F32)
    gate_out[...] = gate
    cum_out[...] = cum
    total = cum[rows - 1 : rows, :]
    keys = gate * jnp.exp(total - cum)
    vals = values[...].astype(F32)
    for h in range(heads):
        ks = keys[:, h * HEAD : (h + 1) * HEAD]
        vs = vals[:, h * HEAD : (h + 1) * HEAD]
        state = lax.dot_general(
            ks, vs, (((0,), (0,)), ((), ())), precision=HI, preferred_element_type=F32
        )
        packed[h * HEAD : (h + 1) * HEAD, :] = state.astype(BF16)
    packed[heads * HEAD :, :] = pack_logs([total[:, h * HEAD : (h + 1) * HEAD] for h in range(heads)])


def local_body(query, gate, cum, values, out):
    rows, width = query.shape
    sub = min(SUB, rows)
    for h in range(width // HEAD):
        lanes = slice(h * HEAD, (h + 1) * HEAD)
        for i in range(rows // sub):
            lo, hi = i * sub, (i + 1) * sub
            mid = cum[lo + sub // 2 - 1 : lo + sub // 2, lanes]
            qs = query[lo:hi, lanes].astype(F32) * (HEAD**-0.5) * jnp.exp(cum[lo:hi, lanes] - mid)
            ks = gate[0:hi, lanes] * jnp.exp(mid - cum[0:hi, lanes])
            scores = lax.dot_general(
                qs, ks, (((1,), (1,)), ((), ())), precision=HI, preferred_element_type=F32
            )
            rr = lax.broadcasted_iota(jnp.int32, (sub, hi), 0) + lo
            cc = lax.broadcasted_iota(jnp.int32, (sub, hi), 1)
            scores = jnp.where(rr >= cc, scores, 0.0)
            out[lo:hi, lanes] = jnp.dot(
                scores, values[0:hi, lanes].astype(F32), precision=HI, preferred_element_type=F32
            )


def kernel_call(body, out_shape, scratch=(), smem=0, n_in=0, mib=16):
    specs = [pl.BlockSpec(memory_space=pltpu.SMEM)] * smem
    specs += [pl.BlockSpec(memory_space=pltpu.VMEM)] * (n_in - smem)
    many = isinstance(out_shape, (list, tuple))
    out_spec = pl.BlockSpec(memory_space=pltpu.VMEM)
    return pl.pallas_call(
        body,
        out_shape=out_shape,
        in_specs=specs,
        out_specs=[out_spec] * len(out_shape) if many else out_spec,
        scratch_shapes=list(scratch),
        compiler_params=pltpu.CompilerParams(vmem_limit_bytes=mib * 1024 * 1024),
    )


def pair_body(place, mine, theirs, out):
    last = place[1] == 1
    heads = (mine.shape[0] - 16) // HEAD
    logs = []
    for h in range(heads):
        rows = slice(h * HEAD, (h + 1) * HEAD)
        own_log, their_log = log_of(mine, heads, h), log_of(theirs, heads, h)
        own_state, their_state = mine[rows, :].astype(F32), theirs[rows, :].astype(F32)
        decay = as_column(jnp.exp(jnp.where(last, own_log, their_log)))
        early = jnp.where(last, their_state, own_state)
        late = jnp.where(last, own_state, their_state)
        out[rows, :] = (decay * early + late).astype(BF16)
        logs.append(own_log + their_log)
    out[heads * HEAD :, :] = pack_logs(logs)


def mix_body(n_cores, *refs):
    place = refs[0]
    query, cum, local, gate_logits, gain, weight, beside = refs[1:8]
    states = refs[8:-4]
    first, second, away, mixed = refs[-4:]
    rows, width = query.shape
    heads = width // HEAD
    last = place[1] == 1
    for h in range(heads):
        lanes = slice(h * HEAD, (h + 1) * HEAD)
        arrived = jnp.where(last, beside[lanes, :].astype(F32), 0.0)
        passed = jnp.where(last, log_of(beside, heads, h), 0.0)
        for s in states:
            arrived = arrived + as_column(jnp.exp(passed)) * s[lanes, :].astype(F32)
            passed = passed + log_of(s, heads, h)
        reach = query[:, lanes].astype(F32) * (HEAD**-0.5) * jnp.exp(cum[:, lanes])
        rec = local[:, lanes] + jnp.dot(reach, arrived, precision=HI, preferred_element_type=F32)
        scale = lax.rsqrt(jnp.mean(rec * rec, axis=-1, keepdims=True) + EPS)
        v = gate_logits[:, lanes].astype(F32)
        mixed[:, lanes] = rec * scale * gain[...] * (v / (1.0 + jnp.exp(-v)))
    y, c = place[2], place[3]
    n_y = 2
    own = rows // (n_y * n_cores)
    picked = []
    for e in range(n_cores):
        for k in range(n_y):
            t = lax.rem(y + k, n_y) * n_cores + lax.rem(c + e, n_cores)
            picked.append(mixed[pl.ds(pl.multiple_of(t * own, own), own), :])
    ordered = jnp.concatenate(picked, axis=0).astype(BF16)
    part = jnp.dot(ordered, weight[...], preferred_element_type=F32)
    first[...] = part[:own]
    second[...] = part[own : n_y * own]
    away[...] = part[n_y * own :].astype(BF16)


def norm_body(own, beside, arrived, residual, gain, stream_out, normed_out):
    rows = own.shape[0]
    stream = own[...] + beside[:rows, :].astype(F32) + arrived[...].astype(F32)
    stream = stream + residual[...].astype(F32)
    stream_out[...] = stream
    scale = lax.rsqrt(jnp.mean(stream * stream, axis=-1, keepdims=True) + EPS)
    normed = (stream * scale * gain[...]).astype(BF16)
    blocks, _, cols = normed_out.shape
    for i in range(blocks):
        normed_out[i] = normed[:, i * cols : (i + 1) * cols]


def lower_half(out_own, out_away, hidden, down, cut):
    acc = jnp.dot(hidden, down, preferred_element_type=F32)
    out_own[...] = acc[:cut]
    out_away[...] = acc[cut:].astype(BF16)


def mixer_body(n_a, n_cores, *refs):
    n_tok = n_a * n_cores
    n_b = 2
    place = refs[0]
    toks = refs[1 : 1 + n_tok]
    ups = refs[1 + n_tok : 1 + n_tok + 2 * n_b * n_a]
    downs = refs[1 + n_tok + 2 * n_b * n_a : -7]
    keep, away, hid_out, rows_x, up_all, hid, down_all = refs[-7:]
    a, b = place[0], place[1]
    _, own, cols = toks[0].shape
    for i in range(n_tok):
        for e in range(n_a):
            for x in range(n_b):
                k = lax.rem(a - e + n_a, n_a) * n_b + lax.rem(b + x, n_b)
                at = (e * n_b + x) * cols
                rows_x[i * own : (i + 1) * own, at : at + cols] = toks[i][k]
    for y in range(2):
        for e in range(n_a):
            for x in range(n_b):
                at = (e * n_b + x) * cols
                src, off = ups[(y * n_b + x) * n_a + e]
                up_all[at : at + cols, :] = src[off : off + cols, :]
        act = jnp.maximum(jnp.dot(rows_x[...], up_all[...], preferred_element_type=F32), 0.0)
        act = (act * act).astype(BF16)
        half = act.shape[1] // n_b
        for x in range(n_b):
            hid[y * n_b + x] = act[:, x * half : (x + 1) * half]
    width = keep.shape[1]
    at = 0
    for y in range(2):
        for x in range(n_b):
            h = hid[y * n_b + lax.rem(b + x, n_b)]
            step = h.shape[1]
            hid_out[:, at : at + step] = h
            for piece in downs[y * n_b + x :] if y * n_b + x == 3 else [downs[y * n_b + x]]:
                n = piece.shape[0]
                down_all[at : at + n, :] = piece[:, :width]
                at += n
    lower_half(keep, away, hid_out[...], down_all[...], n_a * own)


def mixer_rest_body(cut, hidden, *refs):
    downs, (keep, away, down_all) = refs[:-3], refs[-3:]
    width = keep.shape[1]
    at = 0
    for piece in downs:
        n = piece.shape[0]
        down_all[at : at + n, :] = piece[:, width:]
        at += n
    lower_half(keep, away, hidden[...], down_all[...], cut)


def fold_body(keep, got, *outs):
    rows = outs[0].shape[0]
    for d in range(len(outs)):
        at = (d + 1) * rows
        outs[d][...] = (keep[at : at + rows, :] + got[at : at + rows, :].astype(F32)).astype(BF16)


norm_eps = 1e-06
highest_precision = lax.Precision.HIGHEST


def carried_in(part, axis, combine, identity):
    place = lax.axis_index(axis)
    gathered = jax.tree.map(lambda a: lax.all_gather(a, axis), part)
    state = jax.tree.map(lambda a, e: jnp.zeros_like(a) + jnp.asarray(e, a.dtype), part, identity)

    def one(step, state):
        return combine(
            state, jax.tree.map(lambda a: lax.dynamic_index_in_dim(a, step, 0, False), gathered)
        )

    return lax.fori_loop(0, place, one, state)


def block_update(carry_forward_state, block_inputs):
    query_rows_block, gate_rows_block, value_rows_block, log_block = block_inputs
    cumulative_log = jnp.cumsum(log_block, axis=1)
    length = query_rows_block.shape[1]
    causal = jnp.arange(length)[:, None] >= jnp.arange(length)[None, :]
    across_blocks = jnp.einsum(
        "dcj,djw->dcw",
        query_rows_block * jnp.exp(cumulative_log),
        carry_forward_state,
        precision=highest_precision,
    )
    spread = cumulative_log[:, :, None, :] - cumulative_log[:, None, :, :]
    decay_table = jnp.exp(jnp.where(causal[None, :, :, None], spread, -jnp.inf))
    scores = jnp.einsum(
        "htk,hsk,htsk->hts",
        query_rows_block,
        gate_rows_block,
        decay_table,
        precision=highest_precision,
    )
    within = jnp.einsum("hts,hsv->htv", scores, value_rows_block, precision=highest_precision)
    final_log_total = cumulative_log[:, -1:, :]
    updated_state = jnp.exp(final_log_total[:, 0, :])[
        :, :, None
    ] * carry_forward_state + jnp.einsum(
        "tri,trw->tiw",
        gate_rows_block * jnp.exp(final_log_total - cumulative_log),
        value_rows_block,
        precision=highest_precision,
    )
    return (updated_state, across_blocks + within)


def to_blocks(array, inner):
    length = array.shape[0]
    split_up = array.reshape(length // BLOCK, BLOCK, array.shape[1] // inner, inner)
    return jnp.transpose(split_up, (0, 2, 1, 3))


def from_blocks(blocked):
    joined = jnp.transpose(blocked, (0, 2, 1, 3))
    return joined.reshape(joined.shape[0] * joined.shape[1], joined.shape[2], joined.shape[3])


def prepare_inputs(query, forget_logits, written_values, forget_floor_gap, extra_log_decay):
    input_gate_value = forget_floor_gap[None, :] * jax.nn.sigmoid(
        -forget_logits.astype(jnp.float32)
    )
    forget_log_rate = jnp.log1p(-input_gate_value) + extra_log_decay
    scaled_values = query.astype(jnp.float32) * HEAD_K ** (-0.5)
    return (scaled_values, input_gate_value, written_values.astype(jnp.float32), forget_log_rate)


def gate_out(recurrent, output_gate_logits, head_norm_gain):
    normal_part = recurrent * lax.rsqrt(
        jnp.mean(recurrent * recurrent, axis=-1, keepdims=True) + norm_eps
    )
    gating = jax.nn.silu(output_gate_logits.astype(jnp.float32)).reshape(recurrent.shape)
    mixed = normal_part * head_norm_gain * gating
    return mixed.reshape(recurrent.shape[0], -1).astype(jnp.bfloat16)


def normalize(stream, gain):
    scaled_rows = stream * lax.rsqrt(jnp.mean(stream * stream, axis=-1, keepdims=True) + norm_eps)
    return (scaled_rows * gain).astype(jnp.bfloat16)


def chain_states(earlier, later):
    return (earlier[0] + later[0], jnp.exp(later[0])[:, :, None] * earlier[1] + later[1])


def gathered_plan(
    query,
    forget_logits,
    written_values,
    output_gate_logits,
    forget_floor_gap,
    extra_log_decay,
    head_norm_gain,
    output_weight,
    residual,
    mixer_norm_gain,
    mixer_up_weight,
    mixer_down_weight,
):
    scaled_values, input_gate_value, value_rows, forget_log_rate = prepare_inputs(
        query, forget_logits, written_values, forget_floor_gap, extra_log_decay
    )
    row_count, local_width = query.shape
    head_count = local_width // HEAD_K
    start_state = jnp.zeros((head_count, HEAD_K, HEAD_V), jnp.float32)
    local_state, blocked = lax.scan(
        block_update,
        start_state,
        (
            to_blocks(scaled_values, HEAD_K),
            to_blocks(input_gate_value, HEAD_K),
            to_blocks(value_rows, HEAD_V),
            to_blocks(forget_log_rate, HEAD_K),
        ),
    )
    log_total = jnp.sum(forget_log_rate, axis=0).reshape(head_count, HEAD_K)
    arrived_state = carried_in(
        (log_total, local_state),
        "sp",
        chain_states,
        (jnp.zeros_like(log_total), jnp.zeros_like(local_state)),
    )
    running = jnp.cumsum(forget_log_rate, axis=0)
    reached_state = (scaled_values * jnp.exp(running)).reshape(row_count, head_count, HEAD_K)
    carried_over = jnp.einsum(
        "cja,jae->cje", reached_state, arrived_state[1], precision=highest_precision
    )
    mixed = gate_out(from_blocks(blocked) + carried_over, output_gate_logits, head_norm_gain)
    stream_own = lax.psum_scatter(
        jnp.dot(mixed, output_weight, preferred_element_type=jnp.float32).astype(jnp.bfloat16),
        "tp",
        scatter_dimension=0,
        tiled=True,
    ).astype(jnp.float32) + residual.astype(jnp.float32)
    normed = lax.all_gather(normalize(stream_own, mixer_norm_gain), "tp", axis=0, tiled=True)
    columns = normed
    lifted = jnp.dot(
        columns,
        lax.all_gather(mixer_up_weight, "sp", axis=0, tiled=True),
        preferred_element_type=jnp.float32,
    )
    hidden = jnp.square(jax.nn.relu(lifted)).astype(jnp.bfloat16)
    columns = hidden
    projected = jnp.dot(
        columns,
        lax.all_gather(mixer_down_weight, "sp", axis=0, tiled=True),
        preferred_element_type=jnp.float32,
    )
    mlp_own = lax.psum_scatter(
        projected.astype(jnp.bfloat16), "tp", scatter_dimension=0, tiled=True
    ).astype(jnp.float32)
    return (stream_own + mlp_own).astype(jnp.bfloat16)


def solution(mesh):
    specs = dict(
        mesh=mesh,
        in_specs=(
            P("sp", "tp"),
            P("sp", "tp"),
            P("sp", "tp"),
            P("sp", "tp"),
            P("tp"),
            P("sp", "tp"),
            P(),
            P("tp", None),
            P(("sp", "tp"), None),
            P(),
            P("sp", "tp"),
            P(("tp", "sp"), None),
        ),
        out_specs=P(("sp", "tp"), None),
        check_vma=False,
    )
    n_sp, n_tp = mesh.shape["sp"], mesh.shape["tp"]
    n_b, n_y = 2, 2
    n_a, n_c = n_sp // n_b, n_tp // n_y
    if n_sp % n_b or n_tp % n_y or n_a > 4 or n_c != 2:
        return jax.shard_map(gathered_plan, **specs)

    def flat(a, b, y, c):
        return (a % n_a * n_b + b % n_b) * n_tp + y % n_y * n_c + c % n_c

    def send(x, a=0, b=0, y=0, c=0, cyclic=True):
        pairs = [
            (flat(i, j, k, m), flat(i + a, j + b, k + y, m + c))
            for i in range(n_a)
            for j in range(n_b)
            for k in range(n_y)
            for m in range(n_c)
            if cyclic or i + a < n_a
        ]
        return lax.ppermute(x, AXES, pairs)

    def on_device(
        query,
        forget_logits,
        written_values,
        output_gate_logits,
        forget_floor_gap,
        extra_log_decay,
        head_norm_gain,
        output_weight,
        residual,
        mixer_norm_gain,
        mixer_up_weight,
        mixer_down_weight,
    ):
        sp, tp = lax.axis_index("sp"), lax.axis_index("tp")
        a, b, y, c = sp // n_b, sp % n_b, tp // n_c, tp % n_c
        place = jnp.stack([a, b, y, c]).astype(jnp.int32)
        rows, width = query.shape
        model = output_weight.shape[1]
        own = residual.shape[0]
        heads = width // HEAD

        packed_shape = jax.ShapeDtypeStruct((heads * HEAD + 16, HEAD), BF16)
        gate, cum, packed = kernel_call(
            gates_body,
            [
                jax.ShapeDtypeStruct((rows, width), F32),
                jax.ShapeDtypeStruct((rows, width), F32),
                packed_shape,
            ],
            n_in=4,
        )(forget_logits, written_values, forget_floor_gap[None, :], extra_log_decay)
        later_weight, packed = lax.optimization_barrier((mixer_up_weight, packed))

        up_rows, up_cols = mixer_up_weight.shape
        piece = up_cols // n_a
        mine = []
        for d in range(n_a):
            source = mixer_up_weight if d == n_a // 2 else later_weight
            cut = lax.dynamic_slice(source, (0, (a + d) % n_a * piece), (up_rows, piece))
            mine.append(cut if d == 0 else send(cut, a=d))
        groups = [mine[0::2], mine[1::2]]
        up_x, up_y, up_xy = [], [], []
        for g, members in enumerate(groups):
            joined = jnp.concatenate(members, axis=0)
            up_x.append(send(joined, b=1))
            up_y.append(send(joined, y=1))
            if g:
                up_xy.append(send(up_y[g], b=1))
            else:
                up_xy.append(send(up_x[g], y=1))
        up_arrays = mine + up_x + up_y + up_xy

        def up_places(refs):
            found = [(refs[e], 0) for e in range(n_a)]
            for k in range(3):
                found += [
                    (refs[n_a + 2 * k + e % 2], e // 2 * up_rows) for e in range(n_a)
                ]
            return found

        half = mixer_down_weight.shape[0] // 2
        down_x = send(mixer_down_weight, b=1)
        down_y = send(mixer_down_weight, y=1)
        down_xy = [send(down_x[:half], y=1), send(down_y[half:], b=1)]
        down_arrays = [mixer_down_weight, down_x, down_y] + down_xy

        beside = send(packed, b=1)
        pair = kernel_call(pair_body, packed_shape, smem=1, n_in=3)(place, packed, beside)
        states = [send(pair, a=d, cyclic=False) for d in range(1, n_a)]
        local = kernel_call(
            local_body, jax.ShapeDtypeStruct((rows, width), F32), n_in=4
        )(query, gate, cum, written_values)
        first, second, away = kernel_call(
            lambda *refs: mix_body(n_c, *refs),
            [
                jax.ShapeDtypeStruct((own, model), F32),
                jax.ShapeDtypeStruct((own, model), F32),
                jax.ShapeDtypeStruct((n_y * own, model), BF16),
            ],
            scratch=[pltpu.VMEM((rows, width), F32)],
            smem=1,
            n_in=8 + len(states),
        )(
            place,
            query,
            cum,
            local,
            output_gate_logits,
            head_norm_gain[None, :],
            output_weight,
            beside,
            *states,
        )
        got = send(away, c=1)
        other = send((second + got[own:].astype(F32)).astype(BF16), y=1)
        stream, normed = kernel_call(
            norm_body,
            [
                jax.ShapeDtypeStruct((own, model), F32),
                jax.ShapeDtypeStruct((n_sp, own, model // n_sp), BF16),
            ],
            n_in=5,
        )(first, got, other, residual, mixer_norm_gain[None, :])

        line = [normed] + [send(normed, a=d) for d in range(1, n_a)]
        toks = line + [send(u, c=1) for u in line]
        group = n_a * own
        part = model // 2
        sizes = [
            jax.ShapeDtypeStruct((group, part), F32),
            jax.ShapeDtypeStruct((group, part), BF16),
        ]
        units = n_y * piece

        def mixer(*refs):
            n_tok = len(toks)
            ups = up_places(refs[1 + n_tok : 1 + n_tok + len(up_arrays)])
            rest = refs[1 + n_tok + len(up_arrays) :]
            mixer_body(n_a, n_c, *refs[: 1 + n_tok], *ups, *rest)

        keep0, away0, hidden = kernel_call(
            mixer,
            sizes + [jax.ShapeDtypeStruct((n_c * group, units), BF16)],
            scratch=[
                pltpu.VMEM((n_c * group, model), BF16),
                pltpu.VMEM((model, piece), BF16),
                pltpu.VMEM((n_y * n_b, n_c * group, piece // n_b), BF16),
                pltpu.VMEM((units, part), BF16),
            ],
            smem=1,
            n_in=1 + len(toks) + len(up_arrays) + len(down_arrays),
            mib=34,
        )(place, *toks, *up_arrays, *down_arrays)
        got0 = send(away0, c=1)
        keep1, away1 = kernel_call(
            lambda *refs: mixer_rest_body(group, *refs),
            sizes,
            scratch=[pltpu.VMEM((units, part), BF16)],
            n_in=1 + len(down_arrays),
        )(hidden, *down_arrays)
        got1 = send(away1, c=1)
        halves = []
        for k, (keep, got) in enumerate([(keep0, got0), (keep1, got1)]):
            outs = kernel_call(
                fold_body, [jax.ShapeDtypeStruct((own, part), BF16)] * (n_a - 1), n_in=2
            )(keep, got)
            total = stream[:, k * part : (k + 1) * part] + keep[:own] + got[:own].astype(F32)
            for d in range(1, n_a):
                total = total + send(outs[d - 1], a=n_a - d).astype(F32)
            halves.append(total.astype(BF16))
        return jnp.concatenate(halves, axis=1)


    return jax.shard_map(on_device, **specs)
```

profile of v0, /device:TPU:0, one launch (start us, length us, event | category | flops | bytes accessed | tf_op | source)
XLA Modules:
  0.0 156.0 jit_solution(12580686023924922372)
XLA Ops:
  0.0 1.0 copy-done.6
  1.0 0.9 copy-done.10
  1.9 0.9 copy-done.12
  2.9 0.7 copy-done.15
  3.5 1.3 shard_map.118
  4.9 3.0 %collective-permute-start = (bf16[272,128]{1,0:T(8,128)(2,1)S(1)}, bf16[272,128]{1,0:T(8,128)(2,1)S(1)}, u32[]{:S(2)}, u32[]{:S(2)}) collective-permute-start(bf16[272,128]{1,0:T(8,128)(2,1)S(1)} %get-tuple-element.29.mine), channel_id=1, source_target_pairs={{0,4},{1,5},{2,6},{3,7},{4,0},{5,1},{6,2},{7,3},{8,12},{9,13},{10,... | collective-permute-start | bytes 208904 | tf_op jit(solution)/shard_map/ppermute | solution.py:434
  8.0 2.2 %collective-permute-done.theirs.refs_7_ = bf16[272,128]{1,0:T(8,128)(2,1)S(1)} collective-permute-done((bf16[272,128]{1,0:T(8,128)(2,1)S(1)}, bf16[272,128]{1,0:T(8,128)(2,1)S(1)}, u32[]{:S(2)}, u32[]{:S(2)}) %collective-permute-start) | collective-permute-done | bytes 69664 | tf_op jit(solution)/shard_map/ppermute | solution.py:434
  10.2 0.7 shard_map.120
  10.8 6.0 %collective-permute-start.3 = (bf16[272,128]{1,0:T(8,128)(2,1)S(1)}, bf16[272,128]{1,0:T(8,128)(2,1)S(1)}, u32[]{:S(2)}, u32[]{:S(2)}) collective-permute-start(bf16[272,128]{1,0:T(8,128)(2,1)S(1)} %shard_map.120), channel_id=1, source_target_pairs={{0,24},{1,25},{2,26},{3,27},{4,28},{5,29},{6,30},{7,31}} | collective-permute-start | bytes 208904 | tf_op jit(solution)/shard_map/ppermute | solution.py:434
  16.9 1.3 collective-permute-start.2
  18.2 2.5 %collective-permute-start.1 = (bf16[272,128]{1,0:T(8,128)(2,1)S(1)}, bf16[272,128]{1,0:T(8,128)(2,1)S(1)}, u32[]{:S(2)}, u32[]{:S(2)}) collective-permute-start(bf16[272,128]{1,0:T(8,128)(2,1)S(1)} %shard_map.120), channel_id=1, source_target_pairs={{0,8},{1,9},{2,10},{3,11},{4,12},{5,13},{6,14},{7,15},{8,16},{9,17... | collective-permute-start | bytes 208904 | tf_op jit(solution)/shard_map/ppermute | solution.py:434
  20.7 0.9 copy-done.7
  21.6 0.9 copy-done.8
  22.5 3.4 %shard_map.119.refs_3_ = f32[256,256]{1,0:T(8,128)S(1)} custom-call(bf16[256,256]{1,0:T(8,128)(2,1)S(1)} %copy-done.8, f32[256,256]{1,0:T(8,128)S(1)} %get-tuple-element.27.gate, f32[256,256]{1,0:T(8,128)S(1)} %get-tuple-element.26.cum.refs_2_, bf16[256,256]{1,0:T(8,128)(2,1)S(1)} %copy-done.7), custom_call_target="tpu_custom_call" | custom-call | tf_op jit(solution)/shard_map/pallas_call | solution.py:506
  26.1 0.6 copy-done.16
  26.6 2.4 %shard_map.121 = (f32[64,2048]{1,0:T(8,128)S(1)}, f32[64,2048]{1,0:T(8,128)S(1)}, bf16[128,2048]{1,0:T(8,128)(2,1)}) custom-call(s32[4]{0:T(128)S(1)} %pad_add_fusion.place.refs_0_, bf16[256,256]{1,0:T(8,128)(2,1)S(1)} %copy-done.9, f32[256,256]{1,0:T(8,128)S(1)} %get-tuple-element.26.cum.refs_2_, f32[256,256]{1,0:T(8,128)S(1)} %shard_map.119.refs_3_, ...), custom_call_target="tpu_custom_call" | custom-call | tf_op jit(solution)/shard_map/pallas_call | solution.py:509
  29.1 0.9 constant_dynamic-slice_fusion
  30.0 0.1 copy-done.2
  30.1 0.2 copy-done.4
  30.3 3.8 %collective-permute-start.15 = (bf16[256,512]{1,0:T(8,128)(2,1)}, bf16[256,512]{1,0:T(8,128)(2,1)}, u32[]{:S(2)}, u32[]{:S(2)}) collective-permute-start(bf16[256,512]{1,0:T(8,128)(2,1)} %get-tuple-element.47), channel_id=1, source_target_pairs={{0,24},{1,25},{2,26},{3,27},{4,28},{5,29},{6,30},{7,31},{8,0},{9,1... | collective-permute-start | bytes 786440 | tf_op jit(solution)/shard_map/ppermute | solution.py:434
  34.1 1.5 collective-permute-start.23
  35.6 1.5 collective-permute-start.22
  37.1 1.0 constant_dynamic-slice_fusion.1
  38.1 3.5 %collective-permute-done.13.refs_10_ = bf16[256,512]{1,0:T(8,128)(2,1)} collective-permute-done((bf16[256,512]{1,0:T(8,128)(2,1)}, bf16[256,512]{1,0:T(8,128)(2,1)}, u32[]{:S(2)}, u32[]{:S(2)}) %collective-permute-start.13) | collective-permute-done | bytes 262176 | tf_op jit(solution)/shard_map/ppermute | solution.py:434
  41.6 1.0 constant_dynamic-update-slice_fusion.1
  42.6 4.2 %collective-permute-done.15.refs_12_ = bf16[256,512]{1,0:T(8,128)(2,1)} collective-permute-done((bf16[256,512]{1,0:T(8,128)(2,1)}, bf16[256,512]{1,0:T(8,128)(2,1)}, u32[]{:S(2)}, u32[]{:S(2)}) %collective-permute-start.15) | collective-permute-done | bytes 262176 | tf_op jit(solution)/shard_map/ppermute | solution.py:434
  46.7 1.0 constant_dynamic-update-slice_fusion
  47.7 1.6 %collective-permute-start.19 = (bf16[512,512]{1,0:T(8,128)(2,1)S(1)}, bf16[512,512]{1,0:T(8,128)(2,1)S(1)}, u32[]{:S(2)}, u32[]{:S(2)}) collective-permute-start(bf16[512,512]{1,0:T(8,128)(2,1)S(1)} %constant_dynamic-update-slice_fusion), channel_id=1, source_target_pairs={{0,2},{1,3},{2,0},{3,1},{4,6},{5,7},{6,4},{7,5},{8,10},{9,11},{10,... | collective-permute-start | bytes 1572872 | tf_op jit(solution)/shard_map/ppermute | solution.py:434
  49.3 1.0 add_convert_fusion
  50.3 0.6 collective-permute-start.5
  50.9 4.4 %collective-permute-done.14.refs_11_ = bf16[256,512]{1,0:T(8,128)(2,1)S(1)} collective-permute-done((bf16[256,512]{1,0:T(8,128)(2,1)S(1)}, bf16[256,512]{1,0:T(8,128)(2,1)S(1)}, u32[]{:S(2)}, u32[]{:S(2)}) %collective-permute-start.14) | collective-permute-done | bytes 262176 | tf_op jit(solution)/shard_map/ppermute | solution.py:434
  55.3 1.5 collective-permute-start.17
  56.8 14.5 %collective-permute-done.19.refs_16_ = bf16[512,512]{1,0:T(8,128)(2,1)S(1)} collective-permute-done((bf16[512,512]{1,0:T(8,128)(2,1)S(1)}, bf16[512,512]{1,0:T(8,128)(2,1)S(1)}, u32[]{:S(2)}, u32[]{:S(2)}) %collective-permute-start.19) | collective-permute-done | bytes 524320 | tf_op jit(solution)/shard_map/ppermute | solution.py:434
  71.3 1.5 collective-permute-start.18
  72.9 4.1 %collective-permute-done.5.arrived = bf16[64,2048]{1,0:T(8,128)(2,1)S(1)} collective-permute-done((bf16[64,2048]{1,0:T(8,128)(2,1)S(1)}, bf16[64,2048]{1,0:T(8,128)(2,1)S(1)}, u32[]{:S(2)}, u32[]{:S(2)}) %collective-permute-start.5) | collective-permute-done | bytes 262176 | tf_op jit(solution)/shard_map/ppermute | solution.py:434
  77.0 1.5 collective-permute-start.16
  78.5 1.3 shard_map.122
  79.8 7.1 %collective-permute-done.18.refs_15_ = bf16[512,512]{1,0:T(8,128)(2,1)S(1)} collective-permute-done((bf16[512,512]{1,0:T(8,128)(2,1)S(1)}, bf16[512,512]{1,0:T(8,128)(2,1)S(1)}, u32[]{:S(2)}, u32[]{:S(2)}) %collective-permute-start.18) | collective-permute-done | bytes 524320 | tf_op jit(solution)/shard_map/ppermute | solution.py:434
  86.9 1.5 collective-permute-start.21
  88.4 1.5 collective-permute-start.20
  89.9 0.5 collective-permute-start.8
  90.4 1.6 %collective-permute-start.6 = (bf16[8,64,256]{2,1,0:T(8,128)(2,1)S(1)}, bf16[8,64,256]{2,1,0:T(8,128)(2,1)S(1)}, u32[]{:S(2)}, u32[]{:S(2)}) collective-permute-start(bf16[8,64,256]{2,1,0:T(8,128)(2,1)S(1)} %get-tuple-element.34.refs_1_), channel_id=1, source_target_pairs={{0,8},{1,9},{2,10},{3,11},{4,12},{5,13},{6,14},{7,15},{8,16},{9,17... | collective-permute-start | bytes 786440 | tf_op jit(solution)/shard_map/ppermute | solution.py:434
  92.1 5.9 %collective-permute-done.8.refs_4_ = bf16[8,64,256]{2,1,0:T(8,128)(2,1)S(1)} collective-permute-done((bf16[8,64,256]{2,1,0:T(8,128)(2,1)S(1)}, bf16[8,64,256]{2,1,0:T(8,128)(2,1)S(1)}, u32[]{:S(2)}, u32[]{:S(2)}) %collective-permute-start.8) | collective-permute-done | bytes 262176 | tf_op jit(solution)/shard_map/ppermute | solution.py:434
  98.0 1.3 collective-permute-start.25
  99.3 12.3 %collective-permute-done.7.refs_3_ = bf16[8,64,256]{2,1,0:T(8,128)(2,1)S(1)} collective-permute-done((bf16[8,64,256]{2,1,0:T(8,128)(2,1)S(1)}, bf16[8,64,256]{2,1,0:T(8,128)(2,1)S(1)}, u32[]{:S(2)}, u32[]{:S(2)}) %collective-permute-start.7) | collective-permute-done | bytes 262176 | tf_op jit(solution)/shard_map/ppermute | solution.py:434
  111.5 0.5 collective-permute-start.24
  112.1 0.5 collective-permute-start.11
  112.6 0.9 collective-permute-done.12.refs_8_
  113.6 0.4 collective-permute-done.11.refs_7_
  114.0 0.4 collective-permute-done.10.refs_6_
  114.3 8.5 %collective-permute-done.24.refs_22_.refs_4_ = bf16[128,2048]{1,0:T(8,128)(2,1)S(1)} collective-permute-done((bf16[128,2048]{1,0:T(8,128)(2,1)S(1)}, bf16[128,2048]{1,0:T(8,128)(2,1)S(1)}, u32[]{:S(2)}, u32[]{:S(2)}) %collective-permute-start.24) | collective-permute-done | bytes 524320 | tf_op jit(solution)/shard_map/ppermute | solution.py:434
  122.9 4.7 %shard_map.123 = (f32[256,1024]{1,0:T(8,128)S(1)}, bf16[256,1024]{1,0:T(8,128)(2,1)S(1)}, bf16[512,1024]{1,0:T(8,128)(2,1)S(1)}) custom-call(s32[4]{0:T(128)S(1)} %pad_add_fusion.place.refs_0_, bf16[8,64,256]{2,1,0:T(8,128)(2,1)S(1)} %get-tuple-element.34.refs_1_, bf16[8,64,256]{2,1,0:T(8,128)(2,1)S(1)} %collective-permute-done.6.refs_2_, ...), custom_call_target="tpu_custom_call" | custom-call | tf_op jit(solution)/shard_map/pallas_call | solution.py:557
  127.6 1.3 shard_map.125
  128.9 0.5 collective-permute-start.26
  129.4 1.4 collective-permute-done.30.got
  130.9 1.1 collective-permute-start.31
  132.0 1.0 collective-permute-start.33
  133.1 2.9 %collective-permute-start.27 = (bf16[64,1024]{1,0:T(8,128)(2,1)S(1)}, bf16[64,1024]{1,0:T(8,128)(2,1)S(1)}, u32[]{:S(2)}, u32[]{:S(2)}) collective-permute-start(bf16[64,1024]{1,0:T(8,128)(2,1)S(1)} %get-tuple-element.38), channel_id=1, source_target_pairs={{0,24},{1,25},{2,26},{3,27},{4,28},{5,29},{6,30},{7,31},{8,0},{9,1... | collective-permute-start | bytes 393224 | tf_op jit(solution)/shard_map/ppermute | solution.py:434
  135.9 1.1 collective-permute-start.28
  137.0 1.1 collective-permute-done.31
  138.2 7.3 %collective-permute-done.32 = bf16[64,1024]{1,0:T(8,128)(2,1)S(1)} collective-permute-done((bf16[64,1024]{1,0:T(8,128)(2,1)S(1)}, bf16[64,1024]{1,0:T(8,128)(2,1)S(1)}, u32[]{:S(2)}, u32[]{:S(2)}) %collective-permute-start.32) | collective-permute-done | bytes 131104 | tf_op jit(solution)/shard_map/ppermute | solution.py:434
  145.4 9.6 %collective-permute-done.28 = bf16[64,1024]{1,0:T(8,128)(2,1)S(1)} collective-permute-done((bf16[64,1024]{1,0:T(8,128)(2,1)S(1)}, bf16[64,1024]{1,0:T(8,128)(2,1)S(1)}, u32[]{:S(2)}, u32[]{:S(2)}) %collective-permute-start.28) | collective-permute-done | bytes 131104 | tf_op jit(solution)/shard_map/ppermute | solution.py:434
  155.0 0.2 add_convert_fusion.2
  155.3 0.7 pad_maximum_fusion.1
  (60 shorter events, 0.7 us)
Async XLA Ops:
  0.0 26.0 %copy-start.1 = (bf16[256,2048]{1,0:T(8,128)(2,1)S(1)}, bf16[256,2048]{1,0:T(8,128)(2,1)}, u32[]{:S(2)}) copy-start(bf16[256,2048]{1,0:T(8,128)(2,1)} %refs_6_.1) | copy-start | bytes 3145732
  0.0 1.0 copy-start.6
  1.0 0.9 copy-start.10
  1.9 0.9 copy-start.12
  2.9 0.7 copy-start.15
  4.9 5.3 %collective-permute-start = (bf16[272,128]{1,0:T(8,128)(2,1)S(1)}, bf16[272,128]{1,0:T(8,128)(2,1)S(1)}, u32[]{:S(2)}, u32[]{:S(2)}) collective-permute-start(bf16[272,128]{1,0:T(8,128)(2,1)S(1)} %get-tuple-element.29.mine), channel_id=1, source_target_pairs={{0,4},{1,5},{2,6},{3,7},{4,0},{5,1},{6,2},{7,3},{8,12},{9,13},{10,... | collective-permute-start | bytes 208904 | tf_op jit(solution)/shard_map/ppermute | solution.py:434
  10.8 15.2 %collective-permute-start.3 = (bf16[272,128]{1,0:T(8,128)(2,1)S(1)}, bf16[272,128]{1,0:T(8,128)(2,1)S(1)}, u32[]{:S(2)}, u32[]{:S(2)}) collective-permute-start(bf16[272,128]{1,0:T(8,128)(2,1)S(1)} %shard_map.120), channel_id=1, source_target_pairs={{0,24},{1,25},{2,26},{3,27},{4,28},{5,29},{6,30},{7,31}} | collective-permute-start | bytes 208904 | tf_op jit(solution)/shard_map/ppermute | solution.py:434
  16.9 9.1 %collective-permute-start.2 = (bf16[272,128]{1,0:T(8,128)(2,1)S(1)}, bf16[272,128]{1,0:T(8,128)(2,1)S(1)}, u32[]{:S(2)}, u32[]{:S(2)}) collective-permute-start(bf16[272,128]{1,0:T(8,128)(2,1)S(1)} %shard_map.120), channel_id=1, source_target_pairs={{0,16},{1,17},{2,18},{3,19},{4,20},{5,21},{6,22},{7,23},{8,24},{9,... | collective-permute-start | bytes 208904 | tf_op jit(solution)/shard_map/ppermute | solution.py:434
  18.2 7.8 %collective-permute-start.1 = (bf16[272,128]{1,0:T(8,128)(2,1)S(1)}, bf16[272,128]{1,0:T(8,128)(2,1)S(1)}, u32[]{:S(2)}, u32[]{:S(2)}) collective-permute-start(bf16[272,128]{1,0:T(8,128)(2,1)S(1)} %shard_map.120), channel_id=1, source_target_pairs={{0,8},{1,9},{2,10},{3,11},{4,12},{5,13},{6,14},{7,15},{8,16},{9,17... | collective-permute-start | bytes 208904 | tf_op jit(solution)/shard_map/ppermute | solution.py:434
  20.7 0.9 copy-start.7
  21.6 0.9 copy-start.8
  22.5 3.5 %copy-start.9 = (bf16[256,256]{1,0:T(8,128)(2,1)S(1)}, bf16[256,256]{1,0:T(8,128)(2,1)}, u32[]{:S(2)}) copy-start(bf16[256,256]{1,0:T(8,128)(2,1)} %refs_1_.2) | copy-start | bytes 393220
  22.5 3.5 %copy-start.13 = (bf16[256,256]{1,0:T(8,128)(2,1)S(1)}, bf16[256,256]{1,0:T(8,128)(2,1)}, u32[]{:S(2)}) copy-start(bf16[256,256]{1,0:T(8,128)(2,1)} %refs_4_.1) | copy-start | bytes 393220
  26.0 0.7 copy-start.16
  26.6 2.5 %copy-start.17 = (bf16[256,2048]{1,0:T(8,128)(2,1)S(1)}, bf16[256,2048]{1,0:T(8,128)(2,1)}, u32[]{:S(2)}) copy-start(bf16[256,2048]{1,0:T(8,128)(2,1)} %param.22) | copy-start | bytes 3145732
  29.1 1.0 copy-start.2
  29.1 1.1 copy-start.4
  29.1 5.0 %copy-start = (bf16[256,2048]{1,0:T(8,128)(2,1)S(1)}, bf16[256,2048]{1,0:T(8,128)(2,1)}, u32[]{:S(2)}) copy-start(bf16[256,2048]{1,0:T(8,128)(2,1)} %refs_1_.3) | copy-start | bytes 3145732
  29.1 20.2 %collective-permute-start.4 = (bf16[128,2048]{1,0:T(8,128)(2,1)}, bf16[128,2048]{1,0:T(8,128)(2,1)}, u32[]{:S(2)}, u32[]{:S(2)}) collective-permute-start(bf16[128,2048]{1,0:T(8,128)(2,1)} %get-tuple-element.31), channel_id=1, source_target_pairs={{0,1},{1,0},{2,3},{3,2},{4,5},{5,4},{6,7},{7,6},{8,9},{9,8},{10,11... | collective-permute-start | bytes 1572872 | tf_op jit(solution)/shard_map/ppermute | solution.py:434
  30.2 11.3 %collective-permute-start.13 = (bf16[256,512]{1,0:T(8,128)(2,1)}, bf16[256,512]{1,0:T(8,128)(2,1)}, u32[]{:S(2)}, u32[]{:S(2)}) collective-permute-start(bf16[256,512]{1,0:T(8,128)(2,1)} %get-tuple-element.48), channel_id=1, source_target_pairs={{0,8},{1,9},{2,10},{3,11},{4,12},{5,13},{6,14},{7,15},{8,16},{9,17... | collective-permute-start | bytes 786440 | tf_op jit(solution)/shard_map/ppermute | solution.py:434
  30.3 16.5 %collective-permute-start.15 = (bf16[256,512]{1,0:T(8,128)(2,1)}, bf16[256,512]{1,0:T(8,128)(2,1)}, u32[]{:S(2)}, u32[]{:S(2)}) collective-permute-start(bf16[256,512]{1,0:T(8,128)(2,1)} %get-tuple-element.47), channel_id=1, source_target_pairs={{0,24},{1,25},{2,26},{3,27},{4,28},{5,29},{6,30},{7,31},{8,0},{9,1... | collective-permute-start | bytes 786440 | tf_op jit(solution)/shard_map/ppermute | solution.py:434
  34.1 55.8 %collective-permute-start.23 = (bf16[256,2048]{1,0:T(8,128)(2,1)S(1)}, bf16[256,2048]{1,0:T(8,128)(2,1)S(1)}, u32[]{:S(2)}, u32[]{:S(2)}) collective-permute-start(bf16[256,2048]{1,0:T(8,128)(2,1)S(1)} %copy-done), channel_id=1, source_target_pairs={{0,2},{1,3},{2,0},{3,1},{4,6},{5,7},{6,4},{7,5},{8,10},{9,11},{10,... | collective-permute-start | bytes 3145736 | tf_op jit(solution)/shard_map/ppermute | solution.py:434
  35.6 54.8 %collective-permute-start.22 = (bf16[256,2048]{1,0:T(8,128)(2,1)S(1)}, bf16[256,2048]{1,0:T(8,128)(2,1)S(1)}, u32[]{:S(2)}, u32[]{:S(2)}) collective-permute-start(bf16[256,2048]{1,0:T(8,128)(2,1)S(1)} %copy-done), channel_id=1, source_target_pairs={{0,4},{1,5},{2,6},{3,7},{4,0},{5,1},{6,2},{7,3},{8,12},{9,13},{10,... | collective-permute-start | bytes 3145736 | tf_op jit(solution)/shard_map/ppermute | solution.py:434
  38.0 11.3 %copy-start.5 = (f32[64,2048]{1,0:T(8,128)S(1)}, f32[64,2048]{1,0:T(8,128)}, u32[]{:S(2)}) copy-start(f32[64,2048]{1,0:T(8,128)} %copy-done.4) | copy-start | bytes 1572868
  41.6 13.7 %collective-permute-start.14 = (bf16[256,512]{1,0:T(8,128)(2,1)S(1)}, bf16[256,512]{1,0:T(8,128)(2,1)S(1)}, u32[]{:S(2)}, u32[]{:S(2)}) collective-permute-start(bf16[256,512]{1,0:T(8,128)(2,1)S(1)} %constant_dynamic-slice_fusion.1), channel_id=1, source_target_pairs={{0,16},{1,17},{2,18},{3,19},{4,20},{5,21},{6,22},{7,23},{8,24},{9,... | collective-permute-start | bytes 786440 | tf_op jit(solution)/shard_map/ppermute | solution.py:434
  47.7 23.6 %collective-permute-start.19 = (bf16[512,512]{1,0:T(8,128)(2,1)S(1)}, bf16[512,512]{1,0:T(8,128)(2,1)S(1)}, u32[]{:S(2)}, u32[]{:S(2)}) collective-permute-start(bf16[512,512]{1,0:T(8,128)(2,1)S(1)} %constant_dynamic-update-slice_fusion), channel_id=1, source_target_pairs={{0,2},{1,3},{2,0},{3,1},{4,6},{5,7},{6,4},{7,5},{8,10},{9,11},{10,... | collective-permute-start | bytes 1572872 | tf_op jit(solution)/shard_map/ppermute | solution.py:434
  50.3 26.6 %collective-permute-start.5 = (bf16[64,2048]{1,0:T(8,128)(2,1)S(1)}, bf16[64,2048]{1,0:T(8,128)(2,1)S(1)}, u32[]{:S(2)}, u32[]{:S(2)}) collective-permute-start(bf16[64,2048]{1,0:T(8,128)(2,1)S(1)} %add_convert_fusion), channel_id=1, source_target_pairs={{0,2},{1,3},{2,0},{3,1},{4,6},{5,7},{6,4},{7,5},{8,10},{9,11},{10,... | collective-permute-start | bytes 786440 | tf_op jit(solution)/shard_map/ppermute | solution.py:434
  55.3 24.4 %collective-permute-start.17 = (bf16[512,512]{1,0:T(8,128)(2,1)S(1)}, bf16[512,512]{1,0:T(8,128)(2,1)S(1)}, u32[]{:S(2)}, u32[]{:S(2)}) collective-permute-start(bf16[512,512]{1,0:T(8,128)(2,1)S(1)} %constant_dynamic-update-slice_fusion), channel_id=1, source_target_pairs={{0,4},{1,5},{2,6},{3,7},{4,0},{5,1},{6,2},{7,3},{8,12},{9,13},{10,... | collective-permute-start | bytes 1572872 | tf_op jit(solution)/shard_map/ppermute | solution.py:434
  56.8 21.6 %copy-start.3 = (f32[64,2048]{1,0:T(8,128)S(1)}, f32[64,2048]{1,0:T(8,128)}, u32[]{:S(2)}) copy-start(f32[64,2048]{1,0:T(8,128)} %copy-done.2) | copy-start | bytes 1572868
  56.8 21.6 %copy-start.11 = (bf16[64,2048]{1,0:T(8,128)(2,1)S(1)}, bf16[64,2048]{1,0:T(8,128)(2,1)}, u32[]{:S(2)}) copy-start(bf16[64,2048]{1,0:T(8,128)(2,1)} %residual.1) | copy-start | bytes 786436
  56.8 21.6 %copy-start.14 = (f32[2048]{0:T(1024)S(1)}, f32[2048]{0:T(1024)}, u32[]{:S(2)}) copy-start(f32[2048]{0:T(1024)} %param.21) | copy-start | bytes 24580
  71.3 15.6 %collective-permute-start.18 = (bf16[512,512]{1,0:T(8,128)(2,1)S(1)}, bf16[512,512]{1,0:T(8,128)(2,1)S(1)}, u32[]{:S(2)}, u32[]{:S(2)}) collective-permute-start(bf16[512,512]{1,0:T(8,128)(2,1)S(1)} %pad_maximum_fusion), channel_id=1, source_target_pairs={{0,2},{1,3},{2,0},{3,1},{4,6},{5,7},{6,4},{7,5},{8,10},{9,11},{10,... | collective-permute-start | bytes 1572872 | tf_op jit(solution)/shard_map/ppermute | solution.py:434
  77.0 11.4 %collective-permute-start.16 = (bf16[512,512]{1,0:T(8,128)(2,1)S(1)}, bf16[512,512]{1,0:T(8,128)(2,1)S(1)}, u32[]{:S(2)}, u32[]{:S(2)}) collective-permute-start(bf16[512,512]{1,0:T(8,128)(2,1)S(1)} %pad_maximum_fusion), channel_id=1, source_target_pairs={{0,4},{1,5},{2,6},{3,7},{4,0},{5,1},{6,2},{7,3},{8,12},{9,13},{10,... | collective-permute-start | bytes 1572872 | tf_op jit(solution)/shard_map/ppermute | solution.py:434
  79.7 10.7 %collective-permute-start.9 = (bf16[8,64,256]{2,1,0:T(8,128)(2,1)S(1)}, bf16[8,64,256]{2,1,0:T(8,128)(2,1)S(1)}, u32[]{:S(2)}, u32[]{:S(2)}) collective-permute-start(bf16[8,64,256]{2,1,0:T(8,128)(2,1)S(1)} %get-tuple-element.34.refs_1_), channel_id=1, source_target_pairs={{0,1},{1,0},{2,3},{3,2},{4,5},{5,4},{6,7},{7,6},{8,9},{9,8},{10,11... | collective-permute-start | bytes 786440 | tf_op jit(solution)/shard_map/ppermute | solution.py:434
  86.9 25.2 %collective-permute-start.21 = (bf16[512,512]{1,0:T(8,128)(2,1)S(1)}, bf16[512,512]{1,0:T(8,128)(2,1)S(1)}, u32[]{:S(2)}, u32[]{:S(2)}) collective-permute-start(bf16[512,512]{1,0:T(8,128)(2,1)S(1)} %collective-permute-done.19.refs_16_), channel_id=1, source_target_pairs={{0,4},{1,5},{2,6},{3,7},{4,0},{5,1},{6,2},{7,3},{8,12},{9,13},{10,... | collective-permute-start | bytes 1572872 | tf_op jit(solution)/shard_map/ppermute | solution.py:434
  88.4 24.2 %collective-permute-start.20 = (bf16[512,512]{1,0:T(8,128)(2,1)S(1)}, bf16[512,512]{1,0:T(8,128)(2,1)S(1)}, u32[]{:S(2)}, u32[]{:S(2)}) collective-permute-start(bf16[512,512]{1,0:T(8,128)(2,1)S(1)} %collective-permute-done.16.refs_13_), channel_id=1, source_target_pairs={{0,2},{1,3},{2,0},{3,1},{4,6},{5,7},{6,4},{7,5},{8,10},{9,11},{10,... | collective-permute-start | bytes 1572872 | tf_op jit(solution)/shard_map/ppermute | solution.py:434
  89.9 8.1 %collective-permute-start.8 = (bf16[8,64,256]{2,1,0:T(8,128)(2,1)S(1)}, bf16[8,64,256]{2,1,0:T(8,128)(2,1)S(1)}, u32[]{:S(2)}, u32[]{:S(2)}) collective-permute-start(bf16[8,64,256]{2,1,0:T(8,128)(2,1)S(1)} %get-tuple-element.34.refs_1_), channel_id=1, source_target_pairs={{0,24},{1,25},{2,26},{3,27},{4,28},{5,29},{6,30},{7,31},{8,0},{9,1... | collective-permute-start | bytes 786440 | tf_op jit(solution)/shard_map/ppermute | solution.py:434
  90.4 21.1 %collective-permute-start.7 = (bf16[8,64,256]{2,1,0:T(8,128)(2,1)S(1)}, bf16[8,64,256]{2,1,0:T(8,128)(2,1)S(1)}, u32[]{:S(2)}, u32[]{:S(2)}) collective-permute-start(bf16[8,64,256]{2,1,0:T(8,128)(2,1)S(1)} %get-tuple-element.34.refs_1_), channel_id=1, source_target_pairs={{0,16},{1,17},{2,18},{3,19},{4,20},{5,21},{6,22},{7,23},{8,24},{9,... | collective-permute-start | bytes 786440 | tf_op jit(solution)/shard_map/ppermute | solution.py:434
  90.4 21.6 %collective-permute-start.6 = (bf16[8,64,256]{2,1,0:T(8,128)(2,1)S(1)}, bf16[8,64,256]{2,1,0:T(8,128)(2,1)S(1)}, u32[]{:S(2)}, u32[]{:S(2)}) collective-permute-start(bf16[8,64,256]{2,1,0:T(8,128)(2,1)S(1)} %get-tuple-element.34.refs_1_), channel_id=1, source_target_pairs={{0,8},{1,9},{2,10},{3,11},{4,12},{5,13},{6,14},{7,15},{8,16},{9,17... | collective-permute-start | bytes 786440 | tf_op jit(solution)/shard_map/ppermute | solution.py:434
  98.0 16.3 %collective-permute-start.25 = (bf16[128,2048]{1,0:T(8,128)(2,1)S(1)}, bf16[128,2048]{1,0:T(8,128)(2,1)S(1)}, u32[]{:S(2)}, u32[]{:S(2)}) collective-permute-start(bf16[128,2048]{1,0:T(8,128)(2,1)S(1)} %slice.38), channel_id=1, source_target_pairs={{0,4},{1,5},{2,6},{3,7},{4,0},{5,1},{6,2},{7,3},{8,12},{9,13},{10,... | collective-permute-start | bytes 1572872 | tf_op jit(solution)/shard_map/ppermute | solution.py:434
  111.5 11.3 %collective-permute-start.24 = (bf16[128,2048]{1,0:T(8,128)(2,1)S(1)}, bf16[128,2048]{1,0:T(8,128)(2,1)S(1)}, u32[]{:S(2)}, u32[]{:S(2)}) collective-permute-start(bf16[128,2048]{1,0:T(8,128)(2,1)S(1)} %slice.37), channel_id=1, source_target_pairs={{0,2},{1,3},{2,0},{3,1},{4,6},{5,7},{6,4},{7,5},{8,10},{9,11},{10,... | collective-permute-start | bytes 1572872 | tf_op jit(solution)/shard_map/ppermute | solution.py:434
  112.1 1.5 collective-permute-start.12
  112.1 1.9 %collective-permute-start.11 = (bf16[8,64,256]{2,1,0:T(8,128)(2,1)S(1)}, bf16[8,64,256]{2,1,0:T(8,128)(2,1)S(1)}, u32[]{:S(2)}, u32[]{:S(2)}) collective-permute-start(bf16[8,64,256]{2,1,0:T(8,128)(2,1)S(1)} %collective-permute-done.7.refs_3_), channel_id=1, source_target_pairs={{0,1},{1,0},{2,3},{3,2},{4,5},{5,4},{6,7},{7,6},{8,9},{9,8},{10,11... | collective-permute-start | bytes 786440 | tf_op jit(solution)/shard_map/ppermute | solution.py:434
  112.6 1.8 %collective-permute-start.10 = (bf16[8,64,256]{2,1,0:T(8,128)(2,1)S(1)}, bf16[8,64,256]{2,1,0:T(8,128)(2,1)S(1)}, u32[]{:S(2)}, u32[]{:S(2)}) collective-permute-start(bf16[8,64,256]{2,1,0:T(8,128)(2,1)S(1)} %collective-permute-done.6.refs_2_), channel_id=1, source_target_pairs={{0,1},{1,0},{2,3},{3,2},{4,5},{5,4},{6,7},{7,6},{8,9},{9,8},{10,11... | collective-permute-start | bytes 786440 | tf_op jit(solution)/shard_map/ppermute | solution.py:434
  128.9 2.0 %collective-permute-start.30 = (bf16[256,1024]{1,0:T(8,128)(2,1)S(1)}, bf16[256,1024]{1,0:T(8,128)(2,1)S(1)}, u32[]{:S(2)}, u32[]{:S(2)}) collective-permute-start(bf16[256,1024]{1,0:T(8,128)(2,1)S(1)} %get-tuple-element.43), channel_id=1, source_target_pairs={{0,1},{1,0},{2,3},{3,2},{4,5},{5,4},{6,7},{7,6},{8,9},{9,8},{10,11... | collective-permute-start | bytes 1572872 | tf_op jit(solution)/shard_map/ppermute | solution.py:434
  128.9 4.1 %collective-permute-start.26 = (bf16[256,1024]{1,0:T(8,128)(2,1)S(1)}, bf16[256,1024]{1,0:T(8,128)(2,1)S(1)}, u32[]{:S(2)}, u32[]{:S(2)}) collective-permute-start(bf16[256,1024]{1,0:T(8,128)(2,1)S(1)} %get-tuple-element.37), channel_id=1, source_target_pairs={{0,1},{1,0},{2,3},{3,2},{4,5},{5,4},{6,7},{7,6},{8,9},{9,8},{10,11... | collective-permute-start | bytes 1572872 | tf_op jit(solution)/shard_map/ppermute | solution.py:434
  130.9 7.2 %collective-permute-start.31 = (bf16[64,1024]{1,0:T(8,128)(2,1)S(1)}, bf16[64,1024]{1,0:T(8,128)(2,1)S(1)}, u32[]{:S(2)}, u32[]{:S(2)}) collective-permute-start(bf16[64,1024]{1,0:T(8,128)(2,1)S(1)} %get-tuple-element.44), channel_id=1, source_target_pairs={{0,24},{1,25},{2,26},{3,27},{4,28},{5,29},{6,30},{7,31},{8,0},{9,1... | collective-permute-start | bytes 393224 | tf_op jit(solution)/shard_map/ppermute | solution.py:434
  132.0 13.4 %collective-permute-start.32 = (bf16[64,1024]{1,0:T(8,128)(2,1)S(1)}, bf16[64,1024]{1,0:T(8,128)(2,1)S(1)}, u32[]{:S(2)}, u32[]{:S(2)}) collective-permute-start(bf16[64,1024]{1,0:T(8,128)(2,1)S(1)} %get-tuple-element.45), channel_id=1, source_target_pairs={{0,16},{1,17},{2,18},{3,19},{4,20},{5,21},{6,22},{7,23},{8,24},{9,... | collective-permute-start | bytes 393224 | tf_op jit(solution)/shard_map/ppermute | solution.py:434
  132.0 13.4 %collective-permute-start.33 = (bf16[64,1024]{1,0:T(8,128)(2,1)S(1)}, bf16[64,1024]{1,0:T(8,128)(2,1)S(1)}, u32[]{:S(2)}, u32[]{:S(2)}) collective-permute-start(bf16[64,1024]{1,0:T(8,128)(2,1)S(1)} %get-tuple-element.46), channel_id=1, source_target_pairs={{0,8},{1,9},{2,10},{3,11},{4,12},{5,13},{6,14},{7,15},{8,16},{9,17... | collective-permute-start | bytes 393224 | tf_op jit(solution)/shard_map/ppermute | solution.py:434
  133.1 12.4 %collective-permute-start.27 = (bf16[64,1024]{1,0:T(8,128)(2,1)S(1)}, bf16[64,1024]{1,0:T(8,128)(2,1)S(1)}, u32[]{:S(2)}, u32[]{:S(2)}) collective-permute-start(bf16[64,1024]{1,0:T(8,128)(2,1)S(1)} %get-tuple-element.38), channel_id=1, source_target_pairs={{0,24},{1,25},{2,26},{3,27},{4,28},{5,29},{6,30},{7,31},{8,0},{9,1... | collective-permute-start | bytes 393224 | tf_op jit(solution)/shard_map/ppermute | solution.py:434
  135.9 19.1 %collective-permute-start.28 = (bf16[64,1024]{1,0:T(8,128)(2,1)S(1)}, bf16[64,1024]{1,0:T(8,128)(2,1)S(1)}, u32[]{:S(2)}, u32[]{:S(2)}) collective-permute-start(bf16[64,1024]{1,0:T(8,128)(2,1)S(1)} %get-tuple-element.39), channel_id=1, source_target_pairs={{0,16},{1,17},{2,18},{3,19},{4,20},{5,21},{6,22},{7,23},{8,24},{9,... | collective-permute-start | bytes 393224 | tf_op jit(solution)/shard_map/ppermute | solution.py:434
  138.2 16.9 %collective-permute-start.29 = (bf16[64,1024]{1,0:T(8,128)(2,1)S(1)}, bf16[64,1024]{1,0:T(8,128)(2,1)S(1)}, u32[]{:S(2)}, u32[]{:S(2)}) collective-permute-start(bf16[64,1024]{1,0:T(8,128)(2,1)S(1)} %get-tuple-element.40), channel_id=1, source_target_pairs={{0,8},{1,9},{2,10},{3,11},{4,12},{5,13},{6,14},{7,15},{8,16},{9,17... | collective-permute-start | bytes 393224 | tf_op jit(solution)/shard_map/ppermute | solution.py:434
where the time goes:
time: 156 us
  waiting for transfers between devices  87.8 us (56%)
  starting transfers between devices  40.5 us (26%)
  Pallas kernels  15.3 us (10%)
  local copies, waits for them, and re-layouts  10 us (6%)
  other arithmetic  2.08 us (1%)
    ppermute x34, waiting for transfers between devices, send(): return lax.ppermute(x, AXES, pairs)  87.8 us
    ppermute x34, starting transfers between devices, send(): return lax.ppermute(x, AXES, pairs)  40.5 us
    unnamed x37, local copies, waits for them, and re-layouts  7.17 us
    pallas_call x1, Pallas kernels, on_device(): kernel_call(mixer, sizes + [jax.ShapeDtypeStruct((n_c * group, units), BF...  4.73 us
    pallas_call x1, Pallas kernels, on_device(): kernel_call(local_body, jax.ShapeDtypeStruct((rows, width), F32), n_in=4)  3.44 us
  transfers between devices with their start and end apart: 34, of which 17 were waited for; matrix products, arithmetic and copies ran while one was open for 3% of the time, Pallas kernels for 3%

commit v1 on v0

--- a/solution.py
+++ b/solution.py
@@ -171,62 +171,52 @@
         normed_out[i] = normed[:, i * cols : (i + 1) * cols]
 
 
-def lower_half(out_own, out_away, hidden, down, cut):
-    acc = jnp.dot(hidden, down, preferred_element_type=F32)
-    out_own[...] = acc[:cut]
-    out_away[...] = acc[cut:].astype(BF16)
-
-
-def mixer_body(n_a, n_cores, *refs):
-    n_tok = n_a * n_cores
+def hidden_half(rows_x, ups, up_all, cols, out):
+    at = 0
+    for src, off in ups:
+        up_all[at : at + cols, :] = src[off : off + cols, :]
+        at += cols
+    act = jnp.maximum(jnp.dot(rows_x[...], up_all[...], preferred_element_type=F32), 0.0)
+    out[...] = (act * act).astype(BF16)
+
+
+def first_body(n_a, n_cores, place, toks, ups, rows_x, hidden, up_all):
+    a, b = place[0], place[1]
+    n_b = len(ups) // n_a
+    _, own, cols = toks[0].shape
+    for i in range(n_a * n_cores):
+        for x in range(n_b):
+            for e in range(n_a):
+                k = lax.rem(a - e + n_a, n_a) * n_b + lax.rem(b + x, n_b)
+                at = (x * n_a + e) * cols
+                rows_x[i * own : (i + 1) * own, at : at + cols] = toks[i][k]
+    hidden_half(rows_x, ups, up_all, cols, hidden)
+
+
+def down_product(keep, away, units, pieces, down_all):
+    at = 0
+    for group in pieces:
+        for piece in group:
+            n = piece.shape[0]
+            down_all[at : at + n, :] = piece[...]
+            at += n
+    acc = jnp.dot(units, down_all[...], preferred_element_type=F32)
+    cut = keep.shape[0]
+    keep[...] = acc[:cut]
+    away[...] = acc[cut:].astype(BF16)
+
+
+def lower_body(cols, place, rows_x, early, ups, pieces, keep, away, ordered, up_all, late, down_all):
+    hidden_half(rows_x, ups, up_all, cols, late)
     n_b = 2
-    place = refs[0]
-    toks = refs[1 : 1 + n_tok]
-    ups = refs[1 + n_tok : 1 + n_tok + 2 * n_b * n_a]
-    downs = refs[1 + n_tok + 2 * n_b * n_a : -7]
-    keep, away, hid_out, rows_x, up_all, hid, down_all = refs[-7:]
-    a, b = place[0], place[1]
-    _, own, cols = toks[0].shape
-    for i in range(n_tok):
-        for e in range(n_a):
-            for x in range(n_b):
-                k = lax.rem(a - e + n_a, n_a) * n_b + lax.rem(b + x, n_b)
-                at = (e * n_b + x) * cols
-                rows_x[i * own : (i + 1) * own, at : at + cols] = toks[i][k]
-    for y in range(2):
-        for e in range(n_a):
-            for x in range(n_b):
-                at = (e * n_b + x) * cols
-                src, off = ups[(y * n_b + x) * n_a + e]
-                up_all[at : at + cols, :] = src[off : off + cols, :]
-        act = jnp.maximum(jnp.dot(rows_x[...], up_all[...], preferred_element_type=F32), 0.0)
-        act = (act * act).astype(BF16)
-        half = act.shape[1] // n_b
+    b = place[1]
+    half = late.shape[1] // n_b
+    for y, src in enumerate((early, late)):
         for x in range(n_b):
-            hid[y * n_b + x] = act[:, x * half : (x + 1) * half]
-    width = keep.shape[1]
-    at = 0
-    for y in range(2):
-        for x in range(n_b):
-            h = hid[y * n_b + lax.rem(b + x, n_b)]
-            step = h.shape[1]
-            hid_out[:, at : at + step] = h
-            for piece in downs[y * n_b + x :] if y * n_b + x == 3 else [downs[y * n_b + x]]:
-                n = piece.shape[0]
-                down_all[at : at + n, :] = piece[:, :width]
-                at += n
-    lower_half(keep, away, hid_out[...], down_all[...], n_a * own)
-
-
-def mixer_rest_body(cut, hidden, *refs):
-    downs, (keep, away, down_all) = refs[:-3], refs[-3:]
-    width = keep.shape[1]
-    at = 0
-    for piece in downs:
-        n = piece.shape[0]
-        down_all[at : at + n, :] = piece[:, width:]
-        at += n
-    lower_half(keep, away, hidden[...], down_all[...], cut)
+            k = lax.rem(b + x, n_b)
+            at = (y * n_b + x) * half
+            ordered[:, at : at + half] = src[:, pl.ds(pl.multiple_of(k * half, half), half)]
+    down_product(keep, away, ordered[...], pieces, down_all)
 
 
 def fold_body(keep, got, *outs):
@@ -465,40 +455,30 @@
             ],
             n_in=4,
         )(forget_logits, written_values, forget_floor_gap[None, :], extra_log_decay)
-        later_weight, packed = lax.optimization_barrier((mixer_up_weight, packed))
-
         up_rows, up_cols = mixer_up_weight.shape
         piece = up_cols // n_a
         mine = []
         for d in range(n_a):
-            source = mixer_up_weight if d == n_a // 2 else later_weight
-            cut = lax.dynamic_slice(source, (0, (a + d) % n_a * piece), (up_rows, piece))
+            cut = lax.dynamic_slice(mixer_up_weight, (0, (a + d) % n_a * piece), (up_rows, piece))
             mine.append(cut if d == 0 else send(cut, a=d))
-        groups = [mine[0::2], mine[1::2]]
-        up_x, up_y, up_xy = [], [], []
-        for g, members in enumerate(groups):
-            joined = jnp.concatenate(members, axis=0)
+        up_x, up_y = [], []
+        for g in range(2):
+            joined = jnp.concatenate(mine[g::2], axis=0)
             up_x.append(send(joined, b=1))
             up_y.append(send(joined, y=1))
-            if g:
-                up_xy.append(send(up_y[g], b=1))
-            else:
-                up_xy.append(send(up_x[g], y=1))
-        up_arrays = mine + up_x + up_y + up_xy
-
-        def up_places(refs):
-            found = [(refs[e], 0) for e in range(n_a)]
-            for k in range(3):
-                found += [
-                    (refs[n_a + 2 * k + e % 2], e // 2 * up_rows) for e in range(n_a)
-                ]
-            return found
-
+        up_xy = [send(up_y[0], b=1), send(up_x[1], y=1)]
+
+        def grouped(refs):
+            return [(refs[e % 2], e // 2 * up_rows) for e in range(n_a)]
+
+        part = model // 2
         half = mixer_down_weight.shape[0] // 2
-        down_x = send(mixer_down_weight, b=1)
-        down_y = send(mixer_down_weight, y=1)
-        down_xy = [send(down_x[:half], y=1), send(down_y[half:], b=1)]
-        down_arrays = [mixer_down_weight, down_x, down_y] + down_xy
+        down = [mixer_down_weight[:, :part], mixer_down_weight[:, part:]]
+        down_x = [send(u, b=1) for u in down]
+        down_y = [send(u, y=1) for u in down]
+        down_xy = [
+            [send(down_y[0], b=1)], [send(down_x[1][:half], y=1), send(down_y[1][half:], b=1)]
+        ]
 
         beside = send(packed, b=1)
         pair = kernel_call(pair_body, packed_shape, smem=1, n_in=3)(place, packed, beside)
@@ -541,39 +521,57 @@
         line = [normed] + [send(normed, a=d) for d in range(1, n_a)]
         toks = line + [send(u, c=1) for u in line]
         group = n_a * own
-        part = model // 2
+        tokens = n_c * group
+        units = n_y * piece
+        cols = model // n_sp
         sizes = [
             jax.ShapeDtypeStruct((group, part), F32),
-            jax.ShapeDtypeStruct((group, part), BF16),
+            jax.ShapeDtypeStruct((tokens - group, part), BF16),
         ]
-        units = n_y * piece
-
-        def mixer(*refs):
-            n_tok = len(toks)
-            ups = up_places(refs[1 + n_tok : 1 + n_tok + len(up_arrays)])
-            rest = refs[1 + n_tok + len(up_arrays) :]
-            mixer_body(n_a, n_c, *refs[: 1 + n_tok], *ups, *rest)
+
+        def first_half(*refs):
+            t = 1 + len(toks)
+            ups = [(refs[t + e], 0) for e in range(n_a)] + grouped(refs[t + n_a : t + n_a + 2])
+            first_body(n_a, n_c, refs[0], refs[1:t], ups, *refs[-3:])
+
+        rows_x, early = kernel_call(
+            first_half,
+            [
+                jax.ShapeDtypeStruct((tokens, model), BF16),
+                jax.ShapeDtypeStruct((tokens, piece), BF16),
+            ],
+            scratch=[pltpu.VMEM((model, piece), BF16)],
+            smem=1,
+            n_in=1 + len(toks) + n_a + 2,
+            mib=24,
+        )(place, *toks, *mine, *up_x)
+
+        def second_half(*refs):
+            ups = grouped(refs[3:5]) + grouped(refs[5:7])
+            pieces = [[refs[7]], [refs[8]], [refs[9]], [refs[10]]]
+            lower_body(cols, *refs[:3], ups, pieces, *refs[11:])
 
         keep0, away0, hidden = kernel_call(
-            mixer,
-            sizes + [jax.ShapeDtypeStruct((n_c * group, units), BF16)],
+            second_half,
+            sizes + [jax.ShapeDtypeStruct((tokens, units), BF16)],
             scratch=[
-                pltpu.VMEM((n_c * group, model), BF16),
                 pltpu.VMEM((model, piece), BF16),
-                pltpu.VMEM((n_y * n_b, n_c * group, piece // n_b), BF16),
+                pltpu.VMEM((tokens, piece), BF16),
                 pltpu.VMEM((units, part), BF16),
             ],
             smem=1,
-            n_in=1 + len(toks) + len(up_arrays) + len(down_arrays),
-            mib=34,
-        )(place, *toks, *up_arrays, *down_arrays)
+            n_in=11,
+            mib=28,
+        )(place, rows_x, early, *up_y, *up_xy, down[0], down_x[0], down_y[0], *down_xy[0])
         got0 = send(away0, c=1)
+
+        def last_columns(hidden_ref, own_ref, x_ref, y_ref, r0_ref, r1_ref, keep, away, down_all):
+            pieces = [[own_ref], [x_ref], [y_ref], [r0_ref, r1_ref]]
+            down_product(keep, away, hidden_ref[...], pieces, down_all)
+
         keep1, away1 = kernel_call(
-            lambda *refs: mixer_rest_body(group, *refs),
-            sizes,
-            scratch=[pltpu.VMEM((units, part), BF16)],
-            n_in=1 + len(down_arrays),
-        )(hidden, *down_arrays)
+            last_columns, sizes, scratch=[pltpu.VMEM((units, part), BF16)], n_in=6
+        )(hidden, down[1], down_x[1], down_y[1], *down_xy[1])
         got1 = send(away1, c=1)
         halves = []
         for k, (keep, got) in enumerate([(keep0, got0), (keep1, got1)]):

time: 156 us -> 150 us (0.962)
  local copies, waits for them, and re-layouts: 10 us -> 8.07 us
  waiting for transfers between devices: 87.8 us -> 85.9 us
  Pallas kernels: 15.3 us -> 13.5 us
    ppermute x34 -> x37, waiting for transfers between devices: 87.8 us -> 85.9 us  [send(): return lax.ppermute(x, AXES, pairs)]
    dynamic_slice x2 -> x1, local copies, waits for them, and re-layouts: 1.84 us -> 0.12 us  [on_device(): lax.dynamic_slice(mixer_up_weight, (0, (a + d) % n_a * piece), (up_rows,...]
    ppermute x34 -> x37, starting transfers between devices: 40.5 us -> 41.1 us  [send(): return lax.ppermute(x, AXES, pairs)]
    unnamed x37 -> x29, local copies, waits for them, and re-layouts: 7.17 us -> 7.83 us
    pallas_call x2 -> x3, Pallas kernels: 5.99 us -> 6.04 us  [the longest x1 3 us: on_device(): kernel_call(second_half, sizes + [jax.ShapeDtypeStruct((tokens, units), B...]
  transfers between devices with their start and end apart: 34 -> 37, of which waited for: 17 -> 18; matrix products, arithmetic and copies ran while one was open for 3% -> 0% of each run, Pallas kernels for 3% -> 6%
where the time goes in v1:
time: 150 us
  waiting for transfers between devices  85.9 us (57%)
  starting transfers between devices  41.1 us (27%)
  Pallas kernels  13.5 us (9%)
  local copies, waits for them, and re-layouts  8.07 us (5%)
    ppermute x37, waiting for transfers between devices, send(): return lax.ppermute(x, AXES, pairs)  85.9 us
    ppermute x37, starting transfers between devices, send(): return lax.ppermute(x, AXES, pairs)  41.1 us
    unnamed x29, local copies, waits for them, and re-layouts  7.83 us
    pallas_call x1, Pallas kernels, on_device(): kernel_call(local_body, jax.ShapeDtypeStruct((rows, width), F32), n_in=4)  3.44 us
    pallas_call x1, Pallas kernels, on_device(): kernel_call(second_half, sizes + [jax.ShapeDtypeStruct((tokens, units), B...  3 us
  transfers between devices with their start and end apart: 37, of which 18 were waited for; matrix products, arithmetic and copies ran while one was open for 0% of the time, Pallas kernels for 6%

profile of v1, /device:TPU:0, one launch (start us, length us, event | category | flops | bytes accessed | tf_op | source)
XLA Modules:
  0.0 150.1 jit_solution(1832613627184919209)
XLA Ops:
  0.0 1.0 copy-done.1
  1.0 0.9 copy-done.5
  1.9 0.9 copy-done.7
  2.9 0.7 copy-done.10
  3.5 1.3 shard_map.118
  4.9 3.0 %collective-permute-start = (bf16[272,128]{1,0:T(8,128)(2,1)S(1)}, bf16[272,128]{1,0:T(8,128)(2,1)S(1)}, u32[]{:S(2)}, u32[]{:S(2)}) collective-permute-start(bf16[272,128]{1,0:T(8,128)(2,1)S(1)} %get-tuple-element.28.mine), channel_id=1, source_target_pairs={{0,4},{1,5},{2,6},{3,7},{4,0},{5,1},{6,2},{7,3},{8,12},{9,13},{10,... | collective-permute-start | bytes 208904 | tf_op jit(solution)/shard_map/ppermute | solution.py:424
  8.0 2.2 %collective-permute-done.theirs.refs_7_ = bf16[272,128]{1,0:T(8,128)(2,1)S(1)} collective-permute-done((bf16[272,128]{1,0:T(8,128)(2,1)S(1)}, bf16[272,128]{1,0:T(8,128)(2,1)S(1)}, u32[]{:S(2)}, u32[]{:S(2)}) %collective-permute-start) | collective-permute-done | bytes 69664 | tf_op jit(solution)/shard_map/ppermute | solution.py:424
  10.2 0.7 shard_map.120
  10.8 4.0 %collective-permute-start.1 = (bf16[272,128]{1,0:T(8,128)(2,1)S(1)}, bf16[272,128]{1,0:T(8,128)(2,1)S(1)}, u32[]{:S(2)}, u32[]{:S(2)}) collective-permute-start(bf16[272,128]{1,0:T(8,128)(2,1)S(1)} %shard_map.120), channel_id=1, source_target_pairs={{0,8},{1,9},{2,10},{3,11},{4,12},{5,13},{6,14},{7,15},{8,16},{9,17... | collective-permute-start | bytes 208904 | tf_op jit(solution)/shard_map/ppermute | solution.py:424
  14.9 4.5 %collective-permute-start.2 = (bf16[272,128]{1,0:T(8,128)(2,1)S(1)}, bf16[272,128]{1,0:T(8,128)(2,1)S(1)}, u32[]{:S(2)}, u32[]{:S(2)}) collective-permute-start(bf16[272,128]{1,0:T(8,128)(2,1)S(1)} %shard_map.120), channel_id=1, source_target_pairs={{0,16},{1,17},{2,18},{3,19},{4,20},{5,21},{6,22},{7,23},{8,24},{9,... | collective-permute-start | bytes 208904 | tf_op jit(solution)/shard_map/ppermute | solution.py:424
  19.4 1.3 collective-permute-start.3
  20.8 0.9 copy-done.2
  21.7 0.9 copy-done.3
  22.6 3.4 %shard_map.119.refs_3_ = f32[256,256]{1,0:T(8,128)S(1)} custom-call(bf16[256,256]{1,0:T(8,128)(2,1)S(1)} %copy-done.3, f32[256,256]{1,0:T(8,128)S(1)} %get-tuple-element.27.gate, f32[256,256]{1,0:T(8,128)S(1)} %get-tuple-element.26.cum.refs_2_, bf16[256,256]{1,0:T(8,128)(2,1)S(1)} %copy-done.2), custom_call_target="tpu_custom_call" | custom-call | tf_op jit(solution)/shard_map/pallas_call | solution.py:486
  26.1 0.9 copy-done.4
  27.0 0.9 copy-done.8
  27.9 0.7 copy-done.11
  28.5 1.6 %shard_map.121 = (f32[64,2048]{1,0:T(8,128)S(1)}, f32[64,2048]{1,0:T(8,128)S(1)}, bf16[128,2048]{1,0:T(8,128)(2,1)S(1)}) custom-call(s32[4]{0:T(128)S(1)} %pad_add_fusion.place.refs_0_, bf16[256,256]{1,0:T(8,128)(2,1)S(1)} %copy-done.4, f32[256,256]{1,0:T(8,128)S(1)} %get-tuple-element.26.cum.refs_2_, f32[256,256]{1,0:T(8,128)S(1)} %shard_map.119.refs_3_, ...), custom_call_target="tpu_custom_call" | custom-call | tf_op jit(solution)/shard_map/pallas_call | solution.py:489
  30.2 0.1 constant_dynamic-slice_fusion
  30.4 1.3 collective-permute-start.14
  31.8 1.6 %collective-permute-start.23 = (bf16[256,1024]{1,0:T(8,128)(2,1)S(1)}, bf16[256,1024]{1,0:T(8,128)(2,1)S(1)}, u32[]{:S(2)}, u32[]{:S(2)}) collective-permute-start(bf16[256,1024]{1,0:T(8,128)(2,1)S(1)} %get-tuple-element.48.refs_7_), channel_id=1, source_target_pairs={{0,2},{1,3},{2,0},{3,1},{4,6},{5,7},{6,4},{7,5},{8,10},{9,11},{10,... | collective-permute-start | bytes 1572872 | tf_op jit(solution)/shard_map/ppermute | solution.py:424
  33.4 1.5 collective-permute-start.22
  34.9 6.6 %collective-permute-done.13.refs_10_ = bf16[256,512]{1,0:T(8,128)(2,1)S(1)} collective-permute-done((bf16[256,512]{1,0:T(8,128)(2,1)S(1)}, bf16[256,512]{1,0:T(8,128)(2,1)S(1)}, u32[]{:S(2)}, u32[]{:S(2)}) %collective-permute-start.13) | collective-permute-done | bytes 262176 | tf_op jit(solution)/shard_map/ppermute | solution.py:424
  41.5 1.5 collective-permute-start.29
  43.0 8.3 %collective-permute-done.14.refs_11_ = bf16[256,512]{1,0:T(8,128)(2,1)S(1)} collective-permute-done((bf16[256,512]{1,0:T(8,128)(2,1)S(1)}, bf16[256,512]{1,0:T(8,128)(2,1)S(1)}, u32[]{:S(2)}, u32[]{:S(2)}) %collective-permute-start.14) | collective-permute-done | bytes 262176 | tf_op jit(solution)/shard_map/ppermute | solution.py:424
  51.3 1.5 %collective-permute-start.30 = (bf16[256,1024]{1,0:T(8,128)(2,1)S(1)}, bf16[256,1024]{1,0:T(8,128)(2,1)S(1)}, u32[]{:S(2)}, u32[]{:S(2)}) collective-permute-start(bf16[256,1024]{1,0:T(8,128)(2,1)S(1)} %get-tuple-element.47.own_ref), channel_id=1, source_target_pairs={{0,2},{1,3},{2,0},{3,1},{4,6},{5,7},{6,4},{7,5},{8,10},{9,11},{10,... | collective-permute-start | bytes 1572872 | tf_op jit(solution)/shard_map/ppermute | solution.py:424
  53.0 7.5 %collective-permute-done.15.refs_12_ = bf16[256,512]{1,0:T(8,128)(2,1)S(1)} collective-permute-done((bf16[256,512]{1,0:T(8,128)(2,1)S(1)}, bf16[256,512]{1,0:T(8,128)(2,1)S(1)}, u32[]{:S(2)}, u32[]{:S(2)}) %collective-permute-start.15) | collective-permute-done | bytes 262176 | tf_op jit(solution)/shard_map/ppermute | solution.py:424
  60.5 0.5 collective-permute-start.5
  61.0 1.6 %collective-permute-start.17 = (bf16[512,512]{1,0:T(8,128)(2,1)S(1)}, bf16[512,512]{1,0:T(8,128)(2,1)S(1)}, u32[]{:S(2)}, u32[]{:S(2)}) collective-permute-start(bf16[512,512]{1,0:T(8,128)(2,1)S(1)} %constant_dynamic-update-slice_fusion), channel_id=1, source_target_pairs={{0,4},{1,5},{2,6},{3,7},{4,0},{5,1},{6,2},{7,3},{8,12},{9,13},{10,... | collective-permute-start | bytes 1572872 | tf_op jit(solution)/shard_map/ppermute | solution.py:424
  62.6 0.5 collective-permute-start.16
  63.1 1.5 %collective-permute-start.19 = (bf16[512,512]{1,0:T(8,128)(2,1)S(1)}, bf16[512,512]{1,0:T(8,128)(2,1)S(1)}, u32[]{:S(2)}, u32[]{:S(2)}) collective-permute-start(bf16[512,512]{1,0:T(8,128)(2,1)S(1)} %constant_dynamic-update-slice_fusion), channel_id=1, source_target_pairs={{0,2},{1,3},{2,0},{3,1},{4,6},{5,7},{6,4},{7,5},{8,10},{9,11},{10,... | collective-permute-start | bytes 1572872 | tf_op jit(solution)/shard_map/ppermute | solution.py:424
  64.6 7.1 %collective-permute-done.5.arrived = bf16[64,2048]{1,0:T(8,128)(2,1)S(1)} collective-permute-done((bf16[64,2048]{1,0:T(8,128)(2,1)S(1)}, bf16[64,2048]{1,0:T(8,128)(2,1)S(1)}, u32[]{:S(2)}, u32[]{:S(2)}) %collective-permute-start.5) | collective-permute-done | bytes 262176 | tf_op jit(solution)/shard_map/ppermute | solution.py:424
  71.7 1.5 %collective-permute-start.18 = (bf16[512,512]{1,0:T(8,128)(2,1)S(1)}, bf16[512,512]{1,0:T(8,128)(2,1)S(1)}, u32[]{:S(2)}, u32[]{:S(2)}) collective-permute-start(bf16[512,512]{1,0:T(8,128)(2,1)S(1)} %pad_maximum_fusion), channel_id=1, source_target_pairs={{0,2},{1,3},{2,0},{3,1},{4,6},{5,7},{6,4},{7,5},{8,10},{9,11},{10,... | collective-permute-start | bytes 1572872 | tf_op jit(solution)/shard_map/ppermute | solution.py:424
  73.3 0.2 shard_map.122
  73.6 2.3 %collective-permute-done.17.refs_14_ = bf16[512,512]{1,0:T(8,128)(2,1)S(1)} collective-permute-done((bf16[512,512]{1,0:T(8,128)(2,1)S(1)}, bf16[512,512]{1,0:T(8,128)(2,1)S(1)}, u32[]{:S(2)}, u32[]{:S(2)}) %collective-permute-start.17) | collective-permute-done | bytes 524320 | tf_op jit(solution)/shard_map/ppermute | solution.py:424
  75.9 8.5 %collective-permute-done.16.refs_13_ = bf16[512,512]{1,0:T(8,128)(2,1)S(1)} collective-permute-done((bf16[512,512]{1,0:T(8,128)(2,1)S(1)}, bf16[512,512]{1,0:T(8,128)(2,1)S(1)}, u32[]{:S(2)}, u32[]{:S(2)}) %collective-permute-start.16) | collective-permute-done | bytes 524320 | tf_op jit(solution)/shard_map/ppermute | solution.py:424
  84.4 2.4 %collective-permute-start.8 = (bf16[8,64,256]{2,1,0:T(8,128)(2,1)S(1)}, bf16[8,64,256]{2,1,0:T(8,128)(2,1)S(1)}, u32[]{:S(2)}, u32[]{:S(2)}) collective-permute-start(bf16[8,64,256]{2,1,0:T(8,128)(2,1)S(1)} %get-tuple-element.33.refs_1_), channel_id=1, source_target_pairs={{0,24},{1,25},{2,26},{3,27},{4,28},{5,29},{6,30},{7,31},{8,0},{9,1... | collective-permute-start | bytes 786440 | tf_op jit(solution)/shard_map/ppermute | solution.py:424
  86.7 0.5 collective-permute-start.10
  87.2 5.6 %collective-permute-done.18.refs_3_ = bf16[512,512]{1,0:T(8,128)(2,1)S(1)} collective-permute-done((bf16[512,512]{1,0:T(8,128)(2,1)S(1)}, bf16[512,512]{1,0:T(8,128)(2,1)S(1)}, u32[]{:S(2)}, u32[]{:S(2)}) %collective-permute-start.18) | collective-permute-done | bytes 524320 | tf_op jit(solution)/shard_map/ppermute | solution.py:424
  92.9 1.5 collective-permute-start.24
  94.3 1.5 %collective-permute-start.21 = (bf16[512,512]{1,0:T(8,128)(2,1)S(1)}, bf16[512,512]{1,0:T(8,128)(2,1)S(1)}, u32[]{:S(2)}, u32[]{:S(2)}) collective-permute-start(bf16[512,512]{1,0:T(8,128)(2,1)S(1)} %collective-permute-done.17.refs_14_), channel_id=1, source_target_pairs={{0,2},{1,3},{2,0},{3,1},{4,6},{5,7},{6,4},{7,5},{8,10},{9,11},{10,... | collective-permute-start | bytes 1572872 | tf_op jit(solution)/shard_map/ppermute | solution.py:424
  95.9 0.5 collective-permute-start.20
  96.4 0.5 collective-permute-start.12
  97.0 1.0 collective-permute-done.11.refs_7_
  97.9 1.9 %collective-permute-start.31 = (bf16[128,1024]{1,0:T(8,128)(2,1)S(1)}, bf16[128,1024]{1,0:T(8,128)(2,1)S(1)}, u32[]{:S(2)}, u32[]{:S(2)}) collective-permute-start(bf16[128,1024]{1,0:T(8,128)(2,1)S(1)} %slice.46), channel_id=1, source_target_pairs={{0,2},{1,3},{2,0},{3,1},{4,6},{5,7},{6,4},{7,5},{8,10},{9,11},{10,... | collective-permute-start | bytes 786440 | tf_op jit(solution)/shard_map/ppermute | solution.py:424
  99.9 0.5 collective-permute-start.32
  100.4 1.8 %shard_map.123 = (bf16[512,2048]{1,0:T(8,128)(2,1)S(1)}, bf16[512,512]{1,0:T(8,128)(2,1)S(1)}) custom-call(s32[4]{0:T(128)S(1)} %pad_add_fusion.place.refs_0_, bf16[8,64,256]{2,1,0:T(8,128)(2,1)S(1)} %get-tuple-element.33.refs_1_, bf16[8,64,256]{2,1,0:T(8,128)(2,1)S(1)} %collective-permute-done.6.refs_2_, ...), custom_call_target="tpu_custom_call" | custom-call | tf_op jit(solution)/shard_map/pallas_call | solution.py:537
  102.2 5.5 %collective-permute-done.24.refs_10_ = bf16[256,1024]{1,0:T(8,128)(2,1)S(1)} collective-permute-done((bf16[256,1024]{1,0:T(8,128)(2,1)S(1)}, bf16[256,1024]{1,0:T(8,128)(2,1)S(1)}, u32[]{:S(2)}, u32[]{:S(2)}) %collective-permute-start.24) | collective-permute-done | bytes 524320 | tf_op jit(solution)/shard_map/ppermute | solution.py:424
  107.6 1.5 collective-permute-done.21.refs_6_
  109.1 9.7 %collective-permute-done.20.refs_5_ = bf16[512,512]{1,0:T(8,128)(2,1)S(1)} collective-permute-done((bf16[512,512]{1,0:T(8,128)(2,1)S(1)}, bf16[512,512]{1,0:T(8,128)(2,1)S(1)}, u32[]{:S(2)}, u32[]{:S(2)}) %collective-permute-start.20) | collective-permute-done | bytes 524320 | tf_op jit(solution)/shard_map/ppermute | solution.py:424
  118.9 3.0 %shard_map.124 = (f32[256,1024]{1,0:T(8,128)S(1)}, bf16[256,1024]{1,0:T(8,128)(2,1)S(1)}, bf16[512,1024]{1,0:T(8,128)(2,1)S(1)}) custom-call(s32[4]{0:T(128)S(1)} %pad_add_fusion.place.refs_0_, bf16[512,2048]{1,0:T(8,128)(2,1)S(1)} %get-tuple-element.34.refs_1_, bf16[512,512]{1,0:T(8,128)(2,1)S(1)} %get-tuple-element.35.refs_2_, ...), custom_call_target="tpu_custom_call" | custom-call | tf_op jit(solution)/shard_map/pallas_call | solution.py:554
  121.9 0.4 collective-permute-done.32.r1_ref
  122.3 1.3 shard_map.126
  123.6 0.5 collective-permute-start.25
  124.1 1.4 collective-permute-done.33.got
  125.7 1.9 %collective-permute-start.36 = (bf16[64,1024]{1,0:T(8,128)(2,1)S(1)}, bf16[64,1024]{1,0:T(8,128)(2,1)S(1)}, u32[]{:S(2)}, u32[]{:S(2)}) collective-permute-start(bf16[64,1024]{1,0:T(8,128)(2,1)S(1)} %get-tuple-element.46), channel_id=1, source_target_pairs={{0,8},{1,9},{2,10},{3,11},{4,12},{5,13},{6,14},{7,15},{8,16},{9,17... | collective-permute-start | bytes 393224 | tf_op jit(solution)/shard_map/ppermute | solution.py:424
  127.7 0.1 shard_map.125
  127.8 2.4 %collective-permute-start.26 = (bf16[64,1024]{1,0:T(8,128)(2,1)S(1)}, bf16[64,1024]{1,0:T(8,128)(2,1)S(1)}, u32[]{:S(2)}, u32[]{:S(2)}) collective-permute-start(bf16[64,1024]{1,0:T(8,128)(2,1)S(1)} %get-tuple-element.38), channel_id=1, source_target_pairs={{0,24},{1,25},{2,26},{3,27},{4,28},{5,29},{6,30},{7,31},{8,0},{9,1... | collective-permute-start | bytes 393224 | tf_op jit(solution)/shard_map/ppermute | solution.py:424
  130.2 0.6 collective-permute-start.27
  130.8 3.2 %collective-permute-done.34 = bf16[64,1024]{1,0:T(8,128)(2,1)S(1)} collective-permute-done((bf16[64,1024]{1,0:T(8,128)(2,1)S(1)}, bf16[64,1024]{1,0:T(8,128)(2,1)S(1)}, u32[]{:S(2)}, u32[]{:S(2)}) %collective-permute-start.34) | collective-permute-done | bytes 131104 | tf_op jit(solution)/shard_map/ppermute | solution.py:424
  134.1 5.5 %collective-permute-done.35 = bf16[64,1024]{1,0:T(8,128)(2,1)S(1)} collective-permute-done((bf16[64,1024]{1,0:T(8,128)(2,1)S(1)}, bf16[64,1024]{1,0:T(8,128)(2,1)S(1)}, u32[]{:S(2)}, u32[]{:S(2)}) %collective-permute-start.35) | collective-permute-done | bytes 131104 | tf_op jit(solution)/shard_map/ppermute | solution.py:424
  139.6 9.5 %collective-permute-done.27 = bf16[64,1024]{1,0:T(8,128)(2,1)S(1)} collective-permute-done((bf16[64,1024]{1,0:T(8,128)(2,1)S(1)}, bf16[64,1024]{1,0:T(8,128)(2,1)S(1)}, u32[]{:S(2)}, u32[]{:S(2)}) %collective-permute-start.27) | collective-permute-done | bytes 131104 | tf_op jit(solution)/shard_map/ppermute | solution.py:424
  149.1 0.3 add_convert_fusion.2
  149.4 0.7 pad_maximum_fusion.1
  (59 shorter events, 1.0 us)
Async XLA Ops:
  0.0 26.0 %copy-start = (bf16[256,2048]{1,0:T(8,128)(2,1)S(1)}, bf16[256,2048]{1,0:T(8,128)(2,1)}, u32[]{:S(2)}) copy-start(bf16[256,2048]{1,0:T(8,128)(2,1)} %refs_6_.1) | copy-start | bytes 3145732
  0.0 1.0 copy-start.1
  1.0 0.9 copy-start.5
  1.9 0.9 copy-start.7
  2.9 0.7 copy-start.10
  4.9 5.3 %collective-permute-start = (bf16[272,128]{1,0:T(8,128)(2,1)S(1)}, bf16[272,128]{1,0:T(8,128)(2,1)S(1)}, u32[]{:S(2)}, u32[]{:S(2)}) collective-permute-start(bf16[272,128]{1,0:T(8,128)(2,1)S(1)} %get-tuple-element.28.mine), channel_id=1, source_target_pairs={{0,4},{1,5},{2,6},{3,7},{4,0},{5,1},{6,2},{7,3},{8,12},{9,13},{10,... | collective-permute-start | bytes 208904 | tf_op jit(solution)/shard_map/ppermute | solution.py:424
  10.8 15.2 %collective-permute-start.1 = (bf16[272,128]{1,0:T(8,128)(2,1)S(1)}, bf16[272,128]{1,0:T(8,128)(2,1)S(1)}, u32[]{:S(2)}, u32[]{:S(2)}) collective-permute-start(bf16[272,128]{1,0:T(8,128)(2,1)S(1)} %shard_map.120), channel_id=1, source_target_pairs={{0,8},{1,9},{2,10},{3,11},{4,12},{5,13},{6,14},{7,15},{8,16},{9,17... | collective-permute-start | bytes 208904 | tf_op jit(solution)/shard_map/ppermute | solution.py:424
  14.9 11.2 %collective-permute-start.2 = (bf16[272,128]{1,0:T(8,128)(2,1)S(1)}, bf16[272,128]{1,0:T(8,128)(2,1)S(1)}, u32[]{:S(2)}, u32[]{:S(2)}) collective-permute-start(bf16[272,128]{1,0:T(8,128)(2,1)S(1)} %shard_map.120), channel_id=1, source_target_pairs={{0,16},{1,17},{2,18},{3,19},{4,20},{5,21},{6,22},{7,23},{8,24},{9,... | collective-permute-start | bytes 208904 | tf_op jit(solution)/shard_map/ppermute | solution.py:424
  19.4 6.7 %collective-permute-start.3 = (bf16[272,128]{1,0:T(8,128)(2,1)S(1)}, bf16[272,128]{1,0:T(8,128)(2,1)S(1)}, u32[]{:S(2)}, u32[]{:S(2)}) collective-permute-start(bf16[272,128]{1,0:T(8,128)(2,1)S(1)} %shard_map.120), channel_id=1, source_target_pairs={{0,24},{1,25},{2,26},{3,27},{4,28},{5,29},{6,30},{7,31}} | collective-permute-start | bytes 208904 | tf_op jit(solution)/shard_map/ppermute | solution.py:424
  20.7 0.9 copy-start.2
  21.7 0.9 copy-start.3
  26.0 0.9 copy-start.4
  27.0 0.9 copy-start.8
  27.9 0.7 copy-start.11
  28.5 1.7 %copy-start.12 = (bf16[256,2048]{1,0:T(8,128)(2,1)S(1)}, bf16[256,2048]{1,0:T(8,128)(2,1)}, u32[]{:S(2)}) copy-start(bf16[256,2048]{1,0:T(8,128)(2,1)} %param.22) | copy-start | bytes 3145732
  28.5 3.2 %copy-start.13 = (bf16[256,2048]{1,0:T(8,128)(2,1)S(1)}, bf16[256,2048]{1,0:T(8,128)(2,1)}, u32[]{:S(2)}) copy-start(bf16[256,2048]{1,0:T(8,128)(2,1)} %param.23) | copy-start | bytes 3145732
  30.2 22.7 %collective-permute-start.4 = (bf16[128,2048]{1,0:T(8,128)(2,1)S(1)}, bf16[128,2048]{1,0:T(8,128)(2,1)S(1)}, u32[]{:S(2)}, u32[]{:S(2)}) collective-permute-start(bf16[128,2048]{1,0:T(8,128)(2,1)S(1)} %get-tuple-element.30), channel_id=1, source_target_pairs={{0,1},{1,0},{2,3},{3,2},{4,5},{5,4},{6,7},{7,6},{8,9},{9,8},{10,11... | collective-permute-start | bytes 1572872 | tf_op jit(solution)/shard_map/ppermute | solution.py:424
  30.4 11.1 %collective-permute-start.13 = (bf16[256,512]{1,0:T(8,128)(2,1)S(1)}, bf16[256,512]{1,0:T(8,128)(2,1)S(1)}, u32[]{:S(2)}, u32[]{:S(2)}) collective-permute-start(bf16[256,512]{1,0:T(8,128)(2,1)S(1)} %get-tuple-element.50), channel_id=1, source_target_pairs={{0,8},{1,9},{2,10},{3,11},{4,12},{5,13},{6,14},{7,15},{8,16},{9,17... | collective-permute-start | bytes 786440 | tf_op jit(solution)/shard_map/ppermute | solution.py:424
  30.4 20.9 %collective-permute-start.14 = (bf16[256,512]{1,0:T(8,128)(2,1)S(1)}, bf16[256,512]{1,0:T(8,128)(2,1)S(1)}, u32[]{:S(2)}, u32[]{:S(2)}) collective-permute-start(bf16[256,512]{1,0:T(8,128)(2,1)S(1)} %get-tuple-element.52), channel_id=1, source_target_pairs={{0,16},{1,17},{2,18},{3,19},{4,20},{5,21},{6,22},{7,23},{8,24},{9,... | collective-permute-start | bytes 786440 | tf_op jit(solution)/shard_map/ppermute | solution.py:424
  31.8 41.5 %copy-start.6 = (bf16[64,2048]{1,0:T(8,128)(2,1)S(1)}, bf16[64,2048]{1,0:T(8,128)(2,1)}, u32[]{:S(2)}) copy-start(bf16[64,2048]{1,0:T(8,128)(2,1)} %residual.1) | copy-start | bytes 786436
  31.8 41.5 %copy-start.9 = (f32[2048]{0:T(1024)S(1)}, f32[2048]{0:T(1024)}, u32[]{:S(2)}) copy-start(f32[2048]{0:T(1024)} %param.21) | copy-start | bytes 24580
  31.8 29.2 %collective-permute-start.23 = (bf16[256,1024]{1,0:T(8,128)(2,1)S(1)}, bf16[256,1024]{1,0:T(8,128)(2,1)S(1)}, u32[]{:S(2)}, u32[]{:S(2)}) collective-permute-start(bf16[256,1024]{1,0:T(8,128)(2,1)S(1)} %get-tuple-element.48.refs_7_), channel_id=1, source_target_pairs={{0,2},{1,3},{2,0},{3,1},{4,6},{5,7},{6,4},{7,5},{8,10},{9,11},{10,... | collective-permute-start | bytes 1572872 | tf_op jit(solution)/shard_map/ppermute | solution.py:424
  33.4 29.2 %collective-permute-start.22 = (bf16[256,1024]{1,0:T(8,128)(2,1)S(1)}, bf16[256,1024]{1,0:T(8,128)(2,1)S(1)}, u32[]{:S(2)}, u32[]{:S(2)}) collective-permute-start(bf16[256,1024]{1,0:T(8,128)(2,1)S(1)} %get-tuple-element.48.refs_7_), channel_id=1, source_target_pairs={{0,4},{1,5},{2,6},{3,7},{4,0},{5,1},{6,2},{7,3},{8,12},{9,13},{10,... | collective-permute-start | bytes 1572872 | tf_op jit(solution)/shard_map/ppermute | solution.py:424
  41.5 21.6 %collective-permute-start.29 = (bf16[256,1024]{1,0:T(8,128)(2,1)S(1)}, bf16[256,1024]{1,0:T(8,128)(2,1)S(1)}, u32[]{:S(2)}, u32[]{:S(2)}) collective-permute-start(bf16[256,1024]{1,0:T(8,128)(2,1)S(1)} %get-tuple-element.47.own_ref), channel_id=1, source_target_pairs={{0,4},{1,5},{2,6},{3,7},{4,0},{5,1},{6,2},{7,3},{8,12},{9,13},{10,... | collective-permute-start | bytes 1572872 | tf_op jit(solution)/shard_map/ppermute | solution.py:424
  51.3 22.2 %collective-permute-start.30 = (bf16[256,1024]{1,0:T(8,128)(2,1)S(1)}, bf16[256,1024]{1,0:T(8,128)(2,1)S(1)}, u32[]{:S(2)}, u32[]{:S(2)}) collective-permute-start(bf16[256,1024]{1,0:T(8,128)(2,1)S(1)} %get-tuple-element.47.own_ref), channel_id=1, source_target_pairs={{0,2},{1,3},{2,0},{3,1},{4,6},{5,7},{6,4},{7,5},{8,10},{9,11},{10,... | collective-permute-start | bytes 1572872 | tf_op jit(solution)/shard_map/ppermute | solution.py:424
  52.9 7.6 %collective-permute-start.15 = (bf16[256,512]{1,0:T(8,128)(2,1)S(1)}, bf16[256,512]{1,0:T(8,128)(2,1)S(1)}, u32[]{:S(2)}, u32[]{:S(2)}) collective-permute-start(bf16[256,512]{1,0:T(8,128)(2,1)S(1)} %get-tuple-element.49), channel_id=1, source_target_pairs={{0,24},{1,25},{2,26},{3,27},{4,28},{5,29},{6,30},{7,31},{8,0},{9,1... | collective-permute-start | bytes 786440 | tf_op jit(solution)/shard_map/ppermute | solution.py:424
  60.5 11.2 %collective-permute-start.5 = (bf16[64,2048]{1,0:T(8,128)(2,1)S(1)}, bf16[64,2048]{1,0:T(8,128)(2,1)S(1)}, u32[]{:S(2)}, u32[]{:S(2)}) collective-permute-start(bf16[64,2048]{1,0:T(8,128)(2,1)S(1)} %add_convert_fusion), channel_id=1, source_target_pairs={{0,2},{1,3},{2,0},{3,1},{4,6},{5,7},{6,4},{7,5},{8,10},{9,11},{10,... | collective-permute-start | bytes 786440 | tf_op jit(solution)/shard_map/ppermute | solution.py:424
  61.0 14.9 %collective-permute-start.17 = (bf16[512,512]{1,0:T(8,128)(2,1)S(1)}, bf16[512,512]{1,0:T(8,128)(2,1)S(1)}, u32[]{:S(2)}, u32[]{:S(2)}) collective-permute-start(bf16[512,512]{1,0:T(8,128)(2,1)S(1)} %constant_dynamic-update-slice_fusion), channel_id=1, source_target_pairs={{0,4},{1,5},{2,6},{3,7},{4,0},{5,1},{6,2},{7,3},{8,12},{9,13},{10,... | collective-permute-start | bytes 1572872 | tf_op jit(solution)/shard_map/ppermute | solution.py:424
  62.6 21.8 %collective-permute-start.16 = (bf16[512,512]{1,0:T(8,128)(2,1)S(1)}, bf16[512,512]{1,0:T(8,128)(2,1)S(1)}, u32[]{:S(2)}, u32[]{:S(2)}) collective-permute-start(bf16[512,512]{1,0:T(8,128)(2,1)S(1)} %pad_maximum_fusion), channel_id=1, source_target_pairs={{0,4},{1,5},{2,6},{3,7},{4,0},{5,1},{6,2},{7,3},{8,12},{9,13},{10,... | collective-permute-start | bytes 1572872 | tf_op jit(solution)/shard_map/ppermute | solution.py:424
  63.1 23.6 %collective-permute-start.19 = (bf16[512,512]{1,0:T(8,128)(2,1)S(1)}, bf16[512,512]{1,0:T(8,128)(2,1)S(1)}, u32[]{:S(2)}, u32[]{:S(2)}) collective-permute-start(bf16[512,512]{1,0:T(8,128)(2,1)S(1)} %constant_dynamic-update-slice_fusion), channel_id=1, source_target_pairs={{0,2},{1,3},{2,0},{3,1},{4,6},{5,7},{6,4},{7,5},{8,10},{9,11},{10,... | collective-permute-start | bytes 1572872 | tf_op jit(solution)/shard_map/ppermute | solution.py:424
  71.7 21.1 %collective-permute-start.18 = (bf16[512,512]{1,0:T(8,128)(2,1)S(1)}, bf16[512,512]{1,0:T(8,128)(2,1)S(1)}, u32[]{:S(2)}, u32[]{:S(2)}) collective-permute-start(bf16[512,512]{1,0:T(8,128)(2,1)S(1)} %pad_maximum_fusion), channel_id=1, source_target_pairs={{0,2},{1,3},{2,0},{3,1},{4,6},{5,7},{6,4},{7,5},{8,10},{9,11},{10,... | collective-permute-start | bytes 1572872 | tf_op jit(solution)/shard_map/ppermute | solution.py:424
  73.5 13.2 %collective-permute-start.6 = (bf16[8,64,256]{2,1,0:T(8,128)(2,1)S(1)}, bf16[8,64,256]{2,1,0:T(8,128)(2,1)S(1)}, u32[]{:S(2)}, u32[]{:S(2)}) collective-permute-start(bf16[8,64,256]{2,1,0:T(8,128)(2,1)S(1)} %get-tuple-element.33.refs_1_), channel_id=1, source_target_pairs={{0,8},{1,9},{2,10},{3,11},{4,12},{5,13},{6,14},{7,15},{8,16},{9,17... | collective-permute-start | bytes 786440 | tf_op jit(solution)/shard_map/ppermute | solution.py:424
  75.9 18.5 %collective-permute-start.7 = (bf16[8,64,256]{2,1,0:T(8,128)(2,1)S(1)}, bf16[8,64,256]{2,1,0:T(8,128)(2,1)S(1)}, u32[]{:S(2)}, u32[]{:S(2)}) collective-permute-start(bf16[8,64,256]{2,1,0:T(8,128)(2,1)S(1)} %get-tuple-element.33.refs_1_), channel_id=1, source_target_pairs={{0,16},{1,17},{2,18},{3,19},{4,20},{5,21},{6,22},{7,23},{8,24},{9,... | collective-permute-start | bytes 786440 | tf_op jit(solution)/shard_map/ppermute | solution.py:424
  84.4 11.5 %collective-permute-start.8 = (bf16[8,64,256]{2,1,0:T(8,128)(2,1)S(1)}, bf16[8,64,256]{2,1,0:T(8,128)(2,1)S(1)}, u32[]{:S(2)}, u32[]{:S(2)}) collective-permute-start(bf16[8,64,256]{2,1,0:T(8,128)(2,1)S(1)} %get-tuple-element.33.refs_1_), channel_id=1, source_target_pairs={{0,24},{1,25},{2,26},{3,27},{4,28},{5,29},{6,30},{7,31},{8,0},{9,1... | collective-permute-start | bytes 786440 | tf_op jit(solution)/shard_map/ppermute | solution.py:424
  86.7 9.7 %collective-permute-start.9 = (bf16[8,64,256]{2,1,0:T(8,128)(2,1)S(1)}, bf16[8,64,256]{2,1,0:T(8,128)(2,1)S(1)}, u32[]{:S(2)}, u32[]{:S(2)}) collective-permute-start(bf16[8,64,256]{2,1,0:T(8,128)(2,1)S(1)} %get-tuple-element.33.refs_1_), channel_id=1, source_target_pairs={{0,1},{1,0},{2,3},{3,2},{4,5},{5,4},{6,7},{7,6},{8,9},{9,8},{10,11... | collective-permute-start | bytes 786440 | tf_op jit(solution)/shard_map/ppermute | solution.py:424
  86.7 9.7 %collective-permute-start.10 = (bf16[8,64,256]{2,1,0:T(8,128)(2,1)S(1)}, bf16[8,64,256]{2,1,0:T(8,128)(2,1)S(1)}, u32[]{:S(2)}, u32[]{:S(2)}) collective-permute-start(bf16[8,64,256]{2,1,0:T(8,128)(2,1)S(1)} %collective-permute-done.6.refs_2_), channel_id=1, source_target_pairs={{0,1},{1,0},{2,3},{3,2},{4,5},{5,4},{6,7},{7,6},{8,9},{9,8},{10,11... | collective-permute-start | bytes 786440 | tf_op jit(solution)/shard_map/ppermute | solution.py:424
  92.9 14.8 %collective-permute-start.24 = (bf16[256,1024]{1,0:T(8,128)(2,1)S(1)}, bf16[256,1024]{1,0:T(8,128)(2,1)S(1)}, u32[]{:S(2)}, u32[]{:S(2)}) collective-permute-start(bf16[256,1024]{1,0:T(8,128)(2,1)S(1)} %collective-permute-done.23.refs_9_), channel_id=1, source_target_pairs={{0,4},{1,5},{2,6},{3,7},{4,0},{5,1},{6,2},{7,3},{8,12},{9,13},{10,... | collective-permute-start | bytes 1572872 | tf_op jit(solution)/shard_map/ppermute | solution.py:424
  94.3 14.8 %collective-permute-start.21 = (bf16[512,512]{1,0:T(8,128)(2,1)S(1)}, bf16[512,512]{1,0:T(8,128)(2,1)S(1)}, u32[]{:S(2)}, u32[]{:S(2)}) collective-permute-start(bf16[512,512]{1,0:T(8,128)(2,1)S(1)} %collective-permute-done.17.refs_14_), channel_id=1, source_target_pairs={{0,2},{1,3},{2,0},{3,1},{4,6},{5,7},{6,4},{7,5},{8,10},{9,11},{10,... | collective-permute-start | bytes 1572872 | tf_op jit(solution)/shard_map/ppermute | solution.py:424
  95.9 23.0 %collective-permute-start.20 = (bf16[512,512]{1,0:T(8,128)(2,1)S(1)}, bf16[512,512]{1,0:T(8,128)(2,1)S(1)}, u32[]{:S(2)}, u32[]{:S(2)}) collective-permute-start(bf16[512,512]{1,0:T(8,128)(2,1)S(1)} %collective-permute-done.18.refs_3_), channel_id=1, source_target_pairs={{0,4},{1,5},{2,6},{3,7},{4,0},{5,1},{6,2},{7,3},{8,12},{9,13},{10,... | collective-permute-start | bytes 1572872 | tf_op jit(solution)/shard_map/ppermute | solution.py:424
  96.4 1.5 %collective-permute-start.11 = (bf16[8,64,256]{2,1,0:T(8,128)(2,1)S(1)}, bf16[8,64,256]{2,1,0:T(8,128)(2,1)S(1)}, u32[]{:S(2)}, u32[]{:S(2)}) collective-permute-start(bf16[8,64,256]{2,1,0:T(8,128)(2,1)S(1)} %collective-permute-done.7.refs_3_), channel_id=1, source_target_pairs={{0,1},{1,0},{2,3},{3,2},{4,5},{5,4},{6,7},{7,6},{8,9},{9,8},{10,11... | collective-permute-start | bytes 786440 | tf_op jit(solution)/shard_map/ppermute | solution.py:424
  96.4 3.4 %collective-permute-start.12 = (bf16[8,64,256]{2,1,0:T(8,128)(2,1)S(1)}, bf16[8,64,256]{2,1,0:T(8,128)(2,1)S(1)}, u32[]{:S(2)}, u32[]{:S(2)}) collective-permute-start(bf16[8,64,256]{2,1,0:T(8,128)(2,1)S(1)} %collective-permute-done.8.refs_4_), channel_id=1, source_target_pairs={{0,1},{1,0},{2,3},{3,2},{4,5},{5,4},{6,7},{7,6},{8,9},{9,8},{10,11... | collective-permute-start | bytes 786440 | tf_op jit(solution)/shard_map/ppermute | solution.py:424
  97.9 23.9 %collective-permute-start.31 = (bf16[128,1024]{1,0:T(8,128)(2,1)S(1)}, bf16[128,1024]{1,0:T(8,128)(2,1)S(1)}, u32[]{:S(2)}, u32[]{:S(2)}) collective-permute-start(bf16[128,1024]{1,0:T(8,128)(2,1)S(1)} %slice.46), channel_id=1, source_target_pairs={{0,2},{1,3},{2,0},{3,1},{4,6},{5,7},{6,4},{7,5},{8,10},{9,11},{10,... | collective-permute-start | bytes 786440 | tf_op jit(solution)/shard_map/ppermute | solution.py:424
  99.9 22.4 %collective-permute-start.32 = (bf16[128,1024]{1,0:T(8,128)(2,1)S(1)}, bf16[128,1024]{1,0:T(8,128)(2,1)S(1)}, u32[]{:S(2)}, u32[]{:S(2)}) collective-permute-start(bf16[128,1024]{1,0:T(8,128)(2,1)S(1)} %slice.47), channel_id=1, source_target_pairs={{0,4},{1,5},{2,6},{3,7},{4,0},{5,1},{6,2},{7,3},{8,12},{9,13},{10,... | collective-permute-start | bytes 786440 | tf_op jit(solution)/shard_map/ppermute | solution.py:424
  123.6 2.0 %collective-permute-start.33 = (bf16[256,1024]{1,0:T(8,128)(2,1)S(1)}, bf16[256,1024]{1,0:T(8,128)(2,1)S(1)}, u32[]{:S(2)}, u32[]{:S(2)}) collective-permute-start(bf16[256,1024]{1,0:T(8,128)(2,1)S(1)} %get-tuple-element.43), channel_id=1, source_target_pairs={{0,1},{1,0},{2,3},{3,2},{4,5},{5,4},{6,7},{7,6},{8,9},{9,8},{10,11... | collective-permute-start | bytes 1572872 | tf_op jit(solution)/shard_map/ppermute | solution.py:424
  123.6 4.1 %collective-permute-start.25 = (bf16[256,1024]{1,0:T(8,128)(2,1)S(1)}, bf16[256,1024]{1,0:T(8,128)(2,1)S(1)}, u32[]{:S(2)}, u32[]{:S(2)}) collective-permute-start(bf16[256,1024]{1,0:T(8,128)(2,1)S(1)} %get-tuple-element.37), channel_id=1, source_target_pairs={{0,1},{1,0},{2,3},{3,2},{4,5},{5,4},{6,7},{7,6},{8,9},{9,8},{10,11... | collective-permute-start | bytes 1572872 | tf_op jit(solution)/shard_map/ppermute | solution.py:424
  125.6 8.4 %collective-permute-start.34 = (bf16[64,1024]{1,0:T(8,128)(2,1)S(1)}, bf16[64,1024]{1,0:T(8,128)(2,1)S(1)}, u32[]{:S(2)}, u32[]{:S(2)}) collective-permute-start(bf16[64,1024]{1,0:T(8,128)(2,1)S(1)} %get-tuple-element.44), channel_id=1, source_target_pairs={{0,24},{1,25},{2,26},{3,27},{4,28},{5,29},{6,30},{7,31},{8,0},{9,1... | collective-permute-start | bytes 393224 | tf_op jit(solution)/shard_map/ppermute | solution.py:424
  125.7 13.9 %collective-permute-start.35 = (bf16[64,1024]{1,0:T(8,128)(2,1)S(1)}, bf16[64,1024]{1,0:T(8,128)(2,1)S(1)}, u32[]{:S(2)}, u32[]{:S(2)}) collective-permute-start(bf16[64,1024]{1,0:T(8,128)(2,1)S(1)} %get-tuple-element.45), channel_id=1, source_target_pairs={{0,16},{1,17},{2,18},{3,19},{4,20},{5,21},{6,22},{7,23},{8,24},{9,... | collective-permute-start | bytes 393224 | tf_op jit(solution)/shard_map/ppermute | solution.py:424
  125.7 13.8 %collective-permute-start.36 = (bf16[64,1024]{1,0:T(8,128)(2,1)S(1)}, bf16[64,1024]{1,0:T(8,128)(2,1)S(1)}, u32[]{:S(2)}, u32[]{:S(2)}) collective-permute-start(bf16[64,1024]{1,0:T(8,128)(2,1)S(1)} %get-tuple-element.46), channel_id=1, source_target_pairs={{0,8},{1,9},{2,10},{3,11},{4,12},{5,13},{6,14},{7,15},{8,16},{9,17... | collective-permute-start | bytes 393224 | tf_op jit(solution)/shard_map/ppermute | solution.py:424
  127.8 11.8 %collective-permute-start.26 = (bf16[64,1024]{1,0:T(8,128)(2,1)S(1)}, bf16[64,1024]{1,0:T(8,128)(2,1)S(1)}, u32[]{:S(2)}, u32[]{:S(2)}) collective-permute-start(bf16[64,1024]{1,0:T(8,128)(2,1)S(1)} %get-tuple-element.38), channel_id=1, source_target_pairs={{0,24},{1,25},{2,26},{3,27},{4,28},{5,29},{6,30},{7,31},{8,0},{9,1... | collective-permute-start | bytes 393224 | tf_op jit(solution)/shard_map/ppermute | solution.py:424
  130.2 18.9 %collective-permute-start.27 = (bf16[64,1024]{1,0:T(8,128)(2,1)S(1)}, bf16[64,1024]{1,0:T(8,128)(2,1)S(1)}, u32[]{:S(2)}, u32[]{:S(2)}) collective-permute-start(bf16[64,1024]{1,0:T(8,128)(2,1)S(1)} %get-tuple-element.39), channel_id=1, source_target_pairs={{0,16},{1,17},{2,18},{3,19},{4,20},{5,21},{6,22},{7,23},{8,24},{9,... | collective-permute-start | bytes 393224 | tf_op jit(solution)/shard_map/ppermute | solution.py:424
  134.0 15.1 %collective-permute-start.28 = (bf16[64,1024]{1,0:T(8,128)(2,1)S(1)}, bf16[64,1024]{1,0:T(8,128)(2,1)S(1)}, u32[]{:S(2)}, u32[]{:S(2)}) collective-permute-start(bf16[64,1024]{1,0:T(8,128)(2,1)S(1)} %get-tuple-element.40), channel_id=1, source_target_pairs={{0,8},{1,9},{2,10},{3,11},{4,12},{5,13},{6,14},{7,15},{8,16},{9,17... | collective-permute-start | bytes 393224 | tf_op jit(solution)/shard_map/ppermute | solution.py:424

commit v2 on v1

--- a/solution.py
+++ b/solution.py
@@ -93,9 +93,10 @@
             )
 
 
-def kernel_call(body, out_shape, scratch=(), smem=0, n_in=0, mib=16):
+def kernel_call(body, out_shape, scratch=(), smem=0, n_in=0, mib=16, fetched=False):
     specs = [pl.BlockSpec(memory_space=pltpu.SMEM)] * smem
-    specs += [pl.BlockSpec(memory_space=pltpu.VMEM)] * (n_in - smem)
+    space = pltpu.HBM if fetched else pltpu.VMEM
+    specs += [pl.BlockSpec(memory_space=space)] * (n_in - smem)
     many = isinstance(out_shape, (list, tuple))
     out_spec = pl.BlockSpec(memory_space=pltpu.VMEM)
     return pl.pallas_call(
@@ -106,6 +107,22 @@
         scratch_shapes=list(scratch),
         compiler_params=pltpu.CompilerParams(vmem_limit_bytes=mib * 1024 * 1024),
     )
+
+
+def fetch_then(body, n):
+    def run(*refs):
+        sources, outs, held, sems = refs[:n], refs[n : -n - 1], refs[-n - 1 : -1], refs[-1]
+        copies = [
+            pltpu.make_async_copy(src, dst, sems.at[k])
+            for k, (src, dst) in enumerate(zip(sources, held))
+        ]
+        for copy in copies:
+            copy.start()
+        for copy in copies:
+            copy.wait()
+        body(*held, *outs)
+
+    return run
 
 
 def pair_body(place, mine, theirs, out):
@@ -197,8 +214,9 @@
     at = 0
     for group in pieces:
         for piece in group:
-            n = piece.shape[0]
-            down_all[at : at + n, :] = piece[...]
+            src, off = piece
+            n = src.shape[0]
+            down_all[at : at + n, :] = src[:, off : off + down_all.shape[1]]
             at += n
     acc = jnp.dot(units, down_all[...], preferred_element_type=F32)
     cut = keep.shape[0]
@@ -447,13 +465,21 @@
 
         packed_shape = jax.ShapeDtypeStruct((heads * HEAD + 16, HEAD), BF16)
         gate, cum, packed = kernel_call(
-            gates_body,
+            fetch_then(gates_body, 4),
             [
                 jax.ShapeDtypeStruct((rows, width), F32),
                 jax.ShapeDtypeStruct((rows, width), F32),
                 packed_shape,
             ],
+            scratch=[
+                pltpu.VMEM((rows, width), BF16),
+                pltpu.VMEM((rows, width), BF16),
+                pltpu.VMEM((1, width), F32),
+                pltpu.VMEM((rows, width), F32),
+                pltpu.SemaphoreType.DMA((4,)),
+            ],
             n_in=4,
+            fetched=True,
         )(forget_logits, written_values, forget_floor_gap[None, :], extra_log_decay)
         up_rows, up_cols = mixer_up_weight.shape
         piece = up_cols // n_a
@@ -466,19 +492,20 @@
             joined = jnp.concatenate(mine[g::2], axis=0)
             up_x.append(send(joined, b=1))
             up_y.append(send(joined, y=1))
-        up_xy = [send(up_y[0], b=1), send(up_x[1], y=1)]
+        up_xy = [send(up_x[0], y=1), send(up_y[1], b=1)]
 
         def grouped(refs):
             return [(refs[e % 2], e // 2 * up_rows) for e in range(n_a)]
 
         part = model // 2
         half = mixer_down_weight.shape[0] // 2
-        down = [mixer_down_weight[:, :part], mixer_down_weight[:, part:]]
-        down_x = [send(u, b=1) for u in down]
-        down_y = [send(u, y=1) for u in down]
-        down_xy = [
-            [send(down_y[0], b=1)], [send(down_x[1][:half], y=1), send(down_y[1][half:], b=1)]
-        ]
+        down_x = send(mixer_down_weight, b=1)
+        down_y = send(mixer_down_weight, y=1)
+        down_xy = []
+        for k in range(2):
+            lanes = slice(k * part, (k + 1) * part)
+            down_xy.append([send(down_x[:half, lanes], y=1), send(down_y[half:, lanes], b=1)])
+        whole = [mixer_down_weight, down_x, down_y]
 
         beside = send(packed, b=1)
         pair = kernel_call(pair_body, packed_shape, smem=1, n_in=3)(place, packed, beside)
@@ -548,8 +575,8 @@
 
         def second_half(*refs):
             ups = grouped(refs[3:5]) + grouped(refs[5:7])
-            pieces = [[refs[7]], [refs[8]], [refs[9]], [refs[10]]]
-            lower_body(cols, *refs[:3], ups, pieces, *refs[11:])
+            pieces = [[(r, 0)] for r in refs[7:10]] + [[(refs[10], 0), (refs[11], 0)]]
+            lower_body(cols, *refs[:3], ups, pieces, *refs[12:])
 
         keep0, away0, hidden = kernel_call(
             second_half,
@@ -560,18 +587,19 @@
                 pltpu.VMEM((units, part), BF16),
             ],
             smem=1,
-            n_in=11,
-            mib=28,
-        )(place, rows_x, early, *up_y, *up_xy, down[0], down_x[0], down_y[0], *down_xy[0])
+            n_in=12,
+            mib=30,
+        )(place, rows_x, early, *up_y, *up_xy, *whole, *down_xy[0])
         got0 = send(away0, c=1)
 
         def last_columns(hidden_ref, own_ref, x_ref, y_ref, r0_ref, r1_ref, keep, away, down_all):
-            pieces = [[own_ref], [x_ref], [y_ref], [r0_ref, r1_ref]]
+            pieces = [[(r, part)] for r in (own_ref, x_ref, y_ref)]
+            pieces.append([(r0_ref, 0), (r1_ref, 0)])
             down_product(keep, away, hidden_ref[...], pieces, down_all)
 
         keep1, away1 = kernel_call(
             last_columns, sizes, scratch=[pltpu.VMEM((units, part), BF16)], n_in=6
-        )(hidden, down[1], down_x[1], down_y[1], *down_xy[1])
+        )(hidden, *whole, *down_xy[1])
         got1 = send(away1, c=1)
         halves = []
         for k, (keep, got) in enumerate([(keep0, got0), (keep1, got1)]):

time: 150 us -> 157 us (1.047)
  starting transfers between devices: 41.1 us -> 44.4 us
  waiting for transfers between devices: 85.9 us -> 89.1 us
    ppermute x37 -> x36, starting transfers between devices: 41.1 us -> 44.4 us  [send(): return lax.ppermute(x, AXES, pairs)]
    ppermute x37 -> x36, waiting for transfers between devices: 85.9 us -> 89.1 us  [send(): return lax.ppermute(x, AXES, pairs)]
  transfers between devices with their start and end apart: 37 -> 36, of which waited for: 18 -> 17; matrix products, arithmetic and copies ran while one was open for 0% -> 0% of each run, Pallas kernels for 6% -> 5%
where the time goes in v2:
time: 157 us
  waiting for transfers between devices  89.1 us (57%)
  starting transfers between devices  44.4 us (28%)
  Pallas kernels  13.8 us (9%)
  local copies, waits for them, and re-layouts  8.03 us (5%)
    ppermute x36, waiting for transfers between devices, send(): return lax.ppermute(x, AXES, pairs)  89.1 us
    ppermute x36, starting transfers between devices, send(): return lax.ppermute(x, AXES, pairs)  44.4 us
    unnamed x29, local copies, waits for them, and re-layouts  7.83 us
    pallas_call x1, Pallas kernels, on_device(): kernel_call(local_body, jax.ShapeDtypeStruct((rows, width), F32), n_in=4)  3.44 us
  transfers between devices with their start and end apart: 36, of which 17 were waited for; matrix products, arithmetic and copies ran while one was open for 0% of the time, Pallas kernels for 5%

profile of v2, /device:TPU:0, one launch (start us, length us, event | category | flops | bytes accessed | tf_op | source)
XLA Modules:
  0.0 156.8 jit_solution(11767063595951493619)
XLA Ops:
  0.0 1.0 copy-done.2
  1.0 0.9 copy-done.6
  1.9 0.9 copy-done.8
  2.9 0.7 copy-done.11
  3.5 1.7 %shard_map.118 = (f32[256,256]{1,0:T(8,128)S(1)}, f32[256,256]{1,0:T(8,128)S(1)}, bf16[272,128]{1,0:T(8,128)(2,1)S(1)}) custom-call(bf16[256,256]{1,0:T(8,128)(2,1)S(1)} %copy-done.8, bf16[256,256]{1,0:T(8,128)(2,1)S(1)} %copy-done.2, f32[1,256]{1,0:T(1,128)S(1)} %bitcast.8, f32[256,256]{1,0:T(8,128)S(1)} %copy-done.6), custom_call_target="tpu_custom_call" | custom-call | tf_op jit(solution)/shard_map/pallas_call | solution.py:467
  5.2 3.0 %collective-permute-start = (bf16[272,128]{1,0:T(8,128)(2,1)S(1)}, bf16[272,128]{1,0:T(8,128)(2,1)S(1)}, u32[]{:S(2)}, u32[]{:S(2)}) collective-permute-start(bf16[272,128]{1,0:T(8,128)(2,1)S(1)} %get-tuple-element.28.mine), channel_id=1, source_target_pairs={{0,4},{1,5},{2,6},{3,7},{4,0},{5,1},{6,2},{7,3},{8,12},{9,13},{10,... | collective-permute-start | bytes 208904 | tf_op jit(solution)/shard_map/ppermute | solution.py:442
  8.3 2.2 %collective-permute-done.theirs.refs_7_ = bf16[272,128]{1,0:T(8,128)(2,1)S(1)} collective-permute-done((bf16[272,128]{1,0:T(8,128)(2,1)S(1)}, bf16[272,128]{1,0:T(8,128)(2,1)S(1)}, u32[]{:S(2)}, u32[]{:S(2)}) %collective-permute-start) | collective-permute-done | bytes 69664 | tf_op jit(solution)/shard_map/ppermute | solution.py:442
  10.5 0.7 shard_map.120
  11.2 6.0 %collective-permute-start.3 = (bf16[272,128]{1,0:T(8,128)(2,1)S(1)}, bf16[272,128]{1,0:T(8,128)(2,1)S(1)}, u32[]{:S(2)}, u32[]{:S(2)}) collective-permute-start(bf16[272,128]{1,0:T(8,128)(2,1)S(1)} %shard_map.120), channel_id=1, source_target_pairs={{0,24},{1,25},{2,26},{3,27},{4,28},{5,29},{6,30},{7,31}} | collective-permute-start | bytes 208904 | tf_op jit(solution)/shard_map/ppermute | solution.py:442
  17.3 1.3 collective-permute-start.2
  18.6 2.5 %collective-permute-start.1 = (bf16[272,128]{1,0:T(8,128)(2,1)S(1)}, bf16[272,128]{1,0:T(8,128)(2,1)S(1)}, u32[]{:S(2)}, u32[]{:S(2)}) collective-permute-start(bf16[272,128]{1,0:T(8,128)(2,1)S(1)} %shard_map.120), channel_id=1, source_target_pairs={{0,8},{1,9},{2,10},{3,11},{4,12},{5,13},{6,14},{7,15},{8,16},{9,17... | collective-permute-start | bytes 208904 | tf_op jit(solution)/shard_map/ppermute | solution.py:442
  21.1 0.9 copy-done.3
  22.0 0.9 copy-done.4
  22.9 3.4 %shard_map.119.refs_3_ = f32[256,256]{1,0:T(8,128)S(1)} custom-call(bf16[256,256]{1,0:T(8,128)(2,1)S(1)} %copy-done.4, f32[256,256]{1,0:T(8,128)S(1)} %get-tuple-element.27.gate, f32[256,256]{1,0:T(8,128)S(1)} %get-tuple-element.26.cum.refs_2_, bf16[256,256]{1,0:T(8,128)(2,1)S(1)} %copy-done.3), custom_call_target="tpu_custom_call" | custom-call | tf_op jit(solution)/shard_map/pallas_call | solution.py:513
  26.4 0.9 copy-done.5
  27.3 0.9 copy-done.9
  28.2 0.7 copy-done.12
  28.9 1.6 %shard_map.121 = (f32[64,2048]{1,0:T(8,128)S(1)}, f32[64,2048]{1,0:T(8,128)S(1)}, bf16[128,2048]{1,0:T(8,128)(2,1)S(1)}) custom-call(s32[4]{0:T(128)S(1)} %pad_add_fusion.place.refs_0_, bf16[256,256]{1,0:T(8,128)(2,1)S(1)} %copy-done.5, f32[256,256]{1,0:T(8,128)S(1)} %get-tuple-element.26.cum.refs_2_, f32[256,256]{1,0:T(8,128)S(1)} %shard_map.119.refs_3_, ...), custom_call_target="tpu_custom_call" | custom-call | tf_op jit(solution)/shard_map/pallas_call | solution.py:516
  30.6 0.1 constant_dynamic-slice_fusion
  30.8 3.8 %collective-permute-start.15 = (bf16[256,512]{1,0:T(8,128)(2,1)S(1)}, bf16[256,512]{1,0:T(8,128)(2,1)S(1)}, u32[]{:S(2)}, u32[]{:S(2)}) collective-permute-start(bf16[256,512]{1,0:T(8,128)(2,1)S(1)} %get-tuple-element.51), channel_id=1, source_target_pairs={{0,24},{1,25},{2,26},{3,27},{4,28},{5,29},{6,30},{7,31},{8,0},{9,1... | collective-permute-start | bytes 786440 | tf_op jit(solution)/shard_map/ppermute | solution.py:442
  34.6 1.5 collective-permute-start.23
  36.2 1.5 collective-permute-start.22
  37.7 4.2 %collective-permute-done.13.refs_10_ = bf16[256,512]{1,0:T(8,128)(2,1)S(1)} collective-permute-done((bf16[256,512]{1,0:T(8,128)(2,1)S(1)}, bf16[256,512]{1,0:T(8,128)(2,1)S(1)}, u32[]{:S(2)}, u32[]{:S(2)}) %collective-permute-start.13) | collective-permute-done | bytes 262176 | tf_op jit(solution)/shard_map/ppermute | solution.py:442
  41.9 5.6 %collective-permute-done.15.refs_12_ = bf16[256,512]{1,0:T(8,128)(2,1)S(1)} collective-permute-done((bf16[256,512]{1,0:T(8,128)(2,1)S(1)}, bf16[256,512]{1,0:T(8,128)(2,1)S(1)}, u32[]{:S(2)}, u32[]{:S(2)}) %collective-permute-start.15) | collective-permute-done | bytes 262176 | tf_op jit(solution)/shard_map/ppermute | solution.py:442
  47.5 1.6 %collective-permute-start.19 = (bf16[512,512]{1,0:T(8,128)(2,1)S(1)}, bf16[512,512]{1,0:T(8,128)(2,1)S(1)}, u32[]{:S(2)}, u32[]{:S(2)}) collective-permute-start(bf16[512,512]{1,0:T(8,128)(2,1)S(1)} %constant_dynamic-update-slice_fusion), channel_id=1, source_target_pairs={{0,2},{1,3},{2,0},{3,1},{4,6},{5,7},{6,4},{7,5},{8,10},{9,11},{10,... | collective-permute-start | bytes 1572872 | tf_op jit(solution)/shard_map/ppermute | solution.py:442
  49.1 0.6 collective-permute-start.5
  49.7 6.2 %collective-permute-done.14.refs_11_ = bf16[256,512]{1,0:T(8,128)(2,1)S(1)} collective-permute-done((bf16[256,512]{1,0:T(8,128)(2,1)S(1)}, bf16[256,512]{1,0:T(8,128)(2,1)S(1)}, u32[]{:S(2)}, u32[]{:S(2)}) %collective-permute-start.14) | collective-permute-done | bytes 262176 | tf_op jit(solution)/shard_map/ppermute | solution.py:442
  55.9 1.5 collective-permute-start.17
  57.4 14.5 %collective-permute-done.19.refs_4_ = bf16[512,512]{1,0:T(8,128)(2,1)S(1)} collective-permute-done((bf16[512,512]{1,0:T(8,128)(2,1)S(1)}, bf16[512,512]{1,0:T(8,128)(2,1)S(1)}, u32[]{:S(2)}, u32[]{:S(2)}) %collective-permute-start.19) | collective-permute-done | bytes 524320 | tf_op jit(solution)/shard_map/ppermute | solution.py:442
  71.9 1.5 collective-permute-start.18
  73.4 4.1 %collective-permute-done.5.arrived = bf16[64,2048]{1,0:T(8,128)(2,1)S(1)} collective-permute-done((bf16[64,2048]{1,0:T(8,128)(2,1)S(1)}, bf16[64,2048]{1,0:T(8,128)(2,1)S(1)}, u32[]{:S(2)}, u32[]{:S(2)}) %collective-permute-start.5) | collective-permute-done | bytes 262176 | tf_op jit(solution)/shard_map/ppermute | solution.py:442
  77.5 1.5 collective-permute-start.16
  79.0 0.2 shard_map.122
  79.4 8.4 %collective-permute-done.18.refs_3_ = bf16[512,512]{1,0:T(8,128)(2,1)S(1)} collective-permute-done((bf16[512,512]{1,0:T(8,128)(2,1)S(1)}, bf16[512,512]{1,0:T(8,128)(2,1)S(1)}, u32[]{:S(2)}, u32[]{:S(2)}) %collective-permute-start.18) | collective-permute-done | bytes 524320 | tf_op jit(solution)/shard_map/ppermute | solution.py:442
  87.7 0.3 collective-permute-start.8
  88.0 1.4 collective-permute-done.16.refs_13_
  89.4 1.1 collective-permute-start.6
  90.5 1.5 collective-permute-start.21
  92.0 1.5 collective-permute-start.20
  93.5 2.6 %collective-permute-done.8.refs_4_ = bf16[8,64,256]{2,1,0:T(8,128)(2,1)S(1)} collective-permute-done((bf16[8,64,256]{2,1,0:T(8,128)(2,1)S(1)}, bf16[8,64,256]{2,1,0:T(8,128)(2,1)S(1)}, u32[]{:S(2)}, u32[]{:S(2)}) %collective-permute-start.8) | collective-permute-done | bytes 262176 | tf_op jit(solution)/shard_map/ppermute | solution.py:442
  96.1 14.0 %collective-permute-done.7.refs_3_ = bf16[8,64,256]{2,1,0:T(8,128)(2,1)S(1)} collective-permute-done((bf16[8,64,256]{2,1,0:T(8,128)(2,1)S(1)}, bf16[8,64,256]{2,1,0:T(8,128)(2,1)S(1)}, u32[]{:S(2)}, u32[]{:S(2)}) %collective-permute-start.7) | collective-permute-done | bytes 262176 | tf_op jit(solution)/shard_map/ppermute | solution.py:442
  110.1 0.5 collective-permute-start.10
  110.7 1.6 collective-permute-start.25
  112.3 1.5 collective-permute-start.24
  113.8 0.5 collective-permute-start.31
  114.3 0.5 collective-permute-start.30
  114.8 1.8 %shard_map.123 = (bf16[512,2048]{1,0:T(8,128)(2,1)S(1)}, bf16[512,512]{1,0:T(8,128)(2,1)S(1)}) custom-call(s32[4]{0:T(128)S(1)} %pad_add_fusion.place.refs_0_, bf16[8,64,256]{2,1,0:T(8,128)(2,1)S(1)} %get-tuple-element.33.refs_1_, bf16[8,64,256]{2,1,0:T(8,128)(2,1)S(1)} %collective-permute-done.6.refs_2_, ...), custom_call_target="tpu_custom_call" | custom-call | tf_op jit(solution)/shard_map/pallas_call | solution.py:564
  116.6 3.3 %collective-permute-done.25.refs_11_ = bf16[128,1024]{1,0:T(8,128)(2,1)S(1)} collective-permute-done((bf16[128,1024]{1,0:T(8,128)(2,1)S(1)}, bf16[128,1024]{1,0:T(8,128)(2,1)S(1)}, u32[]{:S(2)}, u32[]{:S(2)}) %collective-permute-start.25) | collective-permute-done | bytes 262176 | tf_op jit(solution)/shard_map/ppermute | solution.py:442
  119.9 1.5 collective-permute-done.24.refs_10_
  121.4 3.0 %shard_map.124 = (f32[256,1024]{1,0:T(8,128)S(1)}, bf16[256,1024]{1,0:T(8,128)(2,1)S(1)}, bf16[512,1024]{1,0:T(8,128)(2,1)S(1)}) custom-call(s32[4]{0:T(128)S(1)} %pad_add_fusion.place.refs_0_, bf16[512,2048]{1,0:T(8,128)(2,1)S(1)} %get-tuple-element.34.refs_1_, bf16[512,512]{1,0:T(8,128)(2,1)S(1)} %get-tuple-element.35.refs_2_, ...), custom_call_target="tpu_custom_call" | custom-call | tf_op jit(solution)/shard_map/pallas_call | solution.py:581
  124.4 0.2 collective-permute-done.31.r1_ref
  124.6 1.2 collective-permute-done.30.r0_ref
  125.8 1.3 shard_map.126
  127.2 0.5 collective-permute-start.26
  127.7 1.4 collective-permute-done.32.got
  129.2 3.3 %collective-permute-start.34 = (bf16[64,1024]{1,0:T(8,128)(2,1)S(1)}, bf16[64,1024]{1,0:T(8,128)(2,1)S(1)}, u32[]{:S(2)}, u32[]{:S(2)}) collective-permute-start(bf16[64,1024]{1,0:T(8,128)(2,1)S(1)} %get-tuple-element.45), channel_id=1, source_target_pairs={{0,16},{1,17},{2,18},{3,19},{4,20},{5,21},{6,22},{7,23},{8,24},{9,... | collective-permute-start | bytes 393224 | tf_op jit(solution)/shard_map/ppermute | solution.py:442
  132.5 1.9 %collective-permute-start.35 = (bf16[64,1024]{1,0:T(8,128)(2,1)S(1)}, bf16[64,1024]{1,0:T(8,128)(2,1)S(1)}, u32[]{:S(2)}, u32[]{:S(2)}) collective-permute-start(bf16[64,1024]{1,0:T(8,128)(2,1)S(1)} %get-tuple-element.46), channel_id=1, source_target_pairs={{0,8},{1,9},{2,10},{3,11},{4,12},{5,13},{6,14},{7,15},{8,16},{9,17... | collective-permute-start | bytes 393224 | tf_op jit(solution)/shard_map/ppermute | solution.py:442
  134.4 0.1 shard_map.125
  134.5 1.9 %collective-permute-start.27 = (bf16[64,1024]{1,0:T(8,128)(2,1)S(1)}, bf16[64,1024]{1,0:T(8,128)(2,1)S(1)}, u32[]{:S(2)}, u32[]{:S(2)}) collective-permute-start(bf16[64,1024]{1,0:T(8,128)(2,1)S(1)} %get-tuple-element.38), channel_id=1, source_target_pairs={{0,24},{1,25},{2,26},{3,27},{4,28},{5,29},{6,30},{7,31},{8,0},{9,1... | collective-permute-start | bytes 393224 | tf_op jit(solution)/shard_map/ppermute | solution.py:442
  136.5 1.1 collective-permute-start.29
  137.5 7.8 %collective-permute-done.34 = bf16[64,1024]{1,0:T(8,128)(2,1)S(1)} collective-permute-done((bf16[64,1024]{1,0:T(8,128)(2,1)S(1)}, bf16[64,1024]{1,0:T(8,128)(2,1)S(1)}, u32[]{:S(2)}, u32[]{:S(2)}) %collective-permute-start.34) | collective-permute-done | bytes 131104 | tf_op jit(solution)/shard_map/ppermute | solution.py:442
  145.3 10.5 %collective-permute-done.28 = bf16[64,1024]{1,0:T(8,128)(2,1)S(1)} collective-permute-done((bf16[64,1024]{1,0:T(8,128)(2,1)S(1)}, bf16[64,1024]{1,0:T(8,128)(2,1)S(1)}, u32[]{:S(2)}, u32[]{:S(2)}) %collective-permute-start.28) | collective-permute-done | bytes 131104 | tf_op jit(solution)/shard_map/ppermute | solution.py:442
  155.9 0.2 add_convert_fusion.2
  156.1 0.7 pad_maximum_fusion.1
  (56 shorter events, 0.8 us)
Async XLA Ops:
  0.0 26.4 %copy-start.1 = (bf16[256,2048]{1,0:T(8,128)(2,1)S(1)}, bf16[256,2048]{1,0:T(8,128)(2,1)}, u32[]{:S(2)}) copy-start(bf16[256,2048]{1,0:T(8,128)(2,1)} %refs_6_.1) | copy-start | bytes 3145732
  0.0 1.0 copy-start.2
  1.0 0.9 copy-start.6
  1.9 0.9 copy-start.8
  2.9 0.7 copy-start.11
  5.2 5.3 %collective-permute-start = (bf16[272,128]{1,0:T(8,128)(2,1)S(1)}, bf16[272,128]{1,0:T(8,128)(2,1)S(1)}, u32[]{:S(2)}, u32[]{:S(2)}) collective-permute-start(bf16[272,128]{1,0:T(8,128)(2,1)S(1)} %get-tuple-element.28.mine), channel_id=1, source_target_pairs={{0,4},{1,5},{2,6},{3,7},{4,0},{5,1},{6,2},{7,3},{8,12},{9,13},{10,... | collective-permute-start | bytes 208904 | tf_op jit(solution)/shard_map/ppermute | solution.py:442
  11.2 15.2 %collective-permute-start.3 = (bf16[272,128]{1,0:T(8,128)(2,1)S(1)}, bf16[272,128]{1,0:T(8,128)(2,1)S(1)}, u32[]{:S(2)}, u32[]{:S(2)}) collective-permute-start(bf16[272,128]{1,0:T(8,128)(2,1)S(1)} %shard_map.120), channel_id=1, source_target_pairs={{0,24},{1,25},{2,26},{3,27},{4,28},{5,29},{6,30},{7,31}} | collective-permute-start | bytes 208904 | tf_op jit(solution)/shard_map/ppermute | solution.py:442
  17.3 9.1 %collective-permute-start.2 = (bf16[272,128]{1,0:T(8,128)(2,1)S(1)}, bf16[272,128]{1,0:T(8,128)(2,1)S(1)}, u32[]{:S(2)}, u32[]{:S(2)}) collective-permute-start(bf16[272,128]{1,0:T(8,128)(2,1)S(1)} %shard_map.120), channel_id=1, source_target_pairs={{0,16},{1,17},{2,18},{3,19},{4,20},{5,21},{6,22},{7,23},{8,24},{9,... | collective-permute-start | bytes 208904 | tf_op jit(solution)/shard_map/ppermute | solution.py:442
  18.6 7.8 %collective-permute-start.1 = (bf16[272,128]{1,0:T(8,128)(2,1)S(1)}, bf16[272,128]{1,0:T(8,128)(2,1)S(1)}, u32[]{:S(2)}, u32[]{:S(2)}) collective-permute-start(bf16[272,128]{1,0:T(8,128)(2,1)S(1)} %shard_map.120), channel_id=1, source_target_pairs={{0,8},{1,9},{2,10},{3,11},{4,12},{5,13},{6,14},{7,15},{8,16},{9,17... | collective-permute-start | bytes 208904 | tf_op jit(solution)/shard_map/ppermute | solution.py:442
  21.1 0.9 copy-start.3
  22.0 0.9 copy-start.4
  26.4 0.9 copy-start.5
  27.3 0.9 copy-start.9
  28.2 0.7 copy-start.12
  28.9 1.7 %copy-start.13 = (bf16[256,2048]{1,0:T(8,128)(2,1)S(1)}, bf16[256,2048]{1,0:T(8,128)(2,1)}, u32[]{:S(2)}) copy-start(bf16[256,2048]{1,0:T(8,128)(2,1)} %param.22) | copy-start | bytes 3145732
  28.9 5.8 %copy-start = (bf16[256,2048]{1,0:T(8,128)(2,1)S(1)}, bf16[256,2048]{1,0:T(8,128)(2,1)}, u32[]{:S(2)}) copy-start(bf16[256,2048]{1,0:T(8,128)(2,1)} %own_ref.1) | copy-start | bytes 3145732
  30.5 18.6 %collective-permute-start.4 = (bf16[128,2048]{1,0:T(8,128)(2,1)S(1)}, bf16[128,2048]{1,0:T(8,128)(2,1)S(1)}, u32[]{:S(2)}, u32[]{:S(2)}) collective-permute-start(bf16[128,2048]{1,0:T(8,128)(2,1)S(1)} %get-tuple-element.30), channel_id=1, source_target_pairs={{0,1},{1,0},{2,3},{3,2},{4,5},{5,4},{6,7},{7,6},{8,9},{9,8},{10,11... | collective-permute-start | bytes 1572872 | tf_op jit(solution)/shard_map/ppermute | solution.py:442
  30.7 48.3 %copy-start.7 = (bf16[64,2048]{1,0:T(8,128)(2,1)S(1)}, bf16[64,2048]{1,0:T(8,128)(2,1)}, u32[]{:S(2)}) copy-start(bf16[64,2048]{1,0:T(8,128)(2,1)} %residual.1) | copy-start | bytes 786436
  30.8 48.3 %copy-start.10 = (f32[2048]{0:T(1024)S(1)}, f32[2048]{0:T(1024)}, u32[]{:S(2)}) copy-start(f32[2048]{0:T(1024)} %param.21) | copy-start | bytes 24580
  30.8 11.1 %collective-permute-start.13 = (bf16[256,512]{1,0:T(8,128)(2,1)S(1)}, bf16[256,512]{1,0:T(8,128)(2,1)S(1)}, u32[]{:S(2)}, u32[]{:S(2)}) collective-permute-start(bf16[256,512]{1,0:T(8,128)(2,1)S(1)} %get-tuple-element.52), channel_id=1, source_target_pairs={{0,8},{1,9},{2,10},{3,11},{4,12},{5,13},{6,14},{7,15},{8,16},{9,17... | collective-permute-start | bytes 786440 | tf_op jit(solution)/shard_map/ppermute | solution.py:442
  30.8 16.6 %collective-permute-start.15 = (bf16[256,512]{1,0:T(8,128)(2,1)S(1)}, bf16[256,512]{1,0:T(8,128)(2,1)S(1)}, u32[]{:S(2)}, u32[]{:S(2)}) collective-permute-start(bf16[256,512]{1,0:T(8,128)(2,1)S(1)} %get-tuple-element.51), channel_id=1, source_target_pairs={{0,24},{1,25},{2,26},{3,27},{4,28},{5,29},{6,30},{7,31},{8,0},{9,1... | collective-permute-start | bytes 786440 | tf_op jit(solution)/shard_map/ppermute | solution.py:442
  34.6 54.7 %collective-permute-start.23 = (bf16[256,2048]{1,0:T(8,128)(2,1)S(1)}, bf16[256,2048]{1,0:T(8,128)(2,1)S(1)}, u32[]{:S(2)}, u32[]{:S(2)}) collective-permute-start(bf16[256,2048]{1,0:T(8,128)(2,1)S(1)} %copy-done), channel_id=1, source_target_pairs={{0,2},{1,3},{2,0},{3,1},{4,6},{5,7},{6,4},{7,5},{8,10},{9,11},{10,... | collective-permute-start | bytes 3145736 | tf_op jit(solution)/shard_map/ppermute | solution.py:442
  36.2 54.3 %collective-permute-start.22 = (bf16[256,2048]{1,0:T(8,128)(2,1)S(1)}, bf16[256,2048]{1,0:T(8,128)(2,1)S(1)}, u32[]{:S(2)}, u32[]{:S(2)}) collective-permute-start(bf16[256,2048]{1,0:T(8,128)(2,1)S(1)} %copy-done), channel_id=1, source_target_pairs={{0,4},{1,5},{2,6},{3,7},{4,0},{5,1},{6,2},{7,3},{8,12},{9,13},{10,... | collective-permute-start | bytes 3145736 | tf_op jit(solution)/shard_map/ppermute | solution.py:442
  41.8 14.1 %collective-permute-start.14 = (bf16[256,512]{1,0:T(8,128)(2,1)S(1)}, bf16[256,512]{1,0:T(8,128)(2,1)S(1)}, u32[]{:S(2)}, u32[]{:S(2)}) collective-permute-start(bf16[256,512]{1,0:T(8,128)(2,1)S(1)} %get-tuple-element.54), channel_id=1, source_target_pairs={{0,16},{1,17},{2,18},{3,19},{4,20},{5,21},{6,22},{7,23},{8,24},{9,... | collective-permute-start | bytes 786440 | tf_op jit(solution)/shard_map/ppermute | solution.py:442
  47.5 24.4 %collective-permute-start.19 = (bf16[512,512]{1,0:T(8,128)(2,1)S(1)}, bf16[512,512]{1,0:T(8,128)(2,1)S(1)}, u32[]{:S(2)}, u32[]{:S(2)}) collective-permute-start(bf16[512,512]{1,0:T(8,128)(2,1)S(1)} %constant_dynamic-update-slice_fusion), channel_id=1, source_target_pairs={{0,2},{1,3},{2,0},{3,1},{4,6},{5,7},{6,4},{7,5},{8,10},{9,11},{10,... | collective-permute-start | bytes 1572872 | tf_op jit(solution)/shard_map/ppermute | solution.py:442
  49.1 28.4 %collective-permute-start.5 = (bf16[64,2048]{1,0:T(8,128)(2,1)S(1)}, bf16[64,2048]{1,0:T(8,128)(2,1)S(1)}, u32[]{:S(2)}, u32[]{:S(2)}) collective-permute-start(bf16[64,2048]{1,0:T(8,128)(2,1)S(1)} %add_convert_fusion), channel_id=1, source_target_pairs={{0,2},{1,3},{2,0},{3,1},{4,6},{5,7},{6,4},{7,5},{8,10},{9,11},{10,... | collective-permute-start | bytes 786440 | tf_op jit(solution)/shard_map/ppermute | solution.py:442
  55.9 23.4 %collective-permute-start.17 = (bf16[512,512]{1,0:T(8,128)(2,1)S(1)}, bf16[512,512]{1,0:T(8,128)(2,1)S(1)}, u32[]{:S(2)}, u32[]{:S(2)}) collective-permute-start(bf16[512,512]{1,0:T(8,128)(2,1)S(1)} %constant_dynamic-update-slice_fusion), channel_id=1, source_target_pairs={{0,4},{1,5},{2,6},{3,7},{4,0},{5,1},{6,2},{7,3},{8,12},{9,13},{10,... | collective-permute-start | bytes 1572872 | tf_op jit(solution)/shard_map/ppermute | solution.py:442
  71.9 15.8 %collective-permute-start.18 = (bf16[512,512]{1,0:T(8,128)(2,1)S(1)}, bf16[512,512]{1,0:T(8,128)(2,1)S(1)}, u32[]{:S(2)}, u32[]{:S(2)}) collective-permute-start(bf16[512,512]{1,0:T(8,128)(2,1)S(1)} %pad_maximum_fusion), channel_id=1, source_target_pairs={{0,2},{1,3},{2,0},{3,1},{4,6},{5,7},{6,4},{7,5},{8,10},{9,11},{10,... | collective-permute-start | bytes 1572872 | tf_op jit(solution)/shard_map/ppermute | solution.py:442
  77.5 11.8 %collective-permute-start.16 = (bf16[512,512]{1,0:T(8,128)(2,1)S(1)}, bf16[512,512]{1,0:T(8,128)(2,1)S(1)}, u32[]{:S(2)}, u32[]{:S(2)}) collective-permute-start(bf16[512,512]{1,0:T(8,128)(2,1)S(1)} %pad_maximum_fusion), channel_id=1, source_target_pairs={{0,4},{1,5},{2,6},{3,7},{4,0},{5,1},{6,2},{7,3},{8,12},{9,13},{10,... | collective-permute-start | bytes 1572872 | tf_op jit(solution)/shard_map/ppermute | solution.py:442
  79.3 12.7 %collective-permute-start.9 = (bf16[8,64,256]{2,1,0:T(8,128)(2,1)S(1)}, bf16[8,64,256]{2,1,0:T(8,128)(2,1)S(1)}, u32[]{:S(2)}, u32[]{:S(2)}) collective-permute-start(bf16[8,64,256]{2,1,0:T(8,128)(2,1)S(1)} %get-tuple-element.33.refs_1_), channel_id=1, source_target_pairs={{0,1},{1,0},{2,3},{3,2},{4,5},{5,4},{6,7},{7,6},{8,9},{9,8},{10,11... | collective-permute-start | bytes 786440 | tf_op jit(solution)/shard_map/ppermute | solution.py:442
  87.7 8.4 %collective-permute-start.8 = (bf16[8,64,256]{2,1,0:T(8,128)(2,1)S(1)}, bf16[8,64,256]{2,1,0:T(8,128)(2,1)S(1)}, u32[]{:S(2)}, u32[]{:S(2)}) collective-permute-start(bf16[8,64,256]{2,1,0:T(8,128)(2,1)S(1)} %get-tuple-element.33.refs_1_), channel_id=1, source_target_pairs={{0,24},{1,25},{2,26},{3,27},{4,28},{5,29},{6,30},{7,31},{8,0},{9,1... | collective-permute-start | bytes 786440 | tf_op jit(solution)/shard_map/ppermute | solution.py:442
  89.4 20.7 %collective-permute-start.7 = (bf16[8,64,256]{2,1,0:T(8,128)(2,1)S(1)}, bf16[8,64,256]{2,1,0:T(8,128)(2,1)S(1)}, u32[]{:S(2)}, u32[]{:S(2)}) collective-permute-start(bf16[8,64,256]{2,1,0:T(8,128)(2,1)S(1)} %get-tuple-element.33.refs_1_), channel_id=1, source_target_pairs={{0,16},{1,17},{2,18},{3,19},{4,20},{5,21},{6,22},{7,23},{8,24},{9,... | collective-permute-start | bytes 786440 | tf_op jit(solution)/shard_map/ppermute | solution.py:442
  89.4 20.7 %collective-permute-start.6 = (bf16[8,64,256]{2,1,0:T(8,128)(2,1)S(1)}, bf16[8,64,256]{2,1,0:T(8,128)(2,1)S(1)}, u32[]{:S(2)}, u32[]{:S(2)}) collective-permute-start(bf16[8,64,256]{2,1,0:T(8,128)(2,1)S(1)} %get-tuple-element.33.refs_1_), channel_id=1, source_target_pairs={{0,8},{1,9},{2,10},{3,11},{4,12},{5,13},{6,14},{7,15},{8,16},{9,17... | collective-permute-start | bytes 786440 | tf_op jit(solution)/shard_map/ppermute | solution.py:442
  90.5 20.2 %collective-permute-start.21 = (bf16[512,512]{1,0:T(8,128)(2,1)S(1)}, bf16[512,512]{1,0:T(8,128)(2,1)S(1)}, u32[]{:S(2)}, u32[]{:S(2)}) collective-permute-start(bf16[512,512]{1,0:T(8,128)(2,1)S(1)} %collective-permute-done.19.refs_4_), channel_id=1, source_target_pairs={{0,4},{1,5},{2,6},{3,7},{4,0},{5,1},{6,2},{7,3},{8,12},{9,13},{10,... | collective-permute-start | bytes 1572872 | tf_op jit(solution)/shard_map/ppermute | solution.py:442
  92.0 24.6 %collective-permute-start.20 = (bf16[512,512]{1,0:T(8,128)(2,1)S(1)}, bf16[512,512]{1,0:T(8,128)(2,1)S(1)}, u32[]{:S(2)}, u32[]{:S(2)}) collective-permute-start(bf16[512,512]{1,0:T(8,128)(2,1)S(1)} %collective-permute-done.16.refs_13_), channel_id=1, source_target_pairs={{0,2},{1,3},{2,0},{3,1},{4,6},{5,7},{6,4},{7,5},{8,10},{9,11},{10,... | collective-permute-start | bytes 1572872 | tf_op jit(solution)/shard_map/ppermute | solution.py:442
  96.1 16.1 %collective-permute-start.12 = (bf16[8,64,256]{2,1,0:T(8,128)(2,1)S(1)}, bf16[8,64,256]{2,1,0:T(8,128)(2,1)S(1)}, u32[]{:S(2)}, u32[]{:S(2)}) collective-permute-start(bf16[8,64,256]{2,1,0:T(8,128)(2,1)S(1)} %collective-permute-done.8.refs_4_), channel_id=1, source_target_pairs={{0,1},{1,0},{2,3},{3,2},{4,5},{5,4},{6,7},{7,6},{8,9},{9,8},{10,11... | collective-permute-start | bytes 786440 | tf_op jit(solution)/shard_map/ppermute | solution.py:442
  110.1 3.7 %collective-permute-start.11 = (bf16[8,64,256]{2,1,0:T(8,128)(2,1)S(1)}, bf16[8,64,256]{2,1,0:T(8,128)(2,1)S(1)}, u32[]{:S(2)}, u32[]{:S(2)}) collective-permute-start(bf16[8,64,256]{2,1,0:T(8,128)(2,1)S(1)} %collective-permute-done.7.refs_3_), channel_id=1, source_target_pairs={{0,1},{1,0},{2,3},{3,2},{4,5},{5,4},{6,7},{7,6},{8,9},{9,8},{10,11... | collective-permute-start | bytes 786440 | tf_op jit(solution)/shard_map/ppermute | solution.py:442
  110.1 4.2 %collective-permute-start.10 = (bf16[8,64,256]{2,1,0:T(8,128)(2,1)S(1)}, bf16[8,64,256]{2,1,0:T(8,128)(2,1)S(1)}, u32[]{:S(2)}, u32[]{:S(2)}) collective-permute-start(bf16[8,64,256]{2,1,0:T(8,128)(2,1)S(1)} %collective-permute-done.6.refs_2_), channel_id=1, source_target_pairs={{0,1},{1,0},{2,3},{3,2},{4,5},{5,4},{6,7},{7,6},{8,9},{9,8},{10,11... | collective-permute-start | bytes 786440 | tf_op jit(solution)/shard_map/ppermute | solution.py:442
  110.7 9.2 %collective-permute-start.25 = (bf16[128,1024]{1,0:T(8,128)(2,1)S(1)}, bf16[128,1024]{1,0:T(8,128)(2,1)S(1)}, u32[]{:S(2)}, u32[]{:S(2)}) collective-permute-start(bf16[128,1024]{1,0:T(8,128)(2,1)S(1)} %get-tuple-element.48), channel_id=1, source_target_pairs={{0,4},{1,5},{2,6},{3,7},{4,0},{5,1},{6,2},{7,3},{8,12},{9,13},{10,... | collective-permute-start | bytes 786440 | tf_op jit(solution)/shard_map/ppermute | solution.py:442
  112.3 9.2 %collective-permute-start.24 = (bf16[128,1024]{1,0:T(8,128)(2,1)S(1)}, bf16[128,1024]{1,0:T(8,128)(2,1)S(1)}, u32[]{:S(2)}, u32[]{:S(2)}) collective-permute-start(bf16[128,1024]{1,0:T(8,128)(2,1)S(1)} %get-tuple-element.50), channel_id=1, source_target_pairs={{0,2},{1,3},{2,0},{3,1},{4,6},{5,7},{6,4},{7,5},{8,10},{9,11},{10,... | collective-permute-start | bytes 786440 | tf_op jit(solution)/shard_map/ppermute | solution.py:442
  113.8 10.8 %collective-permute-start.31 = (bf16[128,1024]{1,0:T(8,128)(2,1)S(1)}, bf16[128,1024]{1,0:T(8,128)(2,1)S(1)}, u32[]{:S(2)}, u32[]{:S(2)}) collective-permute-start(bf16[128,1024]{1,0:T(8,128)(2,1)S(1)} %get-tuple-element.47), channel_id=1, source_target_pairs={{0,4},{1,5},{2,6},{3,7},{4,0},{5,1},{6,2},{7,3},{8,12},{9,13},{10,... | collective-permute-start | bytes 786440 | tf_op jit(solution)/shard_map/ppermute | solution.py:442
  114.3 11.5 %collective-permute-start.30 = (bf16[128,1024]{1,0:T(8,128)(2,1)S(1)}, bf16[128,1024]{1,0:T(8,128)(2,1)S(1)}, u32[]{:S(2)}, u32[]{:S(2)}) collective-permute-start(bf16[128,1024]{1,0:T(8,128)(2,1)S(1)} %get-tuple-element.49), channel_id=1, source_target_pairs={{0,2},{1,3},{2,0},{3,1},{4,6},{5,7},{6,4},{7,5},{8,10},{9,11},{10,... | collective-permute-start | bytes 786440 | tf_op jit(solution)/shard_map/ppermute | solution.py:442
  127.1 2.0 %collective-permute-start.32 = (bf16[256,1024]{1,0:T(8,128)(2,1)S(1)}, bf16[256,1024]{1,0:T(8,128)(2,1)S(1)}, u32[]{:S(2)}, u32[]{:S(2)}) collective-permute-start(bf16[256,1024]{1,0:T(8,128)(2,1)S(1)} %get-tuple-element.43), channel_id=1, source_target_pairs={{0,1},{1,0},{2,3},{3,2},{4,5},{5,4},{6,7},{7,6},{8,9},{9,8},{10,11... | collective-permute-start | bytes 1572872 | tf_op jit(solution)/shard_map/ppermute | solution.py:442
  127.2 7.3 %collective-permute-start.26 = (bf16[256,1024]{1,0:T(8,128)(2,1)S(1)}, bf16[256,1024]{1,0:T(8,128)(2,1)S(1)}, u32[]{:S(2)}, u32[]{:S(2)}) collective-permute-start(bf16[256,1024]{1,0:T(8,128)(2,1)S(1)} %get-tuple-element.37), channel_id=1, source_target_pairs={{0,1},{1,0},{2,3},{3,2},{4,5},{5,4},{6,7},{7,6},{8,9},{9,8},{10,11... | collective-permute-start | bytes 1572872 | tf_op jit(solution)/shard_map/ppermute | solution.py:442
  129.1 7.3 %collective-permute-start.33 = (bf16[64,1024]{1,0:T(8,128)(2,1)S(1)}, bf16[64,1024]{1,0:T(8,128)(2,1)S(1)}, u32[]{:S(2)}, u32[]{:S(2)}) collective-permute-start(bf16[64,1024]{1,0:T(8,128)(2,1)S(1)} %get-tuple-element.44), channel_id=1, source_target_pairs={{0,24},{1,25},{2,26},{3,27},{4,28},{5,29},{6,30},{7,31},{8,0},{9,1... | collective-permute-start | bytes 393224 | tf_op jit(solution)/shard_map/ppermute | solution.py:442
  129.2 16.1 %collective-permute-start.34 = (bf16[64,1024]{1,0:T(8,128)(2,1)S(1)}, bf16[64,1024]{1,0:T(8,128)(2,1)S(1)}, u32[]{:S(2)}, u32[]{:S(2)}) collective-permute-start(bf16[64,1024]{1,0:T(8,128)(2,1)S(1)} %get-tuple-element.45), channel_id=1, source_target_pairs={{0,16},{1,17},{2,18},{3,19},{4,20},{5,21},{6,22},{7,23},{8,24},{9,... | collective-permute-start | bytes 393224 | tf_op jit(solution)/shard_map/ppermute | solution.py:442
  132.5 12.9 %collective-permute-start.35 = (bf16[64,1024]{1,0:T(8,128)(2,1)S(1)}, bf16[64,1024]{1,0:T(8,128)(2,1)S(1)}, u32[]{:S(2)}, u32[]{:S(2)}) collective-permute-start(bf16[64,1024]{1,0:T(8,128)(2,1)S(1)} %get-tuple-element.46), channel_id=1, source_target_pairs={{0,8},{1,9},{2,10},{3,11},{4,12},{5,13},{6,14},{7,15},{8,16},{9,17... | collective-permute-start | bytes 393224 | tf_op jit(solution)/shard_map/ppermute | solution.py:442
  134.5 10.8 %collective-permute-start.27 = (bf16[64,1024]{1,0:T(8,128)(2,1)S(1)}, bf16[64,1024]{1,0:T(8,128)(2,1)S(1)}, u32[]{:S(2)}, u32[]{:S(2)}) collective-permute-start(bf16[64,1024]{1,0:T(8,128)(2,1)S(1)} %get-tuple-element.38), channel_id=1, source_target_pairs={{0,24},{1,25},{2,26},{3,27},{4,28},{5,29},{6,30},{7,31},{8,0},{9,1... | collective-permute-start | bytes 393224 | tf_op jit(solution)/shard_map/ppermute | solution.py:442
  136.5 19.4 %collective-permute-start.28 = (bf16[64,1024]{1,0:T(8,128)(2,1)S(1)}, bf16[64,1024]{1,0:T(8,128)(2,1)S(1)}, u32[]{:S(2)}, u32[]{:S(2)}) collective-permute-start(bf16[64,1024]{1,0:T(8,128)(2,1)S(1)} %get-tuple-element.39), channel_id=1, source_target_pairs={{0,16},{1,17},{2,18},{3,19},{4,20},{5,21},{6,22},{7,23},{8,24},{9,... | collective-permute-start | bytes 393224 | tf_op jit(solution)/shard_map/ppermute | solution.py:442
  136.5 19.4 %collective-permute-start.29 = (bf16[64,1024]{1,0:T(8,128)(2,1)S(1)}, bf16[64,1024]{1,0:T(8,128)(2,1)S(1)}, u32[]{:S(2)}, u32[]{:S(2)}) collective-permute-start(bf16[64,1024]{1,0:T(8,128)(2,1)S(1)} %get-tuple-element.40), channel_id=1, source_target_pairs={{0,8},{1,9},{2,10},{3,11},{4,12},{5,13},{6,14},{7,15},{8,16},{9,17... | collective-permute-start | bytes 393224 | tf_op jit(solution)/shard_map/ppermute | solution.py:442

commit v3 on v2

--- a/solution.py
+++ b/solution.py
@@ -237,11 +237,13 @@
     down_product(keep, away, ordered[...], pieces, down_all)
 
 
-def fold_body(keep, got, *outs):
-    rows = outs[0].shape[0]
-    for d in range(len(outs)):
-        at = (d + 1) * rows
-        outs[d][...] = (keep[at : at + rows, :] + got[at : at + rows, :].astype(F32)).astype(BF16)
+def fold_body(keep, got, near, held):
+    rows = near.shape[0] // 2
+    for k in range(2):
+        for out, block in ((held, 2 * k), (near, 2 * k + 1)):
+            src = slice(block * rows, (block + 1) * rows)
+            both = keep[src, :] + got[src, :].astype(F32)
+            out[k * rows : (k + 1) * rows, :] = both.astype(out.dtype)
 
 
 norm_eps = 1e-06
@@ -424,15 +426,15 @@
     n_sp, n_tp = mesh.shape["sp"], mesh.shape["tp"]
     n_b, n_y = 2, 2
     n_a, n_c = n_sp // n_b, n_tp // n_y
-    if n_sp % n_b or n_tp % n_y or n_a > 4 or n_c != 2:
+    if n_sp % n_b or n_tp % n_y or n_a != 4 or n_c != 2:
         return jax.shard_map(gathered_plan, **specs)
 
     def flat(a, b, y, c):
         return (a % n_a * n_b + b % n_b) * n_tp + y % n_y * n_c + c % n_c
 
-    def send(x, a=0, b=0, y=0, c=0, cyclic=True):
+    def send(x, a=0, b=0, y=0, c=0, flip=0, cyclic=True):
         pairs = [
-            (flat(i, j, k, m), flat(i + a, j + b, k + y, m + c))
+            (flat(i, j, k, m), flat((i ^ flip) + a, j + b, k + y, m + c))
             for i in range(n_a)
             for j in range(n_b)
             for k in range(n_y)
@@ -480,6 +482,7 @@
             ],
             n_in=4,
             fetched=True,
+            mib=60,
         )(forget_logits, written_values, forget_floor_gap[None, :], extra_log_decay)
         up_rows, up_cols = mixer_up_weight.shape
         piece = up_cols // n_a
@@ -487,15 +490,9 @@
         for d in range(n_a):
             cut = lax.dynamic_slice(mixer_up_weight, (0, (a + d) % n_a * piece), (up_rows, piece))
             mine.append(cut if d == 0 else send(cut, a=d))
-        up_x, up_y = [], []
-        for g in range(2):
-            joined = jnp.concatenate(mine[g::2], axis=0)
-            up_x.append(send(joined, b=1))
-            up_y.append(send(joined, y=1))
-        up_xy = [send(up_x[0], y=1), send(up_y[1], b=1)]
 
         def grouped(refs):
-            return [(refs[e % 2], e // 2 * up_rows) for e in range(n_a)]
+            return [(refs[0], 0), (refs[2], 0), (refs[1], 0), (refs[2], up_rows)]
 
         part = model // 2
         half = mixer_down_weight.shape[0] // 2
@@ -535,7 +532,14 @@
             *states,
         )
         got = send(away, c=1)
-        other = send((second + got[own:].astype(F32)).astype(BF16), y=1)
+        second = (second + got[own:].astype(F32)).astype(BF16)
+        other = send(second, y=1)
+        late = lax.optimization_barrier((mine[1], mine[3], second))[:2]
+        up_x, up_y = [], []
+        for members in [mine[0], mine[2], jnp.concatenate(late, axis=0)]:
+            up_x.append(send(members, b=1))
+            up_y.append(send(members, y=1))
+        up_xy = [send(up_x[0], y=1), send(up_x[1], y=1), send(up_y[2], b=1)]
         stream, normed = kernel_call(
             norm_body,
             [
@@ -545,7 +549,7 @@
             n_in=5,
         )(first, got, other, residual, mixer_norm_gain[None, :])
 
-        line = [normed] + [send(normed, a=d) for d in range(1, n_a)]
+        line = [normed] + [send(normed, flip=d) for d in range(1, n_a)]
         toks = line + [send(u, c=1) for u in line]
         group = n_a * own
         tokens = n_c * group
@@ -558,7 +562,7 @@
 
         def first_half(*refs):
             t = 1 + len(toks)
-            ups = [(refs[t + e], 0) for e in range(n_a)] + grouped(refs[t + n_a : t + n_a + 2])
+            ups = [(refs[t + e], 0) for e in range(n_a)] + grouped(refs[t + n_a : t + n_a + 3])
             first_body(n_a, n_c, refs[0], refs[1:t], ups, *refs[-3:])
 
         rows_x, early = kernel_call(
@@ -569,14 +573,14 @@
             ],
             scratch=[pltpu.VMEM((model, piece), BF16)],
             smem=1,
-            n_in=1 + len(toks) + n_a + 2,
+            n_in=1 + len(toks) + n_a + 3,
             mib=24,
         )(place, *toks, *mine, *up_x)
 
         def second_half(*refs):
-            ups = grouped(refs[3:5]) + grouped(refs[5:7])
-            pieces = [[(r, 0)] for r in refs[7:10]] + [[(refs[10], 0), (refs[11], 0)]]
-            lower_body(cols, *refs[:3], ups, pieces, *refs[12:])
+            ups = grouped(refs[3:6]) + grouped(refs[6:9])
+            pieces = [[(r, 0)] for r in refs[9:12]] + [[(refs[12], 0), (refs[13], 0)]]
+            lower_body(cols, *refs[:3], ups, pieces, *refs[14:])
 
         keep0, away0, hidden = kernel_call(
             second_half,
@@ -587,7 +591,7 @@
                 pltpu.VMEM((units, part), BF16),
             ],
             smem=1,
-            n_in=12,
+            n_in=14,
             mib=30,
         )(place, rows_x, early, *up_y, *up_xy, *whole, *down_xy[0])
         got0 = send(away0, c=1)
@@ -603,12 +607,19 @@
         got1 = send(away1, c=1)
         halves = []
         for k, (keep, got) in enumerate([(keep0, got0), (keep1, got1)]):
-            outs = kernel_call(
-                fold_body, [jax.ShapeDtypeStruct((own, part), BF16)] * (n_a - 1), n_in=2
+            near, held = kernel_call(
+                fold_body,
+                [
+                    jax.ShapeDtypeStruct((n_b * own, part), BF16),
+                    jax.ShapeDtypeStruct((n_b * own, part), F32),
+                ],
+                n_in=2,
             )(keep, got)
-            total = stream[:, k * part : (k + 1) * part] + keep[:own] + got[:own].astype(F32)
-            for d in range(1, n_a):
-                total = total + send(outs[d - 1], a=n_a - d).astype(F32)
+            near = send(near, flip=1)
+            far = (held[own:] + near[own:].astype(F32)).astype(BF16)
+            far = send(far, flip=2)
+            total = stream[:, k * part : (k + 1) * part] + held[:own] + near[:own].astype(F32)
+            total = total + far.astype(F32)
             halves.append(total.astype(BF16))
         return jnp.concatenate(halves, axis=1)
 

time: 157 us -> 172 us (1.096)
  starting transfers between devices: 44.4 us -> 54 us
  Pallas kernels: 13.8 us -> 16.2 us
    ppermute x36 -> x37, starting transfers between devices: 44.4 us -> 54 us  [send(): return lax.ppermute(x, AXES, pairs)]
    ppermute x36 -> x37, waiting for transfers between devices: 89.1 us -> 90.4 us  [send(): return lax.ppermute(x, AXES, pairs)]
    unnamed x29 -> x27, local copies, waits for them, and re-layouts: 7.83 us -> 8.02 us
  transfers between devices with their start and end apart: 36 -> 37, of which waited for: 17 -> 15; matrix products, arithmetic and copies ran while one was open for 0% -> 1% of each run, Pallas kernels for 5% -> 6%
where the time goes in v3:
time: 172 us; the launch traced here: 171 us
  waiting for transfers between devices  90.4 us (53%)
  starting transfers between devices  54 us (31%)
  Pallas kernels  16.2 us (9%)
  local copies, waits for them, and re-layouts  9.42 us (5%)
    ppermute x37, waiting for transfers between devices, send(): return lax.ppermute(x, AXES, pairs)  90.4 us
    ppermute x37, starting transfers between devices, send(): return lax.ppermute(x, AXES, pairs)  54 us
    unnamed x27, local copies, waits for them, and re-layouts  8.02 us
  transfers between devices with their start and end apart: 37, of which 15 were waited for; matrix products, arithmetic and copies ran while one was open for 1% of the time, Pallas kernels for 6%

profile of v3, /device:TPU:0, one launch (start us, length us, event | category | flops | bytes accessed | tf_op | source)
XLA Modules:
  0.0 171.3 jit_solution(8493243892905818466)
XLA Ops:
  0.0 3.2 %shard_map.118 = (f32[256,256]{1,0:T(8,128)}, f32[256,256]{1,0:T(8,128)}, bf16[272,128]{1,0:T(8,128)(2,1)}) custom-call(bf16[256,256]{1,0:T(8,128)(2,1)} %refs_0_.1, bf16[256,256]{1,0:T(8,128)(2,1)} %values.1, f32[1,256]{1,0:T(1,128)} %bitcast.9, f32[256,256]{1,0:T(8,128)} %refs_3_.1), custom_call_target="tpu_custom_call" | custom-call | tf_op jit(solution)/shard_map/pallas_call | solution.py:469
  3.2 3.0 %collective-permute-start = (bf16[272,128]{1,0:T(8,128)(2,1)}, bf16[272,128]{1,0:T(8,128)(2,1)S(1)}, u32[]{:S(2)}, u32[]{:S(2)}) collective-permute-start(bf16[272,128]{1,0:T(8,128)(2,1)} %get-tuple-element.28.mine), channel_id=1, source_target_pairs={{0,4},{1,5},{2,6},{3,7},{4,0},{5,1},{6,2},{7,3},{8,12},{9,13},{10,... | collective-permute-start | bytes 208904 | tf_op jit(solution)/shard_map/ppermute | solution.py:444
  6.3 2.4 %collective-permute-done.theirs.refs_7_ = bf16[272,128]{1,0:T(8,128)(2,1)S(1)} collective-permute-done((bf16[272,128]{1,0:T(8,128)(2,1)}, bf16[272,128]{1,0:T(8,128)(2,1)S(1)}, u32[]{:S(2)}, u32[]{:S(2)}) %collective-permute-start) | collective-permute-done | bytes 69664 | tf_op jit(solution)/shard_map/ppermute | solution.py:444
  8.7 0.9 copy-done.10
  9.6 0.7 shard_map.120
  10.2 6.0 %collective-permute-start.3 = (bf16[272,128]{1,0:T(8,128)(2,1)S(1)}, bf16[272,128]{1,0:T(8,128)(2,1)S(1)}, u32[]{:S(2)}, u32[]{:S(2)}) collective-permute-start(bf16[272,128]{1,0:T(8,128)(2,1)S(1)} %shard_map.120), channel_id=1, source_target_pairs={{0,24},{1,25},{2,26},{3,27},{4,28},{5,29},{6,30},{7,31}} | collective-permute-start | bytes 208904 | tf_op jit(solution)/shard_map/ppermute | solution.py:444
  16.3 1.3 collective-permute-start.2
  17.6 2.5 %collective-permute-start.1 = (bf16[272,128]{1,0:T(8,128)(2,1)S(1)}, bf16[272,128]{1,0:T(8,128)(2,1)S(1)}, u32[]{:S(2)}, u32[]{:S(2)}) collective-permute-start(bf16[272,128]{1,0:T(8,128)(2,1)S(1)} %shard_map.120), channel_id=1, source_target_pairs={{0,8},{1,9},{2,10},{3,11},{4,12},{5,13},{6,14},{7,15},{8,16},{9,17... | collective-permute-start | bytes 208904 | tf_op jit(solution)/shard_map/ppermute | solution.py:444
  20.1 0.9 copy-done.2
  21.0 0.9 copy-done.4
  21.9 0.9 copy-done.5
  22.8 0.9 copy-done.8
  23.8 3.4 %shard_map.119.refs_3_ = f32[256,256]{1,0:T(8,128)S(1)} custom-call(bf16[256,256]{1,0:T(8,128)(2,1)S(1)} %copy-done.5, f32[256,256]{1,0:T(8,128)S(1)} %copy-done.8, f32[256,256]{1,0:T(8,128)S(1)} %copy-done.2, bf16[256,256]{1,0:T(8,128)(2,1)S(1)} %copy-done.4), custom_call_target="tpu_custom_call" | custom-call | tf_op jit(solution)/shard_map/pallas_call | solution.py:510
  27.3 0.9 copy-done.3
  28.2 0.9 copy-done.6
  29.1 0.9 copy-done.9
  30.0 0.7 copy-done.12
  30.7 2.5 %shard_map.121 = (f32[64,2048]{1,0:T(8,128)S(1)}, f32[64,2048]{1,0:T(8,128)S(1)}, bf16[128,2048]{1,0:T(8,128)(2,1)}) custom-call(s32[4]{0:T(128)S(1)} %pad_add_fusion.place.refs_0_, bf16[256,256]{1,0:T(8,128)(2,1)S(1)} %copy-done.6, f32[256,256]{1,0:T(8,128)S(1)} %copy-done.3, f32[256,256]{1,0:T(8,128)S(1)} %shard_map.119.refs_3_, ...), custom_call_target="tpu_custom_call" | custom-call | tf_op jit(solution)/shard_map/pallas_call | solution.py:513
  33.2 1.3 constant_dynamic-slice_fusion
  34.5 2.0 %collective-permute-start.13 = (bf16[256,512]{1,0:T(8,128)(2,1)S(1)}, bf16[256,512]{1,0:T(8,128)(2,1)S(1)}, u32[]{:S(2)}, u32[]{:S(2)}) collective-permute-start(bf16[256,512]{1,0:T(8,128)(2,1)S(1)} %get-tuple-element.52), channel_id=1, source_target_pairs={{0,8},{1,9},{2,10},{3,11},{4,12},{5,13},{6,14},{7,15},{8,16},{9,17... | collective-permute-start | bytes 786440 | tf_op jit(solution)/shard_map/ppermute | solution.py:444
  36.6 1.5 collective-permute-start.19
  38.1 10.8 %collective-permute-done.15.refs_12_ = bf16[256,512]{1,0:T(8,128)(2,1)S(1)} collective-permute-done((bf16[256,512]{1,0:T(8,128)(2,1)S(1)}, bf16[256,512]{1,0:T(8,128)(2,1)S(1)}, u32[]{:S(2)}, u32[]{:S(2)}) %collective-permute-start.15) | collective-permute-done | bytes 262176 | tf_op jit(solution)/shard_map/ppermute | solution.py:444
  48.9 1.5 collective-permute-start.16
  50.4 1.5 collective-permute-start.26
  51.9 7.7 %collective-permute-done.14.refs_11_ = bf16[256,512]{1,0:T(8,128)(2,1)S(1)} collective-permute-done((bf16[256,512]{1,0:T(8,128)(2,1)S(1)}, bf16[256,512]{1,0:T(8,128)(2,1)S(1)}, u32[]{:S(2)}, u32[]{:S(2)}) %collective-permute-start.14) | collective-permute-done | bytes 262176 | tf_op jit(solution)/shard_map/ppermute | solution.py:444
  59.5 1.5 collective-permute-start.25
  61.0 1.5 collective-permute-start.20
  62.6 0.5 collective-permute-start.17
  63.2 0.6 collective-permute-start.5
  63.7 18.3 %collective-permute-done.20.refs_4_ = bf16[256,512]{1,0:T(8,128)(2,1)S(1)} collective-permute-done((bf16[256,512]{1,0:T(8,128)(2,1)S(1)}, bf16[256,512]{1,0:T(8,128)(2,1)S(1)}, u32[]{:S(2)}, u32[]{:S(2)}) %collective-permute-start.20) | collective-permute-done | bytes 262176 | tf_op jit(solution)/shard_map/ppermute | solution.py:444
  82.0 1.5 collective-permute-start.22
  83.5 6.3 %collective-permute-done.17.refs_14_ = bf16[256,512]{1,0:T(8,128)(2,1)S(1)} collective-permute-done((bf16[256,512]{1,0:T(8,128)(2,1)S(1)}, bf16[256,512]{1,0:T(8,128)(2,1)S(1)}, u32[]{:S(2)}, u32[]{:S(2)}) %collective-permute-start.17) | collective-permute-done | bytes 262176 | tf_op jit(solution)/shard_map/ppermute | solution.py:444
  89.9 1.5 collective-permute-start.23
  91.4 0.6 collective-permute-start.21
  92.0 0.2 shard_map.122
  92.3 6.7 %collective-permute-done.23.refs_7_ = bf16[256,512]{1,0:T(8,128)(2,1)S(1)} collective-permute-done((bf16[256,512]{1,0:T(8,128)(2,1)S(1)}, bf16[256,512]{1,0:T(8,128)(2,1)S(1)}, u32[]{:S(2)}, u32[]{:S(2)}) %collective-permute-start.23) | collective-permute-done | bytes 262176 | tf_op jit(solution)/shard_map/ppermute | solution.py:444
  99.0 3.1 %collective-permute-start.8 = (bf16[8,64,256]{2,1,0:T(8,128)(2,1)S(1)}, bf16[8,64,256]{2,1,0:T(8,128)(2,1)S(1)}, u32[]{:S(2)}, u32[]{:S(2)}) collective-permute-start(bf16[8,64,256]{2,1,0:T(8,128)(2,1)S(1)} %get-tuple-element.33.refs_1_), channel_id=1, source_target_pairs={{0,24},{1,25},{2,26},{3,27},{4,28},{5,29},{6,30},{7,31},{8,16},{9,... | collective-permute-start | bytes 786440 | tf_op jit(solution)/shard_map/ppermute | solution.py:444
  102.1 1.5 collective-permute-start.18
  103.6 3.4 %collective-permute-start.7 = (bf16[8,64,256]{2,1,0:T(8,128)(2,1)S(1)}, bf16[8,64,256]{2,1,0:T(8,128)(2,1)S(1)}, u32[]{:S(2)}, u32[]{:S(2)}) collective-permute-start(bf16[8,64,256]{2,1,0:T(8,128)(2,1)S(1)} %get-tuple-element.33.refs_1_), channel_id=1, source_target_pairs={{0,16},{1,17},{2,18},{3,19},{4,20},{5,21},{6,22},{7,23},{8,24},{9,... | collective-permute-start | bytes 786440 | tf_op jit(solution)/shard_map/ppermute | solution.py:444
  107.0 3.1 %collective-permute-done.8.refs_4_ = bf16[8,64,256]{2,1,0:T(8,128)(2,1)S(1)} collective-permute-done((bf16[8,64,256]{2,1,0:T(8,128)(2,1)S(1)}, bf16[8,64,256]{2,1,0:T(8,128)(2,1)S(1)}, u32[]{:S(2)}, u32[]{:S(2)}) %collective-permute-start.8) | collective-permute-done | bytes 262176 | tf_op jit(solution)/shard_map/ppermute | solution.py:444
  110.1 1.5 collective-permute-start.24
  111.6 11.0 %collective-permute-done.7.refs_3_ = bf16[8,64,256]{2,1,0:T(8,128)(2,1)S(1)} collective-permute-done((bf16[8,64,256]{2,1,0:T(8,128)(2,1)S(1)}, bf16[8,64,256]{2,1,0:T(8,128)(2,1)S(1)}, u32[]{:S(2)}, u32[]{:S(2)}) %collective-permute-start.7) | collective-permute-done | bytes 262176 | tf_op jit(solution)/shard_map/ppermute | solution.py:444
  122.6 0.5 collective-permute-start.10
  123.2 1.0 collective-permute-start.28
  124.2 1.5 collective-permute-start.27
  125.7 1.1 collective-permute-start.33
  126.8 0.5 collective-permute-start.32
  127.3 1.8 %shard_map.123 = (bf16[512,2048]{1,0:T(8,128)(2,1)S(1)}, bf16[512,512]{1,0:T(8,128)(2,1)S(1)}) custom-call(s32[4]{0:T(128)S(1)} %pad_add_fusion.place.refs_0_, bf16[8,64,256]{2,1,0:T(8,128)(2,1)S(1)} %get-tuple-element.33.refs_1_, bf16[8,64,256]{2,1,0:T(8,128)(2,1)S(1)} %collective-permute-done.6.refs_2_, ...), custom_call_target="tpu_custom_call" | custom-call | tf_op jit(solution)/shard_map/pallas_call | solution.py:568
  129.1 3.3 %collective-permute-done.28.refs_13_ = bf16[128,1024]{1,0:T(8,128)(2,1)S(1)} collective-permute-done((bf16[128,1024]{1,0:T(8,128)(2,1)S(1)}, bf16[128,1024]{1,0:T(8,128)(2,1)S(1)}, u32[]{:S(2)}, u32[]{:S(2)}) %collective-permute-start.28) | collective-permute-done | bytes 262176 | tf_op jit(solution)/shard_map/ppermute | solution.py:444
  132.4 0.9 collective-permute-done.27.refs_12_
  133.3 3.0 %shard_map.124 = (f32[256,1024]{1,0:T(8,128)S(1)}, bf16[256,1024]{1,0:T(8,128)(2,1)S(1)}, bf16[512,1024]{1,0:T(8,128)(2,1)S(1)}) custom-call(s32[4]{0:T(128)S(1)} %pad_add_fusion.place.refs_0_, bf16[512,2048]{1,0:T(8,128)(2,1)S(1)} %get-tuple-element.36.refs_1_, bf16[512,512]{1,0:T(8,128)(2,1)S(1)} %get-tuple-element.37.refs_2_, ...), custom_call_target="tpu_custom_call" | custom-call | tf_op jit(solution)/shard_map/pallas_call | solution.py:585
  136.4 0.6 collective-permute-done.33.r1_ref
  137.1 0.6 collective-permute-done.32.r0_ref
  137.7 1.3 shard_map.126
  139.1 0.1 shard_map.125
  139.2 6.8 %collective-permute-start.30 = (bf16[128,1024]{1,0:T(8,128)(2,1)S(1)}, bf16[128,1024]{1,0:T(8,128)(2,1)S(1)}, u32[]{:S(2)}, u32[]{:S(2)}) collective-permute-start(bf16[128,1024]{1,0:T(8,128)(2,1)S(1)} %get-tuple-element.41), channel_id=1, source_target_pairs={{0,8},{1,9},{2,10},{3,11},{4,12},{5,13},{6,14},{7,15},{8,0},{9,1},... | collective-permute-start | bytes 786440 | tf_op jit(solution)/shard_map/ppermute | solution.py:444
  146.0 1.8 %collective-permute-start.35 = (bf16[128,1024]{1,0:T(8,128)(2,1)S(1)}, bf16[128,1024]{1,0:T(8,128)(2,1)S(1)}, u32[]{:S(2)}, u32[]{:S(2)}) collective-permute-start(bf16[128,1024]{1,0:T(8,128)(2,1)S(1)} %get-tuple-element.46), channel_id=1, source_target_pairs={{0,8},{1,9},{2,10},{3,11},{4,12},{5,13},{6,14},{7,15},{8,0},{9,1},... | collective-permute-start | bytes 786440 | tf_op jit(solution)/shard_map/ppermute | solution.py:444
  147.8 5.3 %collective-permute-done.30 = bf16[128,1024]{1,0:T(8,128)(2,1)S(1)} collective-permute-done((bf16[128,1024]{1,0:T(8,128)(2,1)S(1)}, bf16[128,1024]{1,0:T(8,128)(2,1)S(1)}, u32[]{:S(2)}, u32[]{:S(2)}) %collective-permute-start.30) | collective-permute-done | bytes 262176 | tf_op jit(solution)/shard_map/ppermute | solution.py:444
  153.1 3.3 %collective-permute-start.31 = (bf16[64,1024]{1,0:T(8,128)(2,1)S(1)}, bf16[64,1024]{1,0:T(8,128)(2,1)S(1)}, u32[]{:S(2)}, u32[]{:S(2)}) collective-permute-start(bf16[64,1024]{1,0:T(8,128)(2,1)S(1)} %add_convert_fusion.4), channel_id=1, source_target_pairs={{0,16},{1,17},{2,18},{3,19},{4,20},{5,21},{6,22},{7,23},{8,24},{9,... | collective-permute-start | bytes 393224 | tf_op jit(solution)/shard_map/ppermute | solution.py:444
  156.4 4.9 %collective-permute-done.35 = bf16[128,1024]{1,0:T(8,128)(2,1)S(1)} collective-permute-done((bf16[128,1024]{1,0:T(8,128)(2,1)S(1)}, bf16[128,1024]{1,0:T(8,128)(2,1)S(1)}, u32[]{:S(2)}, u32[]{:S(2)}) %collective-permute-start.35) | collective-permute-done | bytes 262176 | tf_op jit(solution)/shard_map/ppermute | solution.py:444
  161.3 0.8 collective-permute-start.36
  162.1 8.3 %collective-permute-done.36 = bf16[64,1024]{1,0:T(8,128)(2,1)S(1)} collective-permute-done((bf16[64,1024]{1,0:T(8,128)(2,1)S(1)}, bf16[64,1024]{1,0:T(8,128)(2,1)S(1)}, u32[]{:S(2)}, u32[]{:S(2)}) %collective-permute-start.36) | collective-permute-done | bytes 131104 | tf_op jit(solution)/shard_map/ppermute | solution.py:444
  170.4 0.1 add_convert_fusion.3
  170.5 0.7 pad_maximum_fusion
  (57 shorter events, 0.7 us)
Async XLA Ops:
  0.0 27.3 %copy-start.1 = (bf16[256,2048]{1,0:T(8,128)(2,1)S(1)}, bf16[256,2048]{1,0:T(8,128)(2,1)}, u32[]{:S(2)}) copy-start(bf16[256,2048]{1,0:T(8,128)(2,1)} %refs_6_.1) | copy-start | bytes 3145732
  3.2 5.5 %collective-permute-start = (bf16[272,128]{1,0:T(8,128)(2,1)}, bf16[272,128]{1,0:T(8,128)(2,1)S(1)}, u32[]{:S(2)}, u32[]{:S(2)}) collective-permute-start(bf16[272,128]{1,0:T(8,128)(2,1)} %get-tuple-element.28.mine), channel_id=1, source_target_pairs={{0,4},{1,5},{2,6},{3,7},{4,0},{5,1},{6,2},{7,3},{8,12},{9,13},{10,... | collective-permute-start | bytes 208904 | tf_op jit(solution)/shard_map/ppermute | solution.py:444
  8.7 0.9 copy-start.10
  10.2 17.0 %collective-permute-start.3 = (bf16[272,128]{1,0:T(8,128)(2,1)S(1)}, bf16[272,128]{1,0:T(8,128)(2,1)S(1)}, u32[]{:S(2)}, u32[]{:S(2)}) collective-permute-start(bf16[272,128]{1,0:T(8,128)(2,1)S(1)} %shard_map.120), channel_id=1, source_target_pairs={{0,24},{1,25},{2,26},{3,27},{4,28},{5,29},{6,30},{7,31}} | collective-permute-start | bytes 208904 | tf_op jit(solution)/shard_map/ppermute | solution.py:444
  16.3 10.9 %collective-permute-start.2 = (bf16[272,128]{1,0:T(8,128)(2,1)S(1)}, bf16[272,128]{1,0:T(8,128)(2,1)S(1)}, u32[]{:S(2)}, u32[]{:S(2)}) collective-permute-start(bf16[272,128]{1,0:T(8,128)(2,1)S(1)} %shard_map.120), channel_id=1, source_target_pairs={{0,16},{1,17},{2,18},{3,19},{4,20},{5,21},{6,22},{7,23},{8,24},{9,... | collective-permute-start | bytes 208904 | tf_op jit(solution)/shard_map/ppermute | solution.py:444
  17.6 9.7 %collective-permute-start.1 = (bf16[272,128]{1,0:T(8,128)(2,1)S(1)}, bf16[272,128]{1,0:T(8,128)(2,1)S(1)}, u32[]{:S(2)}, u32[]{:S(2)}) collective-permute-start(bf16[272,128]{1,0:T(8,128)(2,1)S(1)} %shard_map.120), channel_id=1, source_target_pairs={{0,8},{1,9},{2,10},{3,11},{4,12},{5,13},{6,14},{7,15},{8,16},{9,17... | collective-permute-start | bytes 208904 | tf_op jit(solution)/shard_map/ppermute | solution.py:444
  20.1 1.0 copy-start.2
  21.0 0.9 copy-start.4
  21.9 0.9 copy-start.5
  22.8 0.9 copy-start.8
  27.3 1.0 copy-start.3
  28.2 0.9 copy-start.6
  29.1 0.9 copy-start.9
  30.0 0.7 copy-start.12
  30.7 19.7 %copy-start = (bf16[256,2048]{1,0:T(8,128)(2,1)S(1)}, bf16[256,2048]{1,0:T(8,128)(2,1)}, u32[]{:S(2)}) copy-start(bf16[256,2048]{1,0:T(8,128)(2,1)} %own_ref.1) | copy-start | bytes 3145732
  33.2 29.4 %collective-permute-start.4 = (bf16[128,2048]{1,0:T(8,128)(2,1)}, bf16[128,2048]{1,0:T(8,128)(2,1)S(1)}, u32[]{:S(2)}, u32[]{:S(2)}) collective-permute-start(bf16[128,2048]{1,0:T(8,128)(2,1)} %get-tuple-element.30), channel_id=1, source_target_pairs={{0,1},{1,0},{2,3},{3,2},{4,5},{5,4},{6,7},{7,6},{8,9},{9,8},{10,11... | collective-permute-start | bytes 1572872 | tf_op jit(solution)/shard_map/ppermute | solution.py:444
  33.2 58.8 %copy-start.7 = (bf16[64,2048]{1,0:T(8,128)(2,1)S(1)}, bf16[64,2048]{1,0:T(8,128)(2,1)}, u32[]{:S(2)}) copy-start(bf16[64,2048]{1,0:T(8,128)(2,1)} %residual.1) | copy-start | bytes 786436
  33.2 58.8 %copy-start.11 = (f32[2048]{0:T(1024)S(1)}, f32[2048]{0:T(1024)}, u32[]{:S(2)}) copy-start(f32[2048]{0:T(1024)} %param.21) | copy-start | bytes 24580
  34.5 14.4 %collective-permute-start.15 = (bf16[256,512]{1,0:T(8,128)(2,1)S(1)}, bf16[256,512]{1,0:T(8,128)(2,1)S(1)}, u32[]{:S(2)}, u32[]{:S(2)}) collective-permute-start(bf16[256,512]{1,0:T(8,128)(2,1)S(1)} %get-tuple-element.51), channel_id=1, source_target_pairs={{0,24},{1,25},{2,26},{3,27},{4,28},{5,29},{6,30},{7,31},{8,0},{9,1... | collective-permute-start | bytes 786440 | tf_op jit(solution)/shard_map/ppermute | solution.py:444
  34.5 15.8 %collective-permute-start.13 = (bf16[256,512]{1,0:T(8,128)(2,1)S(1)}, bf16[256,512]{1,0:T(8,128)(2,1)S(1)}, u32[]{:S(2)}, u32[]{:S(2)}) collective-permute-start(bf16[256,512]{1,0:T(8,128)(2,1)S(1)} %get-tuple-element.52), channel_id=1, source_target_pairs={{0,8},{1,9},{2,10},{3,11},{4,12},{5,13},{6,14},{7,15},{8,16},{9,17... | collective-permute-start | bytes 786440 | tf_op jit(solution)/shard_map/ppermute | solution.py:444
  36.5 23.0 %collective-permute-start.14 = (bf16[256,512]{1,0:T(8,128)(2,1)S(1)}, bf16[256,512]{1,0:T(8,128)(2,1)S(1)}, u32[]{:S(2)}, u32[]{:S(2)}) collective-permute-start(bf16[256,512]{1,0:T(8,128)(2,1)S(1)} %get-tuple-element.54), channel_id=1, source_target_pairs={{0,16},{1,17},{2,18},{3,19},{4,20},{5,21},{6,22},{7,23},{8,24},{9,... | collective-permute-start | bytes 786440 | tf_op jit(solution)/shard_map/ppermute | solution.py:444
  36.6 24.5 %collective-permute-start.19 = (bf16[256,512]{1,0:T(8,128)(2,1)S(1)}, bf16[256,512]{1,0:T(8,128)(2,1)S(1)}, u32[]{:S(2)}, u32[]{:S(2)}) collective-permute-start(bf16[256,512]{1,0:T(8,128)(2,1)S(1)} %get-tuple-element.53.refs_9_), channel_id=1, source_target_pairs={{0,2},{1,3},{2,0},{3,1},{4,6},{5,7},{6,4},{7,5},{8,10},{9,11},{10,... | collective-permute-start | bytes 786440 | tf_op jit(solution)/shard_map/ppermute | solution.py:444
  48.9 14.3 %collective-permute-start.16 = (bf16[256,512]{1,0:T(8,128)(2,1)S(1)}, bf16[256,512]{1,0:T(8,128)(2,1)S(1)}, u32[]{:S(2)}, u32[]{:S(2)}) collective-permute-start(bf16[256,512]{1,0:T(8,128)(2,1)S(1)} %get-tuple-element.53.refs_9_), channel_id=1, source_target_pairs={{0,4},{1,5},{2,6},{3,7},{4,0},{5,1},{6,2},{7,3},{8,12},{9,13},{10,... | collective-permute-start | bytes 786440 | tf_op jit(solution)/shard_map/ppermute | solution.py:444
  50.4 51.8 %collective-permute-start.26 = (bf16[256,2048]{1,0:T(8,128)(2,1)S(1)}, bf16[256,2048]{1,0:T(8,128)(2,1)S(1)}, u32[]{:S(2)}, u32[]{:S(2)}) collective-permute-start(bf16[256,2048]{1,0:T(8,128)(2,1)S(1)} %copy-done), channel_id=1, source_target_pairs={{0,2},{1,3},{2,0},{3,1},{4,6},{5,7},{6,4},{7,5},{8,10},{9,11},{10,... | collective-permute-start | bytes 3145736 | tf_op jit(solution)/shard_map/ppermute | solution.py:444
  59.5 44.1 %collective-permute-start.25 = (bf16[256,2048]{1,0:T(8,128)(2,1)S(1)}, bf16[256,2048]{1,0:T(8,128)(2,1)S(1)}, u32[]{:S(2)}, u32[]{:S(2)}) collective-permute-start(bf16[256,2048]{1,0:T(8,128)(2,1)S(1)} %copy-done), channel_id=1, source_target_pairs={{0,4},{1,5},{2,6},{3,7},{4,0},{5,1},{6,2},{7,3},{8,12},{9,13},{10,... | collective-permute-start | bytes 3145736 | tf_op jit(solution)/shard_map/ppermute | solution.py:444
  61.0 21.0 %collective-permute-start.20 = (bf16[256,512]{1,0:T(8,128)(2,1)S(1)}, bf16[256,512]{1,0:T(8,128)(2,1)S(1)}, u32[]{:S(2)}, u32[]{:S(2)}) collective-permute-start(bf16[256,512]{1,0:T(8,128)(2,1)S(1)} %collective-permute-done.14.refs_11_), channel_id=1, source_target_pairs={{0,2},{1,3},{2,0},{3,1},{4,6},{5,7},{6,4},{7,5},{8,10},{9,11},{10,... | collective-permute-start | bytes 786440 | tf_op jit(solution)/shard_map/ppermute | solution.py:444
  62.6 27.3 %collective-permute-start.17 = (bf16[256,512]{1,0:T(8,128)(2,1)S(1)}, bf16[256,512]{1,0:T(8,128)(2,1)S(1)}, u32[]{:S(2)}, u32[]{:S(2)}) collective-permute-start(bf16[256,512]{1,0:T(8,128)(2,1)S(1)} %collective-permute-done.14.refs_11_), channel_id=1, source_target_pairs={{0,4},{1,5},{2,6},{3,7},{4,0},{5,1},{6,2},{7,3},{8,12},{9,13},{10,... | collective-permute-start | bytes 786440 | tf_op jit(solution)/shard_map/ppermute | solution.py:444
  63.2 28.3 %collective-permute-start.5 = (bf16[64,2048]{1,0:T(8,128)(2,1)S(1)}, bf16[64,2048]{1,0:T(8,128)(2,1)S(1)}, u32[]{:S(2)}, u32[]{:S(2)}) collective-permute-start(bf16[64,2048]{1,0:T(8,128)(2,1)S(1)} %add_convert_fusion), channel_id=1, source_target_pairs={{0,2},{1,3},{2,0},{3,1},{4,6},{5,7},{6,4},{7,5},{8,10},{9,11},{10,... | collective-permute-start | bytes 786440 | tf_op jit(solution)/shard_map/ppermute | solution.py:444
  82.0 10.2 %collective-permute-start.22 = (bf16[256,512]{1,0:T(8,128)(2,1)S(1)}, bf16[256,512]{1,0:T(8,128)(2,1)S(1)}, u32[]{:S(2)}, u32[]{:S(2)}) collective-permute-start(bf16[256,512]{1,0:T(8,128)(2,1)S(1)} %collective-permute-done.16.refs_13_), channel_id=1, source_target_pairs={{0,2},{1,3},{2,0},{3,1},{4,6},{5,7},{6,4},{7,5},{8,10},{9,11},{10,... | collective-permute-start | bytes 786440 | tf_op jit(solution)/shard_map/ppermute | solution.py:444
  89.9 9.2 %collective-permute-start.23 = (bf16[256,512]{1,0:T(8,128)(2,1)S(1)}, bf16[256,512]{1,0:T(8,128)(2,1)S(1)}, u32[]{:S(2)}, u32[]{:S(2)}) collective-permute-start(bf16[256,512]{1,0:T(8,128)(2,1)S(1)} %collective-permute-done.17.refs_14_), channel_id=1, source_target_pairs={{0,2},{1,3},{2,0},{3,1},{4,6},{5,7},{6,4},{7,5},{8,10},{9,11},{10,... | collective-permute-start | bytes 786440 | tf_op jit(solution)/shard_map/ppermute | solution.py:444
  91.4 18.7 %collective-permute-start.21 = (bf16[512,512]{1,0:T(8,128)(2,1)S(1)}, bf16[512,512]{1,0:T(8,128)(2,1)S(1)}, u32[]{:S(2)}, u32[]{:S(2)}) collective-permute-start(bf16[512,512]{1,0:T(8,128)(2,1)S(1)} %constant_dynamic-update-slice_fusion), channel_id=1, source_target_pairs={{0,2},{1,3},{2,0},{3,1},{4,6},{5,7},{6,4},{7,5},{8,10},{9,11},{10,... | collective-permute-start | bytes 1572872 | tf_op jit(solution)/shard_map/ppermute | solution.py:444
  92.2 14.7 %collective-permute-start.9 = (bf16[8,64,256]{2,1,0:T(8,128)(2,1)S(1)}, bf16[8,64,256]{2,1,0:T(8,128)(2,1)S(1)}, u32[]{:S(2)}, u32[]{:S(2)}) collective-permute-start(bf16[8,64,256]{2,1,0:T(8,128)(2,1)S(1)} %get-tuple-element.33.refs_1_), channel_id=1, source_target_pairs={{0,1},{1,0},{2,3},{3,2},{4,5},{5,4},{6,7},{7,6},{8,9},{9,8},{10,11... | collective-permute-start | bytes 786440 | tf_op jit(solution)/shard_map/ppermute | solution.py:444
  99.0 11.0 %collective-permute-start.8 = (bf16[8,64,256]{2,1,0:T(8,128)(2,1)S(1)}, bf16[8,64,256]{2,1,0:T(8,128)(2,1)S(1)}, u32[]{:S(2)}, u32[]{:S(2)}) collective-permute-start(bf16[8,64,256]{2,1,0:T(8,128)(2,1)S(1)} %get-tuple-element.33.refs_1_), channel_id=1, source_target_pairs={{0,24},{1,25},{2,26},{3,27},{4,28},{5,29},{6,30},{7,31},{8,16},{9,... | collective-permute-start | bytes 786440 | tf_op jit(solution)/shard_map/ppermute | solution.py:444
  102.1 21.1 %collective-permute-start.18 = (bf16[512,512]{1,0:T(8,128)(2,1)S(1)}, bf16[512,512]{1,0:T(8,128)(2,1)S(1)}, u32[]{:S(2)}, u32[]{:S(2)}) collective-permute-start(bf16[512,512]{1,0:T(8,128)(2,1)S(1)} %constant_dynamic-update-slice_fusion), channel_id=1, source_target_pairs={{0,4},{1,5},{2,6},{3,7},{4,0},{5,1},{6,2},{7,3},{8,12},{9,13},{10,... | collective-permute-start | bytes 1572872 | tf_op jit(solution)/shard_map/ppermute | solution.py:444
  103.6 19.0 %collective-permute-start.7 = (bf16[8,64,256]{2,1,0:T(8,128)(2,1)S(1)}, bf16[8,64,256]{2,1,0:T(8,128)(2,1)S(1)}, u32[]{:S(2)}, u32[]{:S(2)}) collective-permute-start(bf16[8,64,256]{2,1,0:T(8,128)(2,1)S(1)} %get-tuple-element.33.refs_1_), channel_id=1, source_target_pairs={{0,16},{1,17},{2,18},{3,19},{4,20},{5,21},{6,22},{7,23},{8,24},{9,... | collective-permute-start | bytes 786440 | tf_op jit(solution)/shard_map/ppermute | solution.py:444
  107.0 15.7 %collective-permute-start.6 = (bf16[8,64,256]{2,1,0:T(8,128)(2,1)S(1)}, bf16[8,64,256]{2,1,0:T(8,128)(2,1)S(1)}, u32[]{:S(2)}, u32[]{:S(2)}) collective-permute-start(bf16[8,64,256]{2,1,0:T(8,128)(2,1)S(1)} %get-tuple-element.33.refs_1_), channel_id=1, source_target_pairs={{0,8},{1,9},{2,10},{3,11},{4,12},{5,13},{6,14},{7,15},{8,0},{9,1},... | collective-permute-start | bytes 786440 | tf_op jit(solution)/shard_map/ppermute | solution.py:444
  110.1 14.1 %collective-permute-start.12 = (bf16[8,64,256]{2,1,0:T(8,128)(2,1)S(1)}, bf16[8,64,256]{2,1,0:T(8,128)(2,1)S(1)}, u32[]{:S(2)}, u32[]{:S(2)}) collective-permute-start(bf16[8,64,256]{2,1,0:T(8,128)(2,1)S(1)} %collective-permute-done.8.refs_4_), channel_id=1, source_target_pairs={{0,1},{1,0},{2,3},{3,2},{4,5},{5,4},{6,7},{7,6},{8,9},{9,8},{10,11... | collective-permute-start | bytes 786440 | tf_op jit(solution)/shard_map/ppermute | solution.py:444
  110.1 23.3 %collective-permute-start.24 = (bf16[512,512]{1,0:T(8,128)(2,1)S(1)}, bf16[512,512]{1,0:T(8,128)(2,1)S(1)}, u32[]{:S(2)}, u32[]{:S(2)}) collective-permute-start(bf16[512,512]{1,0:T(8,128)(2,1)S(1)} %collective-permute-done.21.refs_5_), channel_id=1, source_target_pairs={{0,4},{1,5},{2,6},{3,7},{4,0},{5,1},{6,2},{7,3},{8,12},{9,13},{10,... | collective-permute-start | bytes 1572872 | tf_op jit(solution)/shard_map/ppermute | solution.py:444
  122.6 3.1 %collective-permute-start.11 = (bf16[8,64,256]{2,1,0:T(8,128)(2,1)S(1)}, bf16[8,64,256]{2,1,0:T(8,128)(2,1)S(1)}, u32[]{:S(2)}, u32[]{:S(2)}) collective-permute-start(bf16[8,64,256]{2,1,0:T(8,128)(2,1)S(1)} %collective-permute-done.7.refs_3_), channel_id=1, source_target_pairs={{0,1},{1,0},{2,3},{3,2},{4,5},{5,4},{6,7},{7,6},{8,9},{9,8},{10,11... | collective-permute-start | bytes 786440 | tf_op jit(solution)/shard_map/ppermute | solution.py:444
  122.6 4.2 %collective-permute-start.10 = (bf16[8,64,256]{2,1,0:T(8,128)(2,1)S(1)}, bf16[8,64,256]{2,1,0:T(8,128)(2,1)S(1)}, u32[]{:S(2)}, u32[]{:S(2)}) collective-permute-start(bf16[8,64,256]{2,1,0:T(8,128)(2,1)S(1)} %collective-permute-done.6.refs_2_), channel_id=1, source_target_pairs={{0,1},{1,0},{2,3},{3,2},{4,5},{5,4},{6,7},{7,6},{8,9},{9,8},{10,11... | collective-permute-start | bytes 786440 | tf_op jit(solution)/shard_map/ppermute | solution.py:444
  123.2 9.2 %collective-permute-start.28 = (bf16[128,1024]{1,0:T(8,128)(2,1)S(1)}, bf16[128,1024]{1,0:T(8,128)(2,1)S(1)}, u32[]{:S(2)}, u32[]{:S(2)}) collective-permute-start(bf16[128,1024]{1,0:T(8,128)(2,1)S(1)} %get-tuple-element.48), channel_id=1, source_target_pairs={{0,4},{1,5},{2,6},{3,7},{4,0},{5,1},{6,2},{7,3},{8,12},{9,13},{10,... | collective-permute-start | bytes 786440 | tf_op jit(solution)/shard_map/ppermute | solution.py:444
  124.2 9.2 %collective-permute-start.27 = (bf16[128,1024]{1,0:T(8,128)(2,1)S(1)}, bf16[128,1024]{1,0:T(8,128)(2,1)S(1)}, u32[]{:S(2)}, u32[]{:S(2)}) collective-permute-start(bf16[128,1024]{1,0:T(8,128)(2,1)S(1)} %get-tuple-element.50), channel_id=1, source_target_pairs={{0,2},{1,3},{2,0},{3,1},{4,6},{5,7},{6,4},{7,5},{8,10},{9,11},{10,... | collective-permute-start | bytes 786440 | tf_op jit(solution)/shard_map/ppermute | solution.py:444
  125.7 11.4 %collective-permute-start.33 = (bf16[128,1024]{1,0:T(8,128)(2,1)S(1)}, bf16[128,1024]{1,0:T(8,128)(2,1)S(1)}, u32[]{:S(2)}, u32[]{:S(2)}) collective-permute-start(bf16[128,1024]{1,0:T(8,128)(2,1)S(1)} %get-tuple-element.47), channel_id=1, source_target_pairs={{0,4},{1,5},{2,6},{3,7},{4,0},{5,1},{6,2},{7,3},{8,12},{9,13},{10,... | collective-permute-start | bytes 786440 | tf_op jit(solution)/shard_map/ppermute | solution.py:444
  126.8 10.9 %collective-permute-start.32 = (bf16[128,1024]{1,0:T(8,128)(2,1)S(1)}, bf16[128,1024]{1,0:T(8,128)(2,1)S(1)}, u32[]{:S(2)}, u32[]{:S(2)}) collective-permute-start(bf16[128,1024]{1,0:T(8,128)(2,1)S(1)} %get-tuple-element.49), channel_id=1, source_target_pairs={{0,2},{1,3},{2,0},{3,1},{4,6},{5,7},{6,4},{7,5},{8,10},{9,11},{10,... | collective-permute-start | bytes 786440 | tf_op jit(solution)/shard_map/ppermute | solution.py:444
  136.4 2.7 %collective-permute-start.29 = (bf16[256,1024]{1,0:T(8,128)(2,1)S(1)}, bf16[256,1024]{1,0:T(8,128)(2,1)S(1)}, u32[]{:S(2)}, u32[]{:S(2)}) collective-permute-start(bf16[256,1024]{1,0:T(8,128)(2,1)S(1)} %get-tuple-element.39), channel_id=1, source_target_pairs={{0,1},{1,0},{2,3},{3,2},{4,5},{5,4},{6,7},{7,6},{8,9},{9,8},{10,11... | collective-permute-start | bytes 1572872 | tf_op jit(solution)/shard_map/ppermute | solution.py:444
  139.0 6.9 %collective-permute-start.34 = (bf16[256,1024]{1,0:T(8,128)(2,1)S(1)}, bf16[256,1024]{1,0:T(8,128)(2,1)S(1)}, u32[]{:S(2)}, u32[]{:S(2)}) collective-permute-start(bf16[256,1024]{1,0:T(8,128)(2,1)S(1)} %get-tuple-element.44), channel_id=1, source_target_pairs={{0,1},{1,0},{2,3},{3,2},{4,5},{5,4},{6,7},{7,6},{8,9},{9,8},{10,11... | collective-permute-start | bytes 1572872 | tf_op jit(solution)/shard_map/ppermute | solution.py:444
  139.2 13.9 %collective-permute-start.30 = (bf16[128,1024]{1,0:T(8,128)(2,1)S(1)}, bf16[128,1024]{1,0:T(8,128)(2,1)S(1)}, u32[]{:S(2)}, u32[]{:S(2)}) collective-permute-start(bf16[128,1024]{1,0:T(8,128)(2,1)S(1)} %get-tuple-element.41), channel_id=1, source_target_pairs={{0,8},{1,9},{2,10},{3,11},{4,12},{5,13},{6,14},{7,15},{8,0},{9,1},... | collective-permute-start | bytes 786440 | tf_op jit(solution)/shard_map/ppermute | solution.py:444
  146.0 15.3 %collective-permute-start.35 = (bf16[128,1024]{1,0:T(8,128)(2,1)S(1)}, bf16[128,1024]{1,0:T(8,128)(2,1)S(1)}, u32[]{:S(2)}, u32[]{:S(2)}) collective-permute-start(bf16[128,1024]{1,0:T(8,128)(2,1)S(1)} %get-tuple-element.46), channel_id=1, source_target_pairs={{0,8},{1,9},{2,10},{3,11},{4,12},{5,13},{6,14},{7,15},{8,0},{9,1},... | collective-permute-start | bytes 786440 | tf_op jit(solution)/shard_map/ppermute | solution.py:444
  153.1 9.0 %collective-permute-start.31 = (bf16[64,1024]{1,0:T(8,128)(2,1)S(1)}, bf16[64,1024]{1,0:T(8,128)(2,1)S(1)}, u32[]{:S(2)}, u32[]{:S(2)}) collective-permute-start(bf16[64,1024]{1,0:T(8,128)(2,1)S(1)} %add_convert_fusion.4), channel_id=1, source_target_pairs={{0,16},{1,17},{2,18},{3,19},{4,20},{5,21},{6,22},{7,23},{8,24},{9,... | collective-permute-start | bytes 393224 | tf_op jit(solution)/shard_map/ppermute | solution.py:444
  161.3 9.1 %collective-permute-start.36 = (bf16[64,1024]{1,0:T(8,128)(2,1)S(1)}, bf16[64,1024]{1,0:T(8,128)(2,1)S(1)}, u32[]{:S(2)}, u32[]{:S(2)}) collective-permute-start(bf16[64,1024]{1,0:T(8,128)(2,1)S(1)} %add_convert_fusion.2), channel_id=1, source_target_pairs={{0,16},{1,17},{2,18},{3,19},{4,20},{5,21},{6,22},{7,23},{8,24},{9,... | collective-permute-start | bytes 393224 | tf_op jit(solution)/shard_map/ppermute | solution.py:444

commit v4 on v3

--- a/solution.py
+++ b/solution.py
@@ -47,17 +47,14 @@
     return jnp.transpose(jnp.broadcast_to(row, (HEAD, HEAD)))
 
 
-def gates_body(logits, values, gap, extra, gate_out, cum_out, packed):
-    rows, width = logits.shape
+def gates_body(values, gates, logs, cum_out, packed):
+    rows, width = gates.shape
     heads = width // HEAD
-    z = logits[...].astype(F32)
-    gate = gap[...] / (1.0 + jnp.exp(z))
-    log_forget = jnp.log1p(-gate) + extra[...]
+    gate, log_forget = gates[...], logs[...]
     r = lax.broadcasted_iota(jnp.int32, (rows, rows), 0)
     c = lax.broadcasted_iota(jnp.int32, (rows, rows), 1)
     lower = (r >= c).astype(F32)
     cum = jnp.dot(lower, log_forget, precision=HI, preferred_element_type=F32)
-    gate_out[...] = gate
     cum_out[...] = cum
     total = cum[rows - 1 : rows, :]
     keys = gate * jnp.exp(total - cum)
@@ -93,10 +90,9 @@
             )
 
 
-def kernel_call(body, out_shape, scratch=(), smem=0, n_in=0, mib=16, fetched=False):
+def kernel_call(body, out_shape, scratch=(), smem=0, n_in=0, mib=16):
     specs = [pl.BlockSpec(memory_space=pltpu.SMEM)] * smem
-    space = pltpu.HBM if fetched else pltpu.VMEM
-    specs += [pl.BlockSpec(memory_space=space)] * (n_in - smem)
+    specs += [pl.BlockSpec(memory_space=pltpu.VMEM)] * (n_in - smem)
     many = isinstance(out_shape, (list, tuple))
     out_spec = pl.BlockSpec(memory_space=pltpu.VMEM)
     return pl.pallas_call(
@@ -107,22 +103,6 @@
         scratch_shapes=list(scratch),
         compiler_params=pltpu.CompilerParams(vmem_limit_bytes=mib * 1024 * 1024),
     )
-
-
-def fetch_then(body, n):
-    def run(*refs):
-        sources, outs, held, sems = refs[:n], refs[n : -n - 1], refs[-n - 1 : -1], refs[-1]
-        copies = [
-            pltpu.make_async_copy(src, dst, sems.at[k])
-            for k, (src, dst) in enumerate(zip(sources, held))
-        ]
-        for copy in copies:
-            copy.start()
-        for copy in copies:
-            copy.wait()
-        body(*held, *outs)
-
-    return run
 
 
 def pair_body(place, mine, theirs, out):
@@ -466,24 +446,12 @@
         heads = width // HEAD
 
         packed_shape = jax.ShapeDtypeStruct((heads * HEAD + 16, HEAD), BF16)
-        gate, cum, packed = kernel_call(
-            fetch_then(gates_body, 4),
-            [
-                jax.ShapeDtypeStruct((rows, width), F32),
-                jax.ShapeDtypeStruct((rows, width), F32),
-                packed_shape,
-            ],
-            scratch=[
-                pltpu.VMEM((rows, width), BF16),
-                pltpu.VMEM((rows, width), BF16),
-                pltpu.VMEM((1, width), F32),
-                pltpu.VMEM((rows, width), F32),
-                pltpu.SemaphoreType.DMA((4,)),
-            ],
-            n_in=4,
-            fetched=True,
-            mib=60,
-        )(forget_logits, written_values, forget_floor_gap[None, :], extra_log_decay)
+        gate = forget_floor_gap[None, :] * jax.nn.sigmoid(-forget_logits.astype(F32))
+        log_forget = jnp.log1p(-gate) + extra_log_decay
+        cum, packed = kernel_call(
+            gates_body, [jax.ShapeDtypeStruct((rows, width), F32), packed_shape], n_in=3
+        )(written_values, gate, log_forget)
+
         up_rows, up_cols = mixer_up_weight.shape
         piece = up_cols // n_a
         mine = []
@@ -501,7 +469,8 @@
         down_xy = []
         for k in range(2):
             lanes = slice(k * part, (k + 1) * part)
-            down_xy.append([send(down_x[:half, lanes], y=1), send(down_y[half:, lanes], b=1)])
+            cut = half if k else half // 2
+            down_xy.append([send(down_x[:cut, lanes], y=1), send(down_y[cut:, lanes], b=1)])
         whole = [mixer_down_weight, down_x, down_y]
 
         beside = send(packed, b=1)

time: 172 us -> 180 us (1.047)
  waiting for transfers between devices: 90.4 us -> 107 us
  starting transfers between devices: 54 us -> 50 us
  local copies, waits for them, and re-layouts: 9.42 us -> 5.69 us
  Pallas kernels: 16.2 us -> 14.2 us
    ppermute x37, waiting for transfers between devices: 90.4 us -> 107 us  [send(): return lax.ppermute(x, AXES, pairs)]
    ppermute x37, starting transfers between devices: 54 us -> 50 us  [send(): return lax.ppermute(x, AXES, pairs)]
    unnamed x27 -> x19, local copies, waits for them, and re-layouts: 8.02 us -> 4.29 us
    pallas_call x1, Pallas kernels: 3.17 us -> 1.18 us  [on_device(): kernel_call(gates_body, [jax.ShapeDtypeStruct((rows, width), F32), packed...]
  transfers between devices with their start and end apart: 37 -> 37, of which waited for: 15 -> 15; matrix products, arithmetic and copies ran while one was open for 1% -> 1% of each run, Pallas kernels for 6% -> 5%
where the time goes in v4:
time: 180 us; the launch traced here: 179 us
  waiting for transfers between devices  107 us (59%)
  starting transfers between devices  50 us (28%)
  Pallas kernels  14.2 us (8%)
  local copies, waits for them, and re-layouts  5.69 us (3%)
  other arithmetic  2.3 us (1%)
    ppermute x37, waiting for transfers between devices, send(): return lax.ppermute(x, AXES, pairs)  107 us
    ppermute x37, starting transfers between devices, send(): return lax.ppermute(x, AXES, pairs)  50 us
    unnamed x19, local copies, waits for them, and re-layouts  4.29 us
  transfers between devices with their start and end apart: 37, of which 15 were waited for; matrix products, arithmetic and copies ran while one was open for 1% of the time, Pallas kernels for 5%

profile of v4, /device:TPU:0, one launch (start us, length us, event | category | flops | bytes accessed | tf_op | source)
XLA Modules:
  0.0 179.4 jit_solution(13381866040302102335)
XLA Ops:
  0.0 1.3 log-plus-one_add_fusion
  1.3 0.9 copy-done.2
  2.2 1.2 shard_map.118
  3.4 3.0 %collective-permute-start = (bf16[272,128]{1,0:T(8,128)(2,1)S(1)}, bf16[272,128]{1,0:T(8,128)(2,1)S(1)}, u32[]{:S(2)}, u32[]{:S(2)}) collective-permute-start(bf16[272,128]{1,0:T(8,128)(2,1)S(1)} %get-tuple-element.26.mine), channel_id=1, source_target_pairs={{0,4},{1,5},{2,6},{3,7},{4,0},{5,1},{6,2},{7,3},{8,12},{9,13},{10,... | collective-permute-start | bytes 208904 | tf_op jit(solution)/shard_map/ppermute | solution.py:424
  6.4 0.1 pad_add_fusion.place.refs_0_
  6.5 2.2 %collective-permute-done.theirs.refs_7_ = bf16[272,128]{1,0:T(8,128)(2,1)S(1)} collective-permute-done((bf16[272,128]{1,0:T(8,128)(2,1)S(1)}, bf16[272,128]{1,0:T(8,128)(2,1)S(1)}, u32[]{:S(2)}, u32[]{:S(2)}) %collective-permute-start) | collective-permute-done | bytes 69664 | tf_op jit(solution)/shard_map/ppermute | solution.py:424
  8.7 0.7 shard_map.120
  9.3 4.0 %collective-permute-start.1 = (bf16[272,128]{1,0:T(8,128)(2,1)S(1)}, bf16[272,128]{1,0:T(8,128)(2,1)S(1)}, u32[]{:S(2)}, u32[]{:S(2)}) collective-permute-start(bf16[272,128]{1,0:T(8,128)(2,1)S(1)} %shard_map.120), channel_id=1, source_target_pairs={{0,8},{1,9},{2,10},{3,11},{4,12},{5,13},{6,14},{7,15},{8,16},{9,17... | collective-permute-start | bytes 208904 | tf_op jit(solution)/shard_map/ppermute | solution.py:424
  13.4 4.5 %collective-permute-start.2 = (bf16[272,128]{1,0:T(8,128)(2,1)S(1)}, bf16[272,128]{1,0:T(8,128)(2,1)S(1)}, u32[]{:S(2)}, u32[]{:S(2)}) collective-permute-start(bf16[272,128]{1,0:T(8,128)(2,1)S(1)} %shard_map.120), channel_id=1, source_target_pairs={{0,16},{1,17},{2,18},{3,19},{4,20},{5,21},{6,22},{7,23},{8,24},{9,... | collective-permute-start | bytes 208904 | tf_op jit(solution)/shard_map/ppermute | solution.py:424
  17.9 1.3 collective-permute-start.3
  19.2 0.9 copy-done.3
  20.1 0.9 copy-done.4
  21.0 3.4 %shard_map.119.refs_3_ = f32[256,256]{1,0:T(8,128)S(1)} custom-call(bf16[256,256]{1,0:T(8,128)(2,1)S(1)} %copy-done.4, f32[256,256]{1,0:T(8,128)S(1)} %get-tuple-element.52.gates.gate, f32[256,256]{1,0:T(8,128)S(1)} %get-tuple-element.25.cum.refs_2_, bf16[256,256]{1,0:T(8,128)(2,1)S(1)} %copy-done.3), custom_call_target="tpu_custom_call" | custom-call | tf_op jit(solution)/shard_map/pallas_call | solution.py:479
  24.5 0.9 copy-done.6
  25.4 0.7 copy-done.8
  26.0 2.5 %shard_map.121 = (f32[64,2048]{1,0:T(8,128)S(1)}, f32[64,2048]{1,0:T(8,128)S(1)}, bf16[128,2048]{1,0:T(8,128)(2,1)}) custom-call(s32[4]{0:T(128)S(1)} %pad_add_fusion.place.refs_0_, bf16[256,256]{1,0:T(8,128)(2,1)S(1)} %copy-done.4, f32[256,256]{1,0:T(8,128)S(1)} %get-tuple-element.25.cum.refs_2_, f32[256,256]{1,0:T(8,128)S(1)} %shard_map.119.refs_3_, ...), custom_call_target="tpu_custom_call" | custom-call | tf_op jit(solution)/shard_map/pallas_call | solution.py:482
  28.5 1.3 constant_dynamic-slice_fusion
  29.9 3.8 %collective-permute-start.15 = (bf16[256,512]{1,0:T(8,128)(2,1)S(1)}, bf16[256,512]{1,0:T(8,128)(2,1)S(1)}, u32[]{:S(2)}, u32[]{:S(2)}) collective-permute-start(bf16[256,512]{1,0:T(8,128)(2,1)S(1)} %get-tuple-element.45), channel_id=1, source_target_pairs={{0,24},{1,25},{2,26},{3,27},{4,28},{5,29},{6,30},{7,31},{8,0},{9,1... | collective-permute-start | bytes 786440 | tf_op jit(solution)/shard_map/ppermute | solution.py:424
  33.7 1.5 collective-permute-start.16
  35.2 5.7 %collective-permute-done.13.refs_10_ = bf16[256,512]{1,0:T(8,128)(2,1)S(1)} collective-permute-done((bf16[256,512]{1,0:T(8,128)(2,1)S(1)}, bf16[256,512]{1,0:T(8,128)(2,1)S(1)}, u32[]{:S(2)}, u32[]{:S(2)}) %collective-permute-start.13) | collective-permute-done | bytes 262176 | tf_op jit(solution)/shard_map/ppermute | solution.py:424
  40.9 1.5 collective-permute-start.19
  42.4 4.4 %collective-permute-done.15.refs_12_ = bf16[256,512]{1,0:T(8,128)(2,1)S(1)} collective-permute-done((bf16[256,512]{1,0:T(8,128)(2,1)S(1)}, bf16[256,512]{1,0:T(8,128)(2,1)S(1)}, u32[]{:S(2)}, u32[]{:S(2)}) %collective-permute-start.15) | collective-permute-done | bytes 262176 | tf_op jit(solution)/shard_map/ppermute | solution.py:424
  46.9 1.5 collective-permute-start.26
  48.4 6.4 %collective-permute-done.14.refs_11_ = bf16[256,512]{1,0:T(8,128)(2,1)S(1)} collective-permute-done((bf16[256,512]{1,0:T(8,128)(2,1)S(1)}, bf16[256,512]{1,0:T(8,128)(2,1)S(1)}, u32[]{:S(2)}, u32[]{:S(2)}) %collective-permute-start.14) | collective-permute-done | bytes 262176 | tf_op jit(solution)/shard_map/ppermute | solution.py:424
  54.8 1.5 collective-permute-start.25
  56.3 0.5 collective-permute-start.17
  56.8 1.5 collective-permute-start.20
  58.4 0.6 collective-permute-start.22
  59.0 26.1 %collective-permute-done.17.refs_14_ = bf16[256,512]{1,0:T(8,128)(2,1)S(1)} collective-permute-done((bf16[256,512]{1,0:T(8,128)(2,1)S(1)}, bf16[256,512]{1,0:T(8,128)(2,1)S(1)}, u32[]{:S(2)}, u32[]{:S(2)}) %collective-permute-start.17) | collective-permute-done | bytes 262176 | tf_op jit(solution)/shard_map/ppermute | solution.py:424
  85.1 1.5 collective-permute-start.5
  86.7 1.6 collective-permute-start.18
  88.3 0.5 collective-permute-start.21
  88.8 5.5 %collective-permute-done.5.arrived = bf16[64,2048]{1,0:T(8,128)(2,1)S(1)} collective-permute-done((bf16[64,2048]{1,0:T(8,128)(2,1)S(1)}, bf16[64,2048]{1,0:T(8,128)(2,1)S(1)}, u32[]{:S(2)}, u32[]{:S(2)}) %collective-permute-start.5) | collective-permute-done | bytes 262176 | tf_op jit(solution)/shard_map/ppermute | solution.py:424
  94.3 1.5 collective-permute-start.23
  95.8 0.2 shard_map.122
  96.1 12.9 %collective-permute-done.23.refs_7_ = bf16[256,512]{1,0:T(8,128)(2,1)S(1)} collective-permute-done((bf16[256,512]{1,0:T(8,128)(2,1)S(1)}, bf16[256,512]{1,0:T(8,128)(2,1)S(1)}, u32[]{:S(2)}, u32[]{:S(2)}) %collective-permute-start.23) | collective-permute-done | bytes 262176 | tf_op jit(solution)/shard_map/ppermute | solution.py:424
  109.0 3.1 %collective-permute-start.7 = (bf16[8,64,256]{2,1,0:T(8,128)(2,1)S(1)}, bf16[8,64,256]{2,1,0:T(8,128)(2,1)S(1)}, u32[]{:S(2)}, u32[]{:S(2)}) collective-permute-start(bf16[8,64,256]{2,1,0:T(8,128)(2,1)S(1)} %get-tuple-element.31.refs_1_), channel_id=1, source_target_pairs={{0,16},{1,17},{2,18},{3,19},{4,20},{5,21},{6,22},{7,23},{8,24},{9,... | collective-permute-start | bytes 786440 | tf_op jit(solution)/shard_map/ppermute | solution.py:424
  112.1 1.3 collective-permute-start.8
  113.4 1.6 collective-permute-start.24
  114.9 4.6 %collective-permute-done.6.refs_2_ = bf16[8,64,256]{2,1,0:T(8,128)(2,1)S(1)} collective-permute-done((bf16[8,64,256]{2,1,0:T(8,128)(2,1)S(1)}, bf16[8,64,256]{2,1,0:T(8,128)(2,1)S(1)}, u32[]{:S(2)}, u32[]{:S(2)}) %collective-permute-start.6) | collective-permute-done | bytes 262176 | tf_op jit(solution)/shard_map/ppermute | solution.py:424
  119.6 10.9 %collective-permute-done.7.refs_3_ = bf16[8,64,256]{2,1,0:T(8,128)(2,1)S(1)} collective-permute-done((bf16[8,64,256]{2,1,0:T(8,128)(2,1)S(1)}, bf16[8,64,256]{2,1,0:T(8,128)(2,1)S(1)}, u32[]{:S(2)}, u32[]{:S(2)}) %collective-permute-start.7) | collective-permute-done | bytes 262176 | tf_op jit(solution)/shard_map/ppermute | solution.py:424
  130.5 0.6 collective-permute-start.12
  131.1 1.5 collective-permute-start.28
  132.6 1.6 collective-permute-start.32
  134.2 0.5 collective-permute-start.33
  134.8 0.6 collective-permute-start.27
  135.4 1.8 shard_map.123
  137.1 6.4 %collective-permute-done.27.refs_12_ = bf16[64,1024]{1,0:T(8,128)(2,1)S(1)} collective-permute-done((bf16[64,1024]{1,0:T(8,128)(2,1)S(1)}, bf16[64,1024]{1,0:T(8,128)(2,1)S(1)}, u32[]{:S(2)}, u32[]{:S(2)}) %collective-permute-start.27) | collective-permute-done | bytes 131104 | tf_op jit(solution)/shard_map/ppermute | solution.py:424
  143.5 3.0 %shard_map.124 = (f32[256,1024]{1,0:T(8,128)S(1)}, bf16[256,1024]{1,0:T(8,128)(2,1)S(1)}, bf16[512,1024]{1,0:T(8,128)(2,1)S(1)}) custom-call(s32[4]{0:T(128)S(1)} %pad_add_fusion.place.refs_0_, bf16[512,2048]{1,0:T(8,128)(2,1)S(1)} %get-tuple-element.34.refs_1_, bf16[512,512]{1,0:T(8,128)(2,1)S(1)} %get-tuple-element.35.refs_2_, ...), custom_call_target="tpu_custom_call" | custom-call | tf_op jit(solution)/shard_map/pallas_call | solution.py:554
  146.6 1.3 collective-permute-done.33.r1_ref
  147.8 1.3 shard_map.126
  149.1 0.5 collective-permute-start.29
  149.6 1.4 collective-permute-done.34.got
  151.0 0.1 shard_map.127
  151.1 3.9 %collective-permute-start.35 = (bf16[128,1024]{1,0:T(8,128)(2,1)S(1)}, bf16[128,1024]{1,0:T(8,128)(2,1)S(1)}, u32[]{:S(2)}, u32[]{:S(2)}) collective-permute-start(bf16[128,1024]{1,0:T(8,128)(2,1)S(1)} %get-tuple-element.44), channel_id=1, source_target_pairs={{0,8},{1,9},{2,10},{3,11},{4,12},{5,13},{6,14},{7,15},{8,0},{9,1},... | collective-permute-start | bytes 786440 | tf_op jit(solution)/shard_map/ppermute | solution.py:424
  155.1 0.1 shard_map.125
  155.2 0.7 collective-permute-start.30
  155.8 6.4 %collective-permute-done.35 = bf16[128,1024]{1,0:T(8,128)(2,1)S(1)} collective-permute-done((bf16[128,1024]{1,0:T(8,128)(2,1)S(1)}, bf16[128,1024]{1,0:T(8,128)(2,1)S(1)}, u32[]{:S(2)}, u32[]{:S(2)}) %collective-permute-start.35) | collective-permute-done | bytes 262176 | tf_op jit(solution)/shard_map/ppermute | solution.py:424
  162.2 3.0 %collective-permute-start.36 = (bf16[64,1024]{1,0:T(8,128)(2,1)S(1)}, bf16[64,1024]{1,0:T(8,128)(2,1)S(1)}, u32[]{:S(2)}, u32[]{:S(2)}) collective-permute-start(bf16[64,1024]{1,0:T(8,128)(2,1)S(1)} %add_convert_fusion.2), channel_id=1, source_target_pairs={{0,16},{1,17},{2,18},{3,19},{4,20},{5,21},{6,22},{7,23},{8,24},{9,... | collective-permute-start | bytes 393224 | tf_op jit(solution)/shard_map/ppermute | solution.py:424
  165.2 4.9 %collective-permute-done.30 = bf16[128,1024]{1,0:T(8,128)(2,1)S(1)} collective-permute-done((bf16[128,1024]{1,0:T(8,128)(2,1)S(1)}, bf16[128,1024]{1,0:T(8,128)(2,1)S(1)}, u32[]{:S(2)}, u32[]{:S(2)}) %collective-permute-start.30) | collective-permute-done | bytes 262176 | tf_op jit(solution)/shard_map/ppermute | solution.py:424
  170.1 0.7 collective-permute-start.31
  170.8 7.7 %collective-permute-done.31 = bf16[64,1024]{1,0:T(8,128)(2,1)S(1)} collective-permute-done((bf16[64,1024]{1,0:T(8,128)(2,1)S(1)}, bf16[64,1024]{1,0:T(8,128)(2,1)S(1)}, u32[]{:S(2)}, u32[]{:S(2)}) %collective-permute-start.31) | collective-permute-done | bytes 131104 | tf_op jit(solution)/shard_map/ppermute | solution.py:424
  178.6 0.1 add_convert_fusion.3
  178.7 0.7 pad_maximum_fusion
  (52 shorter events, 0.4 us)
Async XLA Ops:
  0.0 24.5 %copy-start.1 = (bf16[256,2048]{1,0:T(8,128)(2,1)S(1)}, bf16[256,2048]{1,0:T(8,128)(2,1)}, u32[]{:S(2)}) copy-start(bf16[256,2048]{1,0:T(8,128)(2,1)} %refs_6_.1) | copy-start | bytes 3145732
  1.3 0.9 copy-start.2
  3.4 5.3 %collective-permute-start = (bf16[272,128]{1,0:T(8,128)(2,1)S(1)}, bf16[272,128]{1,0:T(8,128)(2,1)S(1)}, u32[]{:S(2)}, u32[]{:S(2)}) collective-permute-start(bf16[272,128]{1,0:T(8,128)(2,1)S(1)} %get-tuple-element.26.mine), channel_id=1, source_target_pairs={{0,4},{1,5},{2,6},{3,7},{4,0},{5,1},{6,2},{7,3},{8,12},{9,13},{10,... | collective-permute-start | bytes 208904 | tf_op jit(solution)/shard_map/ppermute | solution.py:424
  9.3 15.1 %collective-permute-start.1 = (bf16[272,128]{1,0:T(8,128)(2,1)S(1)}, bf16[272,128]{1,0:T(8,128)(2,1)S(1)}, u32[]{:S(2)}, u32[]{:S(2)}) collective-permute-start(bf16[272,128]{1,0:T(8,128)(2,1)S(1)} %shard_map.120), channel_id=1, source_target_pairs={{0,8},{1,9},{2,10},{3,11},{4,12},{5,13},{6,14},{7,15},{8,16},{9,17... | collective-permute-start | bytes 208904 | tf_op jit(solution)/shard_map/ppermute | solution.py:424
  13.4 11.1 %collective-permute-start.2 = (bf16[272,128]{1,0:T(8,128)(2,1)S(1)}, bf16[272,128]{1,0:T(8,128)(2,1)S(1)}, u32[]{:S(2)}, u32[]{:S(2)}) collective-permute-start(bf16[272,128]{1,0:T(8,128)(2,1)S(1)} %shard_map.120), channel_id=1, source_target_pairs={{0,16},{1,17},{2,18},{3,19},{4,20},{5,21},{6,22},{7,23},{8,24},{9,... | collective-permute-start | bytes 208904 | tf_op jit(solution)/shard_map/ppermute | solution.py:424
  17.9 6.6 %collective-permute-start.3 = (bf16[272,128]{1,0:T(8,128)(2,1)S(1)}, bf16[272,128]{1,0:T(8,128)(2,1)S(1)}, u32[]{:S(2)}, u32[]{:S(2)}) collective-permute-start(bf16[272,128]{1,0:T(8,128)(2,1)S(1)} %shard_map.120), channel_id=1, source_target_pairs={{0,24},{1,25},{2,26},{3,27},{4,28},{5,29},{6,30},{7,31}} | collective-permute-start | bytes 208904 | tf_op jit(solution)/shard_map/ppermute | solution.py:424
  19.2 0.9 copy-start.3
  20.1 0.9 copy-start.4
  24.5 0.9 copy-start.6
  25.4 0.7 copy-start.8
  26.0 20.8 %copy-start = (bf16[256,2048]{1,0:T(8,128)(2,1)S(1)}, bf16[256,2048]{1,0:T(8,128)(2,1)}, u32[]{:S(2)}) copy-start(bf16[256,2048]{1,0:T(8,128)(2,1)} %own_ref.1) | copy-start | bytes 3145732
  28.5 28.3 %collective-permute-start.4 = (bf16[128,2048]{1,0:T(8,128)(2,1)}, bf16[128,2048]{1,0:T(8,128)(2,1)S(1)}, u32[]{:S(2)}, u32[]{:S(2)}) collective-permute-start(bf16[128,2048]{1,0:T(8,128)(2,1)} %get-tuple-element.28), channel_id=1, source_target_pairs={{0,1},{1,0},{2,3},{3,2},{4,5},{5,4},{6,7},{7,6},{8,9},{9,8},{10,11... | collective-permute-start | bytes 1572872 | tf_op jit(solution)/shard_map/ppermute | solution.py:424
  28.5 67.3 %copy-start.5 = (bf16[64,2048]{1,0:T(8,128)(2,1)S(1)}, bf16[64,2048]{1,0:T(8,128)(2,1)}, u32[]{:S(2)}) copy-start(bf16[64,2048]{1,0:T(8,128)(2,1)} %residual.1) | copy-start | bytes 786436
  28.5 67.3 %copy-start.7 = (f32[2048]{0:T(1024)S(1)}, f32[2048]{0:T(1024)}, u32[]{:S(2)}) copy-start(f32[2048]{0:T(1024)} %param.21) | copy-start | bytes 24580
  29.8 11.1 %collective-permute-start.13 = (bf16[256,512]{1,0:T(8,128)(2,1)S(1)}, bf16[256,512]{1,0:T(8,128)(2,1)S(1)}, u32[]{:S(2)}, u32[]{:S(2)}) collective-permute-start(bf16[256,512]{1,0:T(8,128)(2,1)S(1)} %get-tuple-element.46), channel_id=1, source_target_pairs={{0,8},{1,9},{2,10},{3,11},{4,12},{5,13},{6,14},{7,15},{8,16},{9,17... | collective-permute-start | bytes 786440 | tf_op jit(solution)/shard_map/ppermute | solution.py:424
  29.9 17.0 %collective-permute-start.15 = (bf16[256,512]{1,0:T(8,128)(2,1)S(1)}, bf16[256,512]{1,0:T(8,128)(2,1)S(1)}, u32[]{:S(2)}, u32[]{:S(2)}) collective-permute-start(bf16[256,512]{1,0:T(8,128)(2,1)S(1)} %get-tuple-element.45), channel_id=1, source_target_pairs={{0,24},{1,25},{2,26},{3,27},{4,28},{5,29},{6,30},{7,31},{8,0},{9,1... | collective-permute-start | bytes 786440 | tf_op jit(solution)/shard_map/ppermute | solution.py:424
  33.7 21.1 %collective-permute-start.14 = (bf16[256,512]{1,0:T(8,128)(2,1)S(1)}, bf16[256,512]{1,0:T(8,128)(2,1)S(1)}, u32[]{:S(2)}, u32[]{:S(2)}) collective-permute-start(bf16[256,512]{1,0:T(8,128)(2,1)S(1)} %get-tuple-element.48), channel_id=1, source_target_pairs={{0,16},{1,17},{2,18},{3,19},{4,20},{5,21},{6,22},{7,23},{8,24},{9,... | collective-permute-start | bytes 786440 | tf_op jit(solution)/shard_map/ppermute | solution.py:424
  33.7 22.6 %collective-permute-start.16 = (bf16[256,512]{1,0:T(8,128)(2,1)S(1)}, bf16[256,512]{1,0:T(8,128)(2,1)S(1)}, u32[]{:S(2)}, u32[]{:S(2)}) collective-permute-start(bf16[256,512]{1,0:T(8,128)(2,1)S(1)} %get-tuple-element.47.refs_9_), channel_id=1, source_target_pairs={{0,4},{1,5},{2,6},{3,7},{4,0},{5,1},{6,2},{7,3},{8,12},{9,13},{10,... | collective-permute-start | bytes 786440 | tf_op jit(solution)/shard_map/ppermute | solution.py:424
  40.9 17.5 %collective-permute-start.19 = (bf16[256,512]{1,0:T(8,128)(2,1)S(1)}, bf16[256,512]{1,0:T(8,128)(2,1)S(1)}, u32[]{:S(2)}, u32[]{:S(2)}) collective-permute-start(bf16[256,512]{1,0:T(8,128)(2,1)S(1)} %get-tuple-element.47.refs_9_), channel_id=1, source_target_pairs={{0,2},{1,3},{2,0},{3,1},{4,6},{5,7},{6,4},{7,5},{8,10},{9,11},{10,... | collective-permute-start | bytes 786440 | tf_op jit(solution)/shard_map/ppermute | solution.py:424
  46.9 62.1 %collective-permute-start.26 = (bf16[256,2048]{1,0:T(8,128)(2,1)S(1)}, bf16[256,2048]{1,0:T(8,128)(2,1)S(1)}, u32[]{:S(2)}, u32[]{:S(2)}) collective-permute-start(bf16[256,2048]{1,0:T(8,128)(2,1)S(1)} %copy-done), channel_id=1, source_target_pairs={{0,2},{1,3},{2,0},{3,1},{4,6},{5,7},{6,4},{7,5},{8,10},{9,11},{10,... | collective-permute-start | bytes 3145736 | tf_op jit(solution)/shard_map/ppermute | solution.py:424
  54.8 57.3 %collective-permute-start.25 = (bf16[256,2048]{1,0:T(8,128)(2,1)S(1)}, bf16[256,2048]{1,0:T(8,128)(2,1)S(1)}, u32[]{:S(2)}, u32[]{:S(2)}) collective-permute-start(bf16[256,2048]{1,0:T(8,128)(2,1)S(1)} %copy-done), channel_id=1, source_target_pairs={{0,4},{1,5},{2,6},{3,7},{4,0},{5,1},{6,2},{7,3},{8,12},{9,13},{10,... | collective-permute-start | bytes 3145736 | tf_op jit(solution)/shard_map/ppermute | solution.py:424
  56.3 28.8 %collective-permute-start.17 = (bf16[256,512]{1,0:T(8,128)(2,1)S(1)}, bf16[256,512]{1,0:T(8,128)(2,1)S(1)}, u32[]{:S(2)}, u32[]{:S(2)}) collective-permute-start(bf16[256,512]{1,0:T(8,128)(2,1)S(1)} %collective-permute-done.14.refs_11_), channel_id=1, source_target_pairs={{0,4},{1,5},{2,6},{3,7},{4,0},{5,1},{6,2},{7,3},{8,12},{9,13},{10,... | collective-permute-start | bytes 786440 | tf_op jit(solution)/shard_map/ppermute | solution.py:424
  56.8 29.9 %collective-permute-start.20 = (bf16[256,512]{1,0:T(8,128)(2,1)S(1)}, bf16[256,512]{1,0:T(8,128)(2,1)S(1)}, u32[]{:S(2)}, u32[]{:S(2)}) collective-permute-start(bf16[256,512]{1,0:T(8,128)(2,1)S(1)} %collective-permute-done.14.refs_11_), channel_id=1, source_target_pairs={{0,2},{1,3},{2,0},{3,1},{4,6},{5,7},{6,4},{7,5},{8,10},{9,11},{10,... | collective-permute-start | bytes 786440 | tf_op jit(solution)/shard_map/ppermute | solution.py:424
  58.4 29.9 %collective-permute-start.22 = (bf16[256,512]{1,0:T(8,128)(2,1)S(1)}, bf16[256,512]{1,0:T(8,128)(2,1)S(1)}, u32[]{:S(2)}, u32[]{:S(2)}) collective-permute-start(bf16[256,512]{1,0:T(8,128)(2,1)S(1)} %collective-permute-done.16.refs_13_), channel_id=1, source_target_pairs={{0,2},{1,3},{2,0},{3,1},{4,6},{5,7},{6,4},{7,5},{8,10},{9,11},{10,... | collective-permute-start | bytes 786440 | tf_op jit(solution)/shard_map/ppermute | solution.py:424
  85.1 9.2 %collective-permute-start.5 = (bf16[64,2048]{1,0:T(8,128)(2,1)S(1)}, bf16[64,2048]{1,0:T(8,128)(2,1)S(1)}, u32[]{:S(2)}, u32[]{:S(2)}) collective-permute-start(bf16[64,2048]{1,0:T(8,128)(2,1)S(1)} %add_convert_fusion), channel_id=1, source_target_pairs={{0,2},{1,3},{2,0},{3,1},{4,6},{5,7},{6,4},{7,5},{8,10},{9,11},{10,... | collective-permute-start | bytes 786440 | tf_op jit(solution)/shard_map/ppermute | solution.py:424
  86.7 26.7 %collective-permute-start.18 = (bf16[512,512]{1,0:T(8,128)(2,1)S(1)}, bf16[512,512]{1,0:T(8,128)(2,1)S(1)}, u32[]{:S(2)}, u32[]{:S(2)}) collective-permute-start(bf16[512,512]{1,0:T(8,128)(2,1)S(1)} %constant_dynamic-update-slice_fusion), channel_id=1, source_target_pairs={{0,4},{1,5},{2,6},{3,7},{4,0},{5,1},{6,2},{7,3},{8,12},{9,13},{10,... | collective-permute-start | bytes 1572872 | tf_op jit(solution)/shard_map/ppermute | solution.py:424
  88.3 25.1 %collective-permute-start.21 = (bf16[512,512]{1,0:T(8,128)(2,1)S(1)}, bf16[512,512]{1,0:T(8,128)(2,1)S(1)}, u32[]{:S(2)}, u32[]{:S(2)}) collective-permute-start(bf16[512,512]{1,0:T(8,128)(2,1)S(1)} %constant_dynamic-update-slice_fusion), channel_id=1, source_target_pairs={{0,2},{1,3},{2,0},{3,1},{4,6},{5,7},{6,4},{7,5},{8,10},{9,11},{10,... | collective-permute-start | bytes 1572872 | tf_op jit(solution)/shard_map/ppermute | solution.py:424
  94.3 14.7 %collective-permute-start.23 = (bf16[256,512]{1,0:T(8,128)(2,1)S(1)}, bf16[256,512]{1,0:T(8,128)(2,1)S(1)}, u32[]{:S(2)}, u32[]{:S(2)}) collective-permute-start(bf16[256,512]{1,0:T(8,128)(2,1)S(1)} %collective-permute-done.17.refs_14_), channel_id=1, source_target_pairs={{0,2},{1,3},{2,0},{3,1},{4,6},{5,7},{6,4},{7,5},{8,10},{9,11},{10,... | collective-permute-start | bytes 786440 | tf_op jit(solution)/shard_map/ppermute | solution.py:424
  109.0 10.6 %collective-permute-start.6 = (bf16[8,64,256]{2,1,0:T(8,128)(2,1)S(1)}, bf16[8,64,256]{2,1,0:T(8,128)(2,1)S(1)}, u32[]{:S(2)}, u32[]{:S(2)}) collective-permute-start(bf16[8,64,256]{2,1,0:T(8,128)(2,1)S(1)} %get-tuple-element.31.refs_1_), channel_id=1, source_target_pairs={{0,8},{1,9},{2,10},{3,11},{4,12},{5,13},{6,14},{7,15},{8,0},{9,1},... | collective-permute-start | bytes 786440 | tf_op jit(solution)/shard_map/ppermute | solution.py:424
  109.0 21.5 %collective-permute-start.7 = (bf16[8,64,256]{2,1,0:T(8,128)(2,1)S(1)}, bf16[8,64,256]{2,1,0:T(8,128)(2,1)S(1)}, u32[]{:S(2)}, u32[]{:S(2)}) collective-permute-start(bf16[8,64,256]{2,1,0:T(8,128)(2,1)S(1)} %get-tuple-element.31.refs_1_), channel_id=1, source_target_pairs={{0,16},{1,17},{2,18},{3,19},{4,20},{5,21},{6,22},{7,23},{8,24},{9,... | collective-permute-start | bytes 786440 | tf_op jit(solution)/shard_map/ppermute | solution.py:424
  112.1 18.4 %collective-permute-start.8 = (bf16[8,64,256]{2,1,0:T(8,128)(2,1)S(1)}, bf16[8,64,256]{2,1,0:T(8,128)(2,1)S(1)}, u32[]{:S(2)}, u32[]{:S(2)}) collective-permute-start(bf16[8,64,256]{2,1,0:T(8,128)(2,1)S(1)} %get-tuple-element.31.refs_1_), channel_id=1, source_target_pairs={{0,24},{1,25},{2,26},{3,27},{4,28},{5,29},{6,30},{7,31},{8,16},{9,... | collective-permute-start | bytes 786440 | tf_op jit(solution)/shard_map/ppermute | solution.py:424
  113.4 17.7 %collective-permute-start.9 = (bf16[8,64,256]{2,1,0:T(8,128)(2,1)S(1)}, bf16[8,64,256]{2,1,0:T(8,128)(2,1)S(1)}, u32[]{:S(2)}, u32[]{:S(2)}) collective-permute-start(bf16[8,64,256]{2,1,0:T(8,128)(2,1)S(1)} %get-tuple-element.31.refs_1_), channel_id=1, source_target_pairs={{0,1},{1,0},{2,3},{3,2},{4,5},{5,4},{6,7},{7,6},{8,9},{9,8},{10,11... | collective-permute-start | bytes 786440 | tf_op jit(solution)/shard_map/ppermute | solution.py:424
  113.4 30.1 %collective-permute-start.24 = (bf16[512,512]{1,0:T(8,128)(2,1)S(1)}, bf16[512,512]{1,0:T(8,128)(2,1)S(1)}, u32[]{:S(2)}, u32[]{:S(2)}) collective-permute-start(bf16[512,512]{1,0:T(8,128)(2,1)S(1)} %collective-permute-done.21.refs_5_), channel_id=1, source_target_pairs={{0,4},{1,5},{2,6},{3,7},{4,0},{5,1},{6,2},{7,3},{8,12},{9,13},{10,... | collective-permute-start | bytes 1572872 | tf_op jit(solution)/shard_map/ppermute | solution.py:424
  119.6 13.1 %collective-permute-start.10 = (bf16[8,64,256]{2,1,0:T(8,128)(2,1)S(1)}, bf16[8,64,256]{2,1,0:T(8,128)(2,1)S(1)}, u32[]{:S(2)}, u32[]{:S(2)}) collective-permute-start(bf16[8,64,256]{2,1,0:T(8,128)(2,1)S(1)} %collective-permute-done.6.refs_2_), channel_id=1, source_target_pairs={{0,1},{1,0},{2,3},{3,2},{4,5},{5,4},{6,7},{7,6},{8,9},{9,8},{10,11... | collective-permute-start | bytes 786440 | tf_op jit(solution)/shard_map/ppermute | solution.py:424
  130.5 3.8 %collective-permute-start.11 = (bf16[8,64,256]{2,1,0:T(8,128)(2,1)S(1)}, bf16[8,64,256]{2,1,0:T(8,128)(2,1)S(1)}, u32[]{:S(2)}, u32[]{:S(2)}) collective-permute-start(bf16[8,64,256]{2,1,0:T(8,128)(2,1)S(1)} %collective-permute-done.7.refs_3_), channel_id=1, source_target_pairs={{0,1},{1,0},{2,3},{3,2},{4,5},{5,4},{6,7},{7,6},{8,9},{9,8},{10,11... | collective-permute-start | bytes 786440 | tf_op jit(solution)/shard_map/ppermute | solution.py:424
  130.5 4.3 %collective-permute-start.12 = (bf16[8,64,256]{2,1,0:T(8,128)(2,1)S(1)}, bf16[8,64,256]{2,1,0:T(8,128)(2,1)S(1)}, u32[]{:S(2)}, u32[]{:S(2)}) collective-permute-start(bf16[8,64,256]{2,1,0:T(8,128)(2,1)S(1)} %collective-permute-done.8.refs_4_), channel_id=1, source_target_pairs={{0,1},{1,0},{2,3},{3,2},{4,5},{5,4},{6,7},{7,6},{8,9},{9,8},{10,11... | collective-permute-start | bytes 786440 | tf_op jit(solution)/shard_map/ppermute | solution.py:424
  131.1 12.4 %collective-permute-start.28 = (bf16[192,1024]{1,0:T(8,128)(2,1)S(1)}, bf16[192,1024]{1,0:T(8,128)(2,1)S(1)}, u32[]{:S(2)}, u32[]{:S(2)}) collective-permute-start(bf16[192,1024]{1,0:T(8,128)(2,1)S(1)} %slice.62), channel_id=1, source_target_pairs={{0,4},{1,5},{2,6},{3,7},{4,0},{5,1},{6,2},{7,3},{8,12},{9,13},{10,... | collective-permute-start | bytes 1179656 | tf_op jit(solution)/shard_map/ppermute | solution.py:424
  132.6 13.9 %collective-permute-start.32 = (bf16[128,1024]{1,0:T(8,128)(2,1)S(1)}, bf16[128,1024]{1,0:T(8,128)(2,1)S(1)}, u32[]{:S(2)}, u32[]{:S(2)}) collective-permute-start(bf16[128,1024]{1,0:T(8,128)(2,1)S(1)} %slice.65), channel_id=1, source_target_pairs={{0,2},{1,3},{2,0},{3,1},{4,6},{5,7},{6,4},{7,5},{8,10},{9,11},{10,... | collective-permute-start | bytes 786440 | tf_op jit(solution)/shard_map/ppermute | solution.py:424
  134.2 13.6 %collective-permute-start.33 = (bf16[128,1024]{1,0:T(8,128)(2,1)S(1)}, bf16[128,1024]{1,0:T(8,128)(2,1)S(1)}, u32[]{:S(2)}, u32[]{:S(2)}) collective-permute-start(bf16[128,1024]{1,0:T(8,128)(2,1)S(1)} %slice.66), channel_id=1, source_target_pairs={{0,4},{1,5},{2,6},{3,7},{4,0},{5,1},{6,2},{7,3},{8,12},{9,13},{10,... | collective-permute-start | bytes 786440 | tf_op jit(solution)/shard_map/ppermute | solution.py:424
  134.8 8.7 %collective-permute-start.27 = (bf16[64,1024]{1,0:T(8,128)(2,1)S(1)}, bf16[64,1024]{1,0:T(8,128)(2,1)S(1)}, u32[]{:S(2)}, u32[]{:S(2)}) collective-permute-start(bf16[64,1024]{1,0:T(8,128)(2,1)S(1)} %slice.61), channel_id=1, source_target_pairs={{0,2},{1,3},{2,0},{3,1},{4,6},{5,7},{6,4},{7,5},{8,10},{9,11},{10,... | collective-permute-start | bytes 393224 | tf_op jit(solution)/shard_map/ppermute | solution.py:424
  149.1 2.0 %collective-permute-start.34 = (bf16[256,1024]{1,0:T(8,128)(2,1)S(1)}, bf16[256,1024]{1,0:T(8,128)(2,1)S(1)}, u32[]{:S(2)}, u32[]{:S(2)}) collective-permute-start(bf16[256,1024]{1,0:T(8,128)(2,1)S(1)} %get-tuple-element.42), channel_id=1, source_target_pairs={{0,1},{1,0},{2,3},{3,2},{4,5},{5,4},{6,7},{7,6},{8,9},{9,8},{10,11... | collective-permute-start | bytes 1572872 | tf_op jit(solution)/shard_map/ppermute | solution.py:424
  149.1 5.9 %collective-permute-start.29 = (bf16[256,1024]{1,0:T(8,128)(2,1)S(1)}, bf16[256,1024]{1,0:T(8,128)(2,1)S(1)}, u32[]{:S(2)}, u32[]{:S(2)}) collective-permute-start(bf16[256,1024]{1,0:T(8,128)(2,1)S(1)} %get-tuple-element.37), channel_id=1, source_target_pairs={{0,1},{1,0},{2,3},{3,2},{4,5},{5,4},{6,7},{7,6},{8,9},{9,8},{10,11... | collective-permute-start | bytes 1572872 | tf_op jit(solution)/shard_map/ppermute | solution.py:424
  151.1 11.1 %collective-permute-start.35 = (bf16[128,1024]{1,0:T(8,128)(2,1)S(1)}, bf16[128,1024]{1,0:T(8,128)(2,1)S(1)}, u32[]{:S(2)}, u32[]{:S(2)}) collective-permute-start(bf16[128,1024]{1,0:T(8,128)(2,1)S(1)} %get-tuple-element.44), channel_id=1, source_target_pairs={{0,8},{1,9},{2,10},{3,11},{4,12},{5,13},{6,14},{7,15},{8,0},{9,1},... | collective-permute-start | bytes 786440 | tf_op jit(solution)/shard_map/ppermute | solution.py:424
  155.2 14.9 %collective-permute-start.30 = (bf16[128,1024]{1,0:T(8,128)(2,1)S(1)}, bf16[128,1024]{1,0:T(8,128)(2,1)S(1)}, u32[]{:S(2)}, u32[]{:S(2)}) collective-permute-start(bf16[128,1024]{1,0:T(8,128)(2,1)S(1)} %get-tuple-element.39), channel_id=1, source_target_pairs={{0,8},{1,9},{2,10},{3,11},{4,12},{5,13},{6,14},{7,15},{8,0},{9,1},... | collective-permute-start | bytes 786440 | tf_op jit(solution)/shard_map/ppermute | solution.py:424
  162.2 8.6 %collective-permute-start.36 = (bf16[64,1024]{1,0:T(8,128)(2,1)S(1)}, bf16[64,1024]{1,0:T(8,128)(2,1)S(1)}, u32[]{:S(2)}, u32[]{:S(2)}) collective-permute-start(bf16[64,1024]{1,0:T(8,128)(2,1)S(1)} %add_convert_fusion.2), channel_id=1, source_target_pairs={{0,16},{1,17},{2,18},{3,19},{4,20},{5,21},{6,22},{7,23},{8,24},{9,... | collective-permute-start | bytes 393224 | tf_op jit(solution)/shard_map/ppermute | solution.py:424
  170.1 8.5 %collective-permute-start.31 = (bf16[64,1024]{1,0:T(8,128)(2,1)S(1)}, bf16[64,1024]{1,0:T(8,128)(2,1)S(1)}, u32[]{:S(2)}, u32[]{:S(2)}) collective-permute-start(bf16[64,1024]{1,0:T(8,128)(2,1)S(1)} %add_convert_fusion.4), channel_id=1, source_target_pairs={{0,16},{1,17},{2,18},{3,19},{4,20},{5,21},{6,22},{7,23},{8,24},{9,... | collective-permute-start | bytes 393224 | tf_op jit(solution)/shard_map/ppermute | solution.py:424

commit v5 on v4

--- a/solution.py
+++ b/solution.py
@@ -456,7 +456,8 @@
         piece = up_cols // n_a
         mine = []
         for d in range(n_a):
-            cut = lax.dynamic_slice(mixer_up_weight, (0, (a + d) % n_a * piece), (up_rows, piece))
+            start = (0, (a + d) % n_a * piece)
+            cut = lax.dynamic_slice(mixer_up_weight, start, (up_rows, piece))
             mine.append(cut if d == 0 else send(cut, a=d))
 
         def grouped(refs):
@@ -503,12 +504,6 @@
         got = send(away, c=1)
         second = (second + got[own:].astype(F32)).astype(BF16)
         other = send(second, y=1)
-        late = lax.optimization_barrier((mine[1], mine[3], second))[:2]
-        up_x, up_y = [], []
-        for members in [mine[0], mine[2], jnp.concatenate(late, axis=0)]:
-            up_x.append(send(members, b=1))
-            up_y.append(send(members, y=1))
-        up_xy = [send(up_x[0], y=1), send(up_x[1], y=1), send(up_y[2], b=1)]
         stream, normed = kernel_call(
             norm_body,
             [
@@ -517,6 +512,13 @@
             ],
             n_in=5,
         )(first, got, other, residual, mixer_norm_gain[None, :])
+
+        late = lax.optimization_barrier((mine[1], mine[3], normed))[:2]
+        up_x, up_y = [], []
+        for members in [mine[0], mine[2], jnp.concatenate(late, axis=0)]:
+            up_x.append(send(members, b=1))
+            up_y.append(send(members, y=1))
+        up_xy = [send(up_x[0], y=1), send(up_x[1], y=1), send(up_y[2], b=1)]
 
         line = [normed] + [send(normed, flip=d) for d in range(1, n_a)]
         toks = line + [send(u, c=1) for u in line]

time: 180 us -> 156 us (0.87)
  waiting for transfers between devices: 107 us -> 83.6 us
    ppermute x37, waiting for transfers between devices: 107 us -> 83.6 us  [send(): return lax.ppermute(x, AXES, pairs)]
  transfers between devices with their start and end apart: 37 -> 37, of which waited for: 15 -> 19; matrix products, arithmetic and copies ran while one was open for 1% -> 1% of each run, Pallas kernels for 5% -> 6%
where the time goes in v5:
time: 156 us; the launch traced here: 155 us
  waiting for transfers between devices  83.6 us (54%)
  starting transfers between devices  49.3 us (32%)
  Pallas kernels  14.2 us (9%)
  local copies, waits for them, and re-layouts  5.69 us (4%)
  other arithmetic  2.32 us (1%)
    ppermute x37, waiting for transfers between devices, send(): return lax.ppermute(x, AXES, pairs)  83.6 us
    ppermute x37, starting transfers between devices, send(): return lax.ppermute(x, AXES, pairs)  49.3 us
    unnamed x19, local copies, waits for them, and re-layouts  4.29 us
    pallas_call x1, Pallas kernels, on_device(): kernel_call(local_body, jax.ShapeDtypeStruct((rows, width), F32), n_in=4)  3.44 us
  transfers between devices with their start and end apart: 37, of which 19 were waited for; matrix products, arithmetic and copies ran while one was open for 1% of the time, Pallas kernels for 6%

profile of v5, /device:TPU:0, one launch (start us, length us, event | category | flops | bytes accessed | tf_op | source)
XLA Modules:
  0.0 155.3 jit_solution(12591445809979809755)
XLA Ops:
  0.0 1.3 log-plus-one_add_fusion
  1.3 0.9 copy-done.2
  2.2 1.2 shard_map.118
  3.4 3.0 %collective-permute-start = (bf16[272,128]{1,0:T(8,128)(2,1)S(1)}, bf16[272,128]{1,0:T(8,128)(2,1)S(1)}, u32[]{:S(2)}, u32[]{:S(2)}) collective-permute-start(bf16[272,128]{1,0:T(8,128)(2,1)S(1)} %get-tuple-element.26.mine), channel_id=1, source_target_pairs={{0,4},{1,5},{2,6},{3,7},{4,0},{5,1},{6,2},{7,3},{8,12},{9,13},{10,... | collective-permute-start | bytes 208904 | tf_op jit(solution)/shard_map/ppermute | solution.py:424
  6.5 2.2 %collective-permute-done.theirs.refs_7_ = bf16[272,128]{1,0:T(8,128)(2,1)S(1)} collective-permute-done((bf16[272,128]{1,0:T(8,128)(2,1)S(1)}, bf16[272,128]{1,0:T(8,128)(2,1)S(1)}, u32[]{:S(2)}, u32[]{:S(2)}) %collective-permute-start) | collective-permute-done | bytes 69664 | tf_op jit(solution)/shard_map/ppermute | solution.py:424
  8.7 0.7 shard_map.120
  9.3 4.0 %collective-permute-start.1 = (bf16[272,128]{1,0:T(8,128)(2,1)S(1)}, bf16[272,128]{1,0:T(8,128)(2,1)S(1)}, u32[]{:S(2)}, u32[]{:S(2)}) collective-permute-start(bf16[272,128]{1,0:T(8,128)(2,1)S(1)} %shard_map.120), channel_id=1, source_target_pairs={{0,8},{1,9},{2,10},{3,11},{4,12},{5,13},{6,14},{7,15},{8,16},{9,17... | collective-permute-start | bytes 208904 | tf_op jit(solution)/shard_map/ppermute | solution.py:424
  13.4 4.5 %collective-permute-start.2 = (bf16[272,128]{1,0:T(8,128)(2,1)S(1)}, bf16[272,128]{1,0:T(8,128)(2,1)S(1)}, u32[]{:S(2)}, u32[]{:S(2)}) collective-permute-start(bf16[272,128]{1,0:T(8,128)(2,1)S(1)} %shard_map.120), channel_id=1, source_target_pairs={{0,16},{1,17},{2,18},{3,19},{4,20},{5,21},{6,22},{7,23},{8,24},{9,... | collective-permute-start | bytes 208904 | tf_op jit(solution)/shard_map/ppermute | solution.py:424
  17.9 1.3 collective-permute-start.3
  19.2 0.9 copy-done.3
  20.1 0.9 copy-done.4
  21.0 3.4 %shard_map.119.refs_3_ = f32[256,256]{1,0:T(8,128)S(1)} custom-call(bf16[256,256]{1,0:T(8,128)(2,1)S(1)} %copy-done.4, f32[256,256]{1,0:T(8,128)S(1)} %get-tuple-element.52.gates.gate, f32[256,256]{1,0:T(8,128)S(1)} %get-tuple-element.25.cum.refs_2_, bf16[256,256]{1,0:T(8,128)(2,1)S(1)} %copy-done.3), custom_call_target="tpu_custom_call" | custom-call | tf_op jit(solution)/shard_map/pallas_call | solution.py:480
  24.5 0.9 copy-done.6
  25.4 0.7 copy-done.8
  26.0 2.5 %shard_map.121 = (f32[64,2048]{1,0:T(8,128)S(1)}, f32[64,2048]{1,0:T(8,128)S(1)}, bf16[128,2048]{1,0:T(8,128)(2,1)}) custom-call(s32[4]{0:T(128)S(1)} %pad_add_fusion.place.refs_0_, bf16[256,256]{1,0:T(8,128)(2,1)S(1)} %copy-done.4, f32[256,256]{1,0:T(8,128)S(1)} %get-tuple-element.25.cum.refs_2_, f32[256,256]{1,0:T(8,128)S(1)} %shard_map.119.refs_3_, ...), custom_call_target="tpu_custom_call" | custom-call | tf_op jit(solution)/shard_map/pallas_call | solution.py:483
  28.5 1.3 constant_dynamic-slice_fusion
  29.9 1.6 %collective-permute-start.26 = (bf16[256,2048]{1,0:T(8,128)(2,1)S(1)}, bf16[256,2048]{1,0:T(8,128)(2,1)S(1)}, u32[]{:S(2)}, u32[]{:S(2)}) collective-permute-start(bf16[256,2048]{1,0:T(8,128)(2,1)S(1)} %copy-done), channel_id=1, source_target_pairs={{0,2},{1,3},{2,0},{3,1},{4,6},{5,7},{6,4},{7,5},{8,10},{9,11},{10,... | collective-permute-start | bytes 3145736 | tf_op jit(solution)/shard_map/ppermute | solution.py:424
  31.5 1.5 collective-permute-start.25
  33.0 3.7 %collective-permute-start.15 = (bf16[256,512]{1,0:T(8,128)(2,1)S(1)}, bf16[256,512]{1,0:T(8,128)(2,1)S(1)}, u32[]{:S(2)}, u32[]{:S(2)}) collective-permute-start(bf16[256,512]{1,0:T(8,128)(2,1)S(1)} %get-tuple-element.45), channel_id=1, source_target_pairs={{0,24},{1,25},{2,26},{3,27},{4,28},{5,29},{6,30},{7,31},{8,0},{9,1... | collective-permute-start | bytes 786440 | tf_op jit(solution)/shard_map/ppermute | solution.py:424
  36.7 4.2 %collective-permute-done.13.refs_10_ = bf16[256,512]{1,0:T(8,128)(2,1)S(1)} collective-permute-done((bf16[256,512]{1,0:T(8,128)(2,1)S(1)}, bf16[256,512]{1,0:T(8,128)(2,1)S(1)}, u32[]{:S(2)}, u32[]{:S(2)}) %collective-permute-start.13) | collective-permute-done | bytes 262176 | tf_op jit(solution)/shard_map/ppermute | solution.py:424
  40.9 1.5 collective-permute-start.16
  42.4 3.6 %collective-permute-done.15.refs_12_ = bf16[256,512]{1,0:T(8,128)(2,1)S(1)} collective-permute-done((bf16[256,512]{1,0:T(8,128)(2,1)S(1)}, bf16[256,512]{1,0:T(8,128)(2,1)S(1)}, u32[]{:S(2)}, u32[]{:S(2)}) %collective-permute-start.15) | collective-permute-done | bytes 262176 | tf_op jit(solution)/shard_map/ppermute | solution.py:424
  46.1 2.3 %collective-permute-start.5 = (bf16[64,2048]{1,0:T(8,128)(2,1)S(1)}, bf16[64,2048]{1,0:T(8,128)(2,1)S(1)}, u32[]{:S(2)}, u32[]{:S(2)}) collective-permute-start(bf16[64,2048]{1,0:T(8,128)(2,1)S(1)} %add_convert_fusion), channel_id=1, source_target_pairs={{0,2},{1,3},{2,0},{3,1},{4,6},{5,7},{6,4},{7,5},{8,10},{9,11},{10,... | collective-permute-start | bytes 786440 | tf_op jit(solution)/shard_map/ppermute | solution.py:424
  48.4 8.8 %collective-permute-done.14.refs_11_ = bf16[256,512]{1,0:T(8,128)(2,1)S(1)} collective-permute-done((bf16[256,512]{1,0:T(8,128)(2,1)S(1)}, bf16[256,512]{1,0:T(8,128)(2,1)S(1)}, u32[]{:S(2)}, u32[]{:S(2)}) %collective-permute-start.14) | collective-permute-done | bytes 262176 | tf_op jit(solution)/shard_map/ppermute | solution.py:424
  57.2 0.5 collective-permute-start.19
  57.7 4.7 %collective-permute-done.16.refs_13_ = bf16[256,512]{1,0:T(8,128)(2,1)S(1)} collective-permute-done((bf16[256,512]{1,0:T(8,128)(2,1)S(1)}, bf16[256,512]{1,0:T(8,128)(2,1)S(1)}, u32[]{:S(2)}, u32[]{:S(2)}) %collective-permute-start.16) | collective-permute-done | bytes 262176 | tf_op jit(solution)/shard_map/ppermute | solution.py:424
  62.3 1.5 collective-permute-start.17
  63.8 0.5 collective-permute-start.20
  64.3 0.2 shard_map.122
  64.6 2.6 %collective-permute-done.19.refs_3_ = bf16[256,512]{1,0:T(8,128)(2,1)S(1)} collective-permute-done((bf16[256,512]{1,0:T(8,128)(2,1)S(1)}, bf16[256,512]{1,0:T(8,128)(2,1)S(1)}, u32[]{:S(2)}, u32[]{:S(2)}) %collective-permute-start.19) | collective-permute-done | bytes 262176 | tf_op jit(solution)/shard_map/ppermute | solution.py:424
  67.2 1.5 collective-permute-start.22
  68.7 1.1 collective-permute-done.17.refs_14_
  69.9 0.5 collective-permute-start.23
  70.4 2.6 %collective-permute-done.20.refs_4_ = bf16[256,512]{1,0:T(8,128)(2,1)S(1)} collective-permute-done((bf16[256,512]{1,0:T(8,128)(2,1)S(1)}, bf16[256,512]{1,0:T(8,128)(2,1)S(1)}, u32[]{:S(2)}, u32[]{:S(2)}) %collective-permute-start.20) | collective-permute-done | bytes 262176 | tf_op jit(solution)/shard_map/ppermute | solution.py:424
  73.0 1.4 collective-permute-start.21
  74.4 4.3 %collective-permute-done.22.refs_6_ = bf16[256,512]{1,0:T(8,128)(2,1)S(1)} collective-permute-done((bf16[256,512]{1,0:T(8,128)(2,1)S(1)}, bf16[256,512]{1,0:T(8,128)(2,1)S(1)}, u32[]{:S(2)}, u32[]{:S(2)}) %collective-permute-start.22) | collective-permute-done | bytes 262176 | tf_op jit(solution)/shard_map/ppermute | solution.py:424
  78.6 5.6 %collective-permute-done.23.refs_7_ = bf16[256,512]{1,0:T(8,128)(2,1)S(1)} collective-permute-done((bf16[256,512]{1,0:T(8,128)(2,1)S(1)}, bf16[256,512]{1,0:T(8,128)(2,1)S(1)}, u32[]{:S(2)}, u32[]{:S(2)}) %collective-permute-start.23) | collective-permute-done | bytes 262176 | tf_op jit(solution)/shard_map/ppermute | solution.py:424
  84.2 1.3 collective-permute-start.18
  85.6 1.3 collective-permute-start.7
  86.8 2.6 %collective-permute-start.8 = (bf16[8,64,256]{2,1,0:T(8,128)(2,1)S(1)}, bf16[8,64,256]{2,1,0:T(8,128)(2,1)S(1)}, u32[]{:S(2)}, u32[]{:S(2)}) collective-permute-start(bf16[8,64,256]{2,1,0:T(8,128)(2,1)S(1)} %get-tuple-element.31.refs_1_), channel_id=1, source_target_pairs={{0,24},{1,25},{2,26},{3,27},{4,28},{5,29},{6,30},{7,31},{8,16},{9,... | collective-permute-start | bytes 786440 | tf_op jit(solution)/shard_map/ppermute | solution.py:424
  89.4 5.4 %collective-permute-done.21.refs_5_ = bf16[512,512]{1,0:T(8,128)(2,1)S(1)} collective-permute-done((bf16[512,512]{1,0:T(8,128)(2,1)S(1)}, bf16[512,512]{1,0:T(8,128)(2,1)S(1)}, u32[]{:S(2)}, u32[]{:S(2)}) %collective-permute-start.21) | collective-permute-done | bytes 524320 | tf_op jit(solution)/shard_map/ppermute | solution.py:424
  94.8 1.5 collective-permute-start.24
  96.3 9.1 %collective-permute-done.7.refs_3_ = bf16[8,64,256]{2,1,0:T(8,128)(2,1)S(1)} collective-permute-done((bf16[8,64,256]{2,1,0:T(8,128)(2,1)S(1)}, bf16[8,64,256]{2,1,0:T(8,128)(2,1)S(1)}, u32[]{:S(2)}, u32[]{:S(2)}) %collective-permute-start.7) | collective-permute-done | bytes 262176 | tf_op jit(solution)/shard_map/ppermute | solution.py:424
  105.4 0.5 collective-permute-start.11
  106.0 0.6 collective-permute-start.28
  106.7 0.2 collective-permute-done.10.refs_6_
  106.9 1.5 collective-permute-start.32
  108.4 1.3 collective-permute-start.33
  109.8 0.6 collective-permute-start.27
  110.3 1.8 %shard_map.123 = (bf16[512,2048]{1,0:T(8,128)(2,1)S(1)}, bf16[512,512]{1,0:T(8,128)(2,1)S(1)}) custom-call(s32[4]{0:T(128)S(1)} %pad_add_fusion.place.refs_0_, bf16[8,64,256]{2,1,0:T(8,128)(2,1)S(1)} %get-tuple-element.31.refs_1_, bf16[8,64,256]{2,1,0:T(8,128)(2,1)S(1)} %collective-permute-done.6.refs_2_, ...), custom_call_target="tpu_custom_call" | custom-call | tf_op jit(solution)/shard_map/pallas_call | solution.py:539
  112.1 5.9 %collective-permute-done.27.refs_12_ = bf16[64,1024]{1,0:T(8,128)(2,1)S(1)} collective-permute-done((bf16[64,1024]{1,0:T(8,128)(2,1)S(1)}, bf16[64,1024]{1,0:T(8,128)(2,1)S(1)}, u32[]{:S(2)}, u32[]{:S(2)}) %collective-permute-start.27) | collective-permute-done | bytes 131104 | tf_op jit(solution)/shard_map/ppermute | solution.py:424
  118.1 3.0 %shard_map.124 = (f32[256,1024]{1,0:T(8,128)S(1)}, bf16[256,1024]{1,0:T(8,128)(2,1)S(1)}, bf16[512,1024]{1,0:T(8,128)(2,1)S(1)}) custom-call(s32[4]{0:T(128)S(1)} %pad_add_fusion.place.refs_0_, bf16[512,2048]{1,0:T(8,128)(2,1)S(1)} %get-tuple-element.34.refs_1_, bf16[512,512]{1,0:T(8,128)(2,1)S(1)} %get-tuple-element.35.refs_2_, ...), custom_call_target="tpu_custom_call" | custom-call | tf_op jit(solution)/shard_map/pallas_call | solution.py:556
  121.1 2.1 %collective-permute-done.33.r1_ref = bf16[128,1024]{1,0:T(8,128)(2,1)S(1)} collective-permute-done((bf16[128,1024]{1,0:T(8,128)(2,1)S(1)}, bf16[128,1024]{1,0:T(8,128)(2,1)S(1)}, u32[]{:S(2)}, u32[]{:S(2)}) %collective-permute-start.33) | collective-permute-done | bytes 262176 | tf_op jit(solution)/shard_map/ppermute | solution.py:424
  123.1 1.3 shard_map.126
  124.5 0.5 collective-permute-start.29
  125.0 1.4 collective-permute-done.34.got
  126.5 5.2 %collective-permute-start.35 = (bf16[128,1024]{1,0:T(8,128)(2,1)S(1)}, bf16[128,1024]{1,0:T(8,128)(2,1)S(1)}, u32[]{:S(2)}, u32[]{:S(2)}) collective-permute-start(bf16[128,1024]{1,0:T(8,128)(2,1)S(1)} %get-tuple-element.44), channel_id=1, source_target_pairs={{0,8},{1,9},{2,10},{3,11},{4,12},{5,13},{6,14},{7,15},{8,0},{9,1},... | collective-permute-start | bytes 786440 | tf_op jit(solution)/shard_map/ppermute | solution.py:424
  131.8 0.6 collective-permute-start.30
  132.4 6.4 %collective-permute-done.35 = bf16[128,1024]{1,0:T(8,128)(2,1)S(1)} collective-permute-done((bf16[128,1024]{1,0:T(8,128)(2,1)S(1)}, bf16[128,1024]{1,0:T(8,128)(2,1)S(1)}, u32[]{:S(2)}, u32[]{:S(2)}) %collective-permute-start.35) | collective-permute-done | bytes 262176 | tf_op jit(solution)/shard_map/ppermute | solution.py:424
  138.9 2.2 %collective-permute-start.36 = (bf16[64,1024]{1,0:T(8,128)(2,1)S(1)}, bf16[64,1024]{1,0:T(8,128)(2,1)S(1)}, u32[]{:S(2)}, u32[]{:S(2)}) collective-permute-start(bf16[64,1024]{1,0:T(8,128)(2,1)S(1)} %add_convert_fusion.2), channel_id=1, source_target_pairs={{0,16},{1,17},{2,18},{3,19},{4,20},{5,21},{6,22},{7,23},{8,24},{9,... | collective-permute-start | bytes 393224 | tf_op jit(solution)/shard_map/ppermute | solution.py:424
  141.1 5.6 %collective-permute-done.30 = bf16[128,1024]{1,0:T(8,128)(2,1)S(1)} collective-permute-done((bf16[128,1024]{1,0:T(8,128)(2,1)S(1)}, bf16[128,1024]{1,0:T(8,128)(2,1)S(1)}, u32[]{:S(2)}, u32[]{:S(2)}) %collective-permute-start.30) | collective-permute-done | bytes 262176 | tf_op jit(solution)/shard_map/ppermute | solution.py:424
  146.8 7.6 %collective-permute-done.31 = bf16[64,1024]{1,0:T(8,128)(2,1)S(1)} collective-permute-done((bf16[64,1024]{1,0:T(8,128)(2,1)S(1)}, bf16[64,1024]{1,0:T(8,128)(2,1)S(1)}, u32[]{:S(2)}, u32[]{:S(2)}) %collective-permute-start.31) | collective-permute-done | bytes 131104 | tf_op jit(solution)/shard_map/ppermute | solution.py:424
  154.5 0.1 add_convert_fusion.3
  154.6 0.7 pad_maximum_fusion
  (52 shorter events, 0.9 us)
Async XLA Ops:
  0.0 24.5 %copy-start.1 = (bf16[256,2048]{1,0:T(8,128)(2,1)S(1)}, bf16[256,2048]{1,0:T(8,128)(2,1)}, u32[]{:S(2)}) copy-start(bf16[256,2048]{1,0:T(8,128)(2,1)} %refs_6_.1) | copy-start | bytes 3145732
  1.3 0.9 copy-start.2
  3.4 5.3 %collective-permute-start = (bf16[272,128]{1,0:T(8,128)(2,1)S(1)}, bf16[272,128]{1,0:T(8,128)(2,1)S(1)}, u32[]{:S(2)}, u32[]{:S(2)}) collective-permute-start(bf16[272,128]{1,0:T(8,128)(2,1)S(1)} %get-tuple-element.26.mine), channel_id=1, source_target_pairs={{0,4},{1,5},{2,6},{3,7},{4,0},{5,1},{6,2},{7,3},{8,12},{9,13},{10,... | collective-permute-start | bytes 208904 | tf_op jit(solution)/shard_map/ppermute | solution.py:424
  9.3 15.1 %collective-permute-start.1 = (bf16[272,128]{1,0:T(8,128)(2,1)S(1)}, bf16[272,128]{1,0:T(8,128)(2,1)S(1)}, u32[]{:S(2)}, u32[]{:S(2)}) collective-permute-start(bf16[272,128]{1,0:T(8,128)(2,1)S(1)} %shard_map.120), channel_id=1, source_target_pairs={{0,8},{1,9},{2,10},{3,11},{4,12},{5,13},{6,14},{7,15},{8,16},{9,17... | collective-permute-start | bytes 208904 | tf_op jit(solution)/shard_map/ppermute | solution.py:424
  13.4 11.1 %collective-permute-start.2 = (bf16[272,128]{1,0:T(8,128)(2,1)S(1)}, bf16[272,128]{1,0:T(8,128)(2,1)S(1)}, u32[]{:S(2)}, u32[]{:S(2)}) collective-permute-start(bf16[272,128]{1,0:T(8,128)(2,1)S(1)} %shard_map.120), channel_id=1, source_target_pairs={{0,16},{1,17},{2,18},{3,19},{4,20},{5,21},{6,22},{7,23},{8,24},{9,... | collective-permute-start | bytes 208904 | tf_op jit(solution)/shard_map/ppermute | solution.py:424
  17.9 6.6 %collective-permute-start.3 = (bf16[272,128]{1,0:T(8,128)(2,1)S(1)}, bf16[272,128]{1,0:T(8,128)(2,1)S(1)}, u32[]{:S(2)}, u32[]{:S(2)}) collective-permute-start(bf16[272,128]{1,0:T(8,128)(2,1)S(1)} %shard_map.120), channel_id=1, source_target_pairs={{0,24},{1,25},{2,26},{3,27},{4,28},{5,29},{6,30},{7,31}} | collective-permute-start | bytes 208904 | tf_op jit(solution)/shard_map/ppermute | solution.py:424
  19.2 0.9 copy-start.3
  20.1 0.9 copy-start.4
  24.5 0.9 copy-start.6
  25.4 0.7 copy-start.8
  26.0 3.9 %copy-start = (bf16[256,2048]{1,0:T(8,128)(2,1)S(1)}, bf16[256,2048]{1,0:T(8,128)(2,1)}, u32[]{:S(2)}) copy-start(bf16[256,2048]{1,0:T(8,128)(2,1)} %own_ref.1) | copy-start | bytes 3145732
  28.5 35.8 %copy-start.5 = (bf16[64,2048]{1,0:T(8,128)(2,1)S(1)}, bf16[64,2048]{1,0:T(8,128)(2,1)}, u32[]{:S(2)}) copy-start(bf16[64,2048]{1,0:T(8,128)(2,1)} %residual.1) | copy-start | bytes 786436
  28.5 35.8 %copy-start.7 = (f32[2048]{0:T(1024)S(1)}, f32[2048]{0:T(1024)}, u32[]{:S(2)}) copy-start(f32[2048]{0:T(1024)} %param.21) | copy-start | bytes 24580
  28.5 12.4 %collective-permute-start.4 = (bf16[128,2048]{1,0:T(8,128)(2,1)}, bf16[128,2048]{1,0:T(8,128)(2,1)S(1)}, u32[]{:S(2)}, u32[]{:S(2)}) collective-permute-start(bf16[128,2048]{1,0:T(8,128)(2,1)} %get-tuple-element.28), channel_id=1, source_target_pairs={{0,1},{1,0},{2,3},{3,2},{4,5},{5,4},{6,7},{7,6},{8,9},{9,8},{10,11... | collective-permute-start | bytes 1572872 | tf_op jit(solution)/shard_map/ppermute | solution.py:424
  29.8 11.1 %collective-permute-start.13 = (bf16[256,512]{1,0:T(8,128)(2,1)S(1)}, bf16[256,512]{1,0:T(8,128)(2,1)S(1)}, u32[]{:S(2)}, u32[]{:S(2)}) collective-permute-start(bf16[256,512]{1,0:T(8,128)(2,1)S(1)} %get-tuple-element.46), channel_id=1, source_target_pairs={{0,8},{1,9},{2,10},{3,11},{4,12},{5,13},{6,14},{7,15},{8,16},{9,17... | collective-permute-start | bytes 786440 | tf_op jit(solution)/shard_map/ppermute | solution.py:424
  29.9 55.7 %collective-permute-start.26 = (bf16[256,2048]{1,0:T(8,128)(2,1)S(1)}, bf16[256,2048]{1,0:T(8,128)(2,1)S(1)}, u32[]{:S(2)}, u32[]{:S(2)}) collective-permute-start(bf16[256,2048]{1,0:T(8,128)(2,1)S(1)} %copy-done), channel_id=1, source_target_pairs={{0,2},{1,3},{2,0},{3,1},{4,6},{5,7},{6,4},{7,5},{8,10},{9,11},{10,... | collective-permute-start | bytes 3145736 | tf_op jit(solution)/shard_map/ppermute | solution.py:424
  31.5 55.4 %collective-permute-start.25 = (bf16[256,2048]{1,0:T(8,128)(2,1)S(1)}, bf16[256,2048]{1,0:T(8,128)(2,1)S(1)}, u32[]{:S(2)}, u32[]{:S(2)}) collective-permute-start(bf16[256,2048]{1,0:T(8,128)(2,1)S(1)} %copy-done), channel_id=1, source_target_pairs={{0,4},{1,5},{2,6},{3,7},{4,0},{5,1},{6,2},{7,3},{8,12},{9,13},{10,... | collective-permute-start | bytes 3145736 | tf_op jit(solution)/shard_map/ppermute | solution.py:424
  33.0 13.1 %collective-permute-start.15 = (bf16[256,512]{1,0:T(8,128)(2,1)S(1)}, bf16[256,512]{1,0:T(8,128)(2,1)S(1)}, u32[]{:S(2)}, u32[]{:S(2)}) collective-permute-start(bf16[256,512]{1,0:T(8,128)(2,1)S(1)} %get-tuple-element.45), channel_id=1, source_target_pairs={{0,24},{1,25},{2,26},{3,27},{4,28},{5,29},{6,30},{7,31},{8,0},{9,1... | collective-permute-start | bytes 786440 | tf_op jit(solution)/shard_map/ppermute | solution.py:424
  40.9 16.2 %collective-permute-start.14 = (bf16[256,512]{1,0:T(8,128)(2,1)S(1)}, bf16[256,512]{1,0:T(8,128)(2,1)S(1)}, u32[]{:S(2)}, u32[]{:S(2)}) collective-permute-start(bf16[256,512]{1,0:T(8,128)(2,1)S(1)} %get-tuple-element.48), channel_id=1, source_target_pairs={{0,16},{1,17},{2,18},{3,19},{4,20},{5,21},{6,22},{7,23},{8,24},{9,... | collective-permute-start | bytes 786440 | tf_op jit(solution)/shard_map/ppermute | solution.py:424
  40.9 21.4 %collective-permute-start.16 = (bf16[256,512]{1,0:T(8,128)(2,1)S(1)}, bf16[256,512]{1,0:T(8,128)(2,1)S(1)}, u32[]{:S(2)}, u32[]{:S(2)}) collective-permute-start(bf16[256,512]{1,0:T(8,128)(2,1)S(1)} %get-tuple-element.47.refs_9_), channel_id=1, source_target_pairs={{0,4},{1,5},{2,6},{3,7},{4,0},{5,1},{6,2},{7,3},{8,12},{9,13},{10,... | collective-permute-start | bytes 786440 | tf_op jit(solution)/shard_map/ppermute | solution.py:424
  46.1 17.8 %collective-permute-start.5 = (bf16[64,2048]{1,0:T(8,128)(2,1)S(1)}, bf16[64,2048]{1,0:T(8,128)(2,1)S(1)}, u32[]{:S(2)}, u32[]{:S(2)}) collective-permute-start(bf16[64,2048]{1,0:T(8,128)(2,1)S(1)} %add_convert_fusion), channel_id=1, source_target_pairs={{0,2},{1,3},{2,0},{3,1},{4,6},{5,7},{6,4},{7,5},{8,10},{9,11},{10,... | collective-permute-start | bytes 786440 | tf_op jit(solution)/shard_map/ppermute | solution.py:424
  57.2 10.1 %collective-permute-start.19 = (bf16[256,512]{1,0:T(8,128)(2,1)S(1)}, bf16[256,512]{1,0:T(8,128)(2,1)S(1)}, u32[]{:S(2)}, u32[]{:S(2)}) collective-permute-start(bf16[256,512]{1,0:T(8,128)(2,1)S(1)} %get-tuple-element.47.refs_9_), channel_id=1, source_target_pairs={{0,2},{1,3},{2,0},{3,1},{4,6},{5,7},{6,4},{7,5},{8,10},{9,11},{10,... | collective-permute-start | bytes 786440 | tf_op jit(solution)/shard_map/ppermute | solution.py:424
  62.3 7.5 %collective-permute-start.17 = (bf16[256,512]{1,0:T(8,128)(2,1)S(1)}, bf16[256,512]{1,0:T(8,128)(2,1)S(1)}, u32[]{:S(2)}, u32[]{:S(2)}) collective-permute-start(bf16[256,512]{1,0:T(8,128)(2,1)S(1)} %collective-permute-done.14.refs_11_), channel_id=1, source_target_pairs={{0,4},{1,5},{2,6},{3,7},{4,0},{5,1},{6,2},{7,3},{8,12},{9,13},{10,... | collective-permute-start | bytes 786440 | tf_op jit(solution)/shard_map/ppermute | solution.py:424
  63.8 9.2 %collective-permute-start.20 = (bf16[256,512]{1,0:T(8,128)(2,1)S(1)}, bf16[256,512]{1,0:T(8,128)(2,1)S(1)}, u32[]{:S(2)}, u32[]{:S(2)}) collective-permute-start(bf16[256,512]{1,0:T(8,128)(2,1)S(1)} %collective-permute-done.14.refs_11_), channel_id=1, source_target_pairs={{0,2},{1,3},{2,0},{3,1},{4,6},{5,7},{6,4},{7,5},{8,10},{9,11},{10,... | collective-permute-start | bytes 786440 | tf_op jit(solution)/shard_map/ppermute | solution.py:424
  67.2 11.4 %collective-permute-start.22 = (bf16[256,512]{1,0:T(8,128)(2,1)S(1)}, bf16[256,512]{1,0:T(8,128)(2,1)S(1)}, u32[]{:S(2)}, u32[]{:S(2)}) collective-permute-start(bf16[256,512]{1,0:T(8,128)(2,1)S(1)} %collective-permute-done.16.refs_13_), channel_id=1, source_target_pairs={{0,2},{1,3},{2,0},{3,1},{4,6},{5,7},{6,4},{7,5},{8,10},{9,11},{10,... | collective-permute-start | bytes 786440 | tf_op jit(solution)/shard_map/ppermute | solution.py:424
  69.9 14.4 %collective-permute-start.23 = (bf16[256,512]{1,0:T(8,128)(2,1)S(1)}, bf16[256,512]{1,0:T(8,128)(2,1)S(1)}, u32[]{:S(2)}, u32[]{:S(2)}) collective-permute-start(bf16[256,512]{1,0:T(8,128)(2,1)S(1)} %collective-permute-done.17.refs_14_), channel_id=1, source_target_pairs={{0,2},{1,3},{2,0},{3,1},{4,6},{5,7},{6,4},{7,5},{8,10},{9,11},{10,... | collective-permute-start | bytes 786440 | tf_op jit(solution)/shard_map/ppermute | solution.py:424
  73.0 21.8 %collective-permute-start.21 = (bf16[512,512]{1,0:T(8,128)(2,1)S(1)}, bf16[512,512]{1,0:T(8,128)(2,1)S(1)}, u32[]{:S(2)}, u32[]{:S(2)}) collective-permute-start(bf16[512,512]{1,0:T(8,128)(2,1)S(1)} %constant_dynamic-update-slice_fusion), channel_id=1, source_target_pairs={{0,2},{1,3},{2,0},{3,1},{4,6},{5,7},{6,4},{7,5},{8,10},{9,11},{10,... | collective-permute-start | bytes 1572872 | tf_op jit(solution)/shard_map/ppermute | solution.py:424
  78.6 10.8 %collective-permute-start.6 = (bf16[8,64,256]{2,1,0:T(8,128)(2,1)S(1)}, bf16[8,64,256]{2,1,0:T(8,128)(2,1)S(1)}, u32[]{:S(2)}, u32[]{:S(2)}) collective-permute-start(bf16[8,64,256]{2,1,0:T(8,128)(2,1)S(1)} %get-tuple-element.31.refs_1_), channel_id=1, source_target_pairs={{0,8},{1,9},{2,10},{3,11},{4,12},{5,13},{6,14},{7,15},{8,0},{9,1},... | collective-permute-start | bytes 786440 | tf_op jit(solution)/shard_map/ppermute | solution.py:424
  84.2 21.8 %collective-permute-start.18 = (bf16[512,512]{1,0:T(8,128)(2,1)S(1)}, bf16[512,512]{1,0:T(8,128)(2,1)S(1)}, u32[]{:S(2)}, u32[]{:S(2)}) collective-permute-start(bf16[512,512]{1,0:T(8,128)(2,1)S(1)} %constant_dynamic-update-slice_fusion), channel_id=1, source_target_pairs={{0,4},{1,5},{2,6},{3,7},{4,0},{5,1},{6,2},{7,3},{8,12},{9,13},{10,... | collective-permute-start | bytes 1572872 | tf_op jit(solution)/shard_map/ppermute | solution.py:424
  85.6 19.8 %collective-permute-start.7 = (bf16[8,64,256]{2,1,0:T(8,128)(2,1)S(1)}, bf16[8,64,256]{2,1,0:T(8,128)(2,1)S(1)}, u32[]{:S(2)}, u32[]{:S(2)}) collective-permute-start(bf16[8,64,256]{2,1,0:T(8,128)(2,1)S(1)} %get-tuple-element.31.refs_1_), channel_id=1, source_target_pairs={{0,16},{1,17},{2,18},{3,19},{4,20},{5,21},{6,22},{7,23},{8,24},{9,... | collective-permute-start | bytes 786440 | tf_op jit(solution)/shard_map/ppermute | solution.py:424
  86.8 18.5 %collective-permute-start.8 = (bf16[8,64,256]{2,1,0:T(8,128)(2,1)S(1)}, bf16[8,64,256]{2,1,0:T(8,128)(2,1)S(1)}, u32[]{:S(2)}, u32[]{:S(2)}) collective-permute-start(bf16[8,64,256]{2,1,0:T(8,128)(2,1)S(1)} %get-tuple-element.31.refs_1_), channel_id=1, source_target_pairs={{0,24},{1,25},{2,26},{3,27},{4,28},{5,29},{6,30},{7,31},{8,16},{9,... | collective-permute-start | bytes 786440 | tf_op jit(solution)/shard_map/ppermute | solution.py:424
  89.4 16.5 %collective-permute-start.9 = (bf16[8,64,256]{2,1,0:T(8,128)(2,1)S(1)}, bf16[8,64,256]{2,1,0:T(8,128)(2,1)S(1)}, u32[]{:S(2)}, u32[]{:S(2)}) collective-permute-start(bf16[8,64,256]{2,1,0:T(8,128)(2,1)S(1)} %get-tuple-element.31.refs_1_), channel_id=1, source_target_pairs={{0,1},{1,0},{2,3},{3,2},{4,5},{5,4},{6,7},{7,6},{8,9},{9,8},{10,11... | collective-permute-start | bytes 786440 | tf_op jit(solution)/shard_map/ppermute | solution.py:424
  94.8 23.3 %collective-permute-start.24 = (bf16[512,512]{1,0:T(8,128)(2,1)S(1)}, bf16[512,512]{1,0:T(8,128)(2,1)S(1)}, u32[]{:S(2)}, u32[]{:S(2)}) collective-permute-start(bf16[512,512]{1,0:T(8,128)(2,1)S(1)} %collective-permute-done.21.refs_5_), channel_id=1, source_target_pairs={{0,4},{1,5},{2,6},{3,7},{4,0},{5,1},{6,2},{7,3},{8,12},{9,13},{10,... | collective-permute-start | bytes 1572872 | tf_op jit(solution)/shard_map/ppermute | solution.py:424
  105.4 1.5 collective-permute-start.10
  105.4 3.1 %collective-permute-start.11 = (bf16[8,64,256]{2,1,0:T(8,128)(2,1)S(1)}, bf16[8,64,256]{2,1,0:T(8,128)(2,1)S(1)}, u32[]{:S(2)}, u32[]{:S(2)}) collective-permute-start(bf16[8,64,256]{2,1,0:T(8,128)(2,1)S(1)} %collective-permute-done.7.refs_3_), channel_id=1, source_target_pairs={{0,1},{1,0},{2,3},{3,2},{4,5},{5,4},{6,7},{7,6},{8,9},{9,8},{10,11... | collective-permute-start | bytes 786440 | tf_op jit(solution)/shard_map/ppermute | solution.py:424
  105.9 3.8 %collective-permute-start.12 = (bf16[8,64,256]{2,1,0:T(8,128)(2,1)S(1)}, bf16[8,64,256]{2,1,0:T(8,128)(2,1)S(1)}, u32[]{:S(2)}, u32[]{:S(2)}) collective-permute-start(bf16[8,64,256]{2,1,0:T(8,128)(2,1)S(1)} %collective-permute-done.8.refs_4_), channel_id=1, source_target_pairs={{0,1},{1,0},{2,3},{3,2},{4,5},{5,4},{6,7},{7,6},{8,9},{9,8},{10,11... | collective-permute-start | bytes 786440 | tf_op jit(solution)/shard_map/ppermute | solution.py:424
  106.0 12.1 %collective-permute-start.28 = (bf16[192,1024]{1,0:T(8,128)(2,1)S(1)}, bf16[192,1024]{1,0:T(8,128)(2,1)S(1)}, u32[]{:S(2)}, u32[]{:S(2)}) collective-permute-start(bf16[192,1024]{1,0:T(8,128)(2,1)S(1)} %slice.62), channel_id=1, source_target_pairs={{0,4},{1,5},{2,6},{3,7},{4,0},{5,1},{6,2},{7,3},{8,12},{9,13},{10,... | collective-permute-start | bytes 1179656 | tf_op jit(solution)/shard_map/ppermute | solution.py:424
  106.9 14.2 %collective-permute-start.32 = (bf16[128,1024]{1,0:T(8,128)(2,1)S(1)}, bf16[128,1024]{1,0:T(8,128)(2,1)S(1)}, u32[]{:S(2)}, u32[]{:S(2)}) collective-permute-start(bf16[128,1024]{1,0:T(8,128)(2,1)S(1)} %slice.65), channel_id=1, source_target_pairs={{0,2},{1,3},{2,0},{3,1},{4,6},{5,7},{6,4},{7,5},{8,10},{9,11},{10,... | collective-permute-start | bytes 786440 | tf_op jit(solution)/shard_map/ppermute | solution.py:424
  108.4 14.7 %collective-permute-start.33 = (bf16[128,1024]{1,0:T(8,128)(2,1)S(1)}, bf16[128,1024]{1,0:T(8,128)(2,1)S(1)}, u32[]{:S(2)}, u32[]{:S(2)}) collective-permute-start(bf16[128,1024]{1,0:T(8,128)(2,1)S(1)} %slice.66), channel_id=1, source_target_pairs={{0,4},{1,5},{2,6},{3,7},{4,0},{5,1},{6,2},{7,3},{8,12},{9,13},{10,... | collective-permute-start | bytes 786440 | tf_op jit(solution)/shard_map/ppermute | solution.py:424
  109.8 8.3 %collective-permute-start.27 = (bf16[64,1024]{1,0:T(8,128)(2,1)S(1)}, bf16[64,1024]{1,0:T(8,128)(2,1)S(1)}, u32[]{:S(2)}, u32[]{:S(2)}) collective-permute-start(bf16[64,1024]{1,0:T(8,128)(2,1)S(1)} %slice.61), channel_id=1, source_target_pairs={{0,2},{1,3},{2,0},{3,1},{4,6},{5,7},{6,4},{7,5},{8,10},{9,11},{10,... | collective-permute-start | bytes 393224 | tf_op jit(solution)/shard_map/ppermute | solution.py:424
  124.4 2.0 %collective-permute-start.34 = (bf16[256,1024]{1,0:T(8,128)(2,1)S(1)}, bf16[256,1024]{1,0:T(8,128)(2,1)S(1)}, u32[]{:S(2)}, u32[]{:S(2)}) collective-permute-start(bf16[256,1024]{1,0:T(8,128)(2,1)S(1)} %get-tuple-element.42), channel_id=1, source_target_pairs={{0,1},{1,0},{2,3},{3,2},{4,5},{5,4},{6,7},{7,6},{8,9},{9,8},{10,11... | collective-permute-start | bytes 1572872 | tf_op jit(solution)/shard_map/ppermute | solution.py:424
  124.5 7.2 %collective-permute-start.29 = (bf16[256,1024]{1,0:T(8,128)(2,1)S(1)}, bf16[256,1024]{1,0:T(8,128)(2,1)S(1)}, u32[]{:S(2)}, u32[]{:S(2)}) collective-permute-start(bf16[256,1024]{1,0:T(8,128)(2,1)S(1)} %get-tuple-element.37), channel_id=1, source_target_pairs={{0,1},{1,0},{2,3},{3,2},{4,5},{5,4},{6,7},{7,6},{8,9},{9,8},{10,11... | collective-permute-start | bytes 1572872 | tf_op jit(solution)/shard_map/ppermute | solution.py:424
  126.5 12.3 %collective-permute-start.35 = (bf16[128,1024]{1,0:T(8,128)(2,1)S(1)}, bf16[128,1024]{1,0:T(8,128)(2,1)S(1)}, u32[]{:S(2)}, u32[]{:S(2)}) collective-permute-start(bf16[128,1024]{1,0:T(8,128)(2,1)S(1)} %get-tuple-element.44), channel_id=1, source_target_pairs={{0,8},{1,9},{2,10},{3,11},{4,12},{5,13},{6,14},{7,15},{8,0},{9,1},... | collective-permute-start | bytes 786440 | tf_op jit(solution)/shard_map/ppermute | solution.py:424
  131.8 14.9 %collective-permute-start.30 = (bf16[128,1024]{1,0:T(8,128)(2,1)S(1)}, bf16[128,1024]{1,0:T(8,128)(2,1)S(1)}, u32[]{:S(2)}, u32[]{:S(2)}) collective-permute-start(bf16[128,1024]{1,0:T(8,128)(2,1)S(1)} %get-tuple-element.39), channel_id=1, source_target_pairs={{0,8},{1,9},{2,10},{3,11},{4,12},{5,13},{6,14},{7,15},{8,0},{9,1},... | collective-permute-start | bytes 786440 | tf_op jit(solution)/shard_map/ppermute | solution.py:424
  138.9 8.0 %collective-permute-start.36 = (bf16[64,1024]{1,0:T(8,128)(2,1)S(1)}, bf16[64,1024]{1,0:T(8,128)(2,1)S(1)}, u32[]{:S(2)}, u32[]{:S(2)}) collective-permute-start(bf16[64,1024]{1,0:T(8,128)(2,1)S(1)} %add_convert_fusion.2), channel_id=1, source_target_pairs={{0,16},{1,17},{2,18},{3,19},{4,20},{5,21},{6,22},{7,23},{8,24},{9,... | collective-permute-start | bytes 393224 | tf_op jit(solution)/shard_map/ppermute | solution.py:424
  146.7 7.7 %collective-permute-start.31 = (bf16[64,1024]{1,0:T(8,128)(2,1)S(1)}, bf16[64,1024]{1,0:T(8,128)(2,1)S(1)}, u32[]{:S(2)}, u32[]{:S(2)}) collective-permute-start(bf16[64,1024]{1,0:T(8,128)(2,1)S(1)} %add_convert_fusion.4), channel_id=1, source_target_pairs={{0,16},{1,17},{2,18},{3,19},{4,20},{5,21},{6,22},{7,23},{8,24},{9,... | collective-permute-start | bytes 393224 | tf_op jit(solution)/shard_map/ppermute | solution.py:424

commit v6 on v5

--- a/solution.py
+++ b/solution.py
@@ -518,7 +518,12 @@
         for members in [mine[0], mine[2], jnp.concatenate(late, axis=0)]:
             up_x.append(send(members, b=1))
             up_y.append(send(members, y=1))
-        up_xy = [send(up_x[0], y=1), send(up_x[1], y=1), send(up_y[2], b=1)]
+        up_xy = [
+            send(up_y[0], b=1),
+            send(up_x[1], y=1),
+            send(up_y[2][:up_rows], b=1),
+            send(up_x[2][up_rows:], y=1),
+        ]
 
         line = [normed] + [send(normed, flip=d) for d in range(1, n_a)]
         toks = line + [send(u, c=1) for u in line]
@@ -549,9 +554,9 @@
         )(place, *toks, *mine, *up_x)
 
         def second_half(*refs):
-            ups = grouped(refs[3:6]) + grouped(refs[6:9])
-            pieces = [[(r, 0)] for r in refs[9:12]] + [[(refs[12], 0), (refs[13], 0)]]
-            lower_body(cols, *refs[:3], ups, pieces, *refs[14:])
+            ups = grouped(refs[3:6]) + [(refs[6 + k], 0) for k in (0, 2, 1, 3)]
+            pieces = [[(r, 0)] for r in refs[10:13]] + [[(refs[13], 0), (refs[14], 0)]]
+            lower_body(cols, *refs[:3], ups, pieces, *refs[15:])
 
         keep0, away0, hidden = kernel_call(
             second_half,
@@ -562,7 +567,7 @@
                 pltpu.VMEM((units, part), BF16),
             ],
             smem=1,
-            n_in=14,
+            n_in=15,
             mib=30,
         )(place, rows_x, early, *up_y, *up_xy, *whole, *down_xy[0])
         got0 = send(away0, c=1)

time: 156 us -> 155 us (level)
  waiting for transfers between devices: 83.6 us -> 78.9 us
  starting transfers between devices: 49.3 us -> 53.6 us
    ppermute x37 -> x38, waiting for transfers between devices: 83.6 us -> 78.9 us  [send(): return lax.ppermute(x, AXES, pairs)]
    ppermute x37 -> x38, starting transfers between devices: 49.3 us -> 53.6 us  [send(): return lax.ppermute(x, AXES, pairs)]
  transfers between devices with their start and end apart: 37 -> 38, of which waited for: 19 -> 19; matrix products, arithmetic and copies ran while one was open for 1% -> 1% of each run, Pallas kernels for 6% -> 6%
where the time goes in v6:
time: 155 us
  waiting for transfers between devices  78.9 us (51%)
  starting transfers between devices  53.6 us (35%)
  Pallas kernels  14.2 us (9%)
  local copies, waits for them, and re-layouts  5.73 us (4%)
  other arithmetic  2.32 us (1%)
    ppermute x38, waiting for transfers between devices, send(): return lax.ppermute(x, AXES, pairs)  78.9 us
    ppermute x38, starting transfers between devices, send(): return lax.ppermute(x, AXES, pairs)  53.6 us
    unnamed x19, local copies, waits for them, and re-layouts  4.29 us
    pallas_call x1, Pallas kernels, on_device(): kernel_call(local_body, jax.ShapeDtypeStruct((rows, width), F32), n_in=4)  3.44 us
  transfers between devices with their start and end apart: 38, of which 19 were waited for; matrix products, arithmetic and copies ran while one was open for 1% of the time, Pallas kernels for 6%

profile of v6, /device:TPU:0, one launch (start us, length us, event | category | flops | bytes accessed | tf_op | source)
XLA Modules:
  0.0 154.9 jit_solution(13548288201442636144)
XLA Ops:
  0.0 1.3 log-plus-one_add_fusion
  1.3 0.9 copy-done.2
  2.2 1.2 shard_map.118
  3.4 3.0 %collective-permute-start = (bf16[272,128]{1,0:T(8,128)(2,1)S(1)}, bf16[272,128]{1,0:T(8,128)(2,1)S(1)}, u32[]{:S(2)}, u32[]{:S(2)}) collective-permute-start(bf16[272,128]{1,0:T(8,128)(2,1)S(1)} %get-tuple-element.26.mine), channel_id=1, source_target_pairs={{0,4},{1,5},{2,6},{3,7},{4,0},{5,1},{6,2},{7,3},{8,12},{9,13},{10,... | collective-permute-start | bytes 208904 | tf_op jit(solution)/shard_map/ppermute | solution.py:424
  6.5 2.2 %collective-permute-done.theirs.refs_7_ = bf16[272,128]{1,0:T(8,128)(2,1)S(1)} collective-permute-done((bf16[272,128]{1,0:T(8,128)(2,1)S(1)}, bf16[272,128]{1,0:T(8,128)(2,1)S(1)}, u32[]{:S(2)}, u32[]{:S(2)}) %collective-permute-start) | collective-permute-done | bytes 69664 | tf_op jit(solution)/shard_map/ppermute | solution.py:424
  8.7 0.7 shard_map.120
  9.3 4.0 %collective-permute-start.1 = (bf16[272,128]{1,0:T(8,128)(2,1)S(1)}, bf16[272,128]{1,0:T(8,128)(2,1)S(1)}, u32[]{:S(2)}, u32[]{:S(2)}) collective-permute-start(bf16[272,128]{1,0:T(8,128)(2,1)S(1)} %shard_map.120), channel_id=1, source_target_pairs={{0,8},{1,9},{2,10},{3,11},{4,12},{5,13},{6,14},{7,15},{8,16},{9,17... | collective-permute-start | bytes 208904 | tf_op jit(solution)/shard_map/ppermute | solution.py:424
  13.4 4.5 %collective-permute-start.2 = (bf16[272,128]{1,0:T(8,128)(2,1)S(1)}, bf16[272,128]{1,0:T(8,128)(2,1)S(1)}, u32[]{:S(2)}, u32[]{:S(2)}) collective-permute-start(bf16[272,128]{1,0:T(8,128)(2,1)S(1)} %shard_map.120), channel_id=1, source_target_pairs={{0,16},{1,17},{2,18},{3,19},{4,20},{5,21},{6,22},{7,23},{8,24},{9,... | collective-permute-start | bytes 208904 | tf_op jit(solution)/shard_map/ppermute | solution.py:424
  17.9 1.3 collective-permute-start.3
  19.2 0.9 copy-done.3
  20.1 0.9 copy-done.4
  21.0 3.4 %shard_map.119.refs_3_ = f32[256,256]{1,0:T(8,128)S(1)} custom-call(bf16[256,256]{1,0:T(8,128)(2,1)S(1)} %copy-done.4, f32[256,256]{1,0:T(8,128)S(1)} %get-tuple-element.52.gates.gate, f32[256,256]{1,0:T(8,128)S(1)} %get-tuple-element.25.cum.refs_2_, bf16[256,256]{1,0:T(8,128)(2,1)S(1)} %copy-done.3), custom_call_target="tpu_custom_call" | custom-call | tf_op jit(solution)/shard_map/pallas_call | solution.py:480
  24.5 0.9 copy-done.6
  25.4 0.7 copy-done.8
  26.0 2.5 %shard_map.121 = (f32[64,2048]{1,0:T(8,128)S(1)}, f32[64,2048]{1,0:T(8,128)S(1)}, bf16[128,2048]{1,0:T(8,128)(2,1)}) custom-call(s32[4]{0:T(128)S(1)} %pad_add_fusion.place.refs_0_, bf16[256,256]{1,0:T(8,128)(2,1)S(1)} %copy-done.4, f32[256,256]{1,0:T(8,128)S(1)} %get-tuple-element.25.cum.refs_2_, f32[256,256]{1,0:T(8,128)S(1)} %shard_map.119.refs_3_, ...), custom_call_target="tpu_custom_call" | custom-call | tf_op jit(solution)/shard_map/pallas_call | solution.py:483
  28.5 1.3 constant_dynamic-slice_fusion
  29.9 1.6 %collective-permute-start.27 = (bf16[256,2048]{1,0:T(8,128)(2,1)S(1)}, bf16[256,2048]{1,0:T(8,128)(2,1)S(1)}, u32[]{:S(2)}, u32[]{:S(2)}) collective-permute-start(bf16[256,2048]{1,0:T(8,128)(2,1)S(1)} %copy-done), channel_id=1, source_target_pairs={{0,2},{1,3},{2,0},{3,1},{4,6},{5,7},{6,4},{7,5},{8,10},{9,11},{10,... | collective-permute-start | bytes 3145736 | tf_op jit(solution)/shard_map/ppermute | solution.py:424
  31.5 1.5 collective-permute-start.26
  33.0 3.7 %collective-permute-start.15 = (bf16[256,512]{1,0:T(8,128)(2,1)S(1)}, bf16[256,512]{1,0:T(8,128)(2,1)S(1)}, u32[]{:S(2)}, u32[]{:S(2)}) collective-permute-start(bf16[256,512]{1,0:T(8,128)(2,1)S(1)} %get-tuple-element.45), channel_id=1, source_target_pairs={{0,24},{1,25},{2,26},{3,27},{4,28},{5,29},{6,30},{7,31},{8,0},{9,1... | collective-permute-start | bytes 786440 | tf_op jit(solution)/shard_map/ppermute | solution.py:424
  36.7 4.2 %collective-permute-done.13.refs_10_ = bf16[256,512]{1,0:T(8,128)(2,1)S(1)} collective-permute-done((bf16[256,512]{1,0:T(8,128)(2,1)S(1)}, bf16[256,512]{1,0:T(8,128)(2,1)S(1)}, u32[]{:S(2)}, u32[]{:S(2)}) %collective-permute-start.13) | collective-permute-done | bytes 262176 | tf_op jit(solution)/shard_map/ppermute | solution.py:424
  40.9 1.5 collective-permute-start.16
  42.4 3.6 %collective-permute-done.15.refs_12_ = bf16[256,512]{1,0:T(8,128)(2,1)S(1)} collective-permute-done((bf16[256,512]{1,0:T(8,128)(2,1)S(1)}, bf16[256,512]{1,0:T(8,128)(2,1)S(1)}, u32[]{:S(2)}, u32[]{:S(2)}) %collective-permute-start.15) | collective-permute-done | bytes 262176 | tf_op jit(solution)/shard_map/ppermute | solution.py:424
  46.0 2.3 %collective-permute-start.5 = (bf16[64,2048]{1,0:T(8,128)(2,1)S(1)}, bf16[64,2048]{1,0:T(8,128)(2,1)S(1)}, u32[]{:S(2)}, u32[]{:S(2)}) collective-permute-start(bf16[64,2048]{1,0:T(8,128)(2,1)S(1)} %add_convert_fusion), channel_id=1, source_target_pairs={{0,2},{1,3},{2,0},{3,1},{4,6},{5,7},{6,4},{7,5},{8,10},{9,11},{10,... | collective-permute-start | bytes 786440 | tf_op jit(solution)/shard_map/ppermute | solution.py:424
  48.4 8.8 %collective-permute-done.14.refs_11_ = bf16[256,512]{1,0:T(8,128)(2,1)S(1)} collective-permute-done((bf16[256,512]{1,0:T(8,128)(2,1)S(1)}, bf16[256,512]{1,0:T(8,128)(2,1)S(1)}, u32[]{:S(2)}, u32[]{:S(2)}) %collective-permute-start.14) | collective-permute-done | bytes 262176 | tf_op jit(solution)/shard_map/ppermute | solution.py:424
  57.2 0.5 collective-permute-start.19
  57.7 4.7 %collective-permute-done.16.refs_13_ = bf16[256,512]{1,0:T(8,128)(2,1)S(1)} collective-permute-done((bf16[256,512]{1,0:T(8,128)(2,1)S(1)}, bf16[256,512]{1,0:T(8,128)(2,1)S(1)}, u32[]{:S(2)}, u32[]{:S(2)}) %collective-permute-start.16) | collective-permute-done | bytes 262176 | tf_op jit(solution)/shard_map/ppermute | solution.py:424
  62.3 1.5 collective-permute-start.17
  63.8 0.5 collective-permute-start.20
  64.3 0.2 shard_map.122
  64.6 2.6 %collective-permute-done.19.refs_3_ = bf16[256,512]{1,0:T(8,128)(2,1)S(1)} collective-permute-done((bf16[256,512]{1,0:T(8,128)(2,1)S(1)}, bf16[256,512]{1,0:T(8,128)(2,1)S(1)}, u32[]{:S(2)}, u32[]{:S(2)}) %collective-permute-start.19) | collective-permute-done | bytes 262176 | tf_op jit(solution)/shard_map/ppermute | solution.py:424
  67.2 1.5 collective-permute-start.22
  68.7 2.1 %collective-permute-done.17.refs_14_ = bf16[256,512]{1,0:T(8,128)(2,1)S(1)} collective-permute-done((bf16[256,512]{1,0:T(8,128)(2,1)S(1)}, bf16[256,512]{1,0:T(8,128)(2,1)S(1)}, u32[]{:S(2)}, u32[]{:S(2)}) %collective-permute-start.17) | collective-permute-done | bytes 262176 | tf_op jit(solution)/shard_map/ppermute | solution.py:424
  70.8 2.2 %collective-permute-done.20.refs_4_ = bf16[256,512]{1,0:T(8,128)(2,1)S(1)} collective-permute-done((bf16[256,512]{1,0:T(8,128)(2,1)S(1)}, bf16[256,512]{1,0:T(8,128)(2,1)S(1)}, u32[]{:S(2)}, u32[]{:S(2)}) %collective-permute-start.20) | collective-permute-done | bytes 262176 | tf_op jit(solution)/shard_map/ppermute | solution.py:424
  73.0 1.3 collective-permute-start.18
  74.3 1.5 collective-permute-start.21
  75.9 0.6 collective-permute-done.22.refs_6_
  76.4 3.6 %collective-permute-done.23.refs_7_ = bf16[256,512]{1,0:T(8,128)(2,1)S(1)} collective-permute-done((bf16[256,512]{1,0:T(8,128)(2,1)S(1)}, bf16[256,512]{1,0:T(8,128)(2,1)S(1)}, u32[]{:S(2)}, u32[]{:S(2)}) %collective-permute-start.23) | collective-permute-done | bytes 262176 | tf_op jit(solution)/shard_map/ppermute | solution.py:424
  80.0 3.7 %collective-permute-start.7 = (bf16[8,64,256]{2,1,0:T(8,128)(2,1)S(1)}, bf16[8,64,256]{2,1,0:T(8,128)(2,1)S(1)}, u32[]{:S(2)}, u32[]{:S(2)}) collective-permute-start(bf16[8,64,256]{2,1,0:T(8,128)(2,1)S(1)} %get-tuple-element.31.refs_1_), channel_id=1, source_target_pairs={{0,16},{1,17},{2,18},{3,19},{4,20},{5,21},{6,22},{7,23},{8,24},{9,... | collective-permute-start | bytes 786440 | tf_op jit(solution)/shard_map/ppermute | solution.py:424
  83.7 8.2 %collective-permute-done.28.refs_13_ = bf16[64,1024]{1,0:T(8,128)(2,1)S(1)} collective-permute-done((bf16[64,1024]{1,0:T(8,128)(2,1)S(1)}, bf16[64,1024]{1,0:T(8,128)(2,1)S(1)}, u32[]{:S(2)}, u32[]{:S(2)}) %collective-permute-start.28) | collective-permute-done | bytes 131104 | tf_op jit(solution)/shard_map/ppermute | solution.py:424
  92.0 3.5 %collective-permute-start.8 = (bf16[8,64,256]{2,1,0:T(8,128)(2,1)S(1)}, bf16[8,64,256]{2,1,0:T(8,128)(2,1)S(1)}, u32[]{:S(2)}, u32[]{:S(2)}) collective-permute-start(bf16[8,64,256]{2,1,0:T(8,128)(2,1)S(1)} %get-tuple-element.31.refs_1_), channel_id=1, source_target_pairs={{0,24},{1,25},{2,26},{3,27},{4,28},{5,29},{6,30},{7,31},{8,16},{9,... | collective-permute-start | bytes 786440 | tf_op jit(solution)/shard_map/ppermute | solution.py:424
  95.5 0.5 collective-permute-start.10
  96.0 4.7 %collective-permute-done.8.refs_4_ = bf16[8,64,256]{2,1,0:T(8,128)(2,1)S(1)} collective-permute-done((bf16[8,64,256]{2,1,0:T(8,128)(2,1)S(1)}, bf16[8,64,256]{2,1,0:T(8,128)(2,1)S(1)}, u32[]{:S(2)}, u32[]{:S(2)}) %collective-permute-start.8) | collective-permute-done | bytes 262176 | tf_op jit(solution)/shard_map/ppermute | solution.py:424
  100.7 0.5 collective-permute-start.12
  101.3 1.6 %collective-permute-start.29 = (bf16[192,1024]{1,0:T(8,128)(2,1)S(1)}, bf16[192,1024]{1,0:T(8,128)(2,1)S(1)}, u32[]{:S(2)}, u32[]{:S(2)}) collective-permute-start(bf16[192,1024]{1,0:T(8,128)(2,1)S(1)} %slice.72), channel_id=1, source_target_pairs={{0,4},{1,5},{2,6},{3,7},{4,0},{5,1},{6,2},{7,3},{8,12},{9,13},{10,... | collective-permute-start | bytes 1179656 | tf_op jit(solution)/shard_map/ppermute | solution.py:424
  102.9 0.6 collective-permute-start.24
  103.5 2.5 %collective-permute-start.25 = (bf16[256,512]{1,0:T(8,128)(2,1)S(1)}, bf16[256,512]{1,0:T(8,128)(2,1)S(1)}, u32[]{:S(2)}, u32[]{:S(2)}) collective-permute-start(bf16[256,512]{1,0:T(8,128)(2,1)S(1)} %slice.70), channel_id=1, source_target_pairs={{0,2},{1,3},{2,0},{3,1},{4,6},{5,7},{6,4},{7,5},{8,10},{9,11},{10,... | collective-permute-start | bytes 786440 | tf_op jit(solution)/shard_map/ppermute | solution.py:424
  106.1 1.6 %collective-permute-start.34 = (bf16[128,1024]{1,0:T(8,128)(2,1)S(1)}, bf16[128,1024]{1,0:T(8,128)(2,1)S(1)}, u32[]{:S(2)}, u32[]{:S(2)}) collective-permute-start(bf16[128,1024]{1,0:T(8,128)(2,1)S(1)} %slice.76), channel_id=1, source_target_pairs={{0,4},{1,5},{2,6},{3,7},{4,0},{5,1},{6,2},{7,3},{8,12},{9,13},{10,... | collective-permute-start | bytes 786440 | tf_op jit(solution)/shard_map/ppermute | solution.py:424
  107.7 1.8 %shard_map.123 = (bf16[512,2048]{1,0:T(8,128)(2,1)S(1)}, bf16[512,512]{1,0:T(8,128)(2,1)S(1)}) custom-call(s32[4]{0:T(128)S(1)} %pad_add_fusion.place.refs_0_, bf16[8,64,256]{2,1,0:T(8,128)(2,1)S(1)} %get-tuple-element.31.refs_1_, bf16[8,64,256]{2,1,0:T(8,128)(2,1)S(1)} %collective-permute-done.6.refs_2_, ...), custom_call_target="tpu_custom_call" | custom-call | tf_op jit(solution)/shard_map/pallas_call | solution.py:544
  109.5 3.9 %collective-permute-done.29.refs_14_ = bf16[192,1024]{1,0:T(8,128)(2,1)S(1)} collective-permute-done((bf16[192,1024]{1,0:T(8,128)(2,1)S(1)}, bf16[192,1024]{1,0:T(8,128)(2,1)S(1)}, u32[]{:S(2)}, u32[]{:S(2)}) %collective-permute-start.29) | collective-permute-done | bytes 393248 | tf_op jit(solution)/shard_map/ppermute | solution.py:424
  113.3 5.6 %collective-permute-done.24.refs_8_ = bf16[256,512]{1,0:T(8,128)(2,1)S(1)} collective-permute-done((bf16[256,512]{1,0:T(8,128)(2,1)S(1)}, bf16[256,512]{1,0:T(8,128)(2,1)S(1)}, u32[]{:S(2)}, u32[]{:S(2)}) %collective-permute-start.24) | collective-permute-done | bytes 262176 | tf_op jit(solution)/shard_map/ppermute | solution.py:424
  118.9 3.0 %shard_map.124 = (f32[256,1024]{1,0:T(8,128)S(1)}, bf16[256,1024]{1,0:T(8,128)(2,1)S(1)}, bf16[512,1024]{1,0:T(8,128)(2,1)S(1)}) custom-call(s32[4]{0:T(128)S(1)} %pad_add_fusion.place.refs_0_, bf16[512,2048]{1,0:T(8,128)(2,1)S(1)} %get-tuple-element.34.refs_1_, bf16[512,512]{1,0:T(8,128)(2,1)S(1)} %get-tuple-element.35.refs_2_, ...), custom_call_target="tpu_custom_call" | custom-call | tf_op jit(solution)/shard_map/pallas_call | solution.py:561
  122.0 1.6 %collective-permute-done.34.r1_ref = bf16[128,1024]{1,0:T(8,128)(2,1)S(1)} collective-permute-done((bf16[128,1024]{1,0:T(8,128)(2,1)S(1)}, bf16[128,1024]{1,0:T(8,128)(2,1)S(1)}, u32[]{:S(2)}, u32[]{:S(2)}) %collective-permute-start.34) | collective-permute-done | bytes 262176 | tf_op jit(solution)/shard_map/ppermute | solution.py:424
  123.6 1.3 shard_map.126
  124.9 0.5 collective-permute-start.30
  125.4 1.4 collective-permute-done.35.got
  126.9 3.4 %collective-permute-start.36 = (bf16[128,1024]{1,0:T(8,128)(2,1)S(1)}, bf16[128,1024]{1,0:T(8,128)(2,1)S(1)}, u32[]{:S(2)}, u32[]{:S(2)}) collective-permute-start(bf16[128,1024]{1,0:T(8,128)(2,1)S(1)} %get-tuple-element.44), channel_id=1, source_target_pairs={{0,8},{1,9},{2,10},{3,11},{4,12},{5,13},{6,14},{7,15},{8,0},{9,1},... | collective-permute-start | bytes 786440 | tf_op jit(solution)/shard_map/ppermute | solution.py:424
  130.4 0.6 collective-permute-start.31
  131.1 6.4 %collective-permute-done.36 = bf16[128,1024]{1,0:T(8,128)(2,1)S(1)} collective-permute-done((bf16[128,1024]{1,0:T(8,128)(2,1)S(1)}, bf16[128,1024]{1,0:T(8,128)(2,1)S(1)}, u32[]{:S(2)}, u32[]{:S(2)}) %collective-permute-start.36) | collective-permute-done | bytes 262176 | tf_op jit(solution)/shard_map/ppermute | solution.py:424
  137.5 3.2 %collective-permute-start.37 = (bf16[64,1024]{1,0:T(8,128)(2,1)S(1)}, bf16[64,1024]{1,0:T(8,128)(2,1)S(1)}, u32[]{:S(2)}, u32[]{:S(2)}) collective-permute-start(bf16[64,1024]{1,0:T(8,128)(2,1)S(1)} %add_convert_fusion.2), channel_id=1, source_target_pairs={{0,16},{1,17},{2,18},{3,19},{4,20},{5,21},{6,22},{7,23},{8,24},{9,... | collective-permute-start | bytes 393224 | tf_op jit(solution)/shard_map/ppermute | solution.py:424
  140.7 4.6 %collective-permute-done.31 = bf16[128,1024]{1,0:T(8,128)(2,1)S(1)} collective-permute-done((bf16[128,1024]{1,0:T(8,128)(2,1)S(1)}, bf16[128,1024]{1,0:T(8,128)(2,1)S(1)}, u32[]{:S(2)}, u32[]{:S(2)}) %collective-permute-start.31) | collective-permute-done | bytes 262176 | tf_op jit(solution)/shard_map/ppermute | solution.py:424
  145.4 0.9 collective-permute-start.32
  146.3 7.7 %collective-permute-done.32 = bf16[64,1024]{1,0:T(8,128)(2,1)S(1)} collective-permute-done((bf16[64,1024]{1,0:T(8,128)(2,1)S(1)}, bf16[64,1024]{1,0:T(8,128)(2,1)S(1)}, u32[]{:S(2)}, u32[]{:S(2)}) %collective-permute-start.32) | collective-permute-done | bytes 131104 | tf_op jit(solution)/shard_map/ppermute | solution.py:424
  154.1 0.1 add_convert_fusion.3
  154.2 0.7 pad_maximum_fusion
  (56 shorter events, 0.8 us)
Async XLA Ops:
  0.0 24.5 %copy-start.1 = (bf16[256,2048]{1,0:T(8,128)(2,1)S(1)}, bf16[256,2048]{1,0:T(8,128)(2,1)}, u32[]{:S(2)}) copy-start(bf16[256,2048]{1,0:T(8,128)(2,1)} %refs_6_.1) | copy-start | bytes 3145732
  1.3 0.9 copy-start.2
  3.4 5.3 %collective-permute-start = (bf16[272,128]{1,0:T(8,128)(2,1)S(1)}, bf16[272,128]{1,0:T(8,128)(2,1)S(1)}, u32[]{:S(2)}, u32[]{:S(2)}) collective-permute-start(bf16[272,128]{1,0:T(8,128)(2,1)S(1)} %get-tuple-element.26.mine), channel_id=1, source_target_pairs={{0,4},{1,5},{2,6},{3,7},{4,0},{5,1},{6,2},{7,3},{8,12},{9,13},{10,... | collective-permute-start | bytes 208904 | tf_op jit(solution)/shard_map/ppermute | solution.py:424
  9.3 15.1 %collective-permute-start.1 = (bf16[272,128]{1,0:T(8,128)(2,1)S(1)}, bf16[272,128]{1,0:T(8,128)(2,1)S(1)}, u32[]{:S(2)}, u32[]{:S(2)}) collective-permute-start(bf16[272,128]{1,0:T(8,128)(2,1)S(1)} %shard_map.120), channel_id=1, source_target_pairs={{0,8},{1,9},{2,10},{3,11},{4,12},{5,13},{6,14},{7,15},{8,16},{9,17... | collective-permute-start | bytes 208904 | tf_op jit(solution)/shard_map/ppermute | solution.py:424
  13.4 11.1 %collective-permute-start.2 = (bf16[272,128]{1,0:T(8,128)(2,1)S(1)}, bf16[272,128]{1,0:T(8,128)(2,1)S(1)}, u32[]{:S(2)}, u32[]{:S(2)}) collective-permute-start(bf16[272,128]{1,0:T(8,128)(2,1)S(1)} %shard_map.120), channel_id=1, source_target_pairs={{0,16},{1,17},{2,18},{3,19},{4,20},{5,21},{6,22},{7,23},{8,24},{9,... | collective-permute-start | bytes 208904 | tf_op jit(solution)/shard_map/ppermute | solution.py:424
  17.9 6.6 %collective-permute-start.3 = (bf16[272,128]{1,0:T(8,128)(2,1)S(1)}, bf16[272,128]{1,0:T(8,128)(2,1)S(1)}, u32[]{:S(2)}, u32[]{:S(2)}) collective-permute-start(bf16[272,128]{1,0:T(8,128)(2,1)S(1)} %shard_map.120), channel_id=1, source_target_pairs={{0,24},{1,25},{2,26},{3,27},{4,28},{5,29},{6,30},{7,31}} | collective-permute-start | bytes 208904 | tf_op jit(solution)/shard_map/ppermute | solution.py:424
  19.2 0.9 copy-start.3
  20.1 0.9 copy-start.4
  24.5 0.9 copy-start.6
  25.4 0.7 copy-start.8
  26.0 3.8 %copy-start = (bf16[256,2048]{1,0:T(8,128)(2,1)S(1)}, bf16[256,2048]{1,0:T(8,128)(2,1)}, u32[]{:S(2)}) copy-start(bf16[256,2048]{1,0:T(8,128)(2,1)} %own_ref.1) | copy-start | bytes 3145732
  28.5 35.8 %copy-start.5 = (bf16[64,2048]{1,0:T(8,128)(2,1)S(1)}, bf16[64,2048]{1,0:T(8,128)(2,1)}, u32[]{:S(2)}) copy-start(bf16[64,2048]{1,0:T(8,128)(2,1)} %residual.1) | copy-start | bytes 786436
  28.5 35.8 %copy-start.7 = (f32[2048]{0:T(1024)S(1)}, f32[2048]{0:T(1024)}, u32[]{:S(2)}) copy-start(f32[2048]{0:T(1024)} %param.21) | copy-start | bytes 24580
  28.5 12.4 %collective-permute-start.4 = (bf16[128,2048]{1,0:T(8,128)(2,1)}, bf16[128,2048]{1,0:T(8,128)(2,1)S(1)}, u32[]{:S(2)}, u32[]{:S(2)}) collective-permute-start(bf16[128,2048]{1,0:T(8,128)(2,1)} %get-tuple-element.28), channel_id=1, source_target_pairs={{0,1},{1,0},{2,3},{3,2},{4,5},{5,4},{6,7},{7,6},{8,9},{9,8},{10,11... | collective-permute-start | bytes 1572872 | tf_op jit(solution)/shard_map/ppermute | solution.py:424
  29.8 11.1 %collective-permute-start.13 = (bf16[256,512]{1,0:T(8,128)(2,1)S(1)}, bf16[256,512]{1,0:T(8,128)(2,1)S(1)}, u32[]{:S(2)}, u32[]{:S(2)}) collective-permute-start(bf16[256,512]{1,0:T(8,128)(2,1)S(1)} %get-tuple-element.46), channel_id=1, source_target_pairs={{0,8},{1,9},{2,10},{3,11},{4,12},{5,13},{6,14},{7,15},{8,16},{9,17... | collective-permute-start | bytes 786440 | tf_op jit(solution)/shard_map/ppermute | solution.py:424
  29.9 50.1 %collective-permute-start.27 = (bf16[256,2048]{1,0:T(8,128)(2,1)S(1)}, bf16[256,2048]{1,0:T(8,128)(2,1)S(1)}, u32[]{:S(2)}, u32[]{:S(2)}) collective-permute-start(bf16[256,2048]{1,0:T(8,128)(2,1)S(1)} %copy-done), channel_id=1, source_target_pairs={{0,2},{1,3},{2,0},{3,1},{4,6},{5,7},{6,4},{7,5},{8,10},{9,11},{10,... | collective-permute-start | bytes 3145736 | tf_op jit(solution)/shard_map/ppermute | solution.py:424
  31.5 42.9 %collective-permute-start.26 = (bf16[256,2048]{1,0:T(8,128)(2,1)S(1)}, bf16[256,2048]{1,0:T(8,128)(2,1)S(1)}, u32[]{:S(2)}, u32[]{:S(2)}) collective-permute-start(bf16[256,2048]{1,0:T(8,128)(2,1)S(1)} %copy-done), channel_id=1, source_target_pairs={{0,4},{1,5},{2,6},{3,7},{4,0},{5,1},{6,2},{7,3},{8,12},{9,13},{10,... | collective-permute-start | bytes 3145736 | tf_op jit(solution)/shard_map/ppermute | solution.py:424
  33.0 13.1 %collective-permute-start.15 = (bf16[256,512]{1,0:T(8,128)(2,1)S(1)}, bf16[256,512]{1,0:T(8,128)(2,1)S(1)}, u32[]{:S(2)}, u32[]{:S(2)}) collective-permute-start(bf16[256,512]{1,0:T(8,128)(2,1)S(1)} %get-tuple-element.45), channel_id=1, source_target_pairs={{0,24},{1,25},{2,26},{3,27},{4,28},{5,29},{6,30},{7,31},{8,0},{9,1... | collective-permute-start | bytes 786440 | tf_op jit(solution)/shard_map/ppermute | solution.py:424
  40.9 16.2 %collective-permute-start.14 = (bf16[256,512]{1,0:T(8,128)(2,1)S(1)}, bf16[256,512]{1,0:T(8,128)(2,1)S(1)}, u32[]{:S(2)}, u32[]{:S(2)}) collective-permute-start(bf16[256,512]{1,0:T(8,128)(2,1)S(1)} %get-tuple-element.48), channel_id=1, source_target_pairs={{0,16},{1,17},{2,18},{3,19},{4,20},{5,21},{6,22},{7,23},{8,24},{9,... | collective-permute-start | bytes 786440 | tf_op jit(solution)/shard_map/ppermute | solution.py:424
  40.9 21.4 %collective-permute-start.16 = (bf16[256,512]{1,0:T(8,128)(2,1)S(1)}, bf16[256,512]{1,0:T(8,128)(2,1)S(1)}, u32[]{:S(2)}, u32[]{:S(2)}) collective-permute-start(bf16[256,512]{1,0:T(8,128)(2,1)S(1)} %get-tuple-element.47.refs_9_), channel_id=1, source_target_pairs={{0,4},{1,5},{2,6},{3,7},{4,0},{5,1},{6,2},{7,3},{8,12},{9,13},{10,... | collective-permute-start | bytes 786440 | tf_op jit(solution)/shard_map/ppermute | solution.py:424
  46.0 17.8 %collective-permute-start.5 = (bf16[64,2048]{1,0:T(8,128)(2,1)S(1)}, bf16[64,2048]{1,0:T(8,128)(2,1)S(1)}, u32[]{:S(2)}, u32[]{:S(2)}) collective-permute-start(bf16[64,2048]{1,0:T(8,128)(2,1)S(1)} %add_convert_fusion), channel_id=1, source_target_pairs={{0,2},{1,3},{2,0},{3,1},{4,6},{5,7},{6,4},{7,5},{8,10},{9,11},{10,... | collective-permute-start | bytes 786440 | tf_op jit(solution)/shard_map/ppermute | solution.py:424
  57.2 10.1 %collective-permute-start.19 = (bf16[256,512]{1,0:T(8,128)(2,1)S(1)}, bf16[256,512]{1,0:T(8,128)(2,1)S(1)}, u32[]{:S(2)}, u32[]{:S(2)}) collective-permute-start(bf16[256,512]{1,0:T(8,128)(2,1)S(1)} %get-tuple-element.47.refs_9_), channel_id=1, source_target_pairs={{0,2},{1,3},{2,0},{3,1},{4,6},{5,7},{6,4},{7,5},{8,10},{9,11},{10,... | collective-permute-start | bytes 786440 | tf_op jit(solution)/shard_map/ppermute | solution.py:424
  62.3 8.5 %collective-permute-start.17 = (bf16[256,512]{1,0:T(8,128)(2,1)S(1)}, bf16[256,512]{1,0:T(8,128)(2,1)S(1)}, u32[]{:S(2)}, u32[]{:S(2)}) collective-permute-start(bf16[256,512]{1,0:T(8,128)(2,1)S(1)} %collective-permute-done.14.refs_11_), channel_id=1, source_target_pairs={{0,4},{1,5},{2,6},{3,7},{4,0},{5,1},{6,2},{7,3},{8,12},{9,13},{10,... | collective-permute-start | bytes 786440 | tf_op jit(solution)/shard_map/ppermute | solution.py:424
  63.8 9.2 %collective-permute-start.20 = (bf16[256,512]{1,0:T(8,128)(2,1)S(1)}, bf16[256,512]{1,0:T(8,128)(2,1)S(1)}, u32[]{:S(2)}, u32[]{:S(2)}) collective-permute-start(bf16[256,512]{1,0:T(8,128)(2,1)S(1)} %collective-permute-done.14.refs_11_), channel_id=1, source_target_pairs={{0,2},{1,3},{2,0},{3,1},{4,6},{5,7},{6,4},{7,5},{8,10},{9,11},{10,... | collective-permute-start | bytes 786440 | tf_op jit(solution)/shard_map/ppermute | solution.py:424
  67.2 9.2 %collective-permute-start.22 = (bf16[256,512]{1,0:T(8,128)(2,1)S(1)}, bf16[256,512]{1,0:T(8,128)(2,1)S(1)}, u32[]{:S(2)}, u32[]{:S(2)}) collective-permute-start(bf16[256,512]{1,0:T(8,128)(2,1)S(1)} %collective-permute-done.19.refs_3_), channel_id=1, source_target_pairs={{0,4},{1,5},{2,6},{3,7},{4,0},{5,1},{6,2},{7,3},{8,12},{9,13},{10,... | collective-permute-start | bytes 786440 | tf_op jit(solution)/shard_map/ppermute | solution.py:424
  70.8 9.2 %collective-permute-start.23 = (bf16[256,512]{1,0:T(8,128)(2,1)S(1)}, bf16[256,512]{1,0:T(8,128)(2,1)S(1)}, u32[]{:S(2)}, u32[]{:S(2)}) collective-permute-start(bf16[256,512]{1,0:T(8,128)(2,1)S(1)} %collective-permute-done.17.refs_14_), channel_id=1, source_target_pairs={{0,2},{1,3},{2,0},{3,1},{4,6},{5,7},{6,4},{7,5},{8,10},{9,11},{10,... | collective-permute-start | bytes 786440 | tf_op jit(solution)/shard_map/ppermute | solution.py:424
  73.0 27.7 %collective-permute-start.18 = (bf16[512,512]{1,0:T(8,128)(2,1)S(1)}, bf16[512,512]{1,0:T(8,128)(2,1)S(1)}, u32[]{:S(2)}, u32[]{:S(2)}) collective-permute-start(bf16[512,512]{1,0:T(8,128)(2,1)S(1)} %constant_dynamic-update-slice_fusion), channel_id=1, source_target_pairs={{0,4},{1,5},{2,6},{3,7},{4,0},{5,1},{6,2},{7,3},{8,12},{9,13},{10,... | collective-permute-start | bytes 1572872 | tf_op jit(solution)/shard_map/ppermute | solution.py:424
  74.3 26.9 %collective-permute-start.21 = (bf16[512,512]{1,0:T(8,128)(2,1)S(1)}, bf16[512,512]{1,0:T(8,128)(2,1)S(1)}, u32[]{:S(2)}, u32[]{:S(2)}) collective-permute-start(bf16[512,512]{1,0:T(8,128)(2,1)S(1)} %constant_dynamic-update-slice_fusion), channel_id=1, source_target_pairs={{0,2},{1,3},{2,0},{3,1},{4,6},{5,7},{6,4},{7,5},{8,10},{9,11},{10,... | collective-permute-start | bytes 1572872 | tf_op jit(solution)/shard_map/ppermute | solution.py:424
  76.4 15.6 %collective-permute-start.28 = (bf16[64,1024]{1,0:T(8,128)(2,1)S(1)}, bf16[64,1024]{1,0:T(8,128)(2,1)S(1)}, u32[]{:S(2)}, u32[]{:S(2)}) collective-permute-start(bf16[64,1024]{1,0:T(8,128)(2,1)S(1)} %slice.71), channel_id=1, source_target_pairs={{0,2},{1,3},{2,0},{3,1},{4,6},{5,7},{6,4},{7,5},{8,10},{9,11},{10,... | collective-permute-start | bytes 393224 | tf_op jit(solution)/shard_map/ppermute | solution.py:424
  80.0 15.5 %collective-permute-start.6 = (bf16[8,64,256]{2,1,0:T(8,128)(2,1)S(1)}, bf16[8,64,256]{2,1,0:T(8,128)(2,1)S(1)}, u32[]{:S(2)}, u32[]{:S(2)}) collective-permute-start(bf16[8,64,256]{2,1,0:T(8,128)(2,1)S(1)} %get-tuple-element.31.refs_1_), channel_id=1, source_target_pairs={{0,8},{1,9},{2,10},{3,11},{4,12},{5,13},{6,14},{7,15},{8,0},{9,1},... | collective-permute-start | bytes 786440 | tf_op jit(solution)/shard_map/ppermute | solution.py:424
  80.0 15.5 %collective-permute-start.7 = (bf16[8,64,256]{2,1,0:T(8,128)(2,1)S(1)}, bf16[8,64,256]{2,1,0:T(8,128)(2,1)S(1)}, u32[]{:S(2)}, u32[]{:S(2)}) collective-permute-start(bf16[8,64,256]{2,1,0:T(8,128)(2,1)S(1)} %get-tuple-element.31.refs_1_), channel_id=1, source_target_pairs={{0,16},{1,17},{2,18},{3,19},{4,20},{5,21},{6,22},{7,23},{8,24},{9,... | collective-permute-start | bytes 786440 | tf_op jit(solution)/shard_map/ppermute | solution.py:424
  92.0 8.7 %collective-permute-start.8 = (bf16[8,64,256]{2,1,0:T(8,128)(2,1)S(1)}, bf16[8,64,256]{2,1,0:T(8,128)(2,1)S(1)}, u32[]{:S(2)}, u32[]{:S(2)}) collective-permute-start(bf16[8,64,256]{2,1,0:T(8,128)(2,1)S(1)} %get-tuple-element.31.refs_1_), channel_id=1, source_target_pairs={{0,24},{1,25},{2,26},{3,27},{4,28},{5,29},{6,30},{7,31},{8,16},{9,... | collective-permute-start | bytes 786440 | tf_op jit(solution)/shard_map/ppermute | solution.py:424
  95.4 7.5 %collective-permute-start.9 = (bf16[8,64,256]{2,1,0:T(8,128)(2,1)S(1)}, bf16[8,64,256]{2,1,0:T(8,128)(2,1)S(1)}, u32[]{:S(2)}, u32[]{:S(2)}) collective-permute-start(bf16[8,64,256]{2,1,0:T(8,128)(2,1)S(1)} %get-tuple-element.31.refs_1_), channel_id=1, source_target_pairs={{0,1},{1,0},{2,3},{3,2},{4,5},{5,4},{6,7},{7,6},{8,9},{9,8},{10,11... | collective-permute-start | bytes 786440 | tf_op jit(solution)/shard_map/ppermute | solution.py:424
  95.5 8.1 %collective-permute-start.10 = (bf16[8,64,256]{2,1,0:T(8,128)(2,1)S(1)}, bf16[8,64,256]{2,1,0:T(8,128)(2,1)S(1)}, u32[]{:S(2)}, u32[]{:S(2)}) collective-permute-start(bf16[8,64,256]{2,1,0:T(8,128)(2,1)S(1)} %collective-permute-done.6.refs_2_), channel_id=1, source_target_pairs={{0,1},{1,0},{2,3},{3,2},{4,5},{5,4},{6,7},{7,6},{8,9},{9,8},{10,11... | collective-permute-start | bytes 786440 | tf_op jit(solution)/shard_map/ppermute | solution.py:424
  100.7 5.3 %collective-permute-start.11 = (bf16[8,64,256]{2,1,0:T(8,128)(2,1)S(1)}, bf16[8,64,256]{2,1,0:T(8,128)(2,1)S(1)}, u32[]{:S(2)}, u32[]{:S(2)}) collective-permute-start(bf16[8,64,256]{2,1,0:T(8,128)(2,1)S(1)} %collective-permute-done.7.refs_3_), channel_id=1, source_target_pairs={{0,1},{1,0},{2,3},{3,2},{4,5},{5,4},{6,7},{7,6},{8,9},{9,8},{10,11... | collective-permute-start | bytes 786440 | tf_op jit(solution)/shard_map/ppermute | solution.py:424
  100.7 5.4 %collective-permute-start.12 = (bf16[8,64,256]{2,1,0:T(8,128)(2,1)S(1)}, bf16[8,64,256]{2,1,0:T(8,128)(2,1)S(1)}, u32[]{:S(2)}, u32[]{:S(2)}) collective-permute-start(bf16[8,64,256]{2,1,0:T(8,128)(2,1)S(1)} %collective-permute-done.8.refs_4_), channel_id=1, source_target_pairs={{0,1},{1,0},{2,3},{3,2},{4,5},{5,4},{6,7},{7,6},{8,9},{9,8},{10,11... | collective-permute-start | bytes 786440 | tf_op jit(solution)/shard_map/ppermute | solution.py:424
  101.3 12.1 %collective-permute-start.29 = (bf16[192,1024]{1,0:T(8,128)(2,1)S(1)}, bf16[192,1024]{1,0:T(8,128)(2,1)S(1)}, u32[]{:S(2)}, u32[]{:S(2)}) collective-permute-start(bf16[192,1024]{1,0:T(8,128)(2,1)S(1)} %slice.72), channel_id=1, source_target_pairs={{0,4},{1,5},{2,6},{3,7},{4,0},{5,1},{6,2},{7,3},{8,12},{9,13},{10,... | collective-permute-start | bytes 1179656 | tf_op jit(solution)/shard_map/ppermute | solution.py:424
  102.9 16.0 %collective-permute-start.24 = (bf16[256,512]{1,0:T(8,128)(2,1)S(1)}, bf16[256,512]{1,0:T(8,128)(2,1)S(1)}, u32[]{:S(2)}, u32[]{:S(2)}) collective-permute-start(bf16[256,512]{1,0:T(8,128)(2,1)S(1)} %slice.69), channel_id=1, source_target_pairs={{0,4},{1,5},{2,6},{3,7},{4,0},{5,1},{6,2},{7,3},{8,12},{9,13},{10,... | collective-permute-start | bytes 786440 | tf_op jit(solution)/shard_map/ppermute | solution.py:424
  103.5 15.4 %collective-permute-start.25 = (bf16[256,512]{1,0:T(8,128)(2,1)S(1)}, bf16[256,512]{1,0:T(8,128)(2,1)S(1)}, u32[]{:S(2)}, u32[]{:S(2)}) collective-permute-start(bf16[256,512]{1,0:T(8,128)(2,1)S(1)} %slice.70), channel_id=1, source_target_pairs={{0,2},{1,3},{2,0},{3,1},{4,6},{5,7},{6,4},{7,5},{8,10},{9,11},{10,... | collective-permute-start | bytes 786440 | tf_op jit(solution)/shard_map/ppermute | solution.py:424
  106.0 15.9 %collective-permute-start.33 = (bf16[128,1024]{1,0:T(8,128)(2,1)S(1)}, bf16[128,1024]{1,0:T(8,128)(2,1)S(1)}, u32[]{:S(2)}, u32[]{:S(2)}) collective-permute-start(bf16[128,1024]{1,0:T(8,128)(2,1)S(1)} %slice.75), channel_id=1, source_target_pairs={{0,2},{1,3},{2,0},{3,1},{4,6},{5,7},{6,4},{7,5},{8,10},{9,11},{10,... | collective-permute-start | bytes 786440 | tf_op jit(solution)/shard_map/ppermute | solution.py:424
  106.1 17.5 %collective-permute-start.34 = (bf16[128,1024]{1,0:T(8,128)(2,1)S(1)}, bf16[128,1024]{1,0:T(8,128)(2,1)S(1)}, u32[]{:S(2)}, u32[]{:S(2)}) collective-permute-start(bf16[128,1024]{1,0:T(8,128)(2,1)S(1)} %slice.76), channel_id=1, source_target_pairs={{0,4},{1,5},{2,6},{3,7},{4,0},{5,1},{6,2},{7,3},{8,12},{9,13},{10,... | collective-permute-start | bytes 786440 | tf_op jit(solution)/shard_map/ppermute | solution.py:424
  124.9 2.0 %collective-permute-start.35 = (bf16[256,1024]{1,0:T(8,128)(2,1)S(1)}, bf16[256,1024]{1,0:T(8,128)(2,1)S(1)}, u32[]{:S(2)}, u32[]{:S(2)}) collective-permute-start(bf16[256,1024]{1,0:T(8,128)(2,1)S(1)} %get-tuple-element.42), channel_id=1, source_target_pairs={{0,1},{1,0},{2,3},{3,2},{4,5},{5,4},{6,7},{7,6},{8,9},{9,8},{10,11... | collective-permute-start | bytes 1572872 | tf_op jit(solution)/shard_map/ppermute | solution.py:424
  124.9 5.4 %collective-permute-start.30 = (bf16[256,1024]{1,0:T(8,128)(2,1)S(1)}, bf16[256,1024]{1,0:T(8,128)(2,1)S(1)}, u32[]{:S(2)}, u32[]{:S(2)}) collective-permute-start(bf16[256,1024]{1,0:T(8,128)(2,1)S(1)} %get-tuple-element.37), channel_id=1, source_target_pairs={{0,1},{1,0},{2,3},{3,2},{4,5},{5,4},{6,7},{7,6},{8,9},{9,8},{10,11... | collective-permute-start | bytes 1572872 | tf_op jit(solution)/shard_map/ppermute | solution.py:424
  126.9 10.5 %collective-permute-start.36 = (bf16[128,1024]{1,0:T(8,128)(2,1)S(1)}, bf16[128,1024]{1,0:T(8,128)(2,1)S(1)}, u32[]{:S(2)}, u32[]{:S(2)}) collective-permute-start(bf16[128,1024]{1,0:T(8,128)(2,1)S(1)} %get-tuple-element.44), channel_id=1, source_target_pairs={{0,8},{1,9},{2,10},{3,11},{4,12},{5,13},{6,14},{7,15},{8,0},{9,1},... | collective-permute-start | bytes 786440 | tf_op jit(solution)/shard_map/ppermute | solution.py:424
  130.4 14.9 %collective-permute-start.31 = (bf16[128,1024]{1,0:T(8,128)(2,1)S(1)}, bf16[128,1024]{1,0:T(8,128)(2,1)S(1)}, u32[]{:S(2)}, u32[]{:S(2)}) collective-permute-start(bf16[128,1024]{1,0:T(8,128)(2,1)S(1)} %get-tuple-element.39), channel_id=1, source_target_pairs={{0,8},{1,9},{2,10},{3,11},{4,12},{5,13},{6,14},{7,15},{8,0},{9,1},... | collective-permute-start | bytes 786440 | tf_op jit(solution)/shard_map/ppermute | solution.py:424
  137.5 8.8 %collective-permute-start.37 = (bf16[64,1024]{1,0:T(8,128)(2,1)S(1)}, bf16[64,1024]{1,0:T(8,128)(2,1)S(1)}, u32[]{:S(2)}, u32[]{:S(2)}) collective-permute-start(bf16[64,1024]{1,0:T(8,128)(2,1)S(1)} %add_convert_fusion.2), channel_id=1, source_target_pairs={{0,16},{1,17},{2,18},{3,19},{4,20},{5,21},{6,22},{7,23},{8,24},{9,... | collective-permute-start | bytes 393224 | tf_op jit(solution)/shard_map/ppermute | solution.py:424
  145.4 8.7 %collective-permute-start.32 = (bf16[64,1024]{1,0:T(8,128)(2,1)S(1)}, bf16[64,1024]{1,0:T(8,128)(2,1)S(1)}, u32[]{:S(2)}, u32[]{:S(2)}) collective-permute-start(bf16[64,1024]{1,0:T(8,128)(2,1)S(1)} %add_convert_fusion.4), channel_id=1, source_target_pairs={{0,16},{1,17},{2,18},{3,19},{4,20},{5,21},{6,22},{7,23},{8,24},{9,... | collective-permute-start | bytes 393224 | tf_op jit(solution)/shard_map/ppermute | solution.py:424

commit v7 on v5

--- a/solution.py
+++ b/solution.py
@@ -461,7 +461,7 @@
             mine.append(cut if d == 0 else send(cut, a=d))
 
         def grouped(refs):
-            return [(refs[0], 0), (refs[2], 0), (refs[1], 0), (refs[2], up_rows)]
+            return [(refs[0], 0), (refs[1], 0), (refs[2], 0), (refs[2], up_rows)]
 
         part = model // 2
         half = mixer_down_weight.shape[0] // 2
@@ -513,9 +513,9 @@
             n_in=5,
         )(first, got, other, residual, mixer_norm_gain[None, :])
 
-        late = lax.optimization_barrier((mine[1], mine[3], normed))[:2]
+        late = lax.optimization_barrier((mine[2], mine[3], normed))[:2]
         up_x, up_y = [], []
-        for members in [mine[0], mine[2], jnp.concatenate(late, axis=0)]:
+        for members in [mine[0], mine[1], jnp.concatenate(late, axis=0)]:
             up_x.append(send(members, b=1))
             up_y.append(send(members, y=1))
         up_xy = [send(up_x[0], y=1), send(up_x[1], y=1), send(up_y[2], b=1)]

time: 156 us -> 155 us (level)
  waiting for transfers between devices: 83.6 us -> 79.6 us
  starting transfers between devices: 49.3 us -> 52.6 us
    ppermute x37, waiting for transfers between devices: 83.6 us -> 79.6 us  [send(): return lax.ppermute(x, AXES, pairs)]
    ppermute x37, starting transfers between devices: 49.3 us -> 52.6 us  [send(): return lax.ppermute(x, AXES, pairs)]
  transfers between devices with their start and end apart: 37 -> 37, of which waited for: 19 -> 18; matrix products, arithmetic and copies ran while one was open for 1% -> 1% of each run, Pallas kernels for 6% -> 6%
where the time goes in v7:
time: 155 us
  waiting for transfers between devices  79.6 us (51%)
  starting transfers between devices  52.6 us (34%)
  Pallas kernels  14.2 us (9%)
  local copies, waits for them, and re-layouts  5.69 us (4%)
  other arithmetic  2.32 us (1%)
    ppermute x37, waiting for transfers between devices, send(): return lax.ppermute(x, AXES, pairs)  79.6 us
    ppermute x37, starting transfers between devices, send(): return lax.ppermute(x, AXES, pairs)  52.6 us
    unnamed x19, local copies, waits for them, and re-layouts  4.29 us
    pallas_call x1, Pallas kernels, on_device(): kernel_call(local_body, jax.ShapeDtypeStruct((rows, width), F32), n_in=4)  3.44 us
  transfers between devices with their start and end apart: 37, of which 18 were waited for; matrix products, arithmetic and copies ran while one was open for 1% of the time, Pallas kernels for 6%

profile of v7, /device:TPU:0, one launch (start us, length us, event | category | flops | bytes accessed | tf_op | source)
XLA Modules:
  0.0 154.6 jit_solution(17288502173142682613)
XLA Ops:
  0.0 1.3 log-plus-one_add_fusion
  1.3 0.9 copy-done.2
  2.2 1.2 shard_map.118
  3.4 3.0 %collective-permute-start = (bf16[272,128]{1,0:T(8,128)(2,1)S(1)}, bf16[272,128]{1,0:T(8,128)(2,1)S(1)}, u32[]{:S(2)}, u32[]{:S(2)}) collective-permute-start(bf16[272,128]{1,0:T(8,128)(2,1)S(1)} %get-tuple-element.26.mine), channel_id=1, source_target_pairs={{0,4},{1,5},{2,6},{3,7},{4,0},{5,1},{6,2},{7,3},{8,12},{9,13},{10,... | collective-permute-start | bytes 208904 | tf_op jit(solution)/shard_map/ppermute | solution.py:424
  6.5 2.2 %collective-permute-done.theirs.refs_7_ = bf16[272,128]{1,0:T(8,128)(2,1)S(1)} collective-permute-done((bf16[272,128]{1,0:T(8,128)(2,1)S(1)}, bf16[272,128]{1,0:T(8,128)(2,1)S(1)}, u32[]{:S(2)}, u32[]{:S(2)}) %collective-permute-start) | collective-permute-done | bytes 69664 | tf_op jit(solution)/shard_map/ppermute | solution.py:424
  8.7 0.7 shard_map.120
  9.3 4.0 %collective-permute-start.1 = (bf16[272,128]{1,0:T(8,128)(2,1)S(1)}, bf16[272,128]{1,0:T(8,128)(2,1)S(1)}, u32[]{:S(2)}, u32[]{:S(2)}) collective-permute-start(bf16[272,128]{1,0:T(8,128)(2,1)S(1)} %shard_map.120), channel_id=1, source_target_pairs={{0,8},{1,9},{2,10},{3,11},{4,12},{5,13},{6,14},{7,15},{8,16},{9,17... | collective-permute-start | bytes 208904 | tf_op jit(solution)/shard_map/ppermute | solution.py:424
  13.4 4.5 %collective-permute-start.2 = (bf16[272,128]{1,0:T(8,128)(2,1)S(1)}, bf16[272,128]{1,0:T(8,128)(2,1)S(1)}, u32[]{:S(2)}, u32[]{:S(2)}) collective-permute-start(bf16[272,128]{1,0:T(8,128)(2,1)S(1)} %shard_map.120), channel_id=1, source_target_pairs={{0,16},{1,17},{2,18},{3,19},{4,20},{5,21},{6,22},{7,23},{8,24},{9,... | collective-permute-start | bytes 208904 | tf_op jit(solution)/shard_map/ppermute | solution.py:424
  17.9 1.3 collective-permute-start.3
  19.2 0.9 copy-done.3
  20.1 0.9 copy-done.4
  21.0 3.4 %shard_map.119.refs_3_ = f32[256,256]{1,0:T(8,128)S(1)} custom-call(bf16[256,256]{1,0:T(8,128)(2,1)S(1)} %copy-done.4, f32[256,256]{1,0:T(8,128)S(1)} %get-tuple-element.52.gates.gate, f32[256,256]{1,0:T(8,128)S(1)} %get-tuple-element.25.cum.refs_2_, bf16[256,256]{1,0:T(8,128)(2,1)S(1)} %copy-done.3), custom_call_target="tpu_custom_call" | custom-call | tf_op jit(solution)/shard_map/pallas_call | solution.py:480
  24.5 0.9 copy-done.6
  25.4 0.7 copy-done.8
  26.0 2.5 %shard_map.121 = (f32[64,2048]{1,0:T(8,128)S(1)}, f32[64,2048]{1,0:T(8,128)S(1)}, bf16[128,2048]{1,0:T(8,128)(2,1)}) custom-call(s32[4]{0:T(128)S(1)} %pad_add_fusion.place.refs_0_, bf16[256,256]{1,0:T(8,128)(2,1)S(1)} %copy-done.4, f32[256,256]{1,0:T(8,128)S(1)} %get-tuple-element.25.cum.refs_2_, f32[256,256]{1,0:T(8,128)S(1)} %shard_map.119.refs_3_, ...), custom_call_target="tpu_custom_call" | custom-call | tf_op jit(solution)/shard_map/pallas_call | solution.py:483
  28.5 1.3 constant_dynamic-slice_fusion
  29.9 1.6 %collective-permute-start.26 = (bf16[256,2048]{1,0:T(8,128)(2,1)S(1)}, bf16[256,2048]{1,0:T(8,128)(2,1)S(1)}, u32[]{:S(2)}, u32[]{:S(2)}) collective-permute-start(bf16[256,2048]{1,0:T(8,128)(2,1)S(1)} %copy-done), channel_id=1, source_target_pairs={{0,2},{1,3},{2,0},{3,1},{4,6},{5,7},{6,4},{7,5},{8,10},{9,11},{10,... | collective-permute-start | bytes 3145736 | tf_op jit(solution)/shard_map/ppermute | solution.py:424
  31.5 1.5 collective-permute-start.25
  33.0 1.0 collective-permute-start.15
  34.0 9.3 %collective-permute-done.14.refs_11_ = bf16[256,512]{1,0:T(8,128)(2,1)S(1)} collective-permute-done((bf16[256,512]{1,0:T(8,128)(2,1)S(1)}, bf16[256,512]{1,0:T(8,128)(2,1)S(1)}, u32[]{:S(2)}, u32[]{:S(2)}) %collective-permute-start.14) | collective-permute-done | bytes 262176 | tf_op jit(solution)/shard_map/ppermute | solution.py:424
  43.4 5.3 %collective-permute-start.13 = (bf16[256,512]{1,0:T(8,128)(2,1)S(1)}, bf16[256,512]{1,0:T(8,128)(2,1)S(1)}, u32[]{:S(2)}, u32[]{:S(2)}) collective-permute-start(bf16[256,512]{1,0:T(8,128)(2,1)S(1)} %get-tuple-element.46), channel_id=1, source_target_pairs={{0,8},{1,9},{2,10},{3,11},{4,12},{5,13},{6,14},{7,15},{8,16},{9,17... | collective-permute-start | bytes 786440 | tf_op jit(solution)/shard_map/ppermute | solution.py:424
  48.7 1.5 collective-permute-start.16
  50.2 1.6 %collective-permute-start.5 = (bf16[64,2048]{1,0:T(8,128)(2,1)S(1)}, bf16[64,2048]{1,0:T(8,128)(2,1)S(1)}, u32[]{:S(2)}, u32[]{:S(2)}) collective-permute-start(bf16[64,2048]{1,0:T(8,128)(2,1)S(1)} %add_convert_fusion), channel_id=1, source_target_pairs={{0,2},{1,3},{2,0},{3,1},{4,6},{5,7},{6,4},{7,5},{8,10},{9,11},{10,... | collective-permute-start | bytes 786440 | tf_op jit(solution)/shard_map/ppermute | solution.py:424
  51.8 5.7 %collective-permute-done.13.refs_10_ = bf16[256,512]{1,0:T(8,128)(2,1)S(1)} collective-permute-done((bf16[256,512]{1,0:T(8,128)(2,1)S(1)}, bf16[256,512]{1,0:T(8,128)(2,1)S(1)}, u32[]{:S(2)}, u32[]{:S(2)}) %collective-permute-start.13) | collective-permute-done | bytes 262176 | tf_op jit(solution)/shard_map/ppermute | solution.py:424
  57.5 1.5 collective-permute-start.19
  59.1 3.3 %collective-permute-done.16.refs_13_ = bf16[256,512]{1,0:T(8,128)(2,1)S(1)} collective-permute-done((bf16[256,512]{1,0:T(8,128)(2,1)S(1)}, bf16[256,512]{1,0:T(8,128)(2,1)S(1)}, u32[]{:S(2)}, u32[]{:S(2)}) %collective-permute-start.16) | collective-permute-done | bytes 262176 | tf_op jit(solution)/shard_map/ppermute | solution.py:424
  62.4 1.5 collective-permute-start.17
  63.8 0.5 collective-permute-start.20
  64.4 0.2 shard_map.122
  64.6 2.6 %collective-permute-done.19.refs_3_ = bf16[256,512]{1,0:T(8,128)(2,1)S(1)} collective-permute-done((bf16[256,512]{1,0:T(8,128)(2,1)S(1)}, bf16[256,512]{1,0:T(8,128)(2,1)S(1)}, u32[]{:S(2)}, u32[]{:S(2)}) %collective-permute-start.19) | collective-permute-done | bytes 262176 | tf_op jit(solution)/shard_map/ppermute | solution.py:424
  67.2 1.5 collective-permute-start.22
  68.8 1.1 collective-permute-done.17.refs_14_
  69.9 0.5 collective-permute-start.23
  70.4 2.6 %collective-permute-done.20.refs_4_ = bf16[256,512]{1,0:T(8,128)(2,1)S(1)} collective-permute-done((bf16[256,512]{1,0:T(8,128)(2,1)S(1)}, bf16[256,512]{1,0:T(8,128)(2,1)S(1)}, u32[]{:S(2)}, u32[]{:S(2)}) %collective-permute-start.20) | collective-permute-done | bytes 262176 | tf_op jit(solution)/shard_map/ppermute | solution.py:424
  73.0 1.4 collective-permute-start.21
  74.4 4.3 %collective-permute-done.22.refs_6_ = bf16[256,512]{1,0:T(8,128)(2,1)S(1)} collective-permute-done((bf16[256,512]{1,0:T(8,128)(2,1)S(1)}, bf16[256,512]{1,0:T(8,128)(2,1)S(1)}, u32[]{:S(2)}, u32[]{:S(2)}) %collective-permute-start.22) | collective-permute-done | bytes 262176 | tf_op jit(solution)/shard_map/ppermute | solution.py:424
  78.6 1.1 collective-permute-start.6
  79.7 4.5 %collective-permute-done.23.refs_7_ = bf16[256,512]{1,0:T(8,128)(2,1)S(1)} collective-permute-done((bf16[256,512]{1,0:T(8,128)(2,1)S(1)}, bf16[256,512]{1,0:T(8,128)(2,1)S(1)}, u32[]{:S(2)}, u32[]{:S(2)}) %collective-permute-start.23) | collective-permute-done | bytes 262176 | tf_op jit(solution)/shard_map/ppermute | solution.py:424
  84.3 1.3 collective-permute-start.18
  85.6 2.8 %collective-permute-start.7 = (bf16[8,64,256]{2,1,0:T(8,128)(2,1)S(1)}, bf16[8,64,256]{2,1,0:T(8,128)(2,1)S(1)}, u32[]{:S(2)}, u32[]{:S(2)}) collective-permute-start(bf16[8,64,256]{2,1,0:T(8,128)(2,1)S(1)} %get-tuple-element.31.refs_1_), channel_id=1, source_target_pairs={{0,16},{1,17},{2,18},{3,19},{4,20},{5,21},{6,22},{7,23},{8,24},{9,... | collective-permute-start | bytes 786440 | tf_op jit(solution)/shard_map/ppermute | solution.py:424
  88.4 0.8 collective-permute-start.8
  89.2 5.6 %collective-permute-done.21.refs_5_ = bf16[512,512]{1,0:T(8,128)(2,1)S(1)} collective-permute-done((bf16[512,512]{1,0:T(8,128)(2,1)S(1)}, bf16[512,512]{1,0:T(8,128)(2,1)S(1)}, u32[]{:S(2)}, u32[]{:S(2)}) %collective-permute-start.21) | collective-permute-done | bytes 524320 | tf_op jit(solution)/shard_map/ppermute | solution.py:424
  94.8 1.5 collective-permute-start.24
  96.3 8.7 %collective-permute-done.7.refs_3_ = bf16[8,64,256]{2,1,0:T(8,128)(2,1)S(1)} collective-permute-done((bf16[8,64,256]{2,1,0:T(8,128)(2,1)S(1)}, bf16[8,64,256]{2,1,0:T(8,128)(2,1)S(1)}, u32[]{:S(2)}, u32[]{:S(2)}) %collective-permute-start.7) | collective-permute-done | bytes 262176 | tf_op jit(solution)/shard_map/ppermute | solution.py:424
  105.0 0.5 collective-permute-start.11
  105.6 1.0 collective-permute-start.28
  106.7 1.6 %collective-permute-start.32 = (bf16[128,1024]{1,0:T(8,128)(2,1)S(1)}, bf16[128,1024]{1,0:T(8,128)(2,1)S(1)}, u32[]{:S(2)}, u32[]{:S(2)}) collective-permute-start(bf16[128,1024]{1,0:T(8,128)(2,1)S(1)} %slice.65), channel_id=1, source_target_pairs={{0,2},{1,3},{2,0},{3,1},{4,6},{5,7},{6,4},{7,5},{8,10},{9,11},{10,... | collective-permute-start | bytes 786440 | tf_op jit(solution)/shard_map/ppermute | solution.py:424
  108.3 1.1 collective-permute-start.33
  109.4 0.6 collective-permute-start.27
  110.0 1.8 %shard_map.123 = (bf16[512,2048]{1,0:T(8,128)(2,1)S(1)}, bf16[512,512]{1,0:T(8,128)(2,1)S(1)}) custom-call(s32[4]{0:T(128)S(1)} %pad_add_fusion.place.refs_0_, bf16[8,64,256]{2,1,0:T(8,128)(2,1)S(1)} %get-tuple-element.31.refs_1_, bf16[8,64,256]{2,1,0:T(8,128)(2,1)S(1)} %collective-permute-done.6.refs_2_, ...), custom_call_target="tpu_custom_call" | custom-call | tf_op jit(solution)/shard_map/pallas_call | solution.py:539
  111.7 6.2 %collective-permute-done.27.refs_12_ = bf16[64,1024]{1,0:T(8,128)(2,1)S(1)} collective-permute-done((bf16[64,1024]{1,0:T(8,128)(2,1)S(1)}, bf16[64,1024]{1,0:T(8,128)(2,1)S(1)}, u32[]{:S(2)}, u32[]{:S(2)}) %collective-permute-start.27) | collective-permute-done | bytes 131104 | tf_op jit(solution)/shard_map/ppermute | solution.py:424
  117.9 3.0 %shard_map.124 = (f32[256,1024]{1,0:T(8,128)S(1)}, bf16[256,1024]{1,0:T(8,128)(2,1)S(1)}, bf16[512,1024]{1,0:T(8,128)(2,1)S(1)}) custom-call(s32[4]{0:T(128)S(1)} %pad_add_fusion.place.refs_0_, bf16[512,2048]{1,0:T(8,128)(2,1)S(1)} %get-tuple-element.34.refs_1_, bf16[512,512]{1,0:T(8,128)(2,1)S(1)} %get-tuple-element.35.refs_2_, ...), custom_call_target="tpu_custom_call" | custom-call | tf_op jit(solution)/shard_map/pallas_call | solution.py:556
  121.0 1.8 %collective-permute-done.33.r1_ref = bf16[128,1024]{1,0:T(8,128)(2,1)S(1)} collective-permute-done((bf16[128,1024]{1,0:T(8,128)(2,1)S(1)}, bf16[128,1024]{1,0:T(8,128)(2,1)S(1)}, u32[]{:S(2)}, u32[]{:S(2)}) %collective-permute-start.33) | collective-permute-done | bytes 262176 | tf_op jit(solution)/shard_map/ppermute | solution.py:424
  122.7 1.3 shard_map.126
  124.1 0.5 collective-permute-start.29
  124.6 1.4 collective-permute-done.34.got
  126.1 5.6 %collective-permute-start.35 = (bf16[128,1024]{1,0:T(8,128)(2,1)S(1)}, bf16[128,1024]{1,0:T(8,128)(2,1)S(1)}, u32[]{:S(2)}, u32[]{:S(2)}) collective-permute-start(bf16[128,1024]{1,0:T(8,128)(2,1)S(1)} %get-tuple-element.44), channel_id=1, source_target_pairs={{0,8},{1,9},{2,10},{3,11},{4,12},{5,13},{6,14},{7,15},{8,0},{9,1},... | collective-permute-start | bytes 786440 | tf_op jit(solution)/shard_map/ppermute | solution.py:424
  131.8 0.6 collective-permute-start.30
  132.4 6.4 %collective-permute-done.35 = bf16[128,1024]{1,0:T(8,128)(2,1)S(1)} collective-permute-done((bf16[128,1024]{1,0:T(8,128)(2,1)S(1)}, bf16[128,1024]{1,0:T(8,128)(2,1)S(1)}, u32[]{:S(2)}, u32[]{:S(2)}) %collective-permute-start.35) | collective-permute-done | bytes 262176 | tf_op jit(solution)/shard_map/ppermute | solution.py:424
  138.9 1.1 collective-permute-start.36
  139.9 6.2 %collective-permute-done.30 = bf16[128,1024]{1,0:T(8,128)(2,1)S(1)} collective-permute-done((bf16[128,1024]{1,0:T(8,128)(2,1)S(1)}, bf16[128,1024]{1,0:T(8,128)(2,1)S(1)}, u32[]{:S(2)}, u32[]{:S(2)}) %collective-permute-start.30) | collective-permute-done | bytes 262176 | tf_op jit(solution)/shard_map/ppermute | solution.py:424
  146.3 1.2 collective-permute-done.36
  147.5 6.2 %collective-permute-done.31 = bf16[64,1024]{1,0:T(8,128)(2,1)S(1)} collective-permute-done((bf16[64,1024]{1,0:T(8,128)(2,1)S(1)}, bf16[64,1024]{1,0:T(8,128)(2,1)S(1)}, u32[]{:S(2)}, u32[]{:S(2)}) %collective-permute-start.31) | collective-permute-done | bytes 131104 | tf_op jit(solution)/shard_map/ppermute | solution.py:424
  153.9 0.7 pad_maximum_fusion
  (52 shorter events, 1.0 us)
Async XLA Ops:
  0.0 24.5 %copy-start.1 = (bf16[256,2048]{1,0:T(8,128)(2,1)S(1)}, bf16[256,2048]{1,0:T(8,128)(2,1)}, u32[]{:S(2)}) copy-start(bf16[256,2048]{1,0:T(8,128)(2,1)} %refs_6_.1) | copy-start | bytes 3145732
  1.3 0.9 copy-start.2
  3.4 5.3 %collective-permute-start = (bf16[272,128]{1,0:T(8,128)(2,1)S(1)}, bf16[272,128]{1,0:T(8,128)(2,1)S(1)}, u32[]{:S(2)}, u32[]{:S(2)}) collective-permute-start(bf16[272,128]{1,0:T(8,128)(2,1)S(1)} %get-tuple-element.26.mine), channel_id=1, source_target_pairs={{0,4},{1,5},{2,6},{3,7},{4,0},{5,1},{6,2},{7,3},{8,12},{9,13},{10,... | collective-permute-start | bytes 208904 | tf_op jit(solution)/shard_map/ppermute | solution.py:424
  9.3 15.1 %collective-permute-start.1 = (bf16[272,128]{1,0:T(8,128)(2,1)S(1)}, bf16[272,128]{1,0:T(8,128)(2,1)S(1)}, u32[]{:S(2)}, u32[]{:S(2)}) collective-permute-start(bf16[272,128]{1,0:T(8,128)(2,1)S(1)} %shard_map.120), channel_id=1, source_target_pairs={{0,8},{1,9},{2,10},{3,11},{4,12},{5,13},{6,14},{7,15},{8,16},{9,17... | collective-permute-start | bytes 208904 | tf_op jit(solution)/shard_map/ppermute | solution.py:424
  13.4 11.1 %collective-permute-start.2 = (bf16[272,128]{1,0:T(8,128)(2,1)S(1)}, bf16[272,128]{1,0:T(8,128)(2,1)S(1)}, u32[]{:S(2)}, u32[]{:S(2)}) collective-permute-start(bf16[272,128]{1,0:T(8,128)(2,1)S(1)} %shard_map.120), channel_id=1, source_target_pairs={{0,16},{1,17},{2,18},{3,19},{4,20},{5,21},{6,22},{7,23},{8,24},{9,... | collective-permute-start | bytes 208904 | tf_op jit(solution)/shard_map/ppermute | solution.py:424
  17.9 6.6 %collective-permute-start.3 = (bf16[272,128]{1,0:T(8,128)(2,1)S(1)}, bf16[272,128]{1,0:T(8,128)(2,1)S(1)}, u32[]{:S(2)}, u32[]{:S(2)}) collective-permute-start(bf16[272,128]{1,0:T(8,128)(2,1)S(1)} %shard_map.120), channel_id=1, source_target_pairs={{0,24},{1,25},{2,26},{3,27},{4,28},{5,29},{6,30},{7,31}} | collective-permute-start | bytes 208904 | tf_op jit(solution)/shard_map/ppermute | solution.py:424
  19.2 0.9 copy-start.3
  20.1 0.9 copy-start.4
  24.5 0.9 copy-start.6
  25.4 0.7 copy-start.8
  26.0 3.9 %copy-start = (bf16[256,2048]{1,0:T(8,128)(2,1)S(1)}, bf16[256,2048]{1,0:T(8,128)(2,1)}, u32[]{:S(2)}) copy-start(bf16[256,2048]{1,0:T(8,128)(2,1)} %own_ref.1) | copy-start | bytes 3145732
  28.5 35.9 %copy-start.5 = (bf16[64,2048]{1,0:T(8,128)(2,1)S(1)}, bf16[64,2048]{1,0:T(8,128)(2,1)}, u32[]{:S(2)}) copy-start(bf16[64,2048]{1,0:T(8,128)(2,1)} %residual.1) | copy-start | bytes 786436
  28.5 35.9 %copy-start.7 = (f32[2048]{0:T(1024)S(1)}, f32[2048]{0:T(1024)}, u32[]{:S(2)}) copy-start(f32[2048]{0:T(1024)} %param.21) | copy-start | bytes 24580
  28.5 20.1 %collective-permute-start.4 = (bf16[128,2048]{1,0:T(8,128)(2,1)}, bf16[128,2048]{1,0:T(8,128)(2,1)S(1)}, u32[]{:S(2)}, u32[]{:S(2)}) collective-permute-start(bf16[128,2048]{1,0:T(8,128)(2,1)} %get-tuple-element.28), channel_id=1, source_target_pairs={{0,1},{1,0},{2,3},{3,2},{4,5},{5,4},{6,7},{7,6},{8,9},{9,8},{10,11... | collective-permute-start | bytes 1572872 | tf_op jit(solution)/shard_map/ppermute | solution.py:424
  29.8 13.5 %collective-permute-start.14 = (bf16[256,512]{1,0:T(8,128)(2,1)S(1)}, bf16[256,512]{1,0:T(8,128)(2,1)S(1)}, u32[]{:S(2)}, u32[]{:S(2)}) collective-permute-start(bf16[256,512]{1,0:T(8,128)(2,1)S(1)} %get-tuple-element.48), channel_id=1, source_target_pairs={{0,16},{1,17},{2,18},{3,19},{4,20},{5,21},{6,22},{7,23},{8,24},{9,... | collective-permute-start | bytes 786440 | tf_op jit(solution)/shard_map/ppermute | solution.py:424
  29.9 55.7 %collective-permute-start.26 = (bf16[256,2048]{1,0:T(8,128)(2,1)S(1)}, bf16[256,2048]{1,0:T(8,128)(2,1)S(1)}, u32[]{:S(2)}, u32[]{:S(2)}) collective-permute-start(bf16[256,2048]{1,0:T(8,128)(2,1)S(1)} %copy-done), channel_id=1, source_target_pairs={{0,2},{1,3},{2,0},{3,1},{4,6},{5,7},{6,4},{7,5},{8,10},{9,11},{10,... | collective-permute-start | bytes 3145736 | tf_op jit(solution)/shard_map/ppermute | solution.py:424
  31.5 56.9 %collective-permute-start.25 = (bf16[256,2048]{1,0:T(8,128)(2,1)S(1)}, bf16[256,2048]{1,0:T(8,128)(2,1)S(1)}, u32[]{:S(2)}, u32[]{:S(2)}) collective-permute-start(bf16[256,2048]{1,0:T(8,128)(2,1)S(1)} %copy-done), channel_id=1, source_target_pairs={{0,4},{1,5},{2,6},{3,7},{4,0},{5,1},{6,2},{7,3},{8,12},{9,13},{10,... | collective-permute-start | bytes 3145736 | tf_op jit(solution)/shard_map/ppermute | solution.py:424
  33.0 17.2 %collective-permute-start.15 = (bf16[256,512]{1,0:T(8,128)(2,1)S(1)}, bf16[256,512]{1,0:T(8,128)(2,1)S(1)}, u32[]{:S(2)}, u32[]{:S(2)}) collective-permute-start(bf16[256,512]{1,0:T(8,128)(2,1)S(1)} %get-tuple-element.45), channel_id=1, source_target_pairs={{0,24},{1,25},{2,26},{3,27},{4,28},{5,29},{6,30},{7,31},{8,0},{9,1... | collective-permute-start | bytes 786440 | tf_op jit(solution)/shard_map/ppermute | solution.py:424
  43.4 14.2 %collective-permute-start.13 = (bf16[256,512]{1,0:T(8,128)(2,1)S(1)}, bf16[256,512]{1,0:T(8,128)(2,1)S(1)}, u32[]{:S(2)}, u32[]{:S(2)}) collective-permute-start(bf16[256,512]{1,0:T(8,128)(2,1)S(1)} %get-tuple-element.46), channel_id=1, source_target_pairs={{0,8},{1,9},{2,10},{3,11},{4,12},{5,13},{6,14},{7,15},{8,16},{9,17... | collective-permute-start | bytes 786440 | tf_op jit(solution)/shard_map/ppermute | solution.py:424
  48.7 13.7 %collective-permute-start.16 = (bf16[256,512]{1,0:T(8,128)(2,1)S(1)}, bf16[256,512]{1,0:T(8,128)(2,1)S(1)}, u32[]{:S(2)}, u32[]{:S(2)}) collective-permute-start(bf16[256,512]{1,0:T(8,128)(2,1)S(1)} %get-tuple-element.47.refs_9_), channel_id=1, source_target_pairs={{0,4},{1,5},{2,6},{3,7},{4,0},{5,1},{6,2},{7,3},{8,12},{9,13},{10,... | collective-permute-start | bytes 786440 | tf_op jit(solution)/shard_map/ppermute | solution.py:424
  50.2 13.6 %collective-permute-start.5 = (bf16[64,2048]{1,0:T(8,128)(2,1)S(1)}, bf16[64,2048]{1,0:T(8,128)(2,1)S(1)}, u32[]{:S(2)}, u32[]{:S(2)}) collective-permute-start(bf16[64,2048]{1,0:T(8,128)(2,1)S(1)} %add_convert_fusion), channel_id=1, source_target_pairs={{0,2},{1,3},{2,0},{3,1},{4,6},{5,7},{6,4},{7,5},{8,10},{9,11},{10,... | collective-permute-start | bytes 786440 | tf_op jit(solution)/shard_map/ppermute | solution.py:424
  57.5 9.7 %collective-permute-start.19 = (bf16[256,512]{1,0:T(8,128)(2,1)S(1)}, bf16[256,512]{1,0:T(8,128)(2,1)S(1)}, u32[]{:S(2)}, u32[]{:S(2)}) collective-permute-start(bf16[256,512]{1,0:T(8,128)(2,1)S(1)} %get-tuple-element.47.refs_9_), channel_id=1, source_target_pairs={{0,2},{1,3},{2,0},{3,1},{4,6},{5,7},{6,4},{7,5},{8,10},{9,11},{10,... | collective-permute-start | bytes 786440 | tf_op jit(solution)/shard_map/ppermute | solution.py:424
  62.4 7.5 %collective-permute-start.17 = (bf16[256,512]{1,0:T(8,128)(2,1)S(1)}, bf16[256,512]{1,0:T(8,128)(2,1)S(1)}, u32[]{:S(2)}, u32[]{:S(2)}) collective-permute-start(bf16[256,512]{1,0:T(8,128)(2,1)S(1)} %collective-permute-done.13.refs_10_), channel_id=1, source_target_pairs={{0,4},{1,5},{2,6},{3,7},{4,0},{5,1},{6,2},{7,3},{8,12},{9,13},{10,... | collective-permute-start | bytes 786440 | tf_op jit(solution)/shard_map/ppermute | solution.py:424
  63.8 9.2 %collective-permute-start.20 = (bf16[256,512]{1,0:T(8,128)(2,1)S(1)}, bf16[256,512]{1,0:T(8,128)(2,1)S(1)}, u32[]{:S(2)}, u32[]{:S(2)}) collective-permute-start(bf16[256,512]{1,0:T(8,128)(2,1)S(1)} %collective-permute-done.13.refs_10_), channel_id=1, source_target_pairs={{0,2},{1,3},{2,0},{3,1},{4,6},{5,7},{6,4},{7,5},{8,10},{9,11},{10,... | collective-permute-start | bytes 786440 | tf_op jit(solution)/shard_map/ppermute | solution.py:424
  67.2 11.4 %collective-permute-start.22 = (bf16[256,512]{1,0:T(8,128)(2,1)S(1)}, bf16[256,512]{1,0:T(8,128)(2,1)S(1)}, u32[]{:S(2)}, u32[]{:S(2)}) collective-permute-start(bf16[256,512]{1,0:T(8,128)(2,1)S(1)} %collective-permute-done.16.refs_13_), channel_id=1, source_target_pairs={{0,2},{1,3},{2,0},{3,1},{4,6},{5,7},{6,4},{7,5},{8,10},{9,11},{10,... | collective-permute-start | bytes 786440 | tf_op jit(solution)/shard_map/ppermute | solution.py:424
  69.9 14.4 %collective-permute-start.23 = (bf16[256,512]{1,0:T(8,128)(2,1)S(1)}, bf16[256,512]{1,0:T(8,128)(2,1)S(1)}, u32[]{:S(2)}, u32[]{:S(2)}) collective-permute-start(bf16[256,512]{1,0:T(8,128)(2,1)S(1)} %collective-permute-done.17.refs_14_), channel_id=1, source_target_pairs={{0,2},{1,3},{2,0},{3,1},{4,6},{5,7},{6,4},{7,5},{8,10},{9,11},{10,... | collective-permute-start | bytes 786440 | tf_op jit(solution)/shard_map/ppermute | solution.py:424
  73.0 21.8 %collective-permute-start.21 = (bf16[512,512]{1,0:T(8,128)(2,1)S(1)}, bf16[512,512]{1,0:T(8,128)(2,1)S(1)}, u32[]{:S(2)}, u32[]{:S(2)}) collective-permute-start(bf16[512,512]{1,0:T(8,128)(2,1)S(1)} %constant_dynamic-update-slice_fusion), channel_id=1, source_target_pairs={{0,2},{1,3},{2,0},{3,1},{4,6},{5,7},{6,4},{7,5},{8,10},{9,11},{10,... | collective-permute-start | bytes 1572872 | tf_op jit(solution)/shard_map/ppermute | solution.py:424
  78.6 10.6 %collective-permute-start.6 = (bf16[8,64,256]{2,1,0:T(8,128)(2,1)S(1)}, bf16[8,64,256]{2,1,0:T(8,128)(2,1)S(1)}, u32[]{:S(2)}, u32[]{:S(2)}) collective-permute-start(bf16[8,64,256]{2,1,0:T(8,128)(2,1)S(1)} %get-tuple-element.31.refs_1_), channel_id=1, source_target_pairs={{0,8},{1,9},{2,10},{3,11},{4,12},{5,13},{6,14},{7,15},{8,0},{9,1},... | collective-permute-start | bytes 786440 | tf_op jit(solution)/shard_map/ppermute | solution.py:424
  84.3 21.3 %collective-permute-start.18 = (bf16[512,512]{1,0:T(8,128)(2,1)S(1)}, bf16[512,512]{1,0:T(8,128)(2,1)S(1)}, u32[]{:S(2)}, u32[]{:S(2)}) collective-permute-start(bf16[512,512]{1,0:T(8,128)(2,1)S(1)} %constant_dynamic-update-slice_fusion), channel_id=1, source_target_pairs={{0,4},{1,5},{2,6},{3,7},{4,0},{5,1},{6,2},{7,3},{8,12},{9,13},{10,... | collective-permute-start | bytes 1572872 | tf_op jit(solution)/shard_map/ppermute | solution.py:424
  85.6 19.4 %collective-permute-start.7 = (bf16[8,64,256]{2,1,0:T(8,128)(2,1)S(1)}, bf16[8,64,256]{2,1,0:T(8,128)(2,1)S(1)}, u32[]{:S(2)}, u32[]{:S(2)}) collective-permute-start(bf16[8,64,256]{2,1,0:T(8,128)(2,1)S(1)} %get-tuple-element.31.refs_1_), channel_id=1, source_target_pairs={{0,16},{1,17},{2,18},{3,19},{4,20},{5,21},{6,22},{7,23},{8,24},{9,... | collective-permute-start | bytes 786440 | tf_op jit(solution)/shard_map/ppermute | solution.py:424
  88.4 16.5 %collective-permute-start.8 = (bf16[8,64,256]{2,1,0:T(8,128)(2,1)S(1)}, bf16[8,64,256]{2,1,0:T(8,128)(2,1)S(1)}, u32[]{:S(2)}, u32[]{:S(2)}) collective-permute-start(bf16[8,64,256]{2,1,0:T(8,128)(2,1)S(1)} %get-tuple-element.31.refs_1_), channel_id=1, source_target_pairs={{0,24},{1,25},{2,26},{3,27},{4,28},{5,29},{6,30},{7,31},{8,16},{9,... | collective-permute-start | bytes 786440 | tf_op jit(solution)/shard_map/ppermute | solution.py:424
  89.2 16.3 %collective-permute-start.9 = (bf16[8,64,256]{2,1,0:T(8,128)(2,1)S(1)}, bf16[8,64,256]{2,1,0:T(8,128)(2,1)S(1)}, u32[]{:S(2)}, u32[]{:S(2)}) collective-permute-start(bf16[8,64,256]{2,1,0:T(8,128)(2,1)S(1)} %get-tuple-element.31.refs_1_), channel_id=1, source_target_pairs={{0,1},{1,0},{2,3},{3,2},{4,5},{5,4},{6,7},{7,6},{8,9},{9,8},{10,11... | collective-permute-start | bytes 786440 | tf_op jit(solution)/shard_map/ppermute | solution.py:424
  94.8 23.1 %collective-permute-start.24 = (bf16[512,512]{1,0:T(8,128)(2,1)S(1)}, bf16[512,512]{1,0:T(8,128)(2,1)S(1)}, u32[]{:S(2)}, u32[]{:S(2)}) collective-permute-start(bf16[512,512]{1,0:T(8,128)(2,1)S(1)} %collective-permute-done.21.refs_5_), channel_id=1, source_target_pairs={{0,4},{1,5},{2,6},{3,7},{4,0},{5,1},{6,2},{7,3},{8,12},{9,13},{10,... | collective-permute-start | bytes 1572872 | tf_op jit(solution)/shard_map/ppermute | solution.py:424
  105.0 1.7 %collective-permute-start.10 = (bf16[8,64,256]{2,1,0:T(8,128)(2,1)S(1)}, bf16[8,64,256]{2,1,0:T(8,128)(2,1)S(1)}, u32[]{:S(2)}, u32[]{:S(2)}) collective-permute-start(bf16[8,64,256]{2,1,0:T(8,128)(2,1)S(1)} %collective-permute-done.6.refs_2_), channel_id=1, source_target_pairs={{0,1},{1,0},{2,3},{3,2},{4,5},{5,4},{6,7},{7,6},{8,9},{9,8},{10,11... | collective-permute-start | bytes 786440 | tf_op jit(solution)/shard_map/ppermute | solution.py:424
  105.0 3.3 %collective-permute-start.11 = (bf16[8,64,256]{2,1,0:T(8,128)(2,1)S(1)}, bf16[8,64,256]{2,1,0:T(8,128)(2,1)S(1)}, u32[]{:S(2)}, u32[]{:S(2)}) collective-permute-start(bf16[8,64,256]{2,1,0:T(8,128)(2,1)S(1)} %collective-permute-done.7.refs_3_), channel_id=1, source_target_pairs={{0,1},{1,0},{2,3},{3,2},{4,5},{5,4},{6,7},{7,6},{8,9},{9,8},{10,11... | collective-permute-start | bytes 786440 | tf_op jit(solution)/shard_map/ppermute | solution.py:424
  105.5 3.9 %collective-permute-start.12 = (bf16[8,64,256]{2,1,0:T(8,128)(2,1)S(1)}, bf16[8,64,256]{2,1,0:T(8,128)(2,1)S(1)}, u32[]{:S(2)}, u32[]{:S(2)}) collective-permute-start(bf16[8,64,256]{2,1,0:T(8,128)(2,1)S(1)} %collective-permute-done.8.refs_4_), channel_id=1, source_target_pairs={{0,1},{1,0},{2,3},{3,2},{4,5},{5,4},{6,7},{7,6},{8,9},{9,8},{10,11... | collective-permute-start | bytes 786440 | tf_op jit(solution)/shard_map/ppermute | solution.py:424
  105.6 12.3 %collective-permute-start.28 = (bf16[192,1024]{1,0:T(8,128)(2,1)S(1)}, bf16[192,1024]{1,0:T(8,128)(2,1)S(1)}, u32[]{:S(2)}, u32[]{:S(2)}) collective-permute-start(bf16[192,1024]{1,0:T(8,128)(2,1)S(1)} %slice.62), channel_id=1, source_target_pairs={{0,4},{1,5},{2,6},{3,7},{4,0},{5,1},{6,2},{7,3},{8,12},{9,13},{10,... | collective-permute-start | bytes 1179656 | tf_op jit(solution)/shard_map/ppermute | solution.py:424
  106.7 14.2 %collective-permute-start.32 = (bf16[128,1024]{1,0:T(8,128)(2,1)S(1)}, bf16[128,1024]{1,0:T(8,128)(2,1)S(1)}, u32[]{:S(2)}, u32[]{:S(2)}) collective-permute-start(bf16[128,1024]{1,0:T(8,128)(2,1)S(1)} %slice.65), channel_id=1, source_target_pairs={{0,2},{1,3},{2,0},{3,1},{4,6},{5,7},{6,4},{7,5},{8,10},{9,11},{10,... | collective-permute-start | bytes 786440 | tf_op jit(solution)/shard_map/ppermute | solution.py:424
  108.3 14.5 %collective-permute-start.33 = (bf16[128,1024]{1,0:T(8,128)(2,1)S(1)}, bf16[128,1024]{1,0:T(8,128)(2,1)S(1)}, u32[]{:S(2)}, u32[]{:S(2)}) collective-permute-start(bf16[128,1024]{1,0:T(8,128)(2,1)S(1)} %slice.66), channel_id=1, source_target_pairs={{0,4},{1,5},{2,6},{3,7},{4,0},{5,1},{6,2},{7,3},{8,12},{9,13},{10,... | collective-permute-start | bytes 786440 | tf_op jit(solution)/shard_map/ppermute | solution.py:424
  109.4 8.5 %collective-permute-start.27 = (bf16[64,1024]{1,0:T(8,128)(2,1)S(1)}, bf16[64,1024]{1,0:T(8,128)(2,1)S(1)}, u32[]{:S(2)}, u32[]{:S(2)}) collective-permute-start(bf16[64,1024]{1,0:T(8,128)(2,1)S(1)} %slice.61), channel_id=1, source_target_pairs={{0,2},{1,3},{2,0},{3,1},{4,6},{5,7},{6,4},{7,5},{8,10},{9,11},{10,... | collective-permute-start | bytes 393224 | tf_op jit(solution)/shard_map/ppermute | solution.py:424
  124.0 2.0 %collective-permute-start.34 = (bf16[256,1024]{1,0:T(8,128)(2,1)S(1)}, bf16[256,1024]{1,0:T(8,128)(2,1)S(1)}, u32[]{:S(2)}, u32[]{:S(2)}) collective-permute-start(bf16[256,1024]{1,0:T(8,128)(2,1)S(1)} %get-tuple-element.42), channel_id=1, source_target_pairs={{0,1},{1,0},{2,3},{3,2},{4,5},{5,4},{6,7},{7,6},{8,9},{9,8},{10,11... | collective-permute-start | bytes 1572872 | tf_op jit(solution)/shard_map/ppermute | solution.py:424
  124.1 7.6 %collective-permute-start.29 = (bf16[256,1024]{1,0:T(8,128)(2,1)S(1)}, bf16[256,1024]{1,0:T(8,128)(2,1)S(1)}, u32[]{:S(2)}, u32[]{:S(2)}) collective-permute-start(bf16[256,1024]{1,0:T(8,128)(2,1)S(1)} %get-tuple-element.37), channel_id=1, source_target_pairs={{0,1},{1,0},{2,3},{3,2},{4,5},{5,4},{6,7},{7,6},{8,9},{9,8},{10,11... | collective-permute-start | bytes 1572872 | tf_op jit(solution)/shard_map/ppermute | solution.py:424
  126.1 12.7 %collective-permute-start.35 = (bf16[128,1024]{1,0:T(8,128)(2,1)S(1)}, bf16[128,1024]{1,0:T(8,128)(2,1)S(1)}, u32[]{:S(2)}, u32[]{:S(2)}) collective-permute-start(bf16[128,1024]{1,0:T(8,128)(2,1)S(1)} %get-tuple-element.44), channel_id=1, source_target_pairs={{0,8},{1,9},{2,10},{3,11},{4,12},{5,13},{6,14},{7,15},{8,0},{9,1},... | collective-permute-start | bytes 786440 | tf_op jit(solution)/shard_map/ppermute | solution.py:424
  131.8 14.4 %collective-permute-start.30 = (bf16[128,1024]{1,0:T(8,128)(2,1)S(1)}, bf16[128,1024]{1,0:T(8,128)(2,1)S(1)}, u32[]{:S(2)}, u32[]{:S(2)}) collective-permute-start(bf16[128,1024]{1,0:T(8,128)(2,1)S(1)} %get-tuple-element.39), channel_id=1, source_target_pairs={{0,8},{1,9},{2,10},{3,11},{4,12},{5,13},{6,14},{7,15},{8,0},{9,1},... | collective-permute-start | bytes 786440 | tf_op jit(solution)/shard_map/ppermute | solution.py:424
  138.9 8.7 %collective-permute-start.36 = (bf16[64,1024]{1,0:T(8,128)(2,1)S(1)}, bf16[64,1024]{1,0:T(8,128)(2,1)S(1)}, u32[]{:S(2)}, u32[]{:S(2)}) collective-permute-start(bf16[64,1024]{1,0:T(8,128)(2,1)S(1)} %add_convert_fusion.2), channel_id=1, source_target_pairs={{0,16},{1,17},{2,18},{3,19},{4,20},{5,21},{6,22},{7,23},{8,24},{9,... | collective-permute-start | bytes 393224 | tf_op jit(solution)/shard_map/ppermute | solution.py:424
  146.2 7.6 %collective-permute-start.31 = (bf16[64,1024]{1,0:T(8,128)(2,1)S(1)}, bf16[64,1024]{1,0:T(8,128)(2,1)S(1)}, u32[]{:S(2)}, u32[]{:S(2)}) collective-permute-start(bf16[64,1024]{1,0:T(8,128)(2,1)S(1)} %add_convert_fusion.4), channel_id=1, source_target_pairs={{0,16},{1,17},{2,18},{3,19},{4,20},{5,21},{6,22},{7,23},{8,24},{9,... | collective-permute-start | bytes 393224 | tf_op jit(solution)/shard_map/ppermute | solution.py:424
